TPU v7x, 256 devices: a whole 4x4x8 slice. The times are simulated.
256 devices in a mesh: sp: 64 (over z, y, core), tp: 4 (over x).
Axes of the slice: x: 4, y: 4, z: 8, core: 2. Of those that a mesh axis runs over, the one named last changes fastest.
Arguments:
- tokens: bfloat16 [24576, 2048], P('sp', 'tp'), may hold values from -6 to 6
- norm_gain: float32 [3, 2048], replicated, may hold values from 0.1 to 1.9
- w_value: bfloat16 [3, 2048, 1024], P(None, 'sp', 'tp'), may hold values from -0.125 to 0.125
- w_gate: bfloat16 [3, 2048, 1024], P(None, 'sp', 'tp'), may hold values from -0.125 to 0.125
- conv_taps: float32 [3, 31, 1024], P(None, None, 'tp'), may hold values from -2.4 to 2.4
- conv_bias: float32 [3, 1024], P(None, 'tp'), may hold values from -3 to 3
- ln_gain: float32 [3, 1024], P(None, 'tp'), may hold values from 0.1 to 1.9
- ln_shift: float32 [3, 1024], P(None, 'tp'), may hold values from -3 to 3
- w_out: bfloat16 [3, 1024, 2048], P(None, 'tp', 'sp'), may hold values from -0.1875 to 0.1875
Outputs:
- stream: bfloat16 [24576, 2048], P('sp', 'tp')
All inputs are finite; a program needn't handle non-finite values.
Results may differ from a plain program's by a relative error of at most 0.015.
Values may be sent and summed in bfloat16 or wider, within the bound.
No kernel may reach another device: no remote copies, remote signals or barrier semaphores. Data moves between devices by JAX's collectives and lax.ppermute only.
A program may use at most 64 MiB of HBM per device.

v0:
```python
import functools

import jax
import jax.numpy as jnp
from jax import lax
from jax.experimental import pallas as pl
from jax.experimental.pallas import tpu as pltpu
from jax.sharding import Mesh
from jax.sharding import PartitionSpec as P


SP = ("z", "y", "c")
EDGE = 16
LANES = 128
norm_floor = 0.01
bf16, f32 = jnp.bfloat16, jnp.float32


def to_all(array, axis):
    copies = jnp.broadcast_to(array, (lax.axis_size(axis), *array.shape))
    return lax.all_to_all(copies, axis, split_axis=0, concat_axis=0, tiled=True)


def shifted(array, axis, s):
    n = lax.axis_size(axis)
    return lax.ppermute(array, axis, [(i, (i + s) % n) for i in range(n)])


def spread(array, axis):
    n = lax.axis_size(axis)
    pieces = {s: shifted(array, axis, s) for s in (n // 2, 1, n - 1)}
    return [array] + [pieces[s] for s in range(1, n)]


def swap(arrays):
    return [shifted(a, "c", 1) for a in arrays]


def after(arrays, *others):
    return lax.optimization_barrier((tuple(arrays), *others))[0]


def behind(position, s, n):
    return lax.rem(position + (n - s), n)


def row_step(rows):
    return 64 if rows % 64 == 0 else 32


def up_kernel(layer, total, n_s, n_y, first_lane, info, *refs):
    streams, refs = refs[:n_s], refs[n_s:]
    gain, par, refs = refs[0], refs[1], refs[2:]
    pieces, refs = refs[:-7], refs[-7:]
    out, weights, normed, both, padded, columns, sems = refs
    rows, features = normed.shape
    n_x, width = gain.shape[1:]
    keep = rows - 2 * EDGE
    ch = out.shape[-1]
    taps = par.shape[1] - 3
    shift = EDGE - taps // 2
    core, my_x, my_y = info[0], info[1], info[2]

    if n_y:
        copies = []
        for i, piece in enumerate(pieces):
            c = core if i < n_y else 1 - core
            rows_of = weights.at[:, behind(my_y, i % n_y, n_y), c]
            copies.append(pltpu.make_async_copy(piece, rows_of, sems.at[i]))
    else:
        copies = [pltpu.make_async_copy(pieces[0].at[:, pl.ds(first_lane, 2 * ch)], weights, sems.at[0])]
    for copy in copies:
        copy.start()

    step = 32

    def norm(i, carry):
        here = pl.ds(pl.multiple_of(i * step, step), step)
        squares = jnp.zeros((step, width), f32)
        for s in range(n_x):
            value = (streams[s][here] if n_s > 1 else streams[0][s, here]).astype(f32)
            squares += value * value
        mean = jnp.sum(squares, axis=-1, keepdims=True) * (1.0 / features)
        scale = lax.rsqrt(mean + norm_floor)
        for s in range(n_x):
            b = behind(my_x, s, n_x) if n_s > 1 else s
            value = (streams[s][here] if n_s > 1 else streams[0][s, here]).astype(f32)
            value = (value * scale * gain[layer, pl.ds(b, 1), :]).astype(bf16)
            normed[here, pl.ds(pl.multiple_of(b * width, width), width)] = value
        return carry

    lax.fori_loop(0, rows // step, norm, 0)
    for copy in copies:
        copy.wait()
    for half in range(2):
        part = weights[..., half * ch : (half + 1) * ch].reshape(features, ch)
        both[half] = jnp.dot(normed[...], part, preferred_element_type=f32)

    def gate(i, carry):
        first = pl.multiple_of(i * step, step)
        here = pl.ds(first, step)
        gated = both[0, here] * jax.nn.sigmoid(both[1, here])
        t = info[3 + layer] + first + lax.broadcasted_iota(jnp.int32, (step, 1), 0)
        gated = jnp.where((t >= 0) & (t < total), gated, 0.0).astype(bf16)
        padded[here] = gated.astype(f32)
        return carry

    lax.fori_loop(0, rows // step, gate, 0)

    size = row_step(keep)
    window = size + 2 * EDGE
    lane = lax.broadcasted_iota(jnp.int32, (size, LANES), 1)
    columns[pl.ds(keep, 2 * ch - keep)] = jnp.zeros((2 * ch - keep, LANES), f32)

    def chunk(i, carry):
        first = pl.multiple_of(i * size, size)
        accs = []
        for start in range(0, ch, LANES):
            lanes = slice(start, start + LANES)
            win = padded[pl.ds(first, window), lanes]
            acc = jnp.zeros((size, LANES), f32) + par[layer, taps : taps + 1, lanes]
            for r in range(8):
                turned = pltpu.roll(win, window - r, 0) if r else win
                for q in range(window // 8):
                    k = 8 * q + r - shift
                    if 0 <= k < taps:
                        acc = acc + par[layer, k : k + 1, lanes] * turned[8 * q : 8 * q + size]
            accs.append(acc)
        mean = jnp.sum(sum(accs), axis=-1, keepdims=True) * (1.0 / ch)
        for start, acc in zip(range(0, ch, LANES), accs):
            out[pl.ds(first, size), start : start + LANES] = (acc - mean).astype(bf16)
        high = mean.astype(bf16).astype(f32)
        columns[pl.ds(first, size)] = jnp.where(lane == 0, high, jnp.where(lane == 1, mean - high, 0.0))
        return carry

    lax.fori_loop(0, keep // size, chunk, 0)
    across = columns[...].T[:8]
    tail = jnp.concatenate([across[:, :ch], across[:, ch:]], axis=0).astype(bf16)
    out[keep:] = tail


def down_kernel(layer, last, n_s, n_y, n_x, first_lane, info, *refs):
    gated, refs = refs[:n_x], refs[n_x:]
    pars, refs = refs[:n_x], refs[n_x:]
    streams, refs = refs[:n_s], refs[n_s:]
    pieces, refs = refs[:-5], refs[-5:]
    out, weights, act, columns, sems = refs
    rows, ch = gated[0].shape
    keep = rows - EDGE
    core, my_x, my_y = info[0], info[1], info[2]
    width = out.shape[-1]

    copies = []

    def fetch(source, to):
        copies.append(pltpu.make_async_copy(source, to, sems.at[len(copies)]))

    if n_y:
        for i, piece in enumerate(pieces):
            c = core if i < n_y else 1 - core
            fetch(piece, weights.at[:, behind(my_y, i % n_y, n_y), c])
    elif last:
        mine = pl.ds(pl.multiple_of(my_x * width, width), width)
        fetch(pieces[0].at[mine, pl.ds(first_lane, ch)], weights.at[:, pl.ds(0, ch)])
        for s in range(1, n_x):
            fetch(pieces[s], weights.at[:, pl.ds(s * ch, ch)])
    else:
        fetch(pieces[0].at[:, pl.ds(first_lane, n_x * ch)], weights)
    for copy in copies:
        copy.start()

    spans = []
    for s in range(n_x):
        tail = gated[s][keep:].astype(f32)
        spans.append(jnp.concatenate([tail[:8], tail[8:]], axis=1))
    spans.append(jnp.zeros((LANES - 8 * n_x, 2 * ch), f32))
    columns[...] = jnp.concatenate(spans, axis=0).T

    size = row_step(keep)

    def chunk(i, carry):
        here = pl.ds(pl.multiple_of(i * size, size), size)
        cols = columns[here]
        means = [cols[:, 8 * s : 8 * s + 1] + cols[:, 8 * s + 1 : 8 * s + 2] for s in range(n_x)]
        average = sum(means) * (1.0 / n_x)
        squares = jnp.zeros((size, ch), f32)
        for s in range(n_x):
            value = gated[s][here].astype(f32) + (means[s] - average)
            squares += value * value
        mean = jnp.sum(squares, axis=-1, keepdims=True) * (1.0 / (n_x * ch))
        scale = lax.rsqrt(mean + norm_floor)
        for s in range(n_x):
            value = (gated[s][here].astype(f32) + (means[s] - average)) * scale
            value = value * pars[s][layer, 0:1, :] + pars[s][layer, 1:2, :]
            act[here, s * ch : (s + 1) * ch] = (value * jax.nn.sigmoid(value)).astype(bf16)
        return carry

    lax.fori_loop(0, keep // size, chunk, 0)
    for copy in copies:
        copy.wait()
    dims = (((1,), (1,)), ((), ()))
    inner = slice(EDGE, EDGE + keep)
    if last:
        added = lax.dot_general(act[...], weights[...], dims, preferred_element_type=f32)
        out[...] = (streams[0][my_x, inner].astype(f32) + added).astype(bf16)
    else:
        part_rows = weights.shape[0] // n_x

        def block(b, base):
            part = weights[pl.ds(b * part_rows, part_rows)].reshape(width, n_x * ch)
            added = lax.dot_general(act[...], part, dims, preferred_element_type=f32)
            out[b] = (base.astype(f32) + added).astype(bf16)

        if n_s > 1:
            for s in range(n_x):
                block(behind(my_x, s, n_x), streams[s][inner])
        else:
            lax.fori_loop(0, n_x, lambda b, carry: (block(b, streams[0][b, inner]), carry)[1], 0)


def vmem():
    return pl.BlockSpec(memory_space=pltpu.VMEM)


def hbm():
    return pl.BlockSpec(memory_space=pltpu.HBM)


def smem():
    return pl.BlockSpec(memory_space=pltpu.SMEM)


def up(layer, total, info, streams, gain, par, pieces, ch, first_lane=0):
    n_x, width = gain.shape[1:]
    rows = streams[0].shape[-2]
    keep = rows - 2 * EDGE
    n_y = len(pieces) // 2
    shape = (n_x * width,)
    if n_y:
        n_z, n_i, _ = pieces[0].shape
        shape = (n_z, n_y, 2, n_i)
    return pl.pallas_call(
        functools.partial(up_kernel, layer, total, len(streams), n_y, first_lane),
        out_shape=jax.ShapeDtypeStruct((keep + EDGE, ch), bf16),
        in_specs=[smem()] + [vmem()] * (len(streams) + 2) + [hbm()] * len(pieces),
        out_specs=vmem(),
        scratch_shapes=[
            pltpu.VMEM((*shape, 2 * ch), bf16),
            pltpu.VMEM((rows, n_x * width), bf16),
            pltpu.VMEM((2, rows, ch), f32),
            pltpu.VMEM((rows, ch), f32),
            pltpu.VMEM((2 * ch, LANES), f32),
            pltpu.SemaphoreType.DMA((len(pieces),)),
        ],
    )(info, *streams, gain, par, *pieces)


def down(layer, last, info, gated, pars, streams, pieces, paired, first_lane=0):
    rows, ch = gated[0].shape
    n_x = len(gated)
    keep = rows - EDGE
    width = streams[0].shape[-1]
    n_y = len(pieces) // 2 if paired else 0
    shape = (width if last else n_x * width,)
    if paired:
        n_z, n_i, _ = pieces[0].shape
        shape = (n_z, n_y, 2, n_i)
    out_shape = (keep, width) if last else (n_x, keep, width)
    return pl.pallas_call(
        functools.partial(down_kernel, layer, last, len(streams), n_y, n_x, first_lane),
        out_shape=jax.ShapeDtypeStruct(out_shape, bf16),
        in_specs=[smem()] + [vmem()] * (2 * n_x + len(streams)) + [hbm()] * len(pieces),
        out_specs=vmem(),
        scratch_shapes=[
            pltpu.VMEM((*shape, n_x * ch), bf16),
            pltpu.VMEM((keep, n_x * ch), bf16),
            pltpu.VMEM((2 * ch, LANES), f32),
            pltpu.SemaphoreType.DMA((len(pieces),)),
        ],
    )(info, *gated, *pars, *streams, *pieces)


def program(tokens, norm_gain, w_value, w_gate, conv_taps, conv_bias, ln_gain, ln_shift, w_out):
    layers, _, ch = w_value.shape
    n_x = lax.axis_size("x")
    my_x = lax.axis_index("x")
    n_tok, f_loc = tokens.shape
    halo = EDGE * layers
    size = lax.axis_size(SP)
    total = size * n_tok
    place = lax.axis_index(SP) * n_tok
    info = jnp.stack(
        [lax.axis_index("c"), my_x, lax.axis_index("y")]
        + [place - EDGE * (layers - l) for l in range(layers)]
    ).astype(jnp.int32)
    gain = norm_gain.reshape(layers, n_x, f_loc)

    before = lax.ppermute(tokens[n_tok - halo :], SP, [(i, i + 1) for i in range(size - 1)])
    following = lax.ppermute(tokens[:halo], SP, [(i + 1, i) for i in range(size - 1)])
    streams = spread(jnp.concatenate([before, tokens, following], axis=0), "x")

    par = jnp.concatenate([conv_taps, conv_bias[:, None], ln_gain[:, None], ln_shift[:, None]], axis=1)
    pars = spread(jnp.stack([ln_gain, ln_shift], axis=1), "x")

    info = after([info], *pars[1:])[0]

    out_t = jnp.swapaxes(w_out, 1, 2)
    wide = jnp.concatenate(spread(out_t[: layers - 1], "x"), axis=-1)

    packs, lanes, at = [], [], 0
    for l in range(1, layers):
        packs += [w_value[l], w_gate[l], out_t[l] if l == layers - 1 else wide[l]]
        lanes.append((at, at + 2 * ch))
        at += sum(a.shape[1] for a in packs[-3:])
    rest = lax.all_gather(jnp.concatenate(packs, axis=1), SP, axis=0, tiled=True)

    up_first = to_all(jnp.concatenate([w_value[0], w_gate[0]], axis=1), "z")
    up_first = spread(up_first, "y")
    out_first = to_all(wide[0], "z")
    out_first = spread(out_first, "y")

    for l in range(layers):
        last = l == layers - 1
        if l == 0:
            gated = up(l, total, info, streams, gain, par, [*up_first, *swap(up_first)], ch)
            start = 0
        else:
            first, start = lanes[l - 1]
            gated = up(l, total, info, streams, gain, par, [rest], ch, first)
            pieces = [rest]
        gated = spread(gated, "x")
        if l == 0:
            pieces = after(out_first, *gated[1:])
            pieces = [*pieces, *swap(pieces)]
        if last:
            for s in (1, n_x // 2, n_x - 1):
                row = lax.rem(my_x + s, n_x) * f_loc
                block = lax.dynamic_slice(rest, (row, start), (f_loc, ch))
                pieces.append(shifted(block, "x", s))
        stream = down(l, last, info, gated, pars, streams, pieces, l == 0, start)
        streams = [stream]
    return stream


def solution(mesh):
    torus = Mesh(mesh.devices.reshape(8, 4, 2, mesh.shape["tp"]), ("z", "y", "c", "x"))
    return jax.shard_map(
        program,
        mesh=torus,
        in_specs=(
            P(SP, "x"),
            P(),
            P(None, SP, "x"),
            P(None, SP, "x"),
            P(None, None, "x"),
            P(None, "x"),
            P(None, "x"),
            P(None, "x"),
            P(None, "x", SP),
        ),
        out_specs=P(SP, "x"),
        check_vma=False,
    )
```

profile of v0, /device:TPU:1, one launch (start us, length us, event | category | flops | bytes accessed | tf_op | source)
XLA Modules:
  0.0 230.4 jit_solution(12035322474936893727)
XLA Ops:
  7.3 2.0 collective-permute-start.18
  9.3 2.5 %collective-permute-start.19 = (bf16[2,32,256]{2,1,0:T(8,128)(2,1)S(1)}, bf16[2,32,256]{2,1,0:T(8,128)(2,1)S(1)}, u32[]{:S(2)}, u32[]{:S(2)}) collective-permute-start(bf16[2,32,256]{2,1,0:T(8,128)(2,1)S(1)} %slice.48), channel_id=1, source_target_pairs={{0,2},{1,3},{2,0},{3,1},{4,6},{5,7},{6,4},{7,5},{8,10},{9,11},{10,... | collective-permute-start | bytes 98312 | tf_op jit(solution)/shard_map/ppermute | solution.py:26
  11.8 1.2 collective-permute-start.20
  18.5 5.2 %collective-permute-start.3 = (bf16[48,512]{1,0:T(8,128)(2,1)S(1)}, bf16[48,512]{1,0:T(8,128)(2,1)S(1)}, u32[]{:S(2)}, u32[]{:S(2)}) collective-permute-start(bf16[48,512]{1,0:T(8,128)(2,1)S(1)} %get-tuple-element.19), channel_id=1, source_target_pairs={{0,4},{4,8},{8,12},{12,16},{16,20},{20,24},{24,28},{28,32},{32,36}... | collective-permute-start | bytes 147464 | tf_op jit(solution)/shard_map/ppermute | solution.py:298
  23.7 1.9 collective-permute-start.4
  27.1 8.2 %all-to-all-start = ((bf16[8,32,512]{2,1,0:T(8,128)(2,1)}), bf16[8,32,512]{2,1,0:T(8,128)(2,1)S(1)}, u32[]{:S(2)}, u32[]{:S(2)}) async-start(bf16[8,32,512]{2,1,0:T(8,128)(2,1)} %broadcast_in_dim.12), calls=%async_computation | async-start | bytes 524288 | tf_op jit(solution)/shard_map/all_to_all | solution.py:21
  36.4 8.6 %all-to-all-done.refs_6_ = bf16[8,32,512]{2,1,0:T(8,128)(2,1)S(1)} async-done(((bf16[8,32,512]{2,1,0:T(8,128)(2,1)}), bf16[8,32,512]{2,1,0:T(8,128)(2,1)S(1)}, u32[]{:S(2)}, u32[]{:S(2)}) %all-to-all-start) | async-done | bytes 262176 | tf_op jit(solution)/shard_map/all_to_all | solution.py:21
  45.9 3.5 %all-to-all-start.1 = ((bf16[8,32,1024]{2,1,0:T(8,128)(2,1)}), bf16[8,32,1024]{2,1,0:T(8,128)(2,1)S(1)}, u32[]{:S(2)}, u32[]{:S(2)}) async-start(bf16[8,32,1024]{2,1,0:T(8,128)(2,1)} %broadcast_in_dim.13), calls=%async_computation.1 | async-start | bytes 1048576 | tf_op jit(solution)/shard_map/all_to_all | solution.py:21
  49.9 3.2 %collective-permute-start.6 = (bf16[480,512]{1,0:T(8,128)(2,1)S(1)}, bf16[480,512]{1,0:T(8,128)(2,1)S(1)}, u32[]{:S(2)}, u32[]{:S(2)}) collective-permute-start(bf16[480,512]{1,0:T(8,128)(2,1)S(1)} %constant_dynamic-update-slice_fusion.refs_0_.refs_8_), channel_id=1, source_target_pairs={{0,2},{1,3},{2,0},{3,1},{4,6},{5,7},{6,4},{7,5},{8,10},{9,11},{10,... | collective-permute-start | bytes 1474568 | tf_op jit(solution)/shard_map/ppermute | solution.py:26
  54.6 4.2 %collective-permute-start.8 = (bf16[8,32,512]{2,1,0:T(8,128)(2,1)S(1)}, bf16[8,32,512]{2,1,0:T(8,128)(2,1)S(1)}, u32[]{:S(2)}, u32[]{:S(2)}) collective-permute-start(bf16[8,32,512]{2,1,0:T(8,128)(2,1)S(1)} %all-to-all-done.refs_6_), channel_id=1, source_target_pairs={{0,8},{8,16},{16,24},{24,0},{1,9},{9,17},{17,25},{25,1},{2,10},{10... | collective-permute-start | bytes 786440 | tf_op jit(solution)/shard_map/ppermute | solution.py:26
  58.9 1.5 collective-permute-start
  60.4 5.2 %collective-permute-done.refs_5_ = f32[3,2,256]{2,1,0:T(2,128)S(1)} collective-permute-done((f32[3,2,256]{2,1,0:T(2,128)S(1)}, f32[3,2,256]{2,1,0:T(2,128)S(1)}, u32[]{:S(2)}, u32[]{:S(2)}) %collective-permute-start) | collective-permute-done | bytes 6176 | tf_op jit(solution)/shard_map/ppermute | solution.py:26
  65.6 2.9 %collective-permute-start.1 = (f32[3,2,256]{2,1,0:T(2,128)S(1)}, f32[3,2,256]{2,1,0:T(2,128)S(1)}, u32[]{:S(2)}, u32[]{:S(2)}) collective-permute-start(f32[3,2,256]{2,1,0:T(2,128)S(1)} %pad_maximum_fusion.3.refs_4_), channel_id=1, source_target_pairs={{0,2},{1,3},{2,0},{3,1},{4,6},{5,7},{6,4},{7,5},{8,10},{9,11},{10,... | collective-permute-start | bytes 18440 | tf_op jit(solution)/shard_map/ppermute | solution.py:26
  68.5 1.1 collective-permute-done.1.refs_6_
  69.6 3.9 %collective-permute-start.2 = (f32[3,2,256]{2,1,0:T(2,128)S(1)}, f32[3,2,256]{2,1,0:T(2,128)S(1)}, u32[]{:S(2)}, u32[]{:S(2)}) collective-permute-start(f32[3,2,256]{2,1,0:T(2,128)S(1)} %pad_maximum_fusion.3.refs_4_), channel_id=1, source_target_pairs={{0,3},{1,0},{2,1},{3,2},{4,7},{5,4},{6,5},{7,6},{8,11},{9,8},{10,9... | collective-permute-start | bytes 18440 | tf_op jit(solution)/shard_map/ppermute | solution.py:26
  74.3 8.7 %collective-permute-start.9 = (bf16[8,32,512]{2,1,0:T(8,128)(2,1)S(1)}, bf16[8,32,512]{2,1,0:T(8,128)(2,1)}, u32[]{:S(2)}, u32[]{:S(2)}) collective-permute-start(bf16[8,32,512]{2,1,0:T(8,128)(2,1)S(1)} %all-to-all-done.refs_6_), channel_id=1, source_target_pairs={{0,16},{8,24},{16,0},{24,8},{1,17},{9,25},{17,1},{25,9},{2,18},{10... | collective-permute-start | bytes 786440 | tf_op jit(solution)/shard_map/ppermute | solution.py:26
  83.1 2.2 collective-permute-start.10
  85.3 5.1 %collective-permute-start.11 = (bf16[8,32,512]{2,1,0:T(8,128)(2,1)S(1)}, bf16[8,32,512]{2,1,0:T(8,128)(2,1)}, u32[]{:S(2)}, u32[]{:S(2)}) collective-permute-start(bf16[8,32,512]{2,1,0:T(8,128)(2,1)S(1)} %all-to-all-done.refs_6_), channel_id=1, source_target_pairs={{0,4},{4,0},{1,5},{5,1},{2,6},{6,2},{3,7},{7,3},{8,12},{12,8},{9,1... | collective-permute-start | bytes 786440 | tf_op jit(solution)/shard_map/ppermute | solution.py:26
  90.5 3.5 %collective-permute-done.9.refs_8_ = bf16[8,32,512]{2,1,0:T(8,128)(2,1)} collective-permute-done((bf16[8,32,512]{2,1,0:T(8,128)(2,1)S(1)}, bf16[8,32,512]{2,1,0:T(8,128)(2,1)}, u32[]{:S(2)}, u32[]{:S(2)}) %collective-permute-start.9) | collective-permute-done | bytes 262176 | tf_op jit(solution)/shard_map/ppermute | solution.py:26
  94.0 5.6 %collective-permute-start.13 = (bf16[8,32,512]{2,1,0:T(8,128)(2,1)}, bf16[8,32,512]{2,1,0:T(8,128)(2,1)}, u32[]{:S(2)}, u32[]{:S(2)}) collective-permute-start(bf16[8,32,512]{2,1,0:T(8,128)(2,1)} %collective-permute-done.9.refs_8_), channel_id=1, source_target_pairs={{0,4},{4,0},{1,5},{5,1},{2,6},{6,2},{3,7},{7,3},{8,12},{12,8},{9,1... | collective-permute-start | bytes 786440 | tf_op jit(solution)/shard_map/ppermute | solution.py:26
  99.7 5.3 %collective-permute-done.10.refs_9_ = bf16[8,32,512]{2,1,0:T(8,128)(2,1)} collective-permute-done((bf16[8,32,512]{2,1,0:T(8,128)(2,1)S(1)}, bf16[8,32,512]{2,1,0:T(8,128)(2,1)}, u32[]{:S(2)}, u32[]{:S(2)}) %collective-permute-start.10) | collective-permute-done | bytes 262176 | tf_op jit(solution)/shard_map/ppermute | solution.py:26
  105.0 3.0 %collective-permute-start.14 = (bf16[8,32,512]{2,1,0:T(8,128)(2,1)}, bf16[8,32,512]{2,1,0:T(8,128)(2,1)}, u32[]{:S(2)}, u32[]{:S(2)}) collective-permute-start(bf16[8,32,512]{2,1,0:T(8,128)(2,1)} %collective-permute-done.10.refs_9_), channel_id=1, source_target_pairs={{0,4},{4,0},{1,5},{5,1},{2,6},{6,2},{3,7},{7,3},{8,12},{12,8},{9,1... | collective-permute-start | bytes 786440 | tf_op jit(solution)/shard_map/ppermute | solution.py:26
  108.0 1.3 broadcast_in_dim.11
  109.6 2.5 %collective-permute-start.22 = (bf16[8,32,1024]{2,1,0:T(8,128)(2,1)S(1)}, bf16[8,32,1024]{2,1,0:T(8,128)(2,1)}, u32[]{:S(2)}, u32[]{:S(2)}) collective-permute-start(bf16[8,32,1024]{2,1,0:T(8,128)(2,1)S(1)} %all-to-all-done.1.refs_12_), channel_id=1, source_target_pairs={{0,16},{8,24},{16,0},{24,8},{1,17},{9,25},{17,1},{25,9},{2,18},{10... | collective-permute-start | bytes 1572872 | tf_op jit(solution)/shard_map/ppermute | solution.py:26
  112.1 2.0 collective-permute-start.23
  114.1 1.6 pad_maximum_fusion.1.refs_5_.refs_2_
  115.6 1.4 reshape.3.refs_4_.refs_1_
  117.8 7.8 %shard_map.91.refs_0_ = bf16[464,256]{1,0:T(8,128)(2,1)} custom-call(s32[6]{0:T(128)} %stack.36.info, bf16[480,512]{1,0:T(8,128)(2,1)} %copy-done, bf16[480,512]{1,0:T(8,128)(2,1)} %copy-done.2, bf16[480,512]{1,0:T(8,128)(2,1)} %copy-done.3, bf16[480,512]{1,0:T(8,128)(2,1)} %copy-done.4, f32[3,4,512]{2,1,0:T(4,128)} %reshape.3.refs_4_.refs_1_, ...), custom_call_target="tpu_custom_call" | custom-call | tf_op jit(solution)/shard_map/pallas_call | solution.py:242
  125.5 1.3 collective-permute-start.15
  126.8 2.4 %collective-permute-start.16 = (bf16[464,256]{1,0:T(8,128)(2,1)}, bf16[464,256]{1,0:T(8,128)(2,1)S(1)}, u32[]{:S(2)}, u32[]{:S(2)}) collective-permute-start(bf16[464,256]{1,0:T(8,128)(2,1)} %shard_map.91.refs_0_), channel_id=1, source_target_pairs={{0,2},{1,3},{2,0},{3,1},{4,6},{5,7},{6,4},{7,5},{8,10},{9,11},{10,... | collective-permute-start | bytes 712712 | tf_op jit(solution)/shard_map/ppermute | solution.py:26
  129.2 4.4 %collective-permute-done.15.refs_1_ = bf16[464,256]{1,0:T(8,128)(2,1)S(1)} collective-permute-done((bf16[464,256]{1,0:T(8,128)(2,1)}, bf16[464,256]{1,0:T(8,128)(2,1)S(1)}, u32[]{:S(2)}, u32[]{:S(2)}) %collective-permute-start.15) | collective-permute-done | bytes 237600 | tf_op jit(solution)/shard_map/ppermute | solution.py:26
  133.6 1.2 collective-permute-start.17
  134.8 4.7 %collective-permute-done.16.refs_2_ = bf16[464,256]{1,0:T(8,128)(2,1)S(1)} collective-permute-done((bf16[464,256]{1,0:T(8,128)(2,1)}, bf16[464,256]{1,0:T(8,128)(2,1)S(1)}, u32[]{:S(2)}, u32[]{:S(2)}) %collective-permute-start.16) | collective-permute-done | bytes 237600 | tf_op jit(solution)/shard_map/ppermute | solution.py:26
  139.6 2.6 %collective-permute-start.24 = (bf16[8,32,1024]{2,1,0:T(8,128)(2,1)S(1)}, bf16[8,32,1024]{2,1,0:T(8,128)(2,1)S(1)}, u32[]{:S(2)}, u32[]{:S(2)}) collective-permute-start(bf16[8,32,1024]{2,1,0:T(8,128)(2,1)S(1)} %all-to-all-done.1.refs_12_), channel_id=1, source_target_pairs={{0,4},{4,0},{1,5},{5,1},{2,6},{6,2},{3,7},{7,3},{8,12},{12,8},{9,1... | collective-permute-start | bytes 1572872 | tf_op jit(solution)/shard_map/ppermute | solution.py:26
  146.8 8.7 %shard_map.92.refs_0_.refs_8_ = bf16[4,448,512]{2,1,0:T(8,128)(2,1)} custom-call(s32[6]{0:T(128)} %stack.36.info, bf16[464,256]{1,0:T(8,128)(2,1)} %shard_map.91.refs_0_, bf16[464,256]{1,0:T(8,128)(2,1)} %copy-done.15, bf16[464,256]{1,0:T(8,128)(2,1)} %copy-done.16, bf16[464,256]{1,0:T(8,128)(2,1)} %copy-done.17, f32[3,2,256]{2,1,0:T(2,128)} %copy-done.25, ...), custom_call_target="tpu_custom_call" | custom-call | tf_op jit(solution)/shard_map/pallas_call | solution.py:269
  155.5 8.1 %shard_map.93.refs_0_ = bf16[432,256]{1,0:T(8,128)(2,1)} custom-call(s32[6]{0:T(128)} %stack.36.info, bf16[4,448,512]{2,1,0:T(8,128)(2,1)} %shard_map.92.refs_0_.refs_8_, f32[3,4,512]{2,1,0:T(4,128)} %reshape.3.refs_4_.refs_1_, f32[3,34,256]{2,1,0:T(8,128)} %pad_maximum_fusion.1.refs_5_.refs_2_, bf16[2048,2304]{1,0:T(8,128)(2,1)} %all-gather.2.cloned.1.call-done.refs_3_.refs_9_), custom_call_target="tpu_custom_call" | custom-call | tf_op jit(solution)/shard_map/pallas_call | solution.py:242
  164.6 1.2 constant_dynamic-slice_fusion
  165.8 1.1 collective-permute-start.34
  166.9 2.5 %collective-permute-start.29 = (bf16[432,256]{1,0:T(8,128)(2,1)}, bf16[432,256]{1,0:T(8,128)(2,1)S(1)}, u32[]{:S(2)}, u32[]{:S(2)}) collective-permute-start(bf16[432,256]{1,0:T(8,128)(2,1)} %shard_map.93.refs_0_), channel_id=1, source_target_pairs={{0,2},{1,3},{2,0},{3,1},{4,6},{5,7},{6,4},{7,5},{8,10},{9,11},{10,... | collective-permute-start | bytes 663560 | tf_op jit(solution)/shard_map/ppermute | solution.py:26
  169.4 2.0 collective-permute-start.30
  171.4 1.1 collective-permute-done.28.refs_1_
  172.5 1.2 collective-permute-start.36
  173.7 10.1 %collective-permute-done.29.refs_2_ = bf16[432,256]{1,0:T(8,128)(2,1)S(1)} collective-permute-done((bf16[432,256]{1,0:T(8,128)(2,1)}, bf16[432,256]{1,0:T(8,128)(2,1)S(1)}, u32[]{:S(2)}, u32[]{:S(2)}) %collective-permute-start.29) | collective-permute-done | bytes 221216 | tf_op jit(solution)/shard_map/ppermute | solution.py:26
  185.2 11.3 %shard_map.94.refs_0_.refs_8_ = bf16[4,416,512]{2,1,0:T(8,128)(2,1)} custom-call(s32[6]{0:T(128)} %stack.36.info, bf16[432,256]{1,0:T(8,128)(2,1)} %shard_map.93.refs_0_, bf16[432,256]{1,0:T(8,128)(2,1)} %copy-done.18, bf16[432,256]{1,0:T(8,128)(2,1)} %copy-done.19, bf16[432,256]{1,0:T(8,128)(2,1)} %copy-done.20, f32[3,2,256]{2,1,0:T(2,128)} %copy-done.25, ...), custom_call_target="tpu_custom_call" | custom-call | tf_op jit(solution)/shard_map/pallas_call | solution.py:269
  196.5 6.9 %shard_map.95.refs_0_ = bf16[400,256]{1,0:T(8,128)(2,1)} custom-call(s32[6]{0:T(128)} %stack.36.info, bf16[4,416,512]{2,1,0:T(8,128)(2,1)} %shard_map.94.refs_0_.refs_8_, f32[3,4,512]{2,1,0:T(4,128)} %reshape.3.refs_4_.refs_1_, f32[3,34,256]{2,1,0:T(8,128)} %pad_maximum_fusion.1.refs_5_.refs_2_, bf16[2048,2304]{1,0:T(8,128)(2,1)} %all-gather.2.cloned.1.call-done.refs_3_.refs_9_), custom_call_target="tpu_custom_call" | custom-call | tf_op jit(solution)/shard_map/pallas_call | solution.py:242
  203.6 2.6 %collective-permute-start.33 = (bf16[400,256]{1,0:T(8,128)(2,1)}, bf16[400,256]{1,0:T(8,128)(2,1)S(1)}, u32[]{:S(2)}, u32[]{:S(2)}) collective-permute-start(bf16[400,256]{1,0:T(8,128)(2,1)} %shard_map.95.refs_0_), channel_id=1, source_target_pairs={{0,3},{1,0},{2,1},{3,2},{4,7},{5,4},{6,5},{7,6},{8,11},{9,8},{10,9... | collective-permute-start | bytes 614408 | tf_op jit(solution)/shard_map/ppermute | solution.py:26
  206.3 9.6 %collective-permute-done.31.refs_1_ = bf16[400,256]{1,0:T(8,128)(2,1)S(1)} collective-permute-done((bf16[400,256]{1,0:T(8,128)(2,1)}, bf16[400,256]{1,0:T(8,128)(2,1)S(1)}, u32[]{:S(2)}, u32[]{:S(2)}) %collective-permute-start.31) | collective-permute-done | bytes 204832 | tf_op jit(solution)/shard_map/ppermute | solution.py:26
  217.3 6.2 %shard_map.96 = bf16[384,512]{1,0:T(8,128)(2,1)} custom-call(s32[6]{0:T(128)} %stack.36.info, bf16[400,256]{1,0:T(8,128)(2,1)} %shard_map.95.refs_0_, bf16[400,256]{1,0:T(8,128)(2,1)} %copy-done.21, bf16[400,256]{1,0:T(8,128)(2,1)} %copy-done.22, bf16[400,256]{1,0:T(8,128)(2,1)} %copy-done.23, f32[3,2,256]{2,1,0:T(2,128)} %copy-done.25, ...), custom_call_target="tpu_custom_call" | custom-call | tf_op jit(solution)/shard_map/pallas_call | solution.py:269
  (126 shorter events, 22.3 us)
Async XLA Ops:
  6.5 149.0 %all-gather.2.cloned.1.call-start = ((), (), s32[]{:S(2)}) async-start(), calls=%async_computation.2 | async-start | bytes 9584640 | tf_op jit(solution)/shard_map/all_gather | solution.py:315
  7.3 7.1 %collective-permute-start.18 = (bf16[2,32,256]{2,1,0:T(8,128)(2,1)S(1)}, bf16[2,32,256]{2,1,0:T(8,128)(2,1)S(1)}, u32[]{:S(2)}, u32[]{:S(2)}) collective-permute-start(bf16[2,32,256]{2,1,0:T(8,128)(2,1)S(1)} %slice.48), channel_id=1, source_target_pairs={{0,1},{1,2},{2,3},{3,0},{4,5},{5,6},{6,7},{7,4},{8,9},{9,10},{10,1... | collective-permute-start | bytes 98312 | tf_op jit(solution)/shard_map/ppermute | solution.py:26
  9.3 5.0 %collective-permute-start.19 = (bf16[2,32,256]{2,1,0:T(8,128)(2,1)S(1)}, bf16[2,32,256]{2,1,0:T(8,128)(2,1)S(1)}, u32[]{:S(2)}, u32[]{:S(2)}) collective-permute-start(bf16[2,32,256]{2,1,0:T(8,128)(2,1)S(1)} %slice.48), channel_id=1, source_target_pairs={{0,2},{1,3},{2,0},{3,1},{4,6},{5,7},{6,4},{7,5},{8,10},{9,11},{10,... | collective-permute-start | bytes 98312 | tf_op jit(solution)/shard_map/ppermute | solution.py:26
  11.8 3.1 %collective-permute-start.20 = (bf16[2,32,256]{2,1,0:T(8,128)(2,1)S(1)}, bf16[2,32,256]{2,1,0:T(8,128)(2,1)S(1)}, u32[]{:S(2)}, u32[]{:S(2)}) collective-permute-start(bf16[2,32,256]{2,1,0:T(8,128)(2,1)S(1)} %slice.48), channel_id=1, source_target_pairs={{0,3},{1,0},{2,1},{3,2},{4,7},{5,4},{6,5},{7,6},{8,11},{9,8},{10,9... | collective-permute-start | bytes 98312 | tf_op jit(solution)/shard_map/ppermute | solution.py:26
  18.5 16.8 %collective-permute-start.3 = (bf16[48,512]{1,0:T(8,128)(2,1)S(1)}, bf16[48,512]{1,0:T(8,128)(2,1)S(1)}, u32[]{:S(2)}, u32[]{:S(2)}) collective-permute-start(bf16[48,512]{1,0:T(8,128)(2,1)S(1)} %get-tuple-element.19), channel_id=1, source_target_pairs={{0,4},{4,8},{8,12},{12,16},{16,20},{20,24},{24,28},{28,32},{32,36}... | collective-permute-start | bytes 147464 | tf_op jit(solution)/shard_map/ppermute | solution.py:298
  23.7 25.7 %collective-permute-start.4 = (bf16[48,512]{1,0:T(8,128)(2,1)S(1)}, bf16[48,512]{1,0:T(8,128)(2,1)S(1)}, u32[]{:S(2)}, u32[]{:S(2)}) collective-permute-start(bf16[48,512]{1,0:T(8,128)(2,1)S(1)} %get-tuple-element.18), channel_id=1, source_target_pairs={{4,0},{8,4},{12,8},{16,12},{20,16},{24,20},{28,24},{32,28},{36,32}... | collective-permute-start | bytes 147464 | tf_op jit(solution)/shard_map/ppermute | solution.py:299
  27.1 17.9 %all-to-all-start = ((bf16[8,32,512]{2,1,0:T(8,128)(2,1)}), bf16[8,32,512]{2,1,0:T(8,128)(2,1)S(1)}, u32[]{:S(2)}, u32[]{:S(2)}) async-start(bf16[8,32,512]{2,1,0:T(8,128)(2,1)} %broadcast_in_dim.12), calls=%async_computation | async-start | bytes 524288 | tf_op jit(solution)/shard_map/all_to_all | solution.py:21
  45.0 72.7 %copy-start.5 = (bf16[8,32,512]{2,1,0:T(8,128)(2,1)}, bf16[8,32,512]{2,1,0:T(8,128)(2,1)S(1)}, u32[]{:S(2)}) copy-start(bf16[8,32,512]{2,1,0:T(8,128)(2,1)S(1)} %all-to-all-done.refs_6_) | copy-start | bytes 786436
  45.9 63.4 %all-to-all-start.1 = ((bf16[8,32,1024]{2,1,0:T(8,128)(2,1)}), bf16[8,32,1024]{2,1,0:T(8,128)(2,1)S(1)}, u32[]{:S(2)}, u32[]{:S(2)}) async-start(bf16[8,32,1024]{2,1,0:T(8,128)(2,1)} %broadcast_in_dim.13), calls=%async_computation.1 | async-start | bytes 1048576 | tf_op jit(solution)/shard_map/all_to_all | solution.py:21
  49.4 68.3 %copy-start = (bf16[480,512]{1,0:T(8,128)(2,1)}, bf16[480,512]{1,0:T(8,128)(2,1)S(1)}, u32[]{:S(2)}) copy-start(bf16[480,512]{1,0:T(8,128)(2,1)S(1)} %constant_dynamic-update-slice_fusion.refs_0_.refs_8_) | copy-start | bytes 1474564
  49.4 33.6 %collective-permute-start.5 = (bf16[480,512]{1,0:T(8,128)(2,1)S(1)}, bf16[480,512]{1,0:T(8,128)(2,1)S(1)}, u32[]{:S(2)}, u32[]{:S(2)}) collective-permute-start(bf16[480,512]{1,0:T(8,128)(2,1)S(1)} %constant_dynamic-update-slice_fusion.refs_0_.refs_8_), channel_id=1, source_target_pairs={{0,1},{1,2},{2,3},{3,0},{4,5},{5,6},{6,7},{7,4},{8,9},{9,10},{10,1... | collective-permute-start | bytes 1474568 | tf_op jit(solution)/shard_map/ppermute | solution.py:26
  49.9 35.4 %collective-permute-start.6 = (bf16[480,512]{1,0:T(8,128)(2,1)S(1)}, bf16[480,512]{1,0:T(8,128)(2,1)S(1)}, u32[]{:S(2)}, u32[]{:S(2)}) collective-permute-start(bf16[480,512]{1,0:T(8,128)(2,1)S(1)} %constant_dynamic-update-slice_fusion.refs_0_.refs_8_), channel_id=1, source_target_pairs={{0,2},{1,3},{2,0},{3,1},{4,6},{5,7},{6,4},{7,5},{8,10},{9,11},{10,... | collective-permute-start | bytes 1474568 | tf_op jit(solution)/shard_map/ppermute | solution.py:26
  54.5 54.8 %collective-permute-start.7 = (bf16[480,512]{1,0:T(8,128)(2,1)S(1)}, bf16[480,512]{1,0:T(8,128)(2,1)S(1)}, u32[]{:S(2)}, u32[]{:S(2)}) collective-permute-start(bf16[480,512]{1,0:T(8,128)(2,1)S(1)} %constant_dynamic-update-slice_fusion.refs_0_.refs_8_), channel_id=1, source_target_pairs={{0,3},{1,0},{2,1},{3,2},{4,7},{5,4},{6,5},{7,6},{8,11},{9,8},{10,9... | collective-permute-start | bytes 1474568 | tf_op jit(solution)/shard_map/ppermute | solution.py:26
  54.6 35.8 %collective-permute-start.8 = (bf16[8,32,512]{2,1,0:T(8,128)(2,1)S(1)}, bf16[8,32,512]{2,1,0:T(8,128)(2,1)S(1)}, u32[]{:S(2)}, u32[]{:S(2)}) collective-permute-start(bf16[8,32,512]{2,1,0:T(8,128)(2,1)S(1)} %all-to-all-done.refs_6_), channel_id=1, source_target_pairs={{0,8},{8,16},{16,24},{24,0},{1,9},{9,17},{17,25},{25,1},{2,10},{10... | collective-permute-start | bytes 786440 | tf_op jit(solution)/shard_map/ppermute | solution.py:26
  58.9 87.1 %copy-start.25 = (f32[3,2,256]{2,1,0:T(2,128)}, f32[3,2,256]{2,1,0:T(2,128)S(1)}, u32[]{:S(2)}) copy-start(f32[3,2,256]{2,1,0:T(2,128)S(1)} %pad_maximum_fusion.3.refs_4_) | copy-start | bytes 18436
  58.9 6.7 %collective-permute-start = (f32[3,2,256]{2,1,0:T(2,128)S(1)}, f32[3,2,256]{2,1,0:T(2,128)S(1)}, u32[]{:S(2)}, u32[]{:S(2)}) collective-permute-start(f32[3,2,256]{2,1,0:T(2,128)S(1)} %pad_maximum_fusion.3.refs_4_), channel_id=1, source_target_pairs={{0,1},{1,2},{2,3},{3,0},{4,5},{5,6},{6,7},{7,4},{8,9},{9,10},{10,1... | collective-permute-start | bytes 18440 | tf_op jit(solution)/shard_map/ppermute | solution.py:26
  65.6 80.4 %copy-start.26 = (f32[3,2,256]{2,1,0:T(2,128)}, f32[3,2,256]{2,1,0:T(2,128)S(1)}, u32[]{:S(2)}) copy-start(f32[3,2,256]{2,1,0:T(2,128)S(1)} %collective-permute-done.refs_5_) | copy-start | bytes 18436
  65.6 4.0 %collective-permute-start.1 = (f32[3,2,256]{2,1,0:T(2,128)S(1)}, f32[3,2,256]{2,1,0:T(2,128)S(1)}, u32[]{:S(2)}, u32[]{:S(2)}) collective-permute-start(f32[3,2,256]{2,1,0:T(2,128)S(1)} %pad_maximum_fusion.3.refs_4_), channel_id=1, source_target_pairs={{0,2},{1,3},{2,0},{3,1},{4,6},{5,7},{6,4},{7,5},{8,10},{9,11},{10,... | collective-permute-start | bytes 18440 | tf_op jit(solution)/shard_map/ppermute | solution.py:26
  69.6 39.6 %copy-start.27 = (f32[3,2,256]{2,1,0:T(2,128)}, f32[3,2,256]{2,1,0:T(2,128)S(1)}, u32[]{:S(2)}) copy-start(f32[3,2,256]{2,1,0:T(2,128)S(1)} %collective-permute-done.1.refs_6_) | copy-start | bytes 18436
  69.6 4.7 %collective-permute-start.2 = (f32[3,2,256]{2,1,0:T(2,128)S(1)}, f32[3,2,256]{2,1,0:T(2,128)S(1)}, u32[]{:S(2)}, u32[]{:S(2)}) collective-permute-start(f32[3,2,256]{2,1,0:T(2,128)S(1)} %pad_maximum_fusion.3.refs_4_), channel_id=1, source_target_pairs={{0,3},{1,0},{2,1},{3,2},{4,7},{5,4},{6,5},{7,6},{8,11},{9,8},{10,9... | collective-permute-start | bytes 18440 | tf_op jit(solution)/shard_map/ppermute | solution.py:26
  74.3 34.9 %copy-start.28 = (f32[3,2,256]{2,1,0:T(2,128)}, f32[3,2,256]{2,1,0:T(2,128)S(1)}, u32[]{:S(2)}) copy-start(f32[3,2,256]{2,1,0:T(2,128)S(1)} %collective-permute-done.2.refs_7_) | copy-start | bytes 18436
  74.3 19.7 %collective-permute-start.9 = (bf16[8,32,512]{2,1,0:T(8,128)(2,1)S(1)}, bf16[8,32,512]{2,1,0:T(8,128)(2,1)}, u32[]{:S(2)}, u32[]{:S(2)}) collective-permute-start(bf16[8,32,512]{2,1,0:T(8,128)(2,1)S(1)} %all-to-all-done.refs_6_), channel_id=1, source_target_pairs={{0,16},{8,24},{16,0},{24,8},{1,17},{9,25},{17,1},{25,9},{2,18},{10... | collective-permute-start | bytes 786440 | tf_op jit(solution)/shard_map/ppermute | solution.py:26
  83.1 34.7 %copy-start.2 = (bf16[480,512]{1,0:T(8,128)(2,1)}, bf16[480,512]{1,0:T(8,128)(2,1)S(1)}, u32[]{:S(2)}) copy-start(bf16[480,512]{1,0:T(8,128)(2,1)S(1)} %collective-permute-done.5.refs_1_.refs_9_) | copy-start | bytes 1474564
  83.1 21.9 %collective-permute-start.10 = (bf16[8,32,512]{2,1,0:T(8,128)(2,1)S(1)}, bf16[8,32,512]{2,1,0:T(8,128)(2,1)}, u32[]{:S(2)}, u32[]{:S(2)}) collective-permute-start(bf16[8,32,512]{2,1,0:T(8,128)(2,1)S(1)} %all-to-all-done.refs_6_), channel_id=1, source_target_pairs={{0,24},{8,0},{16,8},{24,16},{1,25},{9,1},{17,9},{25,17},{2,26},{10... | collective-permute-start | bytes 786440 | tf_op jit(solution)/shard_map/ppermute | solution.py:26
  85.3 24.2 %collective-permute-start.11 = (bf16[8,32,512]{2,1,0:T(8,128)(2,1)S(1)}, bf16[8,32,512]{2,1,0:T(8,128)(2,1)}, u32[]{:S(2)}, u32[]{:S(2)}) collective-permute-start(bf16[8,32,512]{2,1,0:T(8,128)(2,1)S(1)} %all-to-all-done.refs_6_), channel_id=1, source_target_pairs={{0,4},{4,0},{1,5},{5,1},{2,6},{6,2},{3,7},{7,3},{8,12},{12,8},{9,1... | collective-permute-start | bytes 786440 | tf_op jit(solution)/shard_map/ppermute | solution.py:26
  90.4 21.7 %collective-permute-start.12 = (bf16[8,32,512]{2,1,0:T(8,128)(2,1)S(1)}, bf16[8,32,512]{2,1,0:T(8,128)(2,1)}, u32[]{:S(2)}, u32[]{:S(2)}) collective-permute-start(bf16[8,32,512]{2,1,0:T(8,128)(2,1)S(1)} %collective-permute-done.8.refs_7_), channel_id=1, source_target_pairs={{0,4},{4,0},{1,5},{5,1},{2,6},{6,2},{3,7},{7,3},{8,12},{12,8},{9,1... | collective-permute-start | bytes 786440 | tf_op jit(solution)/shard_map/ppermute | solution.py:26
  94.0 23.7 %collective-permute-start.13 = (bf16[8,32,512]{2,1,0:T(8,128)(2,1)}, bf16[8,32,512]{2,1,0:T(8,128)(2,1)}, u32[]{:S(2)}, u32[]{:S(2)}) collective-permute-start(bf16[8,32,512]{2,1,0:T(8,128)(2,1)} %collective-permute-done.9.refs_8_), channel_id=1, source_target_pairs={{0,4},{4,0},{1,5},{5,1},{2,6},{6,2},{3,7},{7,3},{8,12},{12,8},{9,1... | collective-permute-start | bytes 786440 | tf_op jit(solution)/shard_map/ppermute | solution.py:26
  105.0 12.7 %collective-permute-start.14 = (bf16[8,32,512]{2,1,0:T(8,128)(2,1)}, bf16[8,32,512]{2,1,0:T(8,128)(2,1)}, u32[]{:S(2)}, u32[]{:S(2)}) collective-permute-start(bf16[8,32,512]{2,1,0:T(8,128)(2,1)} %collective-permute-done.10.refs_9_), channel_id=1, source_target_pairs={{0,4},{4,0},{1,5},{5,1},{2,6},{6,2},{3,7},{7,3},{8,12},{12,8},{9,1... | collective-permute-start | bytes 786440 | tf_op jit(solution)/shard_map/ppermute | solution.py:26
  109.3 36.7 %copy-start.1 = (bf16[8,32,1024]{2,1,0:T(8,128)(2,1)}, bf16[8,32,1024]{2,1,0:T(8,128)(2,1)S(1)}, u32[]{:S(2)}) copy-start(bf16[8,32,1024]{2,1,0:T(8,128)(2,1)S(1)} %all-to-all-done.1.refs_12_) | copy-start | bytes 1572868
  109.3 30.3 %collective-permute-start.21 = (bf16[8,32,1024]{2,1,0:T(8,128)(2,1)S(1)}, bf16[8,32,1024]{2,1,0:T(8,128)(2,1)S(1)}, u32[]{:S(2)}, u32[]{:S(2)}) collective-permute-start(bf16[8,32,1024]{2,1,0:T(8,128)(2,1)S(1)} %all-to-all-done.1.refs_12_), channel_id=1, source_target_pairs={{0,8},{8,16},{16,24},{24,0},{1,9},{9,17},{17,25},{25,1},{2,10},{10... | collective-permute-start | bytes 1572872 | tf_op jit(solution)/shard_map/ppermute | solution.py:26
  109.6 30.0 %collective-permute-start.22 = (bf16[8,32,1024]{2,1,0:T(8,128)(2,1)S(1)}, bf16[8,32,1024]{2,1,0:T(8,128)(2,1)}, u32[]{:S(2)}, u32[]{:S(2)}) collective-permute-start(bf16[8,32,1024]{2,1,0:T(8,128)(2,1)S(1)} %all-to-all-done.1.refs_12_), channel_id=1, source_target_pairs={{0,16},{8,24},{16,0},{24,8},{1,17},{9,25},{17,1},{25,9},{2,18},{10... | collective-permute-start | bytes 1572872 | tf_op jit(solution)/shard_map/ppermute | solution.py:26
  112.1 27.5 %collective-permute-start.23 = (bf16[8,32,1024]{2,1,0:T(8,128)(2,1)S(1)}, bf16[8,32,1024]{2,1,0:T(8,128)(2,1)}, u32[]{:S(2)}, u32[]{:S(2)}) collective-permute-start(bf16[8,32,1024]{2,1,0:T(8,128)(2,1)S(1)} %all-to-all-done.1.refs_12_), channel_id=1, source_target_pairs={{0,24},{8,0},{16,8},{24,16},{1,25},{9,1},{17,9},{25,17},{2,26},{10... | collective-permute-start | bytes 1572872 | tf_op jit(solution)/shard_map/ppermute | solution.py:26
  125.5 8.1 %collective-permute-start.15 = (bf16[464,256]{1,0:T(8,128)(2,1)}, bf16[464,256]{1,0:T(8,128)(2,1)S(1)}, u32[]{:S(2)}, u32[]{:S(2)}) collective-permute-start(bf16[464,256]{1,0:T(8,128)(2,1)} %shard_map.91.refs_0_), channel_id=1, source_target_pairs={{0,1},{1,2},{2,3},{3,0},{4,5},{5,6},{6,7},{7,4},{8,9},{9,10},{10,1... | collective-permute-start | bytes 712712 | tf_op jit(solution)/shard_map/ppermute | solution.py:26
  126.8 12.7 %collective-permute-start.16 = (bf16[464,256]{1,0:T(8,128)(2,1)}, bf16[464,256]{1,0:T(8,128)(2,1)S(1)}, u32[]{:S(2)}, u32[]{:S(2)}) collective-permute-start(bf16[464,256]{1,0:T(8,128)(2,1)} %shard_map.91.refs_0_), channel_id=1, source_target_pairs={{0,2},{1,3},{2,0},{3,1},{4,6},{5,7},{6,4},{7,5},{8,10},{9,11},{10,... | collective-permute-start | bytes 712712 | tf_op jit(solution)/shard_map/ppermute | solution.py:26
  133.6 5.9 %collective-permute-start.17 = (bf16[464,256]{1,0:T(8,128)(2,1)}, bf16[464,256]{1,0:T(8,128)(2,1)S(1)}, u32[]{:S(2)}, u32[]{:S(2)}) collective-permute-start(bf16[464,256]{1,0:T(8,128)(2,1)} %shard_map.91.refs_0_), channel_id=1, source_target_pairs={{0,3},{1,0},{2,1},{3,2},{4,7},{5,4},{6,5},{7,6},{8,11},{9,8},{10,9... | collective-permute-start | bytes 712712 | tf_op jit(solution)/shard_map/ppermute | solution.py:26
  139.6 4.1 %collective-permute-start.24 = (bf16[8,32,1024]{2,1,0:T(8,128)(2,1)S(1)}, bf16[8,32,1024]{2,1,0:T(8,128)(2,1)S(1)}, u32[]{:S(2)}, u32[]{:S(2)}) collective-permute-start(bf16[8,32,1024]{2,1,0:T(8,128)(2,1)S(1)} %all-to-all-done.1.refs_12_), channel_id=1, source_target_pairs={{0,4},{4,0},{1,5},{5,1},{2,6},{6,2},{3,7},{7,3},{8,12},{12,8},{9,1... | collective-permute-start | bytes 1572872 | tf_op jit(solution)/shard_map/ppermute | solution.py:26
  142.2 2.3 collective-permute-start.25
  142.3 2.9 %collective-permute-start.26 = (bf16[8,32,1024]{2,1,0:T(8,128)(2,1)}, bf16[8,32,1024]{2,1,0:T(8,128)(2,1)S(1)}, u32[]{:S(2)}, u32[]{:S(2)}) collective-permute-start(bf16[8,32,1024]{2,1,0:T(8,128)(2,1)} %collective-permute-done.22.refs_14_), channel_id=1, source_target_pairs={{0,4},{4,0},{1,5},{5,1},{2,6},{6,2},{3,7},{7,3},{8,12},{12,8},{9,1... | collective-permute-start | bytes 1572872 | tf_op jit(solution)/shard_map/ppermute | solution.py:26
  142.7 3.3 %collective-permute-start.27 = (bf16[8,32,1024]{2,1,0:T(8,128)(2,1)}, bf16[8,32,1024]{2,1,0:T(8,128)(2,1)S(1)}, u32[]{:S(2)}, u32[]{:S(2)}) collective-permute-start(bf16[8,32,1024]{2,1,0:T(8,128)(2,1)} %collective-permute-done.23.refs_15_), channel_id=1, source_target_pairs={{0,4},{4,0},{1,5},{5,1},{2,6},{6,2},{3,7},{7,3},{8,12},{12,8},{9,1... | collective-permute-start | bytes 1572872 | tf_op jit(solution)/shard_map/ppermute | solution.py:26
  163.6 8.9 %collective-permute-start.28 = (bf16[432,256]{1,0:T(8,128)(2,1)}, bf16[432,256]{1,0:T(8,128)(2,1)S(1)}, u32[]{:S(2)}, u32[]{:S(2)}) collective-permute-start(bf16[432,256]{1,0:T(8,128)(2,1)} %shard_map.93.refs_0_), channel_id=1, source_target_pairs={{0,1},{1,2},{2,3},{3,0},{4,5},{5,6},{6,7},{7,4},{8,9},{9,10},{10,1... | collective-permute-start | bytes 663560 | tf_op jit(solution)/shard_map/ppermute | solution.py:26
  165.8 37.8 %collective-permute-start.34 = (bf16[512,256]{1,0:T(8,128)(2,1)S(1)}, bf16[512,256]{1,0:T(8,128)(2,1)S(1)}, u32[]{:S(2)}, u32[]{:S(2)}) collective-permute-start(bf16[512,256]{1,0:T(8,128)(2,1)S(1)} %get-tuple-element.17), channel_id=1, source_target_pairs={{0,1},{1,2},{2,3},{3,0},{4,5},{5,6},{6,7},{7,4},{8,9},{9,10},{10,1... | collective-permute-start | bytes 786440 | tf_op jit(solution)/shard_map/ppermute | solution.py:26
  166.9 16.8 %collective-permute-start.29 = (bf16[432,256]{1,0:T(8,128)(2,1)}, bf16[432,256]{1,0:T(8,128)(2,1)S(1)}, u32[]{:S(2)}, u32[]{:S(2)}) collective-permute-start(bf16[432,256]{1,0:T(8,128)(2,1)} %shard_map.93.refs_0_), channel_id=1, source_target_pairs={{0,2},{1,3},{2,0},{3,1},{4,6},{5,7},{6,4},{7,5},{8,10},{9,11},{10,... | collective-permute-start | bytes 663560 | tf_op jit(solution)/shard_map/ppermute | solution.py:26
  169.4 14.4 %collective-permute-start.30 = (bf16[432,256]{1,0:T(8,128)(2,1)}, bf16[432,256]{1,0:T(8,128)(2,1)S(1)}, u32[]{:S(2)}, u32[]{:S(2)}) collective-permute-start(bf16[432,256]{1,0:T(8,128)(2,1)} %shard_map.93.refs_0_), channel_id=1, source_target_pairs={{0,3},{1,0},{2,1},{3,2},{4,7},{5,4},{6,5},{7,6},{8,11},{9,8},{10,9... | collective-permute-start | bytes 663560 | tf_op jit(solution)/shard_map/ppermute | solution.py:26
  171.4 34.9 %collective-permute-start.35 = (bf16[512,256]{1,0:T(8,128)(2,1)S(1)}, bf16[512,256]{1,0:T(8,128)(2,1)S(1)}, u32[]{:S(2)}, u32[]{:S(2)}) collective-permute-start(bf16[512,256]{1,0:T(8,128)(2,1)S(1)} %get-tuple-element.16), channel_id=1, source_target_pairs={{0,2},{1,3},{2,0},{3,1},{4,6},{5,7},{6,4},{7,5},{8,10},{9,11},{10,... | collective-permute-start | bytes 786440 | tf_op jit(solution)/shard_map/ppermute | solution.py:26
  172.5 33.7 %collective-permute-start.36 = (bf16[512,256]{1,0:T(8,128)(2,1)S(1)}, bf16[512,256]{1,0:T(8,128)(2,1)S(1)}, u32[]{:S(2)}, u32[]{:S(2)}) collective-permute-start(bf16[512,256]{1,0:T(8,128)(2,1)S(1)} %get-tuple-element.15), channel_id=1, source_target_pairs={{0,3},{1,0},{2,1},{3,2},{4,7},{5,4},{6,5},{7,6},{8,11},{9,8},{10,9... | collective-permute-start | bytes 786440 | tf_op jit(solution)/shard_map/ppermute | solution.py:26
  203.4 12.5 %collective-permute-start.31 = (bf16[400,256]{1,0:T(8,128)(2,1)}, bf16[400,256]{1,0:T(8,128)(2,1)S(1)}, u32[]{:S(2)}, u32[]{:S(2)}) collective-permute-start(bf16[400,256]{1,0:T(8,128)(2,1)} %shard_map.95.refs_0_), channel_id=1, source_target_pairs={{0,1},{1,2},{2,3},{3,0},{4,5},{5,6},{6,7},{7,4},{8,9},{9,10},{10,1... | collective-permute-start | bytes 614408 | tf_op jit(solution)/shard_map/ppermute | solution.py:26
  203.5 12.4 %collective-permute-start.32 = (bf16[400,256]{1,0:T(8,128)(2,1)}, bf16[400,256]{1,0:T(8,128)(2,1)S(1)}, u32[]{:S(2)}, u32[]{:S(2)}) collective-permute-start(bf16[400,256]{1,0:T(8,128)(2,1)} %shard_map.95.refs_0_), channel_id=1, source_target_pairs={{0,2},{1,3},{2,0},{3,1},{4,6},{5,7},{6,4},{7,5},{8,10},{9,11},{10,... | collective-permute-start | bytes 614408 | tf_op jit(solution)/shard_map/ppermute | solution.py:26
  203.6 12.3 %collective-permute-start.33 = (bf16[400,256]{1,0:T(8,128)(2,1)}, bf16[400,256]{1,0:T(8,128)(2,1)S(1)}, u32[]{:S(2)}, u32[]{:S(2)}) collective-permute-start(bf16[400,256]{1,0:T(8,128)(2,1)} %shard_map.95.refs_0_), channel_id=1, source_target_pairs={{0,3},{1,0},{2,1},{3,2},{4,7},{5,4},{6,5},{7,6},{8,11},{9,8},{10,9... | collective-permute-start | bytes 614408 | tf_op jit(solution)/shard_map/ppermute | solution.py:26
  (23 other events, 157.9 us)
Sparse Core Ops, SparseCore 0:
  17.8 97.5 all-gather.1
where the time goes:
time: 232 us; the launch traced here: 230 us
  starting transfers between devices  89 us (38%)
  waiting for transfers between devices  58.2 us (25%)
  Pallas kernels  48.9 us (21%)
  local copies, waits for them, and re-layouts  18.8 us (8%)
  between operations  13.8 us (6%)
    ppermute x35, starting transfers between devices, shifted(): return lax.ppermute(array, axis, [(i, (i + s) % n) for i in range(n)])  70.2 us
    ppermute x35, waiting for transfers between devices, shifted(): return lax.ppermute(array, axis, [(i, (i + s) % n) for i in range(n)])  49.6 us
    pallas_call x3, Pallas kernels, down(): pl.pallas_call(functools.partial(down_kernel, layer, last, len(streams),...  26.2 us
    pallas_call x3, Pallas kernels, up(): pl.pallas_call(functools.partial(up_kernel, layer, total, len(streams), n...  22.7 us
    all_to_all x2, starting transfers between devices, to_all(): return lax.all_to_all(copies, axis, split_axis=0, concat_axis=0, tiled=True)  11.7 us
    all_to_all x2, waiting for transfers between devices, to_all(): return lax.all_to_all(copies, axis, split_axis=0, concat_axis=0, tiled=True)  8.64 us
    unnamed x69, local copies, waits for them, and re-layouts  8.23 us
    ppermute x1, starting transfers between devices, program(): lax.ppermute(tokens[n_tok - halo:], SP, [(i, i + 1) for i in range(size -...  5.17 us
  transfers between devices with their start and end apart: 40, of which 16 were waited for; matrix products, arithmetic and copies ran while one was open for 6% of the time, Pallas kernels for 15%

commit v1 on v0

v1 whole, which is shorter than its diff:
```python
import functools

import jax
import jax.numpy as jnp
from jax import lax
from jax.experimental import pallas as pl
from jax.experimental.pallas import tpu as pltpu
from jax.sharding import Mesh
from jax.sharding import PartitionSpec as P


SP = ("z", "y", "c")
EDGE = 16
LANES = 128
norm_floor = 0.01
bf16, f32 = jnp.bfloat16, jnp.float32


def to_all(array, axis):
    copies = jnp.broadcast_to(array, (lax.axis_size(axis), *array.shape))
    return lax.all_to_all(copies, axis, split_axis=0, concat_axis=0, tiled=True)


def shifted(array, axis, s):
    n = lax.axis_size(axis)
    return lax.ppermute(array, axis, [(i, (i + s) % n) for i in range(n)])


def spread(array, axis):
    n = lax.axis_size(axis)
    pieces = {s: shifted(array, axis, s) for s in (n // 2, 1, n - 1)}
    return [array] + [pieces[s] for s in range(1, n)]


def swap(arrays):
    return [shifted(a, "c", 1) for a in arrays]


def after(arrays, *others):
    return lax.optimization_barrier((tuple(arrays), *others))[0]


def behind(position, s, n):
    return lax.rem(position + (n - s), n)


def by_rows(rows, work, step=64):
    def one(i, carry):
        work(pl.multiple_of(i * step, step), step)
        return carry

    lax.fori_loop(0, rows // step, one, 0)
    if rows % step:
        work(rows - rows % step, rows % step)


def up_kernel(layer, total, n_s, n_y, first_lane, info, *refs):
    streams, refs = refs[:n_s], refs[n_s:]
    gain, tap_ref, bias, ln_gain, ln_shift, refs = *refs[:5], refs[5:]
    pieces, refs = refs[:-7], refs[-7:]
    out, weights, normed, both, padded, columns, sems = refs
    rows, features = normed.shape
    width = streams[0].shape[-1]
    n_x = features // width
    keep = rows - 2 * EDGE
    ch = out.shape[-1]
    outs = [out] if len(out.shape) == 2 else [out.at[b] for b in range(n_x)]
    taps = tap_ref.shape[1]
    shift = EDGE - taps // 2
    core, my_x, my_y = info[0], info[1], info[2]

    if n_y:
        copies = []
        for i, piece in enumerate(pieces if len(pieces) > 2 else [p.at[q] for p in pieces for q in range(n_y)]):
            c = core if i < n_y else 1 - core
            rows_of = weights.at[:, behind(my_y, i % n_y, n_y), c]
            copies.append(pltpu.make_async_copy(piece, rows_of, sems.at[i]))
    else:
        copies = [pltpu.make_async_copy(pieces[0].at[:, pl.ds(first_lane, 2 * ch)], weights, sems.at[0])]
    for copy in copies:
        copy.start()

    def norm(first, step):
        here = pl.ds(first, step)
        squares = jnp.zeros((step, width), f32)
        for s in range(n_x):
            value = (streams[s][here] if n_s > 1 else streams[0][s, here]).astype(f32)
            squares += value * value
        mean = jnp.sum(squares, axis=-1, keepdims=True) * (1.0 / features)
        scale = lax.rsqrt(mean + norm_floor)
        for s in range(n_x):
            b = behind(my_x, s, n_x) if n_s > 1 else s
            wide = pl.ds(pl.multiple_of(b * width, width), width)
            value = (streams[s][here] if n_s > 1 else streams[0][s, here]).astype(f32)
            normed[here, wide] = (value * scale * gain[layer : layer + 1, wide]).astype(bf16)

    by_rows(rows, norm)
    for copy in copies:
        copy.wait()
    for half in range(2):
        part = weights[..., half * ch : (half + 1) * ch].reshape(features, ch)
        both[half] = jnp.dot(normed[...], part, preferred_element_type=f32)

    def gate(first, step):
        here = pl.ds(first, step)
        gated = both[0, here] * jax.nn.sigmoid(both[1, here])
        t = info[3 + layer] + first + lax.broadcasted_iota(jnp.int32, (step, 1), 0)
        gated = jnp.where((t >= 0) & (t < total), gated, 0.0).astype(bf16)
        padded[here] = gated.astype(f32)

    by_rows(rows, gate)
    columns[pl.ds(keep, 2 * ch - keep)] = jnp.zeros((2 * ch - keep, LANES), f32)

    def filtered(first, size):
        window = size + 2 * EDGE
        accs = []
        for start in range(0, ch, LANES):
            lanes = slice(start, start + LANES)
            win = padded[pl.ds(first, window), lanes]
            acc = jnp.zeros((size, LANES), f32) + bias[layer : layer + 1, lanes]
            for r in range(8):
                turned = pltpu.roll(win, window - r, 0) if r else win
                for q in range(window // 8):
                    k = 8 * q + r - shift
                    if 0 <= k < taps:
                        acc = acc + tap_ref[layer, k : k + 1, lanes] * turned[8 * q : 8 * q + size]
            accs.append(acc)
        mean = jnp.sum(sum(accs), axis=-1, keepdims=True) * (1.0 / ch)
        for start, acc in zip(range(0, ch, LANES), accs):
            for to in outs:
                to[pl.ds(first, size), start : start + LANES] = (acc - mean).astype(bf16)
        high = mean.astype(bf16).astype(f32)
        lane = lax.broadcasted_iota(jnp.int32, (size, LANES), 1)
        columns[pl.ds(first, size)] = jnp.where(lane == 0, high, jnp.where(lane == 1, mean - high, 0.0))

    by_rows(keep, filtered)
    across = columns[...].T[:8]
    params = jnp.concatenate([ln_gain[layer : layer + 1, :], ln_shift[layer : layer + 1, :]], axis=1)
    row = lax.broadcasted_iota(jnp.int32, across.shape, 0)
    for p in range(3):
        part = params.astype(bf16).astype(f32)
        across = jnp.where(row == 2 + p, part, across)
        params = params - part
    tail = jnp.concatenate([across[:, :ch], across[:, ch:]], axis=0).astype(bf16)
    for to in outs:
        to[keep:] = tail


def down_kernel(last, n_s, n_y, n_x, n_g, first_lane, info, *refs):
    gated, refs = refs[:n_g], refs[n_g:]
    streams, refs = refs[:n_s], refs[n_s:]
    pieces, refs = refs[:-5], refs[-5:]
    out, weights, act, columns, sems = refs
    core, my_x, my_y = info[0], info[1], info[2]
    if n_g == 1:
        gated = [gated[0].at[behind(my_x, s, n_x)] for s in range(n_x)]
    rows, ch = gated[0].shape
    keep = rows - EDGE
    width = out.shape[-1]

    copies = []

    def fetch(source, to):
        copies.append(pltpu.make_async_copy(source, to, sems.at[len(copies)]))

    if n_y:
        for i, piece in enumerate(pieces):
            c = core if i < n_y else 1 - core
            fetch(piece, weights.at[:, behind(my_y, i % n_y, n_y), c])
    elif last:
        mine = pl.ds(pl.multiple_of(my_x * width, width), width)
        fetch(pieces[0].at[mine, pl.ds(first_lane, ch)], weights.at[:, pl.ds(0, ch)])
        for s in range(1, n_x):
            fetch(pieces[s], weights.at[:, pl.ds(s * ch, ch)])
    else:
        fetch(pieces[0].at[:, pl.ds(first_lane, n_x * ch)], weights)
    for copy in copies:
        copy.start()

    spans = []
    for s in range(n_x):
        tail = gated[s][keep:].astype(f32)
        spans.append(jnp.concatenate([tail[:8], tail[8:]], axis=1))
    params = [sum(v[2 + p : 3 + p] for p in range(3)) for v in spans]
    spans.append(jnp.zeros((LANES - 8 * n_x, 2 * ch), f32))
    columns[...] = jnp.concatenate(spans, axis=0).T

    def activate(first, size):
        here = pl.ds(first, size)
        cols = columns[here]
        means = [cols[:, 8 * s : 8 * s + 1] + cols[:, 8 * s + 1 : 8 * s + 2] for s in range(n_x)]
        average = sum(means) * (1.0 / n_x)
        squares = jnp.zeros((size, ch), f32)
        for s in range(n_x):
            value = gated[s][here].astype(f32) + (means[s] - average)
            squares += value * value
        mean = jnp.sum(squares, axis=-1, keepdims=True) * (1.0 / (n_x * ch))
        scale = lax.rsqrt(mean + norm_floor)
        for s in range(n_x):
            value = (gated[s][here].astype(f32) + (means[s] - average)) * scale
            value = value * params[s][:, :ch] + params[s][:, ch:]
            act[here, s * ch : (s + 1) * ch] = (value * jax.nn.sigmoid(value)).astype(bf16)

    by_rows(keep, activate)
    for copy in copies:
        copy.wait()
    dims = (((1,), (1,)), ((), ()))
    inner = slice(EDGE, EDGE + keep)
    if last:
        added = lax.dot_general(act[...], weights[...], dims, preferred_element_type=f32)
        out[...] = (streams[0][my_x, inner].astype(f32) + added).astype(bf16)
    else:
        part_rows = weights.shape[0] // n_x

        def block(b, base):
            part = weights[pl.ds(b * part_rows, part_rows)].reshape(width, n_x * ch)
            added = lax.dot_general(act[...], part, dims, preferred_element_type=f32)
            out[b] = (base.astype(f32) + added).astype(bf16)

        if n_s > 1:
            for s in range(n_x):
                block(behind(my_x, s, n_x), streams[s][inner])
        else:
            lax.fori_loop(0, n_x, lambda b, carry: (block(b, streams[0][b, inner]), carry)[1], 0)


def vmem():
    return pl.BlockSpec(memory_space=pltpu.VMEM)


def hbm():
    return pl.BlockSpec(memory_space=pltpu.HBM)


def smem():
    return pl.BlockSpec(memory_space=pltpu.SMEM)


def up(layer, total, info, streams, params, pieces, ch, fan, first_lane=0):
    rows, width = streams[0].shape[-2:]
    n_x = params[0].shape[1] // width
    keep = rows - 2 * EDGE
    n_y, shape = 0, (n_x * width,)
    if len(pieces) > 1:
        n_z, n_i, _ = pieces[0].shape[-3:]
        n_y = pieces[0].shape[0] if len(pieces) == 2 else len(pieces) // 2
        shape = (n_z, n_y, 2, n_i)
    return pl.pallas_call(
        functools.partial(up_kernel, layer, total, len(streams), n_y, first_lane),
        out_shape=jax.ShapeDtypeStruct((n_x, keep + EDGE, ch) if fan else (keep + EDGE, ch), bf16),
        in_specs=[smem()] + [vmem()] * (len(streams) + len(params)) + [hbm()] * len(pieces),
        out_specs=vmem(),
        scratch_shapes=[
            pltpu.VMEM((*shape, 2 * ch), bf16),
            pltpu.VMEM((rows, n_x * width), bf16),
            pltpu.VMEM((2, rows, ch), f32),
            pltpu.VMEM((rows, ch), f32),
            pltpu.VMEM((2 * ch, LANES), f32),
            pltpu.SemaphoreType.DMA((max(1, 2 * n_y),)),
        ],
    )(info, *streams, *params, *pieces)


def down(last, info, gated, streams, pieces, paired, first_lane=0):
    rows, ch = gated[0].shape[-2:]
    n_x = lax.axis_size("x")
    keep = rows - EDGE
    width = streams[0].shape[-1]
    n_y = len(pieces) // 2 if paired else 0
    shape = (width if last else n_x * width,)
    if paired:
        n_z, n_i, _ = pieces[0].shape
        shape = (n_z, n_y, 2, n_i)
    out_shape = (keep, width) if last else (n_x, keep, width)
    return pl.pallas_call(
        functools.partial(down_kernel, last, len(streams), n_y, n_x, len(gated), first_lane),
        out_shape=jax.ShapeDtypeStruct(out_shape, bf16),
        in_specs=[smem()] + [vmem()] * (len(gated) + len(streams)) + [hbm()] * len(pieces),
        out_specs=vmem(),
        scratch_shapes=[
            pltpu.VMEM((*shape, n_x * ch), bf16),
            pltpu.VMEM((keep, n_x * ch), bf16),
            pltpu.VMEM((2 * ch, LANES), f32),
            pltpu.SemaphoreType.DMA((len(pieces),)),
        ],
    )(info, *gated, *streams, *pieces)


def program(tokens, norm_gain, w_value, w_gate, conv_taps, conv_bias, ln_gain, ln_shift, w_out):
    layers, _, ch = w_value.shape
    n_x = lax.axis_size("x")
    my_x = lax.axis_index("x")
    n_tok, f_loc = tokens.shape
    halo = EDGE * layers
    size = lax.axis_size(SP)
    total = size * n_tok
    place = lax.axis_index(SP) * n_tok
    info = jnp.stack(
        [lax.axis_index("c"), my_x, lax.axis_index("y")]
        + [place - EDGE * (layers - l) for l in range(layers)]
    ).astype(jnp.int32)
    params = (norm_gain, conv_taps, conv_bias, ln_gain, ln_shift)

    def gather_z(array):
        return to_all(array, "z")

    near = 2
    ups = [gather_z(jnp.concatenate([w_value[l], w_gate[l]], axis=1)) for l in range(near)]

    out_t = jnp.swapaxes(w_out, 1, 2)
    wide = jnp.concatenate(spread(out_t[: layers - 1], "x"), axis=-1)

    packs, lanes, at = [], [(0, 0)], 0
    for l in range(1, layers):
        pair = [w_value[l], w_gate[l]] if l >= near else []
        packs += [*pair, out_t[l] if l == layers - 1 else wide[l]]
        lanes.append((at, at + sum(a.shape[1] for a in pair)))
        at = lanes[-1][1] + packs[-1].shape[1]
    rest = lax.all_gather(jnp.concatenate(packs, axis=1), SP, axis=0, tiled=True)

    before = lax.ppermute(tokens[n_tok - halo :], SP, [(i, i + 1) for i in range(size - 1)])
    following = lax.ppermute(tokens[:halo], SP, [(i + 1, i) for i in range(size - 1)])
    streams = spread(jnp.concatenate([before, tokens, following], axis=0), "x")

    ups = [spread(a, "y") for a in ups]
    out_first = spread(gather_z(wide[0]), "y")

    for l in range(layers):
        last = l == layers - 1
        first, start = lanes[l]
        pieces = [rest]
        if l < near:
            pieces = [jnp.stack(after(ups[l], stream))] if l else ups[l]
            pieces = [*pieces, *swap(pieces)]
        gated = up(l, total, info, streams, params, pieces, ch, l > 0, first)
        if l:
            gated = [lax.all_to_all(gated, "x", split_axis=0, concat_axis=0, tiled=True)]
        else:
            gated = spread(gated, "x")
        pieces = [rest]
        if l == 0:
            pieces = after(out_first, *gated[1:])
            pieces = [*pieces, *swap(pieces)]
        if last:
            for s in (1, n_x // 2, n_x - 1):
                row = lax.rem(my_x + s, n_x) * f_loc
                block = lax.dynamic_slice(rest, (row, start), (f_loc, ch))
                pieces.append(shifted(block, "x", s))
        stream = down(last, info, gated, streams, pieces, l == 0, start)
        streams = [stream]
    return stream


def solution(mesh):
    torus = Mesh(mesh.devices.reshape(8, 4, 2, mesh.shape["tp"]), ("z", "y", "c", "x"))
    return jax.shard_map(
        program,
        mesh=torus,
        in_specs=(
            P(SP, "x"),
            P(),
            P(None, SP, "x"),
            P(None, SP, "x"),
            P(None, None, "x"),
            P(None, "x"),
            P(None, "x"),
            P(None, "x"),
            P(None, "x", SP),
        ),
        out_specs=P(SP, "x"),
        check_vma=False,
    )
```

time: 232 us -> 235 us (1.013)
  the two profiles are of different devices: /device:TPU:1 before, /device:TPU:24 now
where the time goes in v1:
time: 235 us; the launch traced here: 234 us
  waiting for transfers between devices  72.2 us (31%)
  starting transfers between devices  68.9 us (29%)
  Pallas kernels  45.4 us (19%)
  blocking collectives  18.2 us (8%)
  between operations  13.7 us (6%)
  local copies, waits for them, and re-layouts  13.3 us (6%)
  other arithmetic  2.47 us (1%)
    ppermute x30, waiting for transfers between devices, shifted(): return lax.ppermute(array, axis, [(i, (i + s) % n) for i in range(n)])  57.8 us
    ppermute x30, starting transfers between devices, shifted(): return lax.ppermute(array, axis, [(i, (i + s) % n) for i in range(n)])  39.4 us
    pallas_call x3, Pallas kernels, down(): pl.pallas_call(functools.partial(down_kernel, last, len(streams), n_y, n_...  23.6 us
    pallas_call x3, Pallas kernels, up(): pl.pallas_call(functools.partial(up_kernel, layer, total, len(streams), n...  21.8 us
    all_to_all x3, starting transfers between devices, to_all(): return lax.all_to_all(copies, axis, split_axis=0, concat_axis=0, tiled=True)  20.4 us
    all_to_all x1, blocking collectives, program(): lax.all_to_all(gated, 'x', split_axis=0, concat_axis=0, tiled=True)  18.2 us
    all_to_all x3, waiting for transfers between devices, to_all(): return lax.all_to_all(copies, axis, split_axis=0, concat_axis=0, tiled=True)  13.7 us
    unnamed x42, local copies, waits for them, and re-layouts  5.35 us
  transfers between devices with their start and end apart: 37, of which 15 were waited for; matrix products, arithmetic and copies ran while one was open for 4% of the time, Pallas kernels for 10%

profile of v1, /device:TPU:24, one launch (start us, length us, event | category | flops | bytes accessed | tf_op | source)
XLA Modules:
  0.0 234.2 jit_solution(9005929029471655150)
XLA Ops:
  7.3 1.5 collective-permute-start.15
  8.8 2.7 %collective-permute-start.16 = (bf16[2,32,256]{2,1,0:T(8,128)(2,1)S(1)}, bf16[2,32,256]{2,1,0:T(8,128)(2,1)S(1)}, u32[]{:S(2)}, u32[]{:S(2)}) collective-permute-start(bf16[2,32,256]{2,1,0:T(8,128)(2,1)S(1)} %slice.48), channel_id=1, source_target_pairs={{0,2},{1,3},{2,0},{3,1},{4,6},{5,7},{6,4},{7,5},{8,10},{9,11},{10,... | collective-permute-start | bytes 98312 | tf_op jit(solution)/shard_map/ppermute | solution.py:26
  11.5 1.4 collective-permute-start.17
  13.0 1.4 slice_bitcast_fusion.3
  16.9 8.5 %all-to-all-start = ((bf16[8,32,512]{2,1,0:T(8,128)(2,1)}), bf16[8,32,512]{2,1,0:T(8,128)(2,1)S(1)}, u32[]{:S(2)}, u32[]{:S(2)}) async-start(bf16[8,32,512]{2,1,0:T(8,128)(2,1)} %broadcast_in_dim.9), calls=%async_computation | async-start | bytes 524288 | tf_op jit(solution)/shard_map/all_to_all | solution.py:21
  26.2 1.9 collective-permute-start
  28.1 3.6 %collective-permute-start.1 = (bf16[48,512]{1,0:T(8,128)(2,1)S(1)}, bf16[48,512]{1,0:T(8,128)(2,1)S(1)}, u32[]{:S(2)}, u32[]{:S(2)}) collective-permute-start(bf16[48,512]{1,0:T(8,128)(2,1)S(1)} %get-tuple-element.24), channel_id=1, source_target_pairs={{4,0},{8,4},{12,8},{16,12},{20,16},{24,20},{28,24},{32,28},{36,32}... | collective-permute-start | bytes 147464 | tf_op jit(solution)/shard_map/ppermute | solution.py:322
  31.8 1.0 constant_dynamic-update-slice_fusion.1
  34.2 2.2 all-to-all-done.refs_9_
  37.3 5.1 %all-to-all-start.1 = ((bf16[8,32,1024]{2,1,0:T(8,128)(2,1)}), bf16[8,32,1024]{2,1,0:T(8,128)(2,1)S(1)}, u32[]{:S(2)}, u32[]{:S(2)}) async-start(bf16[8,32,1024]{2,1,0:T(8,128)(2,1)} %broadcast_in_dim.10), calls=%async_computation.1 | async-start | bytes 1048576 | tf_op jit(solution)/shard_map/all_to_all | solution.py:21
  42.4 3.4 %collective-permute-start.3 = (bf16[480,512]{1,0:T(8,128)(2,1)S(1)}, bf16[480,512]{1,0:T(8,128)(2,1)S(1)}, u32[]{:S(2)}, u32[]{:S(2)}) collective-permute-start(bf16[480,512]{1,0:T(8,128)(2,1)S(1)} %constant_dynamic-update-slice_fusion.refs_0_.refs_4_), channel_id=1, source_target_pairs={{0,2},{1,3},{2,0},{3,1},{4,6},{5,7},{6,4},{7,5},{8,10},{9,11},{10,... | collective-permute-start | bytes 1474568 | tf_op jit(solution)/shard_map/ppermute | solution.py:26
  45.7 1.2 collective-permute-start.6
  47.0 3.2 %collective-permute-start.7 = (bf16[8,32,512]{2,1,0:T(8,128)(2,1)S(1)}, bf16[8,32,512]{2,1,0:T(8,128)(2,1)}, u32[]{:S(2)}, u32[]{:S(2)}) collective-permute-start(bf16[8,32,512]{2,1,0:T(8,128)(2,1)S(1)} %all-to-all-done.refs_9_), channel_id=1, source_target_pairs={{0,24},{8,0},{16,8},{24,16},{1,25},{9,1},{17,9},{25,17},{2,26},{10... | collective-permute-start | bytes 786440 | tf_op jit(solution)/shard_map/ppermute | solution.py:26
  50.2 7.7 %collective-permute-done.3.refs_2_.refs_6_ = bf16[480,512]{1,0:T(8,128)(2,1)S(1)} collective-permute-done((bf16[480,512]{1,0:T(8,128)(2,1)S(1)}, bf16[480,512]{1,0:T(8,128)(2,1)S(1)}, u32[]{:S(2)}, u32[]{:S(2)}) %collective-permute-start.3) | collective-permute-done | bytes 491552 | tf_op jit(solution)/shard_map/ppermute | solution.py:26
  58.0 2.3 %collective-permute-start.8 = (bf16[8,32,512]{2,1,0:T(8,128)(2,1)S(1)}, bf16[8,32,512]{2,1,0:T(8,128)(2,1)}, u32[]{:S(2)}, u32[]{:S(2)}) collective-permute-start(bf16[8,32,512]{2,1,0:T(8,128)(2,1)S(1)} %all-to-all-done.refs_9_), channel_id=1, source_target_pairs={{0,4},{4,0},{1,5},{5,1},{2,6},{6,2},{3,7},{7,3},{8,12},{12,8},{9,1... | collective-permute-start | bytes 786440 | tf_op jit(solution)/shard_map/ppermute | solution.py:26
  60.4 1.7 collective-permute-done.7.refs_12_
  62.6 4.6 %collective-permute-done.4.refs_3_.refs_7_ = bf16[480,512]{1,0:T(8,128)(2,1)S(1)} collective-permute-done((bf16[480,512]{1,0:T(8,128)(2,1)S(1)}, bf16[480,512]{1,0:T(8,128)(2,1)S(1)}, u32[]{:S(2)}, u32[]{:S(2)}) %collective-permute-start.4) | collective-permute-done | bytes 491552 | tf_op jit(solution)/shard_map/ppermute | solution.py:26
  67.2 2.0 collective-permute-start.18
  69.3 1.9 collective-permute-start.19
  71.9 7.3 %shard_map.91.refs_0_ = bf16[464,256]{1,0:T(8,128)(2,1)} custom-call(s32[6]{0:T(128)} %stack.42.info, bf16[480,512]{1,0:T(8,128)(2,1)} %copy-done.2, bf16[480,512]{1,0:T(8,128)(2,1)} %copy-done.4, bf16[480,512]{1,0:T(8,128)(2,1)} %copy-done.5, bf16[480,512]{1,0:T(8,128)(2,1)} %copy-done.6, f32[3,2048]{1,0:T(4,128)} %refs_1_.3, f32[3,31,256]{2,1,0:T(8,128)} %refs_2_.3, ...), custom_call_target="tpu_custom_call" | custom-call | tf_op jit(solution)/shard_map/pallas_call | solution.py:248
  79.2 1.1 collective-permute-start.12
  80.3 3.1 %collective-permute-start.13 = (bf16[464,256]{1,0:T(8,128)(2,1)}, bf16[464,256]{1,0:T(8,128)(2,1)S(1)}, u32[]{:S(2)}, u32[]{:S(2)}) collective-permute-start(bf16[464,256]{1,0:T(8,128)(2,1)} %shard_map.91.refs_0_), channel_id=1, source_target_pairs={{0,2},{1,3},{2,0},{3,1},{4,6},{5,7},{6,4},{7,5},{8,10},{9,11},{10,... | collective-permute-start | bytes 712712 | tf_op jit(solution)/shard_map/ppermute | solution.py:26
  83.4 5.1 %collective-permute-done.12.refs_1_ = bf16[464,256]{1,0:T(8,128)(2,1)S(1)} collective-permute-done((bf16[464,256]{1,0:T(8,128)(2,1)}, bf16[464,256]{1,0:T(8,128)(2,1)S(1)}, u32[]{:S(2)}, u32[]{:S(2)}) %collective-permute-start.12) | collective-permute-done | bytes 237600 | tf_op jit(solution)/shard_map/ppermute | solution.py:26
  88.5 2.3 collective-permute-start.14
  90.8 3.0 %collective-permute-done.13.refs_2_ = bf16[464,256]{1,0:T(8,128)(2,1)S(1)} collective-permute-done((bf16[464,256]{1,0:T(8,128)(2,1)}, bf16[464,256]{1,0:T(8,128)(2,1)S(1)}, u32[]{:S(2)}, u32[]{:S(2)}) %collective-permute-start.13) | collective-permute-done | bytes 237600 | tf_op jit(solution)/shard_map/ppermute | solution.py:26
  93.8 1.0 collective-permute-done.14.refs_3_
  95.5 12.6 %collective-permute-done.20.refs_11_ = bf16[8,32,1024]{2,1,0:T(8,128)(2,1)} collective-permute-done((bf16[8,32,1024]{2,1,0:T(8,128)(2,1)S(1)}, bf16[8,32,1024]{2,1,0:T(8,128)(2,1)}, u32[]{:S(2)}, u32[]{:S(2)}) %collective-permute-start.20) | collective-permute-done | bytes 524320 | tf_op jit(solution)/shard_map/ppermute | solution.py:26
  110.1 6.9 %all-to-all-start.2 = ((bf16[8,32,512]{2,1,0:T(8,128)(2,1)}), bf16[8,32,512]{2,1,0:T(8,128)(2,1)S(1)}, u32[]{:S(2)}, u32[]{:S(2)}) async-start(bf16[8,32,512]{2,1,0:T(8,128)(2,1)} %broadcast_in_dim.11), calls=%async_computation.2 | async-start | bytes 524288 | tf_op jit(solution)/shard_map/all_to_all | solution.py:21
  117.4 11.5 %all-to-all-done.2 = bf16[8,32,512]{2,1,0:T(8,128)(2,1)S(1)} async-done(((bf16[8,32,512]{2,1,0:T(8,128)(2,1)}), bf16[8,32,512]{2,1,0:T(8,128)(2,1)S(1)}, u32[]{:S(2)}, u32[]{:S(2)}) %all-to-all-start.2) | async-done | bytes 262176 | tf_op jit(solution)/shard_map/all_to_all | solution.py:21
  129.0 3.2 %collective-permute-start.25 = (bf16[8,32,512]{2,1,0:T(8,128)(2,1)S(1)}, bf16[8,32,512]{2,1,0:T(8,128)(2,1)S(1)}, u32[]{:S(2)}, u32[]{:S(2)}) collective-permute-start(bf16[8,32,512]{2,1,0:T(8,128)(2,1)S(1)} %all-to-all-done.2), channel_id=1, source_target_pairs={{0,8},{8,16},{16,24},{24,0},{1,9},{9,17},{17,25},{25,1},{2,10},{10... | collective-permute-start | bytes 786440 | tf_op jit(solution)/shard_map/ppermute | solution.py:26
  132.2 1.3 collective-permute-start.26
  134.5 8.7 %shard_map.92.refs_0_.refs_1_ = bf16[4,448,512]{2,1,0:T(8,128)(2,1)} custom-call(s32[6]{0:T(128)} %stack.42.info, bf16[464,256]{1,0:T(8,128)(2,1)} %shard_map.91.refs_0_, bf16[464,256]{1,0:T(8,128)(2,1)} %copy-done.17, bf16[464,256]{1,0:T(8,128)(2,1)} %copy-done.18, bf16[464,256]{1,0:T(8,128)(2,1)} %copy-done.19, bf16[480,512]{1,0:T(8,128)(2,1)} %copy-done.2, ...), custom_call_target="tpu_custom_call" | custom-call | tf_op jit(solution)/shard_map/pallas_call | solution.py:275
  143.2 2.9 %collective-permute-done.27 = bf16[8,32,512]{2,1,0:T(8,128)(2,1)} collective-permute-done((bf16[8,32,512]{2,1,0:T(8,128)(2,1)S(1)}, bf16[8,32,512]{2,1,0:T(8,128)(2,1)}, u32[]{:S(2)}, u32[]{:S(2)}) %collective-permute-start.27) | collective-permute-done | bytes 262176 | tf_op jit(solution)/shard_map/ppermute | solution.py:26
  146.1 1.1 pad_maximum_fusion.refs_6_
  147.3 2.6 %collective-permute-done.28.refs_7_ = bf16[4,8,32,512]{3,2,1,0:T(8,128)(2,1)S(1)} collective-permute-done((bf16[4,8,32,512]{3,2,1,0:T(8,128)(2,1)S(1)}, bf16[4,8,32,512]{3,2,1,0:T(8,128)(2,1)S(1)}, u32[]{:S(2)}, u32[]{:S(2)}) %collective-permute-start.28) | collective-permute-done | bytes 1048608 | tf_op jit(solution)/shard_map/ppermute | solution.py:26
  149.9 1.0 copy-done.7
  150.9 7.4 %shard_map.93 = bf16[4,432,256]{2,1,0:T(8,128)(2,1)} custom-call(s32[6]{0:T(128)} %stack.42.info, bf16[4,448,512]{2,1,0:T(8,128)(2,1)} %shard_map.92.refs_0_.refs_1_, f32[3,2048]{1,0:T(4,128)} %refs_1_.3, f32[3,31,256]{2,1,0:T(8,128)} %refs_2_.3, f32[3,256]{1,0:T(4,128)} %refs_3_.3, f32[3,256]{1,0:T(4,128)} %refs_4_.5, f32[3,256]{1,0:T(4,128)} %refs_5_.5, ...), custom_call_target="tpu_custom_call" | custom-call | tf_op jit(solution)/shard_map/pallas_call | solution.py:248
  158.3 18.2 %all_to_all.25.refs_0_ = bf16[4,432,256]{2,1,0:T(8,128)(2,1)} all-to-all(bf16[4,432,256]{2,1,0:T(8,128)(2,1)} %shard_map.93), channel_id=1, replica_groups=mesh['z'=8,'y'=4,'c'=2,'x'=4] {'x'}, dimensions={0} | all-to-all | bytes 1769472 | tf_op jit(solution)/shard_map/all_to_all | solution.py:337
  176.5 8.9 %shard_map.94.refs_0_.refs_1_ = bf16[4,416,512]{2,1,0:T(8,128)(2,1)} custom-call(s32[6]{0:T(128)} %stack.42.info, bf16[4,432,256]{2,1,0:T(8,128)(2,1)} %all_to_all.25.refs_0_, bf16[4,448,512]{2,1,0:T(8,128)(2,1)} %shard_map.92.refs_0_.refs_1_, bf16[2048,1792]{1,0:T(8,128)(2,1)} %all-gather.2.cloned.1.call-done.refs_2_.refs_6_), custom_call_target="tpu_custom_call" | custom-call | tf_op jit(solution)/shard_map/pallas_call | solution.py:275
  185.4 7.1 %shard_map.95 = bf16[4,400,256]{2,1,0:T(8,128)(2,1)} custom-call(s32[6]{0:T(128)} %stack.42.info, bf16[4,416,512]{2,1,0:T(8,128)(2,1)} %shard_map.94.refs_0_.refs_1_, f32[3,2048]{1,0:T(4,128)} %refs_1_.3, f32[3,31,256]{2,1,0:T(8,128)} %refs_2_.3, f32[3,256]{1,0:T(4,128)} %refs_3_.3, f32[3,256]{1,0:T(4,128)} %refs_4_.5, f32[3,256]{1,0:T(4,128)} %refs_5_.5, ...), custom_call_target="tpu_custom_call" | custom-call | tf_op jit(solution)/shard_map/pallas_call | solution.py:248
  192.5 3.5 %all-to-all-start.4 = ((bf16[4,400,256]{2,1,0:T(8,128)(2,1)}), bf16[4,400,256]{2,1,0:T(8,128)(2,1)S(1)}, u32[]{:S(2)}, u32[]{:S(2)}) async-start(bf16[4,400,256]{2,1,0:T(8,128)(2,1)} %shard_map.95), calls=%async_computation.4 | async-start | bytes 1638400 | tf_op jit(solution)/shard_map/all_to_all | solution.py:337
  196.0 1.2 constant_dynamic-slice_fusion
  197.2 2.0 collective-permute-start.29
  199.2 2.7 %collective-permute-start.30 = (bf16[512,256]{1,0:T(8,128)(2,1)S(1)}, bf16[512,256]{1,0:T(8,128)(2,1)S(1)}, u32[]{:S(2)}, u32[]{:S(2)}) collective-permute-start(bf16[512,256]{1,0:T(8,128)(2,1)S(1)} %get-tuple-element.22), channel_id=1, source_target_pairs={{0,2},{1,3},{2,0},{3,1},{4,6},{5,7},{6,4},{7,5},{8,10},{9,11},{10,... | collective-permute-start | bytes 786440 | tf_op jit(solution)/shard_map/ppermute | solution.py:26
  201.9 1.5 collective-permute-start.31
  203.4 11.6 %collective-permute-done.29.refs_3_ = bf16[512,256]{1,0:T(8,128)(2,1)S(1)} collective-permute-done((bf16[512,256]{1,0:T(8,128)(2,1)S(1)}, bf16[512,256]{1,0:T(8,128)(2,1)S(1)}, u32[]{:S(2)}, u32[]{:S(2)}) %collective-permute-start.29) | collective-permute-done | bytes 262176 | tf_op jit(solution)/shard_map/ppermute | solution.py:26
  215.0 4.6 %collective-permute-done.30.refs_4_ = bf16[512,256]{1,0:T(8,128)(2,1)S(1)} collective-permute-done((bf16[512,256]{1,0:T(8,128)(2,1)S(1)}, bf16[512,256]{1,0:T(8,128)(2,1)S(1)}, u32[]{:S(2)}, u32[]{:S(2)}) %collective-permute-start.30) | collective-permute-done | bytes 262176 | tf_op jit(solution)/shard_map/ppermute | solution.py:26
  221.3 6.0 %shard_map.96 = bf16[384,512]{1,0:T(8,128)(2,1)} custom-call(s32[6]{0:T(128)} %stack.42.info, bf16[4,400,256]{2,1,0:T(8,128)(2,1)} %copy-done.1, bf16[4,416,512]{2,1,0:T(8,128)(2,1)} %shard_map.94.refs_0_.refs_1_, bf16[2048,1792]{1,0:T(8,128)(2,1)} %all-gather.2.cloned.1.call-done.refs_2_.refs_6_, bf16[512,256]{1,0:T(8,128)(2,1)} %copy-done.13, ...), custom_call_target="tpu_custom_call" | custom-call | tf_op jit(solution)/shard_map/pallas_call | solution.py:275
  (92 shorter events, 13.7 us)
Async XLA Ops:
  6.5 170.0 %all-gather.2.cloned.1.call-start = ((), (), s32[]{:S(2)}) async-start(), calls=%async_computation.5 | async-start | bytes 7454720 | tf_op jit(solution)/shard_map/all_gather | solution.py:319
  7.3 7.8 %collective-permute-start.15 = (bf16[2,32,256]{2,1,0:T(8,128)(2,1)S(1)}, bf16[2,32,256]{2,1,0:T(8,128)(2,1)S(1)}, u32[]{:S(2)}, u32[]{:S(2)}) collective-permute-start(bf16[2,32,256]{2,1,0:T(8,128)(2,1)S(1)} %slice.48), channel_id=1, source_target_pairs={{0,1},{1,2},{2,3},{3,0},{4,5},{5,6},{6,7},{7,4},{8,9},{9,10},{10,1... | collective-permute-start | bytes 98312 | tf_op jit(solution)/shard_map/ppermute | solution.py:26
  8.8 6.3 %collective-permute-start.16 = (bf16[2,32,256]{2,1,0:T(8,128)(2,1)S(1)}, bf16[2,32,256]{2,1,0:T(8,128)(2,1)S(1)}, u32[]{:S(2)}, u32[]{:S(2)}) collective-permute-start(bf16[2,32,256]{2,1,0:T(8,128)(2,1)S(1)} %slice.48), channel_id=1, source_target_pairs={{0,2},{1,3},{2,0},{3,1},{4,6},{5,7},{6,4},{7,5},{8,10},{9,11},{10,... | collective-permute-start | bytes 98312 | tf_op jit(solution)/shard_map/ppermute | solution.py:26
  11.5 3.9 %collective-permute-start.17 = (bf16[2,32,256]{2,1,0:T(8,128)(2,1)S(1)}, bf16[2,32,256]{2,1,0:T(8,128)(2,1)S(1)}, u32[]{:S(2)}, u32[]{:S(2)}) collective-permute-start(bf16[2,32,256]{2,1,0:T(8,128)(2,1)S(1)} %slice.48), channel_id=1, source_target_pairs={{0,3},{1,0},{2,1},{3,2},{4,7},{5,4},{6,5},{7,6},{8,11},{9,8},{10,9... | collective-permute-start | bytes 98312 | tf_op jit(solution)/shard_map/ppermute | solution.py:26
  16.9 19.5 %all-to-all-start = ((bf16[8,32,512]{2,1,0:T(8,128)(2,1)}), bf16[8,32,512]{2,1,0:T(8,128)(2,1)S(1)}, u32[]{:S(2)}, u32[]{:S(2)}) async-start(bf16[8,32,512]{2,1,0:T(8,128)(2,1)} %broadcast_in_dim.9), calls=%async_computation | async-start | bytes 524288 | tf_op jit(solution)/shard_map/all_to_all | solution.py:21
  26.2 5.6 %collective-permute-start = (bf16[48,512]{1,0:T(8,128)(2,1)S(1)}, bf16[48,512]{1,0:T(8,128)(2,1)S(1)}, u32[]{:S(2)}, u32[]{:S(2)}) collective-permute-start(bf16[48,512]{1,0:T(8,128)(2,1)S(1)} %get-tuple-element.25), channel_id=1, source_target_pairs={{0,4},{4,8},{8,12},{12,16},{16,20},{20,24},{24,28},{28,32},{32,36}... | collective-permute-start | bytes 147464 | tf_op jit(solution)/shard_map/ppermute | solution.py:321
  28.1 5.4 %collective-permute-start.1 = (bf16[48,512]{1,0:T(8,128)(2,1)S(1)}, bf16[48,512]{1,0:T(8,128)(2,1)S(1)}, u32[]{:S(2)}, u32[]{:S(2)}) collective-permute-start(bf16[48,512]{1,0:T(8,128)(2,1)S(1)} %get-tuple-element.24), channel_id=1, source_target_pairs={{4,0},{8,4},{12,8},{16,12},{20,16},{24,20},{28,24},{32,28},{36,32}... | collective-permute-start | bytes 147464 | tf_op jit(solution)/shard_map/ppermute | solution.py:322
  33.5 38.4 %copy-start.2 = (bf16[480,512]{1,0:T(8,128)(2,1)}, bf16[480,512]{1,0:T(8,128)(2,1)S(1)}, u32[]{:S(2)}) copy-start(bf16[480,512]{1,0:T(8,128)(2,1)S(1)} %constant_dynamic-update-slice_fusion.refs_0_.refs_4_) | copy-start | bytes 1474564
  33.5 16.7 %collective-permute-start.2 = (bf16[480,512]{1,0:T(8,128)(2,1)S(1)}, bf16[480,512]{1,0:T(8,128)(2,1)S(1)}, u32[]{:S(2)}, u32[]{:S(2)}) collective-permute-start(bf16[480,512]{1,0:T(8,128)(2,1)S(1)} %constant_dynamic-update-slice_fusion.refs_0_.refs_4_), channel_id=1, source_target_pairs={{0,1},{1,2},{2,3},{3,0},{4,5},{5,6},{6,7},{7,4},{8,9},{9,10},{10,1... | collective-permute-start | bytes 1474568 | tf_op jit(solution)/shard_map/ppermute | solution.py:26
  36.4 35.5 %copy-start.8 = (bf16[8,32,512]{2,1,0:T(8,128)(2,1)}, bf16[8,32,512]{2,1,0:T(8,128)(2,1)S(1)}, u32[]{:S(2)}) copy-start(bf16[8,32,512]{2,1,0:T(8,128)(2,1)S(1)} %all-to-all-done.refs_9_) | copy-start | bytes 786436
  37.3 29.9 %all-to-all-start.1 = ((bf16[8,32,1024]{2,1,0:T(8,128)(2,1)}), bf16[8,32,1024]{2,1,0:T(8,128)(2,1)S(1)}, u32[]{:S(2)}, u32[]{:S(2)}) async-start(bf16[8,32,1024]{2,1,0:T(8,128)(2,1)} %broadcast_in_dim.10), calls=%async_computation.1 | async-start | bytes 1048576 | tf_op jit(solution)/shard_map/all_to_all | solution.py:21
  42.4 15.6 %collective-permute-start.3 = (bf16[480,512]{1,0:T(8,128)(2,1)S(1)}, bf16[480,512]{1,0:T(8,128)(2,1)S(1)}, u32[]{:S(2)}, u32[]{:S(2)}) collective-permute-start(bf16[480,512]{1,0:T(8,128)(2,1)S(1)} %constant_dynamic-update-slice_fusion.refs_0_.refs_4_), channel_id=1, source_target_pairs={{0,2},{1,3},{2,0},{3,1},{4,6},{5,7},{6,4},{7,5},{8,10},{9,11},{10,... | collective-permute-start | bytes 1474568 | tf_op jit(solution)/shard_map/ppermute | solution.py:26
  45.7 14.6 %collective-permute-start.6 = (bf16[8,32,512]{2,1,0:T(8,128)(2,1)S(1)}, bf16[8,32,512]{2,1,0:T(8,128)(2,1)S(1)}, u32[]{:S(2)}, u32[]{:S(2)}) collective-permute-start(bf16[8,32,512]{2,1,0:T(8,128)(2,1)S(1)} %all-to-all-done.refs_9_), channel_id=1, source_target_pairs={{0,16},{8,24},{16,0},{24,8},{1,17},{9,25},{17,1},{25,9},{2,18},{10... | collective-permute-start | bytes 786440 | tf_op jit(solution)/shard_map/ppermute | solution.py:26
  47.0 20.2 %collective-permute-start.4 = (bf16[480,512]{1,0:T(8,128)(2,1)S(1)}, bf16[480,512]{1,0:T(8,128)(2,1)S(1)}, u32[]{:S(2)}, u32[]{:S(2)}) collective-permute-start(bf16[480,512]{1,0:T(8,128)(2,1)S(1)} %constant_dynamic-update-slice_fusion.refs_0_.refs_4_), channel_id=1, source_target_pairs={{0,3},{1,0},{2,1},{3,2},{4,7},{5,4},{6,5},{7,6},{8,11},{9,8},{10,9... | collective-permute-start | bytes 1474568 | tf_op jit(solution)/shard_map/ppermute | solution.py:26
  47.0 15.1 %collective-permute-start.7 = (bf16[8,32,512]{2,1,0:T(8,128)(2,1)S(1)}, bf16[8,32,512]{2,1,0:T(8,128)(2,1)}, u32[]{:S(2)}, u32[]{:S(2)}) collective-permute-start(bf16[8,32,512]{2,1,0:T(8,128)(2,1)S(1)} %all-to-all-done.refs_9_), channel_id=1, source_target_pairs={{0,24},{8,0},{16,8},{24,16},{1,25},{9,1},{17,9},{25,17},{2,26},{10... | collective-permute-start | bytes 786440 | tf_op jit(solution)/shard_map/ppermute | solution.py:26
  50.2 21.7 %copy-start.4 = (bf16[480,512]{1,0:T(8,128)(2,1)}, bf16[480,512]{1,0:T(8,128)(2,1)S(1)}, u32[]{:S(2)}) copy-start(bf16[480,512]{1,0:T(8,128)(2,1)S(1)} %collective-permute-done.2.refs_1_.refs_5_) | copy-start | bytes 1474564
  50.2 12.0 %collective-permute-start.5 = (bf16[8,32,512]{2,1,0:T(8,128)(2,1)S(1)}, bf16[8,32,512]{2,1,0:T(8,128)(2,1)}, u32[]{:S(2)}, u32[]{:S(2)}) collective-permute-start(bf16[8,32,512]{2,1,0:T(8,128)(2,1)S(1)} %all-to-all-done.refs_9_), channel_id=1, source_target_pairs={{0,8},{8,16},{16,24},{24,0},{1,9},{9,17},{17,25},{25,1},{2,10},{10... | collective-permute-start | bytes 786440 | tf_op jit(solution)/shard_map/ppermute | solution.py:26
  58.0 13.9 %copy-start.5 = (bf16[480,512]{1,0:T(8,128)(2,1)}, bf16[480,512]{1,0:T(8,128)(2,1)S(1)}, u32[]{:S(2)}) copy-start(bf16[480,512]{1,0:T(8,128)(2,1)S(1)} %collective-permute-done.3.refs_2_.refs_6_) | copy-start | bytes 1474564
  58.0 11.3 %collective-permute-start.8 = (bf16[8,32,512]{2,1,0:T(8,128)(2,1)S(1)}, bf16[8,32,512]{2,1,0:T(8,128)(2,1)}, u32[]{:S(2)}, u32[]{:S(2)}) collective-permute-start(bf16[8,32,512]{2,1,0:T(8,128)(2,1)S(1)} %all-to-all-done.refs_9_), channel_id=1, source_target_pairs={{0,4},{4,0},{1,5},{5,1},{2,6},{6,2},{3,7},{7,3},{8,12},{12,8},{9,1... | collective-permute-start | bytes 786440 | tf_op jit(solution)/shard_map/ppermute | solution.py:26
  60.3 11.6 %copy-start.16 = (bf16[8,32,512]{2,1,0:T(8,128)(2,1)}, bf16[8,32,512]{2,1,0:T(8,128)(2,1)S(1)}, u32[]{:S(2)}) copy-start(bf16[8,32,512]{2,1,0:T(8,128)(2,1)S(1)} %collective-permute-done.6.refs_11_) | copy-start | bytes 786436
  60.3 10.8 %collective-permute-start.10 = (bf16[8,32,512]{2,1,0:T(8,128)(2,1)S(1)}, bf16[8,32,512]{2,1,0:T(8,128)(2,1)}, u32[]{:S(2)}, u32[]{:S(2)}) collective-permute-start(bf16[8,32,512]{2,1,0:T(8,128)(2,1)S(1)} %collective-permute-done.6.refs_11_), channel_id=1, source_target_pairs={{0,4},{4,0},{1,5},{5,1},{2,6},{6,2},{3,7},{7,3},{8,12},{12,8},{9,1... | collective-permute-start | bytes 786440 | tf_op jit(solution)/shard_map/ppermute | solution.py:26
  62.1 9.8 %collective-permute-start.11 = (bf16[8,32,512]{2,1,0:T(8,128)(2,1)}, bf16[8,32,512]{2,1,0:T(8,128)(2,1)}, u32[]{:S(2)}, u32[]{:S(2)}) collective-permute-start(bf16[8,32,512]{2,1,0:T(8,128)(2,1)} %collective-permute-done.7.refs_12_), channel_id=1, source_target_pairs={{0,4},{4,0},{1,5},{5,1},{2,6},{6,2},{3,7},{7,3},{8,12},{12,8},{9,1... | collective-permute-start | bytes 786440 | tf_op jit(solution)/shard_map/ppermute | solution.py:26
  62.2 9.6 %collective-permute-start.9 = (bf16[8,32,512]{2,1,0:T(8,128)(2,1)}, bf16[8,32,512]{2,1,0:T(8,128)(2,1)}, u32[]{:S(2)}, u32[]{:S(2)}) collective-permute-start(bf16[8,32,512]{2,1,0:T(8,128)(2,1)} %collective-permute-done.5.refs_10_), channel_id=1, source_target_pairs={{0,4},{4,0},{1,5},{5,1},{2,6},{6,2},{3,7},{7,3},{8,12},{12,8},{9,1... | collective-permute-start | bytes 786440 | tf_op jit(solution)/shard_map/ppermute | solution.py:26
  67.2 4.7 %copy-start.6 = (bf16[480,512]{1,0:T(8,128)(2,1)}, bf16[480,512]{1,0:T(8,128)(2,1)S(1)}, u32[]{:S(2)}) copy-start(bf16[480,512]{1,0:T(8,128)(2,1)S(1)} %collective-permute-done.4.refs_3_.refs_7_) | copy-start | bytes 1474564
  67.2 66.3 %copy-start.3 = (bf16[8,32,1024]{2,1,0:T(8,128)(2,1)}, bf16[8,32,1024]{2,1,0:T(8,128)(2,1)S(1)}, u32[]{:S(2)}) copy-start(bf16[8,32,1024]{2,1,0:T(8,128)(2,1)S(1)} %all-to-all-done.1.refs_8_) | copy-start | bytes 1572868
  67.2 27.6 %collective-permute-start.18 = (bf16[8,32,1024]{2,1,0:T(8,128)(2,1)S(1)}, bf16[8,32,1024]{2,1,0:T(8,128)(2,1)S(1)}, u32[]{:S(2)}, u32[]{:S(2)}) collective-permute-start(bf16[8,32,1024]{2,1,0:T(8,128)(2,1)S(1)} %all-to-all-done.1.refs_8_), channel_id=1, source_target_pairs={{0,8},{8,16},{16,24},{24,0},{1,9},{9,17},{17,25},{25,1},{2,10},{10... | collective-permute-start | bytes 1572872 | tf_op jit(solution)/shard_map/ppermute | solution.py:26
  69.3 25.6 %collective-permute-start.19 = (bf16[8,32,1024]{2,1,0:T(8,128)(2,1)S(1)}, bf16[8,32,1024]{2,1,0:T(8,128)(2,1)}, u32[]{:S(2)}, u32[]{:S(2)}) collective-permute-start(bf16[8,32,1024]{2,1,0:T(8,128)(2,1)S(1)} %all-to-all-done.1.refs_8_), channel_id=1, source_target_pairs={{0,16},{8,24},{16,0},{24,8},{1,17},{9,25},{17,1},{25,9},{2,18},{10... | collective-permute-start | bytes 1572872 | tf_op jit(solution)/shard_map/ppermute | solution.py:26
  71.2 36.9 %collective-permute-start.20 = (bf16[8,32,1024]{2,1,0:T(8,128)(2,1)S(1)}, bf16[8,32,1024]{2,1,0:T(8,128)(2,1)}, u32[]{:S(2)}, u32[]{:S(2)}) collective-permute-start(bf16[8,32,1024]{2,1,0:T(8,128)(2,1)S(1)} %all-to-all-done.1.refs_8_), channel_id=1, source_target_pairs={{0,24},{8,0},{16,8},{24,16},{1,25},{9,1},{17,9},{25,17},{2,26},{10... | collective-permute-start | bytes 1572872 | tf_op jit(solution)/shard_map/ppermute | solution.py:26
  79.2 9.3 %collective-permute-start.12 = (bf16[464,256]{1,0:T(8,128)(2,1)}, bf16[464,256]{1,0:T(8,128)(2,1)S(1)}, u32[]{:S(2)}, u32[]{:S(2)}) collective-permute-start(bf16[464,256]{1,0:T(8,128)(2,1)} %shard_map.91.refs_0_), channel_id=1, source_target_pairs={{0,1},{1,2},{2,3},{3,0},{4,5},{5,6},{6,7},{7,4},{8,9},{9,10},{10,1... | collective-permute-start | bytes 712712 | tf_op jit(solution)/shard_map/ppermute | solution.py:26
  80.3 13.5 %collective-permute-start.13 = (bf16[464,256]{1,0:T(8,128)(2,1)}, bf16[464,256]{1,0:T(8,128)(2,1)S(1)}, u32[]{:S(2)}, u32[]{:S(2)}) collective-permute-start(bf16[464,256]{1,0:T(8,128)(2,1)} %shard_map.91.refs_0_), channel_id=1, source_target_pairs={{0,2},{1,3},{2,0},{3,1},{4,6},{5,7},{6,4},{7,5},{8,10},{9,11},{10,... | collective-permute-start | bytes 712712 | tf_op jit(solution)/shard_map/ppermute | solution.py:26
  88.5 21.6 %copy-start.17 = (bf16[464,256]{1,0:T(8,128)(2,1)}, bf16[464,256]{1,0:T(8,128)(2,1)S(1)}, u32[]{:S(2)}) copy-start(bf16[464,256]{1,0:T(8,128)(2,1)S(1)} %collective-permute-done.12.refs_1_) | copy-start | bytes 712708
  88.5 6.3 %collective-permute-start.14 = (bf16[464,256]{1,0:T(8,128)(2,1)}, bf16[464,256]{1,0:T(8,128)(2,1)S(1)}, u32[]{:S(2)}, u32[]{:S(2)}) collective-permute-start(bf16[464,256]{1,0:T(8,128)(2,1)} %shard_map.91.refs_0_), channel_id=1, source_target_pairs={{0,3},{1,0},{2,1},{3,2},{4,7},{5,4},{6,5},{7,6},{8,11},{9,8},{10,9... | collective-permute-start | bytes 712712 | tf_op jit(solution)/shard_map/ppermute | solution.py:26
  94.8 38.8 %copy-start.9 = (bf16[8,32,1024]{2,1,0:T(8,128)(2,1)}, bf16[8,32,1024]{2,1,0:T(8,128)(2,1)S(1)}, u32[]{:S(2)}) copy-start(bf16[8,32,1024]{2,1,0:T(8,128)(2,1)S(1)} %collective-permute-done.18.refs_9_) | copy-start | bytes 1572868
  108.1 24.1 %collective-permute-start.21 = (bf16[8,32,1024]{2,1,0:T(8,128)(2,1)S(1)}, bf16[8,32,1024]{2,1,0:T(8,128)(2,1)S(1)}, u32[]{:S(2)}, u32[]{:S(2)}) collective-permute-start(bf16[8,32,1024]{2,1,0:T(8,128)(2,1)S(1)} %all-to-all-done.1.refs_8_), channel_id=1, source_target_pairs={{0,4},{4,0},{1,5},{5,1},{2,6},{6,2},{3,7},{7,3},{8,12},{12,8},{9,1... | collective-permute-start | bytes 1572872 | tf_op jit(solution)/shard_map/ppermute | solution.py:26
  108.1 25.4 %collective-permute-start.22 = (bf16[8,32,1024]{2,1,0:T(8,128)(2,1)S(1)}, bf16[8,32,1024]{2,1,0:T(8,128)(2,1)S(1)}, u32[]{:S(2)}, u32[]{:S(2)}) collective-permute-start(bf16[8,32,1024]{2,1,0:T(8,128)(2,1)S(1)} %collective-permute-done.18.refs_9_), channel_id=1, source_target_pairs={{0,4},{4,0},{1,5},{5,1},{2,6},{6,2},{3,7},{7,3},{8,12},{12,8},{9,1... | collective-permute-start | bytes 1572872 | tf_op jit(solution)/shard_map/ppermute | solution.py:26
  110.1 18.9 %all-to-all-start.2 = ((bf16[8,32,512]{2,1,0:T(8,128)(2,1)}), bf16[8,32,512]{2,1,0:T(8,128)(2,1)S(1)}, u32[]{:S(2)}, u32[]{:S(2)}) async-start(bf16[8,32,512]{2,1,0:T(8,128)(2,1)} %broadcast_in_dim.11), calls=%async_computation.2 | async-start | bytes 524288 | tf_op jit(solution)/shard_map/all_to_all | solution.py:21
  116.9 16.6 %collective-permute-start.23 = (bf16[8,32,1024]{2,1,0:T(8,128)(2,1)}, bf16[8,32,1024]{2,1,0:T(8,128)(2,1)S(1)}, u32[]{:S(2)}, u32[]{:S(2)}) collective-permute-start(bf16[8,32,1024]{2,1,0:T(8,128)(2,1)} %collective-permute-done.19.refs_10_), channel_id=1, source_target_pairs={{0,4},{4,0},{1,5},{5,1},{2,6},{6,2},{3,7},{7,3},{8,12},{12,8},{9,1... | collective-permute-start | bytes 1572872 | tf_op jit(solution)/shard_map/ppermute | solution.py:26
  116.9 16.6 %collective-permute-start.24 = (bf16[8,32,1024]{2,1,0:T(8,128)(2,1)}, bf16[8,32,1024]{2,1,0:T(8,128)(2,1)}, u32[]{:S(2)}, u32[]{:S(2)}) collective-permute-start(bf16[8,32,1024]{2,1,0:T(8,128)(2,1)} %collective-permute-done.20.refs_11_), channel_id=1, source_target_pairs={{0,4},{4,0},{1,5},{5,1},{2,6},{6,2},{3,7},{7,3},{8,12},{12,8},{9,1... | collective-permute-start | bytes 1572872 | tf_op jit(solution)/shard_map/ppermute | solution.py:26
  129.0 14.2 %collective-permute-start.25 = (bf16[8,32,512]{2,1,0:T(8,128)(2,1)S(1)}, bf16[8,32,512]{2,1,0:T(8,128)(2,1)S(1)}, u32[]{:S(2)}, u32[]{:S(2)}) collective-permute-start(bf16[8,32,512]{2,1,0:T(8,128)(2,1)S(1)} %all-to-all-done.2), channel_id=1, source_target_pairs={{0,8},{8,16},{16,24},{24,0},{1,9},{9,17},{17,25},{25,1},{2,10},{10... | collective-permute-start | bytes 786440 | tf_op jit(solution)/shard_map/ppermute | solution.py:26
  132.2 11.0 %collective-permute-start.26 = (bf16[8,32,512]{2,1,0:T(8,128)(2,1)S(1)}, bf16[8,32,512]{2,1,0:T(8,128)(2,1)S(1)}, u32[]{:S(2)}, u32[]{:S(2)}) collective-permute-start(bf16[8,32,512]{2,1,0:T(8,128)(2,1)S(1)} %all-to-all-done.2), channel_id=1, source_target_pairs={{0,16},{8,24},{16,0},{24,8},{1,17},{9,25},{17,1},{25,9},{2,18},{10... | collective-permute-start | bytes 786440 | tf_op jit(solution)/shard_map/ppermute | solution.py:26
  133.5 12.6 %collective-permute-start.27 = (bf16[8,32,512]{2,1,0:T(8,128)(2,1)S(1)}, bf16[8,32,512]{2,1,0:T(8,128)(2,1)}, u32[]{:S(2)}, u32[]{:S(2)}) collective-permute-start(bf16[8,32,512]{2,1,0:T(8,128)(2,1)S(1)} %all-to-all-done.2), channel_id=1, source_target_pairs={{0,24},{8,0},{16,8},{24,16},{1,25},{9,1},{17,9},{25,17},{2,26},{10... | collective-permute-start | bytes 786440 | tf_op jit(solution)/shard_map/ppermute | solution.py:26
  147.2 2.8 %copy-start = (bf16[4,8,32,512]{3,2,1,0:T(8,128)(2,1)}, bf16[4,8,32,512]{3,2,1,0:T(8,128)(2,1)S(1)}, u32[]{:S(2)}) copy-start(bf16[4,8,32,512]{3,2,1,0:T(8,128)(2,1)S(1)} %pad_maximum_fusion.refs_6_) | copy-start | bytes 3145732
  147.2 2.7 %collective-permute-start.28 = (bf16[4,8,32,512]{3,2,1,0:T(8,128)(2,1)S(1)}, bf16[4,8,32,512]{3,2,1,0:T(8,128)(2,1)S(1)}, u32[]{:S(2)}, u32[]{:S(2)}) collective-permute-start(bf16[4,8,32,512]{3,2,1,0:T(8,128)(2,1)S(1)} %pad_maximum_fusion.refs_6_), channel_id=1, source_target_pairs={{0,4},{4,0},{1,5},{5,1},{2,6},{6,2},{3,7},{7,3},{8,12},{12,8},{9,1... | collective-permute-start | bytes 3145736 | tf_op jit(solution)/shard_map/ppermute | solution.py:26
  192.5 27.1 %all-to-all-start.4 = ((bf16[4,400,256]{2,1,0:T(8,128)(2,1)}), bf16[4,400,256]{2,1,0:T(8,128)(2,1)S(1)}, u32[]{:S(2)}, u32[]{:S(2)}) async-start(bf16[4,400,256]{2,1,0:T(8,128)(2,1)} %shard_map.95), calls=%async_computation.4 | async-start | bytes 1638400 | tf_op jit(solution)/shard_map/all_to_all | solution.py:337
  197.2 17.8 %collective-permute-start.29 = (bf16[512,256]{1,0:T(8,128)(2,1)S(1)}, bf16[512,256]{1,0:T(8,128)(2,1)S(1)}, u32[]{:S(2)}, u32[]{:S(2)}) collective-permute-start(bf16[512,256]{1,0:T(8,128)(2,1)S(1)} %get-tuple-element.23), channel_id=1, source_target_pairs={{0,1},{1,2},{2,3},{3,0},{4,5},{5,6},{6,7},{7,4},{8,9},{9,10},{10,1... | collective-permute-start | bytes 786440 | tf_op jit(solution)/shard_map/ppermute | solution.py:26
  199.2 20.4 %collective-permute-start.30 = (bf16[512,256]{1,0:T(8,128)(2,1)S(1)}, bf16[512,256]{1,0:T(8,128)(2,1)S(1)}, u32[]{:S(2)}, u32[]{:S(2)}) collective-permute-start(bf16[512,256]{1,0:T(8,128)(2,1)S(1)} %get-tuple-element.22), channel_id=1, source_target_pairs={{0,2},{1,3},{2,0},{3,1},{4,6},{5,7},{6,4},{7,5},{8,10},{9,11},{10,... | collective-permute-start | bytes 786440 | tf_op jit(solution)/shard_map/ppermute | solution.py:26
  201.9 17.7 %collective-permute-start.31 = (bf16[512,256]{1,0:T(8,128)(2,1)S(1)}, bf16[512,256]{1,0:T(8,128)(2,1)S(1)}, u32[]{:S(2)}, u32[]{:S(2)}) collective-permute-start(bf16[512,256]{1,0:T(8,128)(2,1)S(1)} %get-tuple-element.21), channel_id=1, source_target_pairs={{0,3},{1,0},{2,1},{3,2},{4,7},{5,4},{6,5},{7,6},{8,11},{9,8},{10,9... | collective-permute-start | bytes 786440 | tf_op jit(solution)/shard_map/ppermute | solution.py:26
  215.0 4.6 %copy-start.13 = (bf16[512,256]{1,0:T(8,128)(2,1)}, bf16[512,256]{1,0:T(8,128)(2,1)S(1)}, u32[]{:S(2)}) copy-start(bf16[512,256]{1,0:T(8,128)(2,1)S(1)} %collective-permute-done.29.refs_3_) | copy-start | bytes 786436
  (9 other events, 8.3 us)
Sparse Core Ops, SparseCore 0:
  16.3 103.1 all-gather.1

commit v2 on v1

--- a/solution.py
+++ b/solution.py
@@ -57,8 +57,8 @@
 def up_kernel(layer, total, n_s, n_y, first_lane, info, *refs):
     streams, refs = refs[:n_s], refs[n_s:]
     gain, tap_ref, bias, ln_gain, ln_shift, refs = *refs[:5], refs[5:]
-    pieces, refs = refs[:-7], refs[-7:]
-    out, weights, normed, both, padded, columns, sems = refs
+    pieces, refs = refs[:-8], refs[-8:]
+    out, weights, normed, scales, both, padded, columns, sems = refs
     rows, features = normed.shape
     width = streams[0].shape[-1]
     n_x = features // width
@@ -71,10 +71,10 @@
 
     if n_y:
         copies = []
-        for i, piece in enumerate(pieces if len(pieces) > 2 else [p.at[q] for p in pieces for q in range(n_y)]):
+        for i, piece in enumerate(pieces):
             c = core if i < n_y else 1 - core
             rows_of = weights.at[:, behind(my_y, i % n_y, n_y), c]
-            copies.append(pltpu.make_async_copy(piece, rows_of, sems.at[i]))
+            copies.append(pltpu.make_async_copy(piece.at[:, :, pl.ds(first_lane, 2 * ch)], rows_of, sems.at[i]))
     else:
         copies = [pltpu.make_async_copy(pieces[0].at[:, pl.ds(first_lane, 2 * ch)], weights, sems.at[0])]
     for copy in copies:
@@ -84,15 +84,13 @@
         here = pl.ds(first, step)
         squares = jnp.zeros((step, width), f32)
         for s in range(n_x):
-            value = (streams[s][here] if n_s > 1 else streams[0][s, here]).astype(f32)
-            squares += value * value
-        mean = jnp.sum(squares, axis=-1, keepdims=True) * (1.0 / features)
-        scale = lax.rsqrt(mean + norm_floor)
-        for s in range(n_x):
             b = behind(my_x, s, n_x) if n_s > 1 else s
             wide = pl.ds(pl.multiple_of(b * width, width), width)
             value = (streams[s][here] if n_s > 1 else streams[0][s, here]).astype(f32)
-            normed[here, wide] = (value * scale * gain[layer : layer + 1, wide]).astype(bf16)
+            squares += value * value
+            normed[here, wide] = (value * gain[layer : layer + 1, wide]).astype(bf16)
+        mean = jnp.sum(squares, axis=-1, keepdims=True) * (1.0 / features)
+        scales[here] = jnp.broadcast_to(lax.rsqrt(mean + norm_floor), (step, LANES))
 
     by_rows(rows, norm)
     for copy in copies:
@@ -103,7 +101,8 @@
 
     def gate(first, step):
         here = pl.ds(first, step)
-        gated = both[0, here] * jax.nn.sigmoid(both[1, here])
+        scale = scales[here, 0:1]
+        gated = both[0, here] * scale * jax.nn.sigmoid(both[1, here] * scale)
         t = info[3 + layer] + first + lax.broadcasted_iota(jnp.int32, (step, 1), 0)
         gated = jnp.where((t >= 0) & (t < total), gated, 0.0).astype(bf16)
         padded[here] = gated.astype(f32)
@@ -169,9 +168,7 @@
             fetch(piece, weights.at[:, behind(my_y, i % n_y, n_y), c])
     elif last:
         mine = pl.ds(pl.multiple_of(my_x * width, width), width)
-        fetch(pieces[0].at[mine, pl.ds(first_lane, ch)], weights.at[:, pl.ds(0, ch)])
-        for s in range(1, n_x):
-            fetch(pieces[s], weights.at[:, pl.ds(s * ch, ch)])
+        fetch(pieces[0].at[mine, pl.ds(first_lane, n_x * ch)], weights)
     else:
         fetch(pieces[0].at[:, pl.ds(first_lane, n_x * ch)], weights)
     for copy in copies:
@@ -243,7 +240,7 @@
     n_y, shape = 0, (n_x * width,)
     if len(pieces) > 1:
         n_z, n_i, _ = pieces[0].shape[-3:]
-        n_y = pieces[0].shape[0] if len(pieces) == 2 else len(pieces) // 2
+        n_y = len(pieces) // 2
         shape = (n_z, n_y, 2, n_i)
     return pl.pallas_call(
         functools.partial(up_kernel, layer, total, len(streams), n_y, first_lane),
@@ -253,6 +250,7 @@
         scratch_shapes=[
             pltpu.VMEM((*shape, 2 * ch), bf16),
             pltpu.VMEM((rows, n_x * width), bf16),
+            pltpu.VMEM((rows, LANES), f32),
             pltpu.VMEM((2, rows, ch), f32),
             pltpu.VMEM((rows, ch), f32),
             pltpu.VMEM((2 * ch, LANES), f32),
@@ -290,7 +288,7 @@
     layers, _, ch = w_value.shape
     n_x = lax.axis_size("x")
     my_x = lax.axis_index("x")
-    n_tok, f_loc = tokens.shape
+    n_tok, _ = tokens.shape
     halo = EDGE * layers
     size = lax.axis_size(SP)
     total = size * n_tok
@@ -304,49 +302,38 @@
     def gather_z(array):
         return to_all(array, "z")
 
-    near = 2
-    ups = [gather_z(jnp.concatenate([w_value[l], w_gate[l]], axis=1)) for l in range(near)]
-
-    out_t = jnp.swapaxes(w_out, 1, 2)
-    wide = jnp.concatenate(spread(out_t[: layers - 1], "x"), axis=-1)
+    near = min(2, layers)
+    pairs = [w for l in range(near) for w in (w_value[l], w_gate[l])]
+    ups = gather_z(jnp.concatenate(pairs, axis=1))
+
+    wide = jnp.concatenate(spread(jnp.swapaxes(w_out, 1, 2), "x"), axis=-1)
 
     packs, lanes, at = [], [(0, 0)], 0
     for l in range(1, layers):
         pair = [w_value[l], w_gate[l]] if l >= near else []
-        packs += [*pair, out_t[l] if l == layers - 1 else wide[l]]
-        lanes.append((at, at + sum(a.shape[1] for a in pair)))
-        at = lanes[-1][1] + packs[-1].shape[1]
+        packs += [*pair, wide[l]]
+        first = at if pair else 2 * ch * l
+        lanes.append((first, at + 2 * ch * bool(pair)))
+        at = lanes[-1][1] + n_x * ch
     rest = lax.all_gather(jnp.concatenate(packs, axis=1), SP, axis=0, tiled=True)
 
     before = lax.ppermute(tokens[n_tok - halo :], SP, [(i, i + 1) for i in range(size - 1)])
     following = lax.ppermute(tokens[:halo], SP, [(i + 1, i) for i in range(size - 1)])
     streams = spread(jnp.concatenate([before, tokens, following], axis=0), "x")
 
-    ups = [spread(a, "y") for a in ups]
-    out_first = spread(gather_z(wide[0]), "y")
+    ups = spread(ups, "y")
+    outs = spread(gather_z(wide[0]), "y")
+    ups = [*ups, *swap(ups)]
 
     for l in range(layers):
-        last = l == layers - 1
         first, start = lanes[l]
-        pieces = [rest]
-        if l < near:
-            pieces = [jnp.stack(after(ups[l], stream))] if l else ups[l]
-            pieces = [*pieces, *swap(pieces)]
-        gated = up(l, total, info, streams, params, pieces, ch, l > 0, first)
-        if l:
-            gated = [lax.all_to_all(gated, "x", split_axis=0, concat_axis=0, tiled=True)]
-        else:
-            gated = spread(gated, "x")
+        gated = up(l, total, info, streams, params, ups if l < near else [rest], ch, True, first)
+        gated = lax.all_to_all(gated, "x", split_axis=0, concat_axis=0, tiled=True)
         pieces = [rest]
         if l == 0:
-            pieces = after(out_first, *gated[1:])
+            pieces = after(outs, gated)
             pieces = [*pieces, *swap(pieces)]
-        if last:
-            for s in (1, n_x // 2, n_x - 1):
-                row = lax.rem(my_x + s, n_x) * f_loc
-                block = lax.dynamic_slice(rest, (row, start), (f_loc, ch))
-                pieces.append(shifted(block, "x", s))
-        stream = down(last, info, gated, streams, pieces, l == 0, start)
+        stream = down(l == layers - 1, info, [gated], streams, pieces, l == 0, start)
         streams = [stream]
     return stream
 

time: 235 us -> 207 us (0.88)
  the two profiles are of different devices: /device:TPU:24 before, /device:TPU:120 now
where the time goes in v2:
time: 207 us; the launch traced here: 203 us
  waiting for transfers between devices  56.6 us (27%)
  Pallas kernels  46.9 us (23%)
  starting transfers between devices  46.2 us (22%)
  blocking collectives  34.5 us (17%)
  between operations  13.7 us (7%)
  local copies, waits for them, and re-layouts  4.07 us (2%)
    ppermute x20, waiting for transfers between devices, shifted(): return lax.ppermute(array, axis, [(i, (i + s) % n) for i in range(n)])  49.1 us
    all_to_all x2, blocking collectives, program(): gated = lax.all_to_all(gated, 'x', split_axis=0, concat_axis=0, tiled=True)  34.5 us
    pallas_call x3, Pallas kernels, up(): pl.pallas_call(functools.partial(up_kernel, layer, total, len(streams), n...  23.5 us
    pallas_call x3, Pallas kernels, down(): pl.pallas_call(functools.partial(down_kernel, last, len(streams), n_y, n_...  23.4 us
    ppermute x20, starting transfers between devices, shifted(): return lax.ppermute(array, axis, [(i, (i + s) % n) for i in range(n)])  20.1 us
    all_to_all x2, starting transfers between devices, to_all(): return lax.all_to_all(copies, axis, split_axis=0, concat_axis=0, tiled=True)  15.5 us
    all_to_all x2, waiting for transfers between devices, to_all(): return lax.all_to_all(copies, axis, split_axis=0, concat_axis=0, tiled=True)  7.43 us
    all_to_all x1, starting transfers between devices, program(): gated = lax.all_to_all(gated, 'x', split_axis=0, concat_axis=0, tiled=True)  5 us
  transfers between devices with their start and end apart: 26, of which 14 were waited for; matrix products, arithmetic and copies ran while one was open for 2% of the time, Pallas kernels for 12%

profile of v2, /device:TPU:120, one launch (start us, length us, event | category | flops | bytes accessed | tf_op | source)
XLA Modules:
  0.0 203.4 jit_solution(16092362630803421704)
XLA Ops:
  6.5 1.5 collective-permute-start.12
  8.0 2.7 %collective-permute-start.13 = (bf16[3,32,256]{2,1,0:T(8,128)(2,1)}, bf16[3,32,256]{2,1,0:T(8,128)(2,1)S(1)}, u32[]{:S(2)}, u32[]{:S(2)}) collective-permute-start(bf16[3,32,256]{2,1,0:T(8,128)(2,1)} %bitcast.26), channel_id=1, source_target_pairs={{0,2},{1,3},{2,0},{3,1},{4,6},{5,7},{6,4},{7,5},{8,10},{9,11},{10,... | collective-permute-start | bytes 147464 | tf_op jit(solution)/shard_map/ppermute | solution.py:26
  10.8 1.4 collective-permute-start.14
  12.2 0.8 slice_bitcast_fusion.3
  13.0 0.8 collective-permute-done.13
  13.8 1.2 collective-permute-done.14
  15.1 0.8 pad_maximum_fusion
  15.9 0.7 pad_maximum_fusion.1
  16.6 0.9 broadcast_in_dim.6
  17.5 7.7 %all-to-all-start = ((bf16[8,32,1024]{2,1,0:T(8,128)(2,1)}), bf16[8,32,1024]{2,1,0:T(8,128)(2,1)S(1)}, u32[]{:S(2)}, u32[]{:S(2)}) async-start(bf16[8,32,1024]{2,1,0:T(8,128)(2,1)} %broadcast_in_dim.6), calls=%async_computation | async-start | bytes 1048576 | tf_op jit(solution)/shard_map/all_to_all | solution.py:21
  25.2 1.9 collective-permute-start
  27.1 3.6 %collective-permute-start.1 = (bf16[48,512]{1,0:T(8,128)(2,1)S(1)}, bf16[48,512]{1,0:T(8,128)(2,1)S(1)}, u32[]{:S(2)}, u32[]{:S(2)}) collective-permute-start(bf16[48,512]{1,0:T(8,128)(2,1)S(1)} %get-tuple-element.13), channel_id=1, source_target_pairs={{4,0},{8,4},{12,8},{16,12},{20,16},{24,20},{28,24},{32,28},{36,32}... | collective-permute-start | bytes 147464 | tf_op jit(solution)/shard_map/ppermute | solution.py:321
  30.8 7.4 %all-to-all-done.refs_9_.refs_6_ = bf16[8,32,1024]{2,1,0:T(8,128)(2,1)S(1)} async-done(((bf16[8,32,1024]{2,1,0:T(8,128)(2,1)}), bf16[8,32,1024]{2,1,0:T(8,128)(2,1)S(1)}, u32[]{:S(2)}, u32[]{:S(2)}) %all-to-all-start) | async-done | bytes 524320 | tf_op jit(solution)/shard_map/all_to_all | solution.py:21
  38.2 1.2 collective-permute-start.6
  39.5 1.1 collective-permute-start.7
  40.5 2.2 %collective-permute-start.5 = (bf16[8,32,1024]{2,1,0:T(8,128)(2,1)S(1)}, bf16[8,32,1024]{2,1,0:T(8,128)(2,1)S(1)}, u32[]{:S(2)}, u32[]{:S(2)}) collective-permute-start(bf16[8,32,1024]{2,1,0:T(8,128)(2,1)S(1)} %all-to-all-done.refs_9_.refs_6_), channel_id=1, source_target_pairs={{0,8},{8,16},{16,24},{24,0},{1,9},{9,17},{17,25},{25,1},{2,10},{10... | collective-permute-start | bytes 1572872 | tf_op jit(solution)/shard_map/ppermute | solution.py:26
  43.0 3.6 %collective-permute-start.3 = (bf16[480,512]{1,0:T(8,128)(2,1)S(1)}, bf16[480,512]{1,0:T(8,128)(2,1)}, u32[]{:S(2)}, u32[]{:S(2)}) collective-permute-start(bf16[480,512]{1,0:T(8,128)(2,1)S(1)} %constant_dynamic-update-slice_fusion.refs_0_.refs_1_), channel_id=1, source_target_pairs={{0,2},{1,3},{2,0},{3,1},{4,6},{5,7},{6,4},{7,5},{8,10},{9,11},{10,... | collective-permute-start | bytes 1474568 | tf_op jit(solution)/shard_map/ppermute | solution.py:26
  46.6 0.9 broadcast_in_dim.7
  47.5 7.8 %all-to-all-start.2 = ((bf16[8,32,1024]{2,1,0:T(8,128)(2,1)}), bf16[8,32,1024]{2,1,0:T(8,128)(2,1)S(1)}, u32[]{:S(2)}, u32[]{:S(2)}) async-start(bf16[8,32,1024]{2,1,0:T(8,128)(2,1)} %broadcast_in_dim.7), calls=%async_computation.2 | async-start | bytes 1048576 | tf_op jit(solution)/shard_map/all_to_all | solution.py:21
  55.3 2.5 %collective-permute-done.2.refs_1_.refs_2_ = bf16[480,512]{1,0:T(8,128)(2,1)} collective-permute-done((bf16[480,512]{1,0:T(8,128)(2,1)S(1)}, bf16[480,512]{1,0:T(8,128)(2,1)}, u32[]{:S(2)}, u32[]{:S(2)}) %collective-permute-start.2) | collective-permute-done | bytes 491552 | tf_op jit(solution)/shard_map/ppermute | solution.py:26
  57.8 0.5 collective-permute-start.10
  58.3 5.0 %collective-permute-done.7.refs_12_.refs_9_ = bf16[8,32,1024]{2,1,0:T(8,128)(2,1)S(1)} collective-permute-done((bf16[8,32,1024]{2,1,0:T(8,128)(2,1)S(1)}, bf16[8,32,1024]{2,1,0:T(8,128)(2,1)S(1)}, u32[]{:S(2)}, u32[]{:S(2)}) %collective-permute-start.7) | collective-permute-done | bytes 524320 | tf_op jit(solution)/shard_map/ppermute | solution.py:26
  63.4 0.5 collective-permute-start.9
  63.9 0.8 collective-permute-done.3.refs_2_.refs_3_
  64.7 1.6 collective-permute-start.4
  66.3 0.6 stack.27.info
  66.9 10.3 %collective-permute-done.4.refs_3_.refs_4_ = bf16[480,512]{1,0:T(8,128)(2,1)} collective-permute-done((bf16[480,512]{1,0:T(8,128)(2,1)S(1)}, bf16[480,512]{1,0:T(8,128)(2,1)}, u32[]{:S(2)}, u32[]{:S(2)}) %collective-permute-start.4) | collective-permute-done | bytes 491552 | tf_op jit(solution)/shard_map/ppermute | solution.py:26
  77.3 8.2 %shard_map.91 = bf16[4,464,256]{2,1,0:T(8,128)(2,1)} custom-call(s32[6]{0:T(128)} %stack.27.info, bf16[480,512]{1,0:T(8,128)(2,1)} %copy-done.2, bf16[480,512]{1,0:T(8,128)(2,1)} %collective-permute-done.2.refs_1_.refs_2_, bf16[480,512]{1,0:T(8,128)(2,1)} %collective-permute-done.3.refs_2_.refs_3_, bf16[480,512]{1,0:T(8,128)(2,1)} %collective-permute-done.4.refs_3_.refs_4_, ...), custom_call_target="tpu_custom_call" | custom-call | tf_op jit(solution)/shard_map/pallas_call | solution.py:245
  85.6 5.0 %all-to-all-start.1 = ((bf16[4,464,256]{2,1,0:T(8,128)(2,1)}), bf16[4,464,256]{2,1,0:T(8,128)(2,1)S(1)}, u32[]{:S(2)}, u32[]{:S(2)}) async-start(bf16[4,464,256]{2,1,0:T(8,128)(2,1)} %shard_map.91), calls=%async_computation.1 | async-start | bytes 1900544 | tf_op jit(solution)/shard_map/all_to_all | solution.py:331
  90.6 0.7 collective-permute-start.15
  91.3 1.2 collective-permute-start.16
  92.5 0.5 collective-permute-start.17
  93.0 14.5 %collective-permute-done.15.refs_6_ = bf16[8,32,1024]{2,1,0:T(8,128)(2,1)S(1)} collective-permute-done((bf16[8,32,1024]{2,1,0:T(8,128)(2,1)S(1)}, bf16[8,32,1024]{2,1,0:T(8,128)(2,1)S(1)}, u32[]{:S(2)}, u32[]{:S(2)}) %collective-permute-start.15) | collective-permute-done | bytes 524320 | tf_op jit(solution)/shard_map/ppermute | solution.py:26
  107.4 1.0 collective-permute-done.16.refs_7_
  108.5 10.4 %collective-permute-done.17.refs_8_ = bf16[8,32,1024]{2,1,0:T(8,128)(2,1)S(1)} collective-permute-done((bf16[8,32,1024]{2,1,0:T(8,128)(2,1)S(1)}, bf16[8,32,1024]{2,1,0:T(8,128)(2,1)S(1)}, u32[]{:S(2)}, u32[]{:S(2)}) %collective-permute-start.17) | collective-permute-done | bytes 524320 | tf_op jit(solution)/shard_map/ppermute | solution.py:26
  119.0 0.5 collective-permute-start.19
  119.6 0.4 collective-permute-start.21
  120.0 0.9 collective-permute-done.18.refs_9_
  120.9 0.7 collective-permute-done.19.refs_10_
  121.6 0.7 collective-permute-done.20.refs_11_
  122.4 0.8 copy-done.13
  123.3 8.6 %shard_map.92.refs_0_.refs_1_ = bf16[4,448,512]{2,1,0:T(8,128)(2,1)} custom-call(s32[6]{0:T(128)} %stack.27.info, bf16[4,464,256]{2,1,0:T(8,128)(2,1)} %copy-done.1, bf16[480,512]{1,0:T(8,128)(2,1)} %copy-done.2, bf16[480,512]{1,0:T(8,128)(2,1)} %collective-permute-done.2.refs_1_.refs_2_, bf16[480,512]{1,0:T(8,128)(2,1)} %collective-permute-done.3.refs_2_.refs_3_, ...), custom_call_target="tpu_custom_call" | custom-call | tf_op jit(solution)/shard_map/pallas_call | solution.py:273
  131.9 7.8 %shard_map.93 = bf16[4,432,256]{2,1,0:T(8,128)(2,1)} custom-call(s32[6]{0:T(128)} %stack.27.info, bf16[4,448,512]{2,1,0:T(8,128)(2,1)} %shard_map.92.refs_0_.refs_1_, f32[3,2048]{1,0:T(4,128)} %refs_1_.3, f32[3,31,256]{2,1,0:T(8,128)} %refs_2_.3, f32[3,256]{1,0:T(4,128)} %refs_3_.3, f32[3,256]{1,0:T(4,128)} %refs_4_.5, f32[3,256]{1,0:T(4,128)} %refs_5_.5, ...), custom_call_target="tpu_custom_call" | custom-call | tf_op jit(solution)/shard_map/pallas_call | solution.py:245
  139.7 18.2 %all_to_all.25.refs_0_ = bf16[4,432,256]{2,1,0:T(8,128)(2,1)} all-to-all(bf16[4,432,256]{2,1,0:T(8,128)(2,1)} %shard_map.93), channel_id=1, replica_groups=mesh['z'=8,'y'=4,'c'=2,'x'=4] {'x'}, dimensions={0} | all-to-all | bytes 1769472 | tf_op jit(solution)/shard_map/all_to_all | solution.py:331
  157.9 8.9 %shard_map.94.refs_0_.refs_1_ = bf16[4,416,512]{2,1,0:T(8,128)(2,1)} custom-call(s32[6]{0:T(128)} %stack.27.info, bf16[4,432,256]{2,1,0:T(8,128)(2,1)} %all_to_all.25.refs_0_, bf16[4,448,512]{2,1,0:T(8,128)(2,1)} %shard_map.92.refs_0_.refs_1_, bf16[2048,2560]{1,0:T(8,128)(2,1)} %all-gather.2.cloned.1.call-done.refs_2_.refs_6_), custom_call_target="tpu_custom_call" | custom-call | tf_op jit(solution)/shard_map/pallas_call | solution.py:273
  166.8 7.5 %shard_map.95 = bf16[4,400,256]{2,1,0:T(8,128)(2,1)} custom-call(s32[6]{0:T(128)} %stack.27.info, bf16[4,416,512]{2,1,0:T(8,128)(2,1)} %shard_map.94.refs_0_.refs_1_, f32[3,2048]{1,0:T(4,128)} %refs_1_.3, f32[3,31,256]{2,1,0:T(8,128)} %refs_2_.3, f32[3,256]{1,0:T(4,128)} %refs_3_.3, f32[3,256]{1,0:T(4,128)} %refs_4_.5, f32[3,256]{1,0:T(4,128)} %refs_5_.5, ...), custom_call_target="tpu_custom_call" | custom-call | tf_op jit(solution)/shard_map/pallas_call | solution.py:245
  174.3 16.3 %all_to_all.26.refs_0_ = bf16[4,400,256]{2,1,0:T(8,128)(2,1)} all-to-all(bf16[4,400,256]{2,1,0:T(8,128)(2,1)} %shard_map.95), channel_id=1, replica_groups=mesh['z'=8,'y'=4,'c'=2,'x'=4] {'x'}, dimensions={0} | all-to-all | bytes 1638400 | tf_op jit(solution)/shard_map/all_to_all | solution.py:331
  190.6 6.0 %shard_map.96 = bf16[384,512]{1,0:T(8,128)(2,1)} custom-call(s32[6]{0:T(128)} %stack.27.info, bf16[4,400,256]{2,1,0:T(8,128)(2,1)} %all_to_all.26.refs_0_, bf16[4,416,512]{2,1,0:T(8,128)(2,1)} %shard_map.94.refs_0_.refs_1_, bf16[2048,2560]{1,0:T(8,128)(2,1)} %all-gather.2.cloned.1.call-done.refs_2_.refs_6_), custom_call_target="tpu_custom_call" | custom-call | tf_op jit(solution)/shard_map/pallas_call | solution.py:273
  (53 shorter events, 0.7 us)
Async XLA Ops:
  6.5 18.6 %copy-start.7 = (bf16[384,512]{1,0:T(8,128)(2,1)S(1)}, bf16[384,512]{1,0:T(8,128)(2,1)}, u32[]{:S(2)}) copy-start(bf16[384,512]{1,0:T(8,128)(2,1)} %param.9) | copy-start | bytes 1179652
  6.5 151.4 %all-gather.2.cloned.1.call-start = ((), (), s32[]{:S(2)}) async-start(), calls=%async_computation.5 | async-start | bytes 10649600 | tf_op jit(solution)/shard_map/all_gather | solution.py:318
  6.5 6.5 %collective-permute-start.12 = (bf16[3,32,256]{2,1,0:T(8,128)(2,1)}, bf16[3,32,256]{2,1,0:T(8,128)(2,1)S(1)}, u32[]{:S(2)}, u32[]{:S(2)}) collective-permute-start(bf16[3,32,256]{2,1,0:T(8,128)(2,1)} %bitcast.25), channel_id=1, source_target_pairs={{0,1},{1,2},{2,3},{3,0},{4,5},{5,6},{6,7},{7,4},{8,9},{9,10},{10,1... | collective-permute-start | bytes 147464 | tf_op jit(solution)/shard_map/ppermute | solution.py:26
  8.0 5.8 %collective-permute-start.13 = (bf16[3,32,256]{2,1,0:T(8,128)(2,1)}, bf16[3,32,256]{2,1,0:T(8,128)(2,1)S(1)}, u32[]{:S(2)}, u32[]{:S(2)}) collective-permute-start(bf16[3,32,256]{2,1,0:T(8,128)(2,1)} %bitcast.26), channel_id=1, source_target_pairs={{0,2},{1,3},{2,0},{3,1},{4,6},{5,7},{6,4},{7,5},{8,10},{9,11},{10,... | collective-permute-start | bytes 147464 | tf_op jit(solution)/shard_map/ppermute | solution.py:26
  10.8 4.3 %collective-permute-start.14 = (bf16[3,32,256]{2,1,0:T(8,128)(2,1)}, bf16[3,32,256]{2,1,0:T(8,128)(2,1)S(1)}, u32[]{:S(2)}, u32[]{:S(2)}) collective-permute-start(bf16[3,32,256]{2,1,0:T(8,128)(2,1)} %bitcast.27), channel_id=1, source_target_pairs={{0,3},{1,0},{2,1},{3,2},{4,7},{5,4},{6,5},{7,6},{8,11},{9,8},{10,9... | collective-permute-start | bytes 147464 | tf_op jit(solution)/shard_map/ppermute | solution.py:26
  17.5 20.7 %all-to-all-start = ((bf16[8,32,1024]{2,1,0:T(8,128)(2,1)}), bf16[8,32,1024]{2,1,0:T(8,128)(2,1)S(1)}, u32[]{:S(2)}, u32[]{:S(2)}) async-start(bf16[8,32,1024]{2,1,0:T(8,128)(2,1)} %broadcast_in_dim.6), calls=%async_computation | async-start | bytes 1048576 | tf_op jit(solution)/shard_map/all_to_all | solution.py:21
  25.2 5.6 %collective-permute-start = (bf16[48,512]{1,0:T(8,128)(2,1)S(1)}, bf16[48,512]{1,0:T(8,128)(2,1)S(1)}, u32[]{:S(2)}, u32[]{:S(2)}) collective-permute-start(bf16[48,512]{1,0:T(8,128)(2,1)S(1)} %get-tuple-element.14), channel_id=1, source_target_pairs={{0,4},{4,8},{8,12},{12,16},{16,20},{20,24},{24,28},{28,32},{32,36}... | collective-permute-start | bytes 147464 | tf_op jit(solution)/shard_map/ppermute | solution.py:320
  27.1 15.6 %collective-permute-start.1 = (bf16[48,512]{1,0:T(8,128)(2,1)S(1)}, bf16[48,512]{1,0:T(8,128)(2,1)S(1)}, u32[]{:S(2)}, u32[]{:S(2)}) collective-permute-start(bf16[48,512]{1,0:T(8,128)(2,1)S(1)} %get-tuple-element.13), channel_id=1, source_target_pairs={{4,0},{8,4},{12,8},{16,12},{20,16},{24,20},{28,24},{32,28},{36,32}... | collective-permute-start | bytes 147464 | tf_op jit(solution)/shard_map/ppermute | solution.py:321
  38.2 39.0 %copy-start = (bf16[8,32,1024]{2,1,0:T(8,128)(2,1)}, bf16[8,32,1024]{2,1,0:T(8,128)(2,1)S(1)}, u32[]{:S(2)}) copy-start(bf16[8,32,1024]{2,1,0:T(8,128)(2,1)S(1)} %all-to-all-done.refs_9_.refs_6_) | copy-start | bytes 1572868
  38.2 19.6 %collective-permute-start.6 = (bf16[8,32,1024]{2,1,0:T(8,128)(2,1)S(1)}, bf16[8,32,1024]{2,1,0:T(8,128)(2,1)S(1)}, u32[]{:S(2)}, u32[]{:S(2)}) collective-permute-start(bf16[8,32,1024]{2,1,0:T(8,128)(2,1)S(1)} %all-to-all-done.refs_9_.refs_6_), channel_id=1, source_target_pairs={{0,16},{8,24},{16,0},{24,8},{1,17},{9,25},{17,1},{25,9},{2,18},{10... | collective-permute-start | bytes 1572872 | tf_op jit(solution)/shard_map/ppermute | solution.py:26
  39.5 23.9 %collective-permute-start.7 = (bf16[8,32,1024]{2,1,0:T(8,128)(2,1)S(1)}, bf16[8,32,1024]{2,1,0:T(8,128)(2,1)S(1)}, u32[]{:S(2)}, u32[]{:S(2)}) collective-permute-start(bf16[8,32,1024]{2,1,0:T(8,128)(2,1)S(1)} %all-to-all-done.refs_9_.refs_6_), channel_id=1, source_target_pairs={{0,24},{8,0},{16,8},{24,16},{1,25},{9,1},{17,9},{25,17},{2,26},{10... | collective-permute-start | bytes 1572872 | tf_op jit(solution)/shard_map/ppermute | solution.py:26
  40.5 22.9 %collective-permute-start.5 = (bf16[8,32,1024]{2,1,0:T(8,128)(2,1)S(1)}, bf16[8,32,1024]{2,1,0:T(8,128)(2,1)S(1)}, u32[]{:S(2)}, u32[]{:S(2)}) collective-permute-start(bf16[8,32,1024]{2,1,0:T(8,128)(2,1)S(1)} %all-to-all-done.refs_9_.refs_6_), channel_id=1, source_target_pairs={{0,8},{8,16},{16,24},{24,0},{1,9},{9,17},{17,25},{25,1},{2,10},{10... | collective-permute-start | bytes 1572872 | tf_op jit(solution)/shard_map/ppermute | solution.py:26
  42.7 34.6 %copy-start.2 = (bf16[480,512]{1,0:T(8,128)(2,1)}, bf16[480,512]{1,0:T(8,128)(2,1)S(1)}, u32[]{:S(2)}) copy-start(bf16[480,512]{1,0:T(8,128)(2,1)S(1)} %constant_dynamic-update-slice_fusion.refs_0_.refs_1_) | copy-start | bytes 1474564
  42.7 15.1 %collective-permute-start.2 = (bf16[480,512]{1,0:T(8,128)(2,1)S(1)}, bf16[480,512]{1,0:T(8,128)(2,1)}, u32[]{:S(2)}, u32[]{:S(2)}) collective-permute-start(bf16[480,512]{1,0:T(8,128)(2,1)S(1)} %constant_dynamic-update-slice_fusion.refs_0_.refs_1_), channel_id=1, source_target_pairs={{0,1},{1,2},{2,3},{3,0},{4,5},{5,6},{6,7},{7,4},{8,9},{9,10},{10,1... | collective-permute-start | bytes 1474568 | tf_op jit(solution)/shard_map/ppermute | solution.py:26
  43.0 21.7 %collective-permute-start.3 = (bf16[480,512]{1,0:T(8,128)(2,1)S(1)}, bf16[480,512]{1,0:T(8,128)(2,1)}, u32[]{:S(2)}, u32[]{:S(2)}) collective-permute-start(bf16[480,512]{1,0:T(8,128)(2,1)S(1)} %constant_dynamic-update-slice_fusion.refs_0_.refs_1_), channel_id=1, source_target_pairs={{0,2},{1,3},{2,0},{3,1},{4,6},{5,7},{6,4},{7,5},{8,10},{9,11},{10,... | collective-permute-start | bytes 1474568 | tf_op jit(solution)/shard_map/ppermute | solution.py:26
  47.5 38.1 %all-to-all-start.2 = ((bf16[8,32,1024]{2,1,0:T(8,128)(2,1)}), bf16[8,32,1024]{2,1,0:T(8,128)(2,1)S(1)}, u32[]{:S(2)}, u32[]{:S(2)}) async-start(bf16[8,32,1024]{2,1,0:T(8,128)(2,1)} %broadcast_in_dim.7), calls=%async_computation.2 | async-start | bytes 1048576 | tf_op jit(solution)/shard_map/all_to_all | solution.py:21
  57.8 19.4 %collective-permute-start.8 = (bf16[8,32,1024]{2,1,0:T(8,128)(2,1)S(1)}, bf16[8,32,1024]{2,1,0:T(8,128)(2,1)}, u32[]{:S(2)}, u32[]{:S(2)}) collective-permute-start(bf16[8,32,1024]{2,1,0:T(8,128)(2,1)S(1)} %all-to-all-done.refs_9_.refs_6_), channel_id=1, source_target_pairs={{0,4},{4,0},{1,5},{5,1},{2,6},{6,2},{3,7},{7,3},{8,12},{12,8},{9,1... | collective-permute-start | bytes 1572872 | tf_op jit(solution)/shard_map/ppermute | solution.py:26
  57.8 19.4 %copy-start.4 = (bf16[8,32,1024]{2,1,0:T(8,128)(2,1)}, bf16[8,32,1024]{2,1,0:T(8,128)(2,1)S(1)}, u32[]{:S(2)}) copy-start(bf16[8,32,1024]{2,1,0:T(8,128)(2,1)S(1)} %collective-permute-done.6.refs_11_.refs_8_) | copy-start | bytes 1572868
  57.8 19.4 %collective-permute-start.10 = (bf16[8,32,1024]{2,1,0:T(8,128)(2,1)S(1)}, bf16[8,32,1024]{2,1,0:T(8,128)(2,1)}, u32[]{:S(2)}, u32[]{:S(2)}) collective-permute-start(bf16[8,32,1024]{2,1,0:T(8,128)(2,1)S(1)} %collective-permute-done.6.refs_11_.refs_8_), channel_id=1, source_target_pairs={{0,4},{4,0},{1,5},{5,1},{2,6},{6,2},{3,7},{7,3},{8,12},{12,8},{9,1... | collective-permute-start | bytes 1572872 | tf_op jit(solution)/shard_map/ppermute | solution.py:26
  63.4 13.9 %copy-start.5 = (bf16[8,32,1024]{2,1,0:T(8,128)(2,1)}, bf16[8,32,1024]{2,1,0:T(8,128)(2,1)S(1)}, u32[]{:S(2)}) copy-start(bf16[8,32,1024]{2,1,0:T(8,128)(2,1)S(1)} %collective-permute-done.7.refs_12_.refs_9_) | copy-start | bytes 1572868
  63.4 13.9 %collective-permute-start.11 = (bf16[8,32,1024]{2,1,0:T(8,128)(2,1)S(1)}, bf16[8,32,1024]{2,1,0:T(8,128)(2,1)}, u32[]{:S(2)}, u32[]{:S(2)}) collective-permute-start(bf16[8,32,1024]{2,1,0:T(8,128)(2,1)S(1)} %collective-permute-done.7.refs_12_.refs_9_), channel_id=1, source_target_pairs={{0,4},{4,0},{1,5},{5,1},{2,6},{6,2},{3,7},{7,3},{8,12},{12,8},{9,1... | collective-permute-start | bytes 1572872 | tf_op jit(solution)/shard_map/ppermute | solution.py:26
  63.4 13.9 %copy-start.6 = (bf16[8,32,1024]{2,1,0:T(8,128)(2,1)}, bf16[8,32,1024]{2,1,0:T(8,128)(2,1)S(1)}, u32[]{:S(2)}) copy-start(bf16[8,32,1024]{2,1,0:T(8,128)(2,1)S(1)} %collective-permute-done.5.refs_10_.refs_7_) | copy-start | bytes 1572868
  63.4 13.8 %collective-permute-start.9 = (bf16[8,32,1024]{2,1,0:T(8,128)(2,1)S(1)}, bf16[8,32,1024]{2,1,0:T(8,128)(2,1)}, u32[]{:S(2)}, u32[]{:S(2)}) collective-permute-start(bf16[8,32,1024]{2,1,0:T(8,128)(2,1)S(1)} %collective-permute-done.5.refs_10_.refs_7_), channel_id=1, source_target_pairs={{0,4},{4,0},{1,5},{5,1},{2,6},{6,2},{3,7},{7,3},{8,12},{12,8},{9,1... | collective-permute-start | bytes 1572872 | tf_op jit(solution)/shard_map/ppermute | solution.py:26
  64.7 12.5 %collective-permute-start.4 = (bf16[480,512]{1,0:T(8,128)(2,1)S(1)}, bf16[480,512]{1,0:T(8,128)(2,1)}, u32[]{:S(2)}, u32[]{:S(2)}) collective-permute-start(bf16[480,512]{1,0:T(8,128)(2,1)S(1)} %constant_dynamic-update-slice_fusion.refs_0_.refs_1_), channel_id=1, source_target_pairs={{0,3},{1,0},{2,1},{3,2},{4,7},{5,4},{6,5},{7,6},{8,11},{9,8},{10,9... | collective-permute-start | bytes 1474568 | tf_op jit(solution)/shard_map/ppermute | solution.py:26
  85.5 37.7 %copy-start.3 = (bf16[8,32,1024]{2,1,0:T(8,128)(2,1)}, bf16[8,32,1024]{2,1,0:T(8,128)(2,1)S(1)}, u32[]{:S(2)}) copy-start(bf16[8,32,1024]{2,1,0:T(8,128)(2,1)S(1)} %all-to-all-done.2.refs_5_) | copy-start | bytes 1572868
  85.6 33.3 %all-to-all-start.1 = ((bf16[4,464,256]{2,1,0:T(8,128)(2,1)}), bf16[4,464,256]{2,1,0:T(8,128)(2,1)S(1)}, u32[]{:S(2)}, u32[]{:S(2)}) async-start(bf16[4,464,256]{2,1,0:T(8,128)(2,1)} %shard_map.91), calls=%async_computation.1 | async-start | bytes 1900544 | tf_op jit(solution)/shard_map/all_to_all | solution.py:331
  90.6 16.9 %collective-permute-start.15 = (bf16[8,32,1024]{2,1,0:T(8,128)(2,1)S(1)}, bf16[8,32,1024]{2,1,0:T(8,128)(2,1)S(1)}, u32[]{:S(2)}, u32[]{:S(2)}) collective-permute-start(bf16[8,32,1024]{2,1,0:T(8,128)(2,1)S(1)} %all-to-all-done.2.refs_5_), channel_id=1, source_target_pairs={{0,8},{8,16},{16,24},{24,0},{1,9},{9,17},{17,25},{25,1},{2,10},{10... | collective-permute-start | bytes 1572872 | tf_op jit(solution)/shard_map/ppermute | solution.py:26
  91.3 17.2 %collective-permute-start.16 = (bf16[8,32,1024]{2,1,0:T(8,128)(2,1)S(1)}, bf16[8,32,1024]{2,1,0:T(8,128)(2,1)S(1)}, u32[]{:S(2)}, u32[]{:S(2)}) collective-permute-start(bf16[8,32,1024]{2,1,0:T(8,128)(2,1)S(1)} %all-to-all-done.2.refs_5_), channel_id=1, source_target_pairs={{0,16},{8,24},{16,0},{24,8},{1,17},{9,25},{17,1},{25,9},{2,18},{10... | collective-permute-start | bytes 1572872 | tf_op jit(solution)/shard_map/ppermute | solution.py:26
  92.5 26.3 %collective-permute-start.17 = (bf16[8,32,1024]{2,1,0:T(8,128)(2,1)S(1)}, bf16[8,32,1024]{2,1,0:T(8,128)(2,1)S(1)}, u32[]{:S(2)}, u32[]{:S(2)}) collective-permute-start(bf16[8,32,1024]{2,1,0:T(8,128)(2,1)S(1)} %all-to-all-done.2.refs_5_), channel_id=1, source_target_pairs={{0,24},{8,0},{16,8},{24,16},{1,25},{9,1},{17,9},{25,17},{2,26},{10... | collective-permute-start | bytes 1572872 | tf_op jit(solution)/shard_map/ppermute | solution.py:26
  107.4 15.8 %copy-start.8 = (bf16[8,32,1024]{2,1,0:T(8,128)(2,1)}, bf16[8,32,1024]{2,1,0:T(8,128)(2,1)S(1)}, u32[]{:S(2)}) copy-start(bf16[8,32,1024]{2,1,0:T(8,128)(2,1)S(1)} %collective-permute-done.15.refs_6_) | copy-start | bytes 1572868
  108.5 14.8 %copy-start.9 = (bf16[8,32,1024]{2,1,0:T(8,128)(2,1)}, bf16[8,32,1024]{2,1,0:T(8,128)(2,1)S(1)}, u32[]{:S(2)}) copy-start(bf16[8,32,1024]{2,1,0:T(8,128)(2,1)S(1)} %collective-permute-done.16.refs_7_) | copy-start | bytes 1572868
  118.9 4.4 %copy-start.10 = (bf16[8,32,1024]{2,1,0:T(8,128)(2,1)}, bf16[8,32,1024]{2,1,0:T(8,128)(2,1)S(1)}, u32[]{:S(2)}) copy-start(bf16[8,32,1024]{2,1,0:T(8,128)(2,1)S(1)} %collective-permute-done.17.refs_8_) | copy-start | bytes 1572868
  118.9 4.4 %copy-start.1 = (bf16[4,464,256]{2,1,0:T(8,128)(2,1)}, bf16[4,464,256]{2,1,0:T(8,128)(2,1)S(1)}, u32[]{:S(2)}) copy-start(bf16[4,464,256]{2,1,0:T(8,128)(2,1)S(1)} %all-to-all-done.1.refs_0_) | copy-start | bytes 2850820
  118.9 2.0 collective-permute-start.18
  119.0 2.6 %collective-permute-start.19 = (bf16[8,32,1024]{2,1,0:T(8,128)(2,1)S(1)}, bf16[8,32,1024]{2,1,0:T(8,128)(2,1)S(1)}, u32[]{:S(2)}, u32[]{:S(2)}) collective-permute-start(bf16[8,32,1024]{2,1,0:T(8,128)(2,1)S(1)} %collective-permute-done.15.refs_6_), channel_id=1, source_target_pairs={{0,4},{4,0},{1,5},{5,1},{2,6},{6,2},{3,7},{7,3},{8,12},{12,8},{9,1... | collective-permute-start | bytes 1572872 | tf_op jit(solution)/shard_map/ppermute | solution.py:26
  119.5 2.9 %collective-permute-start.20 = (bf16[8,32,1024]{2,1,0:T(8,128)(2,1)S(1)}, bf16[8,32,1024]{2,1,0:T(8,128)(2,1)S(1)}, u32[]{:S(2)}, u32[]{:S(2)}) collective-permute-start(bf16[8,32,1024]{2,1,0:T(8,128)(2,1)S(1)} %collective-permute-done.16.refs_7_), channel_id=1, source_target_pairs={{0,4},{4,0},{1,5},{5,1},{2,6},{6,2},{3,7},{7,3},{8,12},{12,8},{9,1... | collective-permute-start | bytes 1572872 | tf_op jit(solution)/shard_map/ppermute | solution.py:26
  119.6 3.7 %collective-permute-start.21 = (bf16[8,32,1024]{2,1,0:T(8,128)(2,1)S(1)}, bf16[8,32,1024]{2,1,0:T(8,128)(2,1)}, u32[]{:S(2)}, u32[]{:S(2)}) collective-permute-start(bf16[8,32,1024]{2,1,0:T(8,128)(2,1)S(1)} %collective-permute-done.17.refs_8_), channel_id=1, source_target_pairs={{0,4},{4,0},{1,5},{5,1},{2,6},{6,2},{3,7},{7,3},{8,12},{12,8},{9,1... | collective-permute-start | bytes 1572872 | tf_op jit(solution)/shard_map/ppermute | solution.py:26
  120.9 1.5 copy-start.11
  121.6 0.8 copy-start.12
  122.4 0.8 copy-start.13
Sparse Core Ops, SparseCore 0:
  16.7 101.3 all-gather.1

commit v3 on v2

--- a/solution.py
+++ b/solution.py
@@ -57,8 +57,8 @@
 def up_kernel(layer, total, n_s, n_y, first_lane, info, *refs):
     streams, refs = refs[:n_s], refs[n_s:]
     gain, tap_ref, bias, ln_gain, ln_shift, refs = *refs[:5], refs[5:]
-    pieces, refs = refs[:-8], refs[-8:]
-    out, weights, normed, scales, both, padded, columns, sems = refs
+    pieces, refs = refs[:-7], refs[-7:]
+    out, weights, normed, both, padded, columns, sems = refs
     rows, features = normed.shape
     width = streams[0].shape[-1]
     n_x = features // width
@@ -84,13 +84,15 @@
         here = pl.ds(first, step)
         squares = jnp.zeros((step, width), f32)
         for s in range(n_x):
+            value = (streams[s][here] if n_s > 1 else streams[0][s, here]).astype(f32)
+            squares += value * value
+        mean = jnp.sum(squares, axis=-1, keepdims=True) * (1.0 / features)
+        scale = lax.rsqrt(mean + norm_floor)
+        for s in range(n_x):
             b = behind(my_x, s, n_x) if n_s > 1 else s
             wide = pl.ds(pl.multiple_of(b * width, width), width)
             value = (streams[s][here] if n_s > 1 else streams[0][s, here]).astype(f32)
-            squares += value * value
-            normed[here, wide] = (value * gain[layer : layer + 1, wide]).astype(bf16)
-        mean = jnp.sum(squares, axis=-1, keepdims=True) * (1.0 / features)
-        scales[here] = jnp.broadcast_to(lax.rsqrt(mean + norm_floor), (step, LANES))
+            normed[here, wide] = (value * scale * gain[layer : layer + 1, wide]).astype(bf16)
 
     by_rows(rows, norm)
     for copy in copies:
@@ -101,8 +103,7 @@
 
     def gate(first, step):
         here = pl.ds(first, step)
-        scale = scales[here, 0:1]
-        gated = both[0, here] * scale * jax.nn.sigmoid(both[1, here] * scale)
+        gated = both[0, here] * jax.nn.sigmoid(both[1, here])
         t = info[3 + layer] + first + lax.broadcasted_iota(jnp.int32, (step, 1), 0)
         gated = jnp.where((t >= 0) & (t < total), gated, 0.0).astype(bf16)
         padded[here] = gated.astype(f32)
@@ -214,11 +215,11 @@
             added = lax.dot_general(act[...], part, dims, preferred_element_type=f32)
             out[b] = (base.astype(f32) + added).astype(bf16)
 
-        if n_s > 1:
-            for s in range(n_x):
+        for s in range(n_x):
+            if n_s > 1:
                 block(behind(my_x, s, n_x), streams[s][inner])
-        else:
-            lax.fori_loop(0, n_x, lambda b, carry: (block(b, streams[0][b, inner]), carry)[1], 0)
+            else:
+                block(s, streams[0][s, inner])
 
 
 def vmem():
@@ -250,7 +251,6 @@
         scratch_shapes=[
             pltpu.VMEM((*shape, 2 * ch), bf16),
             pltpu.VMEM((rows, n_x * width), bf16),
-            pltpu.VMEM((rows, LANES), f32),
             pltpu.VMEM((2, rows, ch), f32),
             pltpu.VMEM((rows, ch), f32),
             pltpu.VMEM((2 * ch, LANES), f32),

time: 207 us -> 206 us (level)
  the two profiles are of different devices: /device:TPU:120 before, /device:TPU:8 now
where the time goes in v3:
time: 206 us; the launch traced here: 205 us
  waiting for transfers between devices  60.2 us (29%)
  starting transfers between devices  45.5 us (22%)
  Pallas kernels  45 us (22%)
  blocking collectives  35.3 us (17%)
  between operations  13.7 us (7%)
  local copies, waits for them, and re-layouts  4.07 us (2%)
    ppermute x20, waiting for transfers between devices, shifted(): return lax.ppermute(array, axis, [(i, (i + s) % n) for i in range(n)])  48.2 us
    all_to_all x2, blocking collectives, program(): gated = lax.all_to_all(gated, 'x', split_axis=0, concat_axis=0, tiled=True)  35.3 us
    ppermute x20, starting transfers between devices, shifted(): return lax.ppermute(array, axis, [(i, (i + s) % n) for i in range(n)])  23.7 us
    pallas_call x3, Pallas kernels, down(): pl.pallas_call(functools.partial(down_kernel, last, len(streams), n_y, n_...  22.8 us
    pallas_call x3, Pallas kernels, up(): pl.pallas_call(functools.partial(up_kernel, layer, total, len(streams), n...  22.2 us
    all_to_all x2, waiting for transfers between devices, to_all(): return lax.all_to_all(copies, axis, split_axis=0, concat_axis=0, tiled=True)  12 us
    all_to_all x2, starting transfers between devices, to_all(): return lax.all_to_all(copies, axis, split_axis=0, concat_axis=0, tiled=True)  12 us
    all_to_all x1, starting transfers between devices, program(): gated = lax.all_to_all(gated, 'x', split_axis=0, concat_axis=0, tiled=True)  4.3 us
  transfers between devices with their start and end apart: 26, of which 15 were waited for; matrix products, arithmetic and copies ran while one was open for 2% of the time, Pallas kernels for 12%

profile of v3, /device:TPU:8, one launch (start us, length us, event | category | flops | bytes accessed | tf_op | source)
XLA Modules:
  0.0 205.2 jit_solution(2327720492561643999)
XLA Ops:
  6.5 1.5 collective-permute-start.12
  8.0 2.7 %collective-permute-start.13 = (bf16[3,32,256]{2,1,0:T(8,128)(2,1)}, bf16[3,32,256]{2,1,0:T(8,128)(2,1)S(1)}, u32[]{:S(2)}, u32[]{:S(2)}) collective-permute-start(bf16[3,32,256]{2,1,0:T(8,128)(2,1)} %bitcast.26), channel_id=1, source_target_pairs={{0,2},{1,3},{2,0},{3,1},{4,6},{5,7},{6,4},{7,5},{8,10},{9,11},{10,... | collective-permute-start | bytes 147464 | tf_op jit(solution)/shard_map/ppermute | solution.py:26
  10.8 1.4 collective-permute-start.14
  12.2 0.8 slice_bitcast_fusion.3
  13.0 0.8 collective-permute-done.13
  13.8 1.2 collective-permute-done.14
  15.1 0.8 pad_maximum_fusion
  15.9 0.7 pad_maximum_fusion.1
  16.6 0.9 broadcast_in_dim.6
  17.5 8.5 %all-to-all-start = ((bf16[8,32,1024]{2,1,0:T(8,128)(2,1)}), bf16[8,32,1024]{2,1,0:T(8,128)(2,1)S(1)}, u32[]{:S(2)}, u32[]{:S(2)}) async-start(bf16[8,32,1024]{2,1,0:T(8,128)(2,1)} %broadcast_in_dim.6), calls=%async_computation | async-start | bytes 1048576 | tf_op jit(solution)/shard_map/all_to_all | solution.py:21
  26.0 1.9 collective-permute-start
  27.9 3.6 %collective-permute-start.1 = (bf16[48,512]{1,0:T(8,128)(2,1)S(1)}, bf16[48,512]{1,0:T(8,128)(2,1)S(1)}, u32[]{:S(2)}, u32[]{:S(2)}) collective-permute-start(bf16[48,512]{1,0:T(8,128)(2,1)S(1)} %get-tuple-element.13), channel_id=1, source_target_pairs={{4,0},{8,4},{12,8},{16,12},{20,16},{24,20},{28,24},{32,28},{36,32}... | collective-permute-start | bytes 147464 | tf_op jit(solution)/shard_map/ppermute | solution.py:321
  31.6 12.0 %all-to-all-done.refs_9_.refs_6_ = bf16[8,32,1024]{2,1,0:T(8,128)(2,1)S(1)} async-done(((bf16[8,32,1024]{2,1,0:T(8,128)(2,1)}), bf16[8,32,1024]{2,1,0:T(8,128)(2,1)S(1)}, u32[]{:S(2)}, u32[]{:S(2)}) %all-to-all-start) | async-done | bytes 524320 | tf_op jit(solution)/shard_map/all_to_all | solution.py:21
  43.6 3.1 %collective-permute-start.6 = (bf16[8,32,1024]{2,1,0:T(8,128)(2,1)S(1)}, bf16[8,32,1024]{2,1,0:T(8,128)(2,1)S(1)}, u32[]{:S(2)}, u32[]{:S(2)}) collective-permute-start(bf16[8,32,1024]{2,1,0:T(8,128)(2,1)S(1)} %all-to-all-done.refs_9_.refs_6_), channel_id=1, source_target_pairs={{0,16},{8,24},{16,0},{24,8},{1,17},{9,25},{17,1},{25,9},{2,18},{10... | collective-permute-start | bytes 1572872 | tf_op jit(solution)/shard_map/ppermute | solution.py:26
  46.7 0.6 collective-permute-start.7
  47.2 1.5 collective-permute-start.5
  48.8 3.7 %collective-permute-start.3 = (bf16[480,512]{1,0:T(8,128)(2,1)S(1)}, bf16[480,512]{1,0:T(8,128)(2,1)}, u32[]{:S(2)}, u32[]{:S(2)}) collective-permute-start(bf16[480,512]{1,0:T(8,128)(2,1)S(1)} %constant_dynamic-update-slice_fusion.refs_0_.refs_1_), channel_id=1, source_target_pairs={{0,2},{1,3},{2,0},{3,1},{4,6},{5,7},{6,4},{7,5},{8,10},{9,11},{10,... | collective-permute-start | bytes 1474568 | tf_op jit(solution)/shard_map/ppermute | solution.py:26
  52.5 0.9 broadcast_in_dim.7
  53.4 3.5 %all-to-all-start.2 = ((bf16[8,32,1024]{2,1,0:T(8,128)(2,1)}), bf16[8,32,1024]{2,1,0:T(8,128)(2,1)S(1)}, u32[]{:S(2)}, u32[]{:S(2)}) async-start(bf16[8,32,1024]{2,1,0:T(8,128)(2,1)} %broadcast_in_dim.7), calls=%async_computation.2 | async-start | bytes 1048576 | tf_op jit(solution)/shard_map/all_to_all | solution.py:21
  56.9 6.4 %collective-permute-done.2.refs_1_.refs_2_ = bf16[480,512]{1,0:T(8,128)(2,1)} collective-permute-done((bf16[480,512]{1,0:T(8,128)(2,1)S(1)}, bf16[480,512]{1,0:T(8,128)(2,1)}, u32[]{:S(2)}, u32[]{:S(2)}) %collective-permute-start.2) | collective-permute-done | bytes 491552 | tf_op jit(solution)/shard_map/ppermute | solution.py:26
  63.3 0.5 collective-permute-start.10
  63.8 3.5 %collective-permute-done.7.refs_12_.refs_9_ = bf16[8,32,1024]{2,1,0:T(8,128)(2,1)S(1)} collective-permute-done((bf16[8,32,1024]{2,1,0:T(8,128)(2,1)S(1)}, bf16[8,32,1024]{2,1,0:T(8,128)(2,1)S(1)}, u32[]{:S(2)}, u32[]{:S(2)}) %collective-permute-start.7) | collective-permute-done | bytes 524320 | tf_op jit(solution)/shard_map/ppermute | solution.py:26
  67.4 0.4 collective-permute-start.9
  67.8 0.8 collective-permute-done.3.refs_2_.refs_3_
  68.6 1.0 collective-permute-start.4
  69.6 0.6 stack.27.info
  70.2 10.9 %collective-permute-done.4.refs_3_.refs_4_ = bf16[480,512]{1,0:T(8,128)(2,1)} collective-permute-done((bf16[480,512]{1,0:T(8,128)(2,1)S(1)}, bf16[480,512]{1,0:T(8,128)(2,1)}, u32[]{:S(2)}, u32[]{:S(2)}) %collective-permute-start.4) | collective-permute-done | bytes 491552 | tf_op jit(solution)/shard_map/ppermute | solution.py:26
  81.2 7.7 %shard_map.91 = bf16[4,464,256]{2,1,0:T(8,128)(2,1)} custom-call(s32[6]{0:T(128)} %stack.27.info, bf16[480,512]{1,0:T(8,128)(2,1)} %copy-done.2, bf16[480,512]{1,0:T(8,128)(2,1)} %collective-permute-done.2.refs_1_.refs_2_, bf16[480,512]{1,0:T(8,128)(2,1)} %collective-permute-done.3.refs_2_.refs_3_, bf16[480,512]{1,0:T(8,128)(2,1)} %collective-permute-done.4.refs_3_.refs_4_, ...), custom_call_target="tpu_custom_call" | custom-call | tf_op jit(solution)/shard_map/pallas_call | solution.py:246
  89.0 4.3 %all-to-all-start.1 = ((bf16[4,464,256]{2,1,0:T(8,128)(2,1)}), bf16[4,464,256]{2,1,0:T(8,128)(2,1)S(1)}, u32[]{:S(2)}, u32[]{:S(2)}) async-start(bf16[4,464,256]{2,1,0:T(8,128)(2,1)} %shard_map.91), calls=%async_computation.1 | async-start | bytes 1900544 | tf_op jit(solution)/shard_map/all_to_all | solution.py:331
  93.3 1.6 collective-permute-start.15
  94.8 2.0 collective-permute-start.16
  96.9 2.5 %collective-permute-start.17 = (bf16[8,32,1024]{2,1,0:T(8,128)(2,1)S(1)}, bf16[8,32,1024]{2,1,0:T(8,128)(2,1)S(1)}, u32[]{:S(2)}, u32[]{:S(2)}) collective-permute-start(bf16[8,32,1024]{2,1,0:T(8,128)(2,1)S(1)} %all-to-all-done.2.refs_5_), channel_id=1, source_target_pairs={{0,24},{8,0},{16,8},{24,16},{1,25},{9,1},{17,9},{25,17},{2,26},{10... | collective-permute-start | bytes 1572872 | tf_op jit(solution)/shard_map/ppermute | solution.py:26
  99.4 10.8 %collective-permute-done.15.refs_6_ = bf16[8,32,1024]{2,1,0:T(8,128)(2,1)S(1)} collective-permute-done((bf16[8,32,1024]{2,1,0:T(8,128)(2,1)S(1)}, bf16[8,32,1024]{2,1,0:T(8,128)(2,1)S(1)}, u32[]{:S(2)}, u32[]{:S(2)}) %collective-permute-start.15) | collective-permute-done | bytes 524320 | tf_op jit(solution)/shard_map/ppermute | solution.py:26
  110.2 1.0 collective-permute-done.16.refs_7_
  111.2 9.4 %collective-permute-done.17.refs_8_ = bf16[8,32,1024]{2,1,0:T(8,128)(2,1)S(1)} collective-permute-done((bf16[8,32,1024]{2,1,0:T(8,128)(2,1)S(1)}, bf16[8,32,1024]{2,1,0:T(8,128)(2,1)S(1)}, u32[]{:S(2)}, u32[]{:S(2)}) %collective-permute-start.17) | collective-permute-done | bytes 524320 | tf_op jit(solution)/shard_map/ppermute | solution.py:26
  120.8 0.4 collective-permute-start.19
  121.3 0.4 collective-permute-start.21
  121.7 1.4 collective-permute-done.18.refs_9_
  123.0 1.1 collective-permute-done.19.refs_10_
  124.1 0.7 collective-permute-done.20.refs_11_
  124.9 0.8 copy-done.13
  125.8 8.6 %shard_map.92.refs_0_.refs_1_ = bf16[4,448,512]{2,1,0:T(8,128)(2,1)} custom-call(s32[6]{0:T(128)} %stack.27.info, bf16[4,464,256]{2,1,0:T(8,128)(2,1)} %copy-done.1, bf16[480,512]{1,0:T(8,128)(2,1)} %copy-done.2, bf16[480,512]{1,0:T(8,128)(2,1)} %collective-permute-done.2.refs_1_.refs_2_, bf16[480,512]{1,0:T(8,128)(2,1)} %collective-permute-done.3.refs_2_.refs_3_, ...), custom_call_target="tpu_custom_call" | custom-call | tf_op jit(solution)/shard_map/pallas_call | solution.py:273
  134.4 7.4 %shard_map.93 = bf16[4,432,256]{2,1,0:T(8,128)(2,1)} custom-call(s32[6]{0:T(128)} %stack.27.info, bf16[4,448,512]{2,1,0:T(8,128)(2,1)} %shard_map.92.refs_0_.refs_1_, f32[3,2048]{1,0:T(4,128)} %refs_1_.3, f32[3,31,256]{2,1,0:T(8,128)} %refs_2_.3, f32[3,256]{1,0:T(4,128)} %refs_3_.3, f32[3,256]{1,0:T(4,128)} %refs_4_.5, f32[3,256]{1,0:T(4,128)} %refs_5_.5, ...), custom_call_target="tpu_custom_call" | custom-call | tf_op jit(solution)/shard_map/pallas_call | solution.py:246
  141.8 18.5 %all_to_all.25.refs_0_ = bf16[4,432,256]{2,1,0:T(8,128)(2,1)} all-to-all(bf16[4,432,256]{2,1,0:T(8,128)(2,1)} %shard_map.93), channel_id=1, replica_groups=mesh['z'=8,'y'=4,'c'=2,'x'=4] {'x'}, dimensions={0} | all-to-all | bytes 1769472 | tf_op jit(solution)/shard_map/all_to_all | solution.py:331
  160.2 8.2 %shard_map.94.refs_0_.refs_1_ = bf16[4,416,512]{2,1,0:T(8,128)(2,1)} custom-call(s32[6]{0:T(128)} %stack.27.info, bf16[4,432,256]{2,1,0:T(8,128)(2,1)} %all_to_all.25.refs_0_, bf16[4,448,512]{2,1,0:T(8,128)(2,1)} %shard_map.92.refs_0_.refs_1_, bf16[2048,2560]{1,0:T(8,128)(2,1)} %all-gather.2.cloned.1.call-done.refs_2_.refs_6_), custom_call_target="tpu_custom_call" | custom-call | tf_op jit(solution)/shard_map/pallas_call | solution.py:273
  168.5 7.0 %shard_map.95 = bf16[4,400,256]{2,1,0:T(8,128)(2,1)} custom-call(s32[6]{0:T(128)} %stack.27.info, bf16[4,416,512]{2,1,0:T(8,128)(2,1)} %shard_map.94.refs_0_.refs_1_, f32[3,2048]{1,0:T(4,128)} %refs_1_.3, f32[3,31,256]{2,1,0:T(8,128)} %refs_2_.3, f32[3,256]{1,0:T(4,128)} %refs_3_.3, f32[3,256]{1,0:T(4,128)} %refs_4_.5, f32[3,256]{1,0:T(4,128)} %refs_5_.5, ...), custom_call_target="tpu_custom_call" | custom-call | tf_op jit(solution)/shard_map/pallas_call | solution.py:246
  175.5 16.9 %all_to_all.26.refs_0_ = bf16[4,400,256]{2,1,0:T(8,128)(2,1)} all-to-all(bf16[4,400,256]{2,1,0:T(8,128)(2,1)} %shard_map.95), channel_id=1, replica_groups=mesh['z'=8,'y'=4,'c'=2,'x'=4] {'x'}, dimensions={0} | all-to-all | bytes 1638400 | tf_op jit(solution)/shard_map/all_to_all | solution.py:331
  192.4 6.0 %shard_map.96 = bf16[384,512]{1,0:T(8,128)(2,1)} custom-call(s32[6]{0:T(128)} %stack.27.info, bf16[4,400,256]{2,1,0:T(8,128)(2,1)} %all_to_all.26.refs_0_, bf16[4,416,512]{2,1,0:T(8,128)(2,1)} %shard_map.94.refs_0_.refs_1_, bf16[2048,2560]{1,0:T(8,128)(2,1)} %all-gather.2.cloned.1.call-done.refs_2_.refs_6_), custom_call_target="tpu_custom_call" | custom-call | tf_op jit(solution)/shard_map/pallas_call | solution.py:273
  (53 shorter events, 0.8 us)
Async XLA Ops:
  6.5 19.4 %copy-start.7 = (bf16[384,512]{1,0:T(8,128)(2,1)S(1)}, bf16[384,512]{1,0:T(8,128)(2,1)}, u32[]{:S(2)}) copy-start(bf16[384,512]{1,0:T(8,128)(2,1)} %param.9) | copy-start | bytes 1179652
  6.5 153.7 %all-gather.2.cloned.1.call-start = ((), (), s32[]{:S(2)}) async-start(), calls=%async_computation.5 | async-start | bytes 10649600 | tf_op jit(solution)/shard_map/all_gather | solution.py:318
  6.5 6.5 %collective-permute-start.12 = (bf16[3,32,256]{2,1,0:T(8,128)(2,1)}, bf16[3,32,256]{2,1,0:T(8,128)(2,1)S(1)}, u32[]{:S(2)}, u32[]{:S(2)}) collective-permute-start(bf16[3,32,256]{2,1,0:T(8,128)(2,1)} %bitcast.25), channel_id=1, source_target_pairs={{0,1},{1,2},{2,3},{3,0},{4,5},{5,6},{6,7},{7,4},{8,9},{9,10},{10,1... | collective-permute-start | bytes 147464 | tf_op jit(solution)/shard_map/ppermute | solution.py:26
  8.0 5.8 %collective-permute-start.13 = (bf16[3,32,256]{2,1,0:T(8,128)(2,1)}, bf16[3,32,256]{2,1,0:T(8,128)(2,1)S(1)}, u32[]{:S(2)}, u32[]{:S(2)}) collective-permute-start(bf16[3,32,256]{2,1,0:T(8,128)(2,1)} %bitcast.26), channel_id=1, source_target_pairs={{0,2},{1,3},{2,0},{3,1},{4,6},{5,7},{6,4},{7,5},{8,10},{9,11},{10,... | collective-permute-start | bytes 147464 | tf_op jit(solution)/shard_map/ppermute | solution.py:26
  10.8 4.3 %collective-permute-start.14 = (bf16[3,32,256]{2,1,0:T(8,128)(2,1)}, bf16[3,32,256]{2,1,0:T(8,128)(2,1)S(1)}, u32[]{:S(2)}, u32[]{:S(2)}) collective-permute-start(bf16[3,32,256]{2,1,0:T(8,128)(2,1)} %bitcast.27), channel_id=1, source_target_pairs={{0,3},{1,0},{2,1},{3,2},{4,7},{5,4},{6,5},{7,6},{8,11},{9,8},{10,9... | collective-permute-start | bytes 147464 | tf_op jit(solution)/shard_map/ppermute | solution.py:26
  17.5 26.1 %all-to-all-start = ((bf16[8,32,1024]{2,1,0:T(8,128)(2,1)}), bf16[8,32,1024]{2,1,0:T(8,128)(2,1)S(1)}, u32[]{:S(2)}, u32[]{:S(2)}) async-start(bf16[8,32,1024]{2,1,0:T(8,128)(2,1)} %broadcast_in_dim.6), calls=%async_computation | async-start | bytes 1048576 | tf_op jit(solution)/shard_map/all_to_all | solution.py:21
  26.0 5.6 %collective-permute-start = (bf16[48,512]{1,0:T(8,128)(2,1)S(1)}, bf16[48,512]{1,0:T(8,128)(2,1)S(1)}, u32[]{:S(2)}, u32[]{:S(2)}) collective-permute-start(bf16[48,512]{1,0:T(8,128)(2,1)S(1)} %get-tuple-element.14), channel_id=1, source_target_pairs={{0,4},{4,8},{8,12},{12,16},{16,20},{20,24},{24,28},{28,32},{32,36}... | collective-permute-start | bytes 147464 | tf_op jit(solution)/shard_map/ppermute | solution.py:320
  27.9 20.8 %collective-permute-start.1 = (bf16[48,512]{1,0:T(8,128)(2,1)S(1)}, bf16[48,512]{1,0:T(8,128)(2,1)S(1)}, u32[]{:S(2)}, u32[]{:S(2)}) collective-permute-start(bf16[48,512]{1,0:T(8,128)(2,1)S(1)} %get-tuple-element.13), channel_id=1, source_target_pairs={{4,0},{8,4},{12,8},{16,12},{20,16},{24,20},{28,24},{32,28},{36,32}... | collective-permute-start | bytes 147464 | tf_op jit(solution)/shard_map/ppermute | solution.py:321
  43.6 37.6 %copy-start = (bf16[8,32,1024]{2,1,0:T(8,128)(2,1)}, bf16[8,32,1024]{2,1,0:T(8,128)(2,1)S(1)}, u32[]{:S(2)}) copy-start(bf16[8,32,1024]{2,1,0:T(8,128)(2,1)S(1)} %all-to-all-done.refs_9_.refs_6_) | copy-start | bytes 1572868
  43.6 19.8 %collective-permute-start.6 = (bf16[8,32,1024]{2,1,0:T(8,128)(2,1)S(1)}, bf16[8,32,1024]{2,1,0:T(8,128)(2,1)S(1)}, u32[]{:S(2)}, u32[]{:S(2)}) collective-permute-start(bf16[8,32,1024]{2,1,0:T(8,128)(2,1)S(1)} %all-to-all-done.refs_9_.refs_6_), channel_id=1, source_target_pairs={{0,16},{8,24},{16,0},{24,8},{1,17},{9,25},{17,1},{25,9},{2,18},{10... | collective-permute-start | bytes 1572872 | tf_op jit(solution)/shard_map/ppermute | solution.py:26
  46.7 20.6 %collective-permute-start.7 = (bf16[8,32,1024]{2,1,0:T(8,128)(2,1)S(1)}, bf16[8,32,1024]{2,1,0:T(8,128)(2,1)S(1)}, u32[]{:S(2)}, u32[]{:S(2)}) collective-permute-start(bf16[8,32,1024]{2,1,0:T(8,128)(2,1)S(1)} %all-to-all-done.refs_9_.refs_6_), channel_id=1, source_target_pairs={{0,24},{8,0},{16,8},{24,16},{1,25},{9,1},{17,9},{25,17},{2,26},{10... | collective-permute-start | bytes 1572872 | tf_op jit(solution)/shard_map/ppermute | solution.py:26
  47.2 20.2 %collective-permute-start.5 = (bf16[8,32,1024]{2,1,0:T(8,128)(2,1)S(1)}, bf16[8,32,1024]{2,1,0:T(8,128)(2,1)S(1)}, u32[]{:S(2)}, u32[]{:S(2)}) collective-permute-start(bf16[8,32,1024]{2,1,0:T(8,128)(2,1)S(1)} %all-to-all-done.refs_9_.refs_6_), channel_id=1, source_target_pairs={{0,8},{8,16},{16,24},{24,0},{1,9},{9,17},{17,25},{25,1},{2,10},{10... | collective-permute-start | bytes 1572872 | tf_op jit(solution)/shard_map/ppermute | solution.py:26
  48.7 32.5 %copy-start.2 = (bf16[480,512]{1,0:T(8,128)(2,1)}, bf16[480,512]{1,0:T(8,128)(2,1)S(1)}, u32[]{:S(2)}) copy-start(bf16[480,512]{1,0:T(8,128)(2,1)S(1)} %constant_dynamic-update-slice_fusion.refs_0_.refs_1_) | copy-start | bytes 1474564
  48.7 14.6 %collective-permute-start.2 = (bf16[480,512]{1,0:T(8,128)(2,1)S(1)}, bf16[480,512]{1,0:T(8,128)(2,1)}, u32[]{:S(2)}, u32[]{:S(2)}) collective-permute-start(bf16[480,512]{1,0:T(8,128)(2,1)S(1)} %constant_dynamic-update-slice_fusion.refs_0_.refs_1_), channel_id=1, source_target_pairs={{0,1},{1,2},{2,3},{3,0},{4,5},{5,6},{6,7},{7,4},{8,9},{9,10},{10,1... | collective-permute-start | bytes 1474568 | tf_op jit(solution)/shard_map/ppermute | solution.py:26
  48.8 19.8 %collective-permute-start.3 = (bf16[480,512]{1,0:T(8,128)(2,1)S(1)}, bf16[480,512]{1,0:T(8,128)(2,1)}, u32[]{:S(2)}, u32[]{:S(2)}) collective-permute-start(bf16[480,512]{1,0:T(8,128)(2,1)S(1)} %constant_dynamic-update-slice_fusion.refs_0_.refs_1_), channel_id=1, source_target_pairs={{0,2},{1,3},{2,0},{3,1},{4,6},{5,7},{6,4},{7,5},{8,10},{9,11},{10,... | collective-permute-start | bytes 1474568 | tf_op jit(solution)/shard_map/ppermute | solution.py:26
  53.4 35.6 %all-to-all-start.2 = ((bf16[8,32,1024]{2,1,0:T(8,128)(2,1)}), bf16[8,32,1024]{2,1,0:T(8,128)(2,1)S(1)}, u32[]{:S(2)}, u32[]{:S(2)}) async-start(bf16[8,32,1024]{2,1,0:T(8,128)(2,1)} %broadcast_in_dim.7), calls=%async_computation.2 | async-start | bytes 1048576 | tf_op jit(solution)/shard_map/all_to_all | solution.py:21
  63.3 17.8 %collective-permute-start.8 = (bf16[8,32,1024]{2,1,0:T(8,128)(2,1)S(1)}, bf16[8,32,1024]{2,1,0:T(8,128)(2,1)}, u32[]{:S(2)}, u32[]{:S(2)}) collective-permute-start(bf16[8,32,1024]{2,1,0:T(8,128)(2,1)S(1)} %all-to-all-done.refs_9_.refs_6_), channel_id=1, source_target_pairs={{0,4},{4,0},{1,5},{5,1},{2,6},{6,2},{3,7},{7,3},{8,12},{12,8},{9,1... | collective-permute-start | bytes 1572872 | tf_op jit(solution)/shard_map/ppermute | solution.py:26
  63.3 17.9 %copy-start.4 = (bf16[8,32,1024]{2,1,0:T(8,128)(2,1)}, bf16[8,32,1024]{2,1,0:T(8,128)(2,1)S(1)}, u32[]{:S(2)}) copy-start(bf16[8,32,1024]{2,1,0:T(8,128)(2,1)S(1)} %collective-permute-done.6.refs_11_.refs_8_) | copy-start | bytes 1572868
  63.3 17.8 %collective-permute-start.10 = (bf16[8,32,1024]{2,1,0:T(8,128)(2,1)S(1)}, bf16[8,32,1024]{2,1,0:T(8,128)(2,1)}, u32[]{:S(2)}, u32[]{:S(2)}) collective-permute-start(bf16[8,32,1024]{2,1,0:T(8,128)(2,1)S(1)} %collective-permute-done.6.refs_11_.refs_8_), channel_id=1, source_target_pairs={{0,4},{4,0},{1,5},{5,1},{2,6},{6,2},{3,7},{7,3},{8,12},{12,8},{9,1... | collective-permute-start | bytes 1572872 | tf_op jit(solution)/shard_map/ppermute | solution.py:26
  67.3 13.9 %copy-start.5 = (bf16[8,32,1024]{2,1,0:T(8,128)(2,1)}, bf16[8,32,1024]{2,1,0:T(8,128)(2,1)S(1)}, u32[]{:S(2)}) copy-start(bf16[8,32,1024]{2,1,0:T(8,128)(2,1)S(1)} %collective-permute-done.7.refs_12_.refs_9_) | copy-start | bytes 1572868
  67.3 13.9 %collective-permute-start.11 = (bf16[8,32,1024]{2,1,0:T(8,128)(2,1)S(1)}, bf16[8,32,1024]{2,1,0:T(8,128)(2,1)}, u32[]{:S(2)}, u32[]{:S(2)}) collective-permute-start(bf16[8,32,1024]{2,1,0:T(8,128)(2,1)S(1)} %collective-permute-done.7.refs_12_.refs_9_), channel_id=1, source_target_pairs={{0,4},{4,0},{1,5},{5,1},{2,6},{6,2},{3,7},{7,3},{8,12},{12,8},{9,1... | collective-permute-start | bytes 1572872 | tf_op jit(solution)/shard_map/ppermute | solution.py:26
  67.4 13.8 %copy-start.6 = (bf16[8,32,1024]{2,1,0:T(8,128)(2,1)}, bf16[8,32,1024]{2,1,0:T(8,128)(2,1)S(1)}, u32[]{:S(2)}) copy-start(bf16[8,32,1024]{2,1,0:T(8,128)(2,1)S(1)} %collective-permute-done.5.refs_10_.refs_7_) | copy-start | bytes 1572868
  67.4 13.8 %collective-permute-start.9 = (bf16[8,32,1024]{2,1,0:T(8,128)(2,1)S(1)}, bf16[8,32,1024]{2,1,0:T(8,128)(2,1)}, u32[]{:S(2)}, u32[]{:S(2)}) collective-permute-start(bf16[8,32,1024]{2,1,0:T(8,128)(2,1)S(1)} %collective-permute-done.5.refs_10_.refs_7_), channel_id=1, source_target_pairs={{0,4},{4,0},{1,5},{5,1},{2,6},{6,2},{3,7},{7,3},{8,12},{12,8},{9,1... | collective-permute-start | bytes 1572872 | tf_op jit(solution)/shard_map/ppermute | solution.py:26
  68.6 12.6 %collective-permute-start.4 = (bf16[480,512]{1,0:T(8,128)(2,1)S(1)}, bf16[480,512]{1,0:T(8,128)(2,1)}, u32[]{:S(2)}, u32[]{:S(2)}) collective-permute-start(bf16[480,512]{1,0:T(8,128)(2,1)S(1)} %constant_dynamic-update-slice_fusion.refs_0_.refs_1_), channel_id=1, source_target_pairs={{0,3},{1,0},{2,1},{3,2},{4,7},{5,4},{6,5},{7,6},{8,11},{9,8},{10,9... | collective-permute-start | bytes 1474568 | tf_op jit(solution)/shard_map/ppermute | solution.py:26
  89.0 36.8 %copy-start.3 = (bf16[8,32,1024]{2,1,0:T(8,128)(2,1)}, bf16[8,32,1024]{2,1,0:T(8,128)(2,1)S(1)}, u32[]{:S(2)}) copy-start(bf16[8,32,1024]{2,1,0:T(8,128)(2,1)S(1)} %all-to-all-done.2.refs_5_) | copy-start | bytes 1572868
  89.0 31.6 %all-to-all-start.1 = ((bf16[4,464,256]{2,1,0:T(8,128)(2,1)}), bf16[4,464,256]{2,1,0:T(8,128)(2,1)S(1)}, u32[]{:S(2)}, u32[]{:S(2)}) async-start(bf16[4,464,256]{2,1,0:T(8,128)(2,1)} %shard_map.91), calls=%async_computation.1 | async-start | bytes 1900544 | tf_op jit(solution)/shard_map/all_to_all | solution.py:331
  93.3 16.9 %collective-permute-start.15 = (bf16[8,32,1024]{2,1,0:T(8,128)(2,1)S(1)}, bf16[8,32,1024]{2,1,0:T(8,128)(2,1)S(1)}, u32[]{:S(2)}, u32[]{:S(2)}) collective-permute-start(bf16[8,32,1024]{2,1,0:T(8,128)(2,1)S(1)} %all-to-all-done.2.refs_5_), channel_id=1, source_target_pairs={{0,8},{8,16},{16,24},{24,0},{1,9},{9,17},{17,25},{25,1},{2,10},{10... | collective-permute-start | bytes 1572872 | tf_op jit(solution)/shard_map/ppermute | solution.py:26
  94.8 16.3 %collective-permute-start.16 = (bf16[8,32,1024]{2,1,0:T(8,128)(2,1)S(1)}, bf16[8,32,1024]{2,1,0:T(8,128)(2,1)S(1)}, u32[]{:S(2)}, u32[]{:S(2)}) collective-permute-start(bf16[8,32,1024]{2,1,0:T(8,128)(2,1)S(1)} %all-to-all-done.2.refs_5_), channel_id=1, source_target_pairs={{0,16},{8,24},{16,0},{24,8},{1,17},{9,25},{17,1},{25,9},{2,18},{10... | collective-permute-start | bytes 1572872 | tf_op jit(solution)/shard_map/ppermute | solution.py:26
  96.9 23.7 %collective-permute-start.17 = (bf16[8,32,1024]{2,1,0:T(8,128)(2,1)S(1)}, bf16[8,32,1024]{2,1,0:T(8,128)(2,1)S(1)}, u32[]{:S(2)}, u32[]{:S(2)}) collective-permute-start(bf16[8,32,1024]{2,1,0:T(8,128)(2,1)S(1)} %all-to-all-done.2.refs_5_), channel_id=1, source_target_pairs={{0,24},{8,0},{16,8},{24,16},{1,25},{9,1},{17,9},{25,17},{2,26},{10... | collective-permute-start | bytes 1572872 | tf_op jit(solution)/shard_map/ppermute | solution.py:26
  110.2 15.6 %copy-start.8 = (bf16[8,32,1024]{2,1,0:T(8,128)(2,1)}, bf16[8,32,1024]{2,1,0:T(8,128)(2,1)S(1)}, u32[]{:S(2)}) copy-start(bf16[8,32,1024]{2,1,0:T(8,128)(2,1)S(1)} %collective-permute-done.15.refs_6_) | copy-start | bytes 1572868
  111.2 14.6 %copy-start.9 = (bf16[8,32,1024]{2,1,0:T(8,128)(2,1)}, bf16[8,32,1024]{2,1,0:T(8,128)(2,1)S(1)}, u32[]{:S(2)}) copy-start(bf16[8,32,1024]{2,1,0:T(8,128)(2,1)S(1)} %collective-permute-done.16.refs_7_) | copy-start | bytes 1572868
  120.6 5.2 %copy-start.10 = (bf16[8,32,1024]{2,1,0:T(8,128)(2,1)}, bf16[8,32,1024]{2,1,0:T(8,128)(2,1)S(1)}, u32[]{:S(2)}) copy-start(bf16[8,32,1024]{2,1,0:T(8,128)(2,1)S(1)} %collective-permute-done.17.refs_8_) | copy-start | bytes 1572868
  120.6 5.2 %copy-start.1 = (bf16[4,464,256]{2,1,0:T(8,128)(2,1)}, bf16[4,464,256]{2,1,0:T(8,128)(2,1)S(1)}, u32[]{:S(2)}) copy-start(bf16[4,464,256]{2,1,0:T(8,128)(2,1)S(1)} %all-to-all-done.1.refs_0_) | copy-start | bytes 2850820
  120.6 2.5 %collective-permute-start.18 = (bf16[8,32,1024]{2,1,0:T(8,128)(2,1)S(1)}, bf16[8,32,1024]{2,1,0:T(8,128)(2,1)S(1)}, u32[]{:S(2)}, u32[]{:S(2)}) collective-permute-start(bf16[8,32,1024]{2,1,0:T(8,128)(2,1)S(1)} %all-to-all-done.2.refs_5_), channel_id=1, source_target_pairs={{0,4},{4,0},{1,5},{5,1},{2,6},{6,2},{3,7},{7,3},{8,12},{12,8},{9,1... | collective-permute-start | bytes 1572872 | tf_op jit(solution)/shard_map/ppermute | solution.py:26
  120.8 3.3 %collective-permute-start.19 = (bf16[8,32,1024]{2,1,0:T(8,128)(2,1)S(1)}, bf16[8,32,1024]{2,1,0:T(8,128)(2,1)S(1)}, u32[]{:S(2)}, u32[]{:S(2)}) collective-permute-start(bf16[8,32,1024]{2,1,0:T(8,128)(2,1)S(1)} %collective-permute-done.15.refs_6_), channel_id=1, source_target_pairs={{0,4},{4,0},{1,5},{5,1},{2,6},{6,2},{3,7},{7,3},{8,12},{12,8},{9,1... | collective-permute-start | bytes 1572872 | tf_op jit(solution)/shard_map/ppermute | solution.py:26
  121.2 3.7 %collective-permute-start.20 = (bf16[8,32,1024]{2,1,0:T(8,128)(2,1)S(1)}, bf16[8,32,1024]{2,1,0:T(8,128)(2,1)S(1)}, u32[]{:S(2)}, u32[]{:S(2)}) collective-permute-start(bf16[8,32,1024]{2,1,0:T(8,128)(2,1)S(1)} %collective-permute-done.16.refs_7_), channel_id=1, source_target_pairs={{0,4},{4,0},{1,5},{5,1},{2,6},{6,2},{3,7},{7,3},{8,12},{12,8},{9,1... | collective-permute-start | bytes 1572872 | tf_op jit(solution)/shard_map/ppermute | solution.py:26
  121.3 4.4 %collective-permute-start.21 = (bf16[8,32,1024]{2,1,0:T(8,128)(2,1)S(1)}, bf16[8,32,1024]{2,1,0:T(8,128)(2,1)}, u32[]{:S(2)}, u32[]{:S(2)}) collective-permute-start(bf16[8,32,1024]{2,1,0:T(8,128)(2,1)S(1)} %collective-permute-done.17.refs_8_), channel_id=1, source_target_pairs={{0,4},{4,0},{1,5},{5,1},{2,6},{6,2},{3,7},{7,3},{8,12},{12,8},{9,1... | collective-permute-start | bytes 1572872 | tf_op jit(solution)/shard_map/ppermute | solution.py:26
  123.0 1.8 copy-start.11
  124.1 0.8 copy-start.12
  124.9 0.8 copy-start.13
Sparse Core Ops, SparseCore 0:
  16.7 107.2 all-gather.1

commit v4 on v3

--- a/solution.py
+++ b/solution.py
@@ -55,16 +55,39 @@
 
 
 def up_kernel(layer, total, n_s, n_y, first_lane, info, *refs):
-    streams, refs = refs[:n_s], refs[n_s:]
-    gain, tap_ref, bias, ln_gain, ln_shift, refs = *refs[:5], refs[5:]
+    streams, params, refs = refs[:n_s], refs[n_s : n_s + 5], refs[n_s + 5 :]
     pieces, refs = refs[:-7], refs[-7:]
-    out, weights, normed, both, padded, columns, sems = refs
+    up_work(layer, total, n_y, first_lane, info, streams, params, pieces, *refs)
+
+
+def mid_kernel(layer, total, n_s, n_out, down_lane, n_up, up_lane, n_x, info, *refs):
+    gated, streams, params, refs = refs[0], refs[1 : 1 + n_s], refs[1 + n_s : 6 + n_s], refs[6 + n_s :]
+    split = max(1, 2 * n_out)
+    down_pieces, up_pieces, refs = refs[:split], refs[split:-12], refs[-12:]
+    stream, out, refs = refs[0], refs[1], refs[2:]
+    down_scratch, up_scratch = refs[:4], refs[4:]
+
+    def first():
+        down_work(False, n_out, n_x, down_lane, info, gated, streams, down_pieces, stream, *down_scratch)
+
+    up_work(layer + 1, total, n_up, up_lane, info, [stream], params, up_pieces, out, *up_scratch, first=first)
+
+
+def down_kernel(n_x, first_lane, info, gated, stream, piece, out, *scratch):
+    down_work(True, 0, n_x, first_lane, info, gated, [stream], [piece], out, *scratch)
+
+
+def up_work(
+    layer, total, n_y, first_lane, info, streams, params, pieces, out, weights, normed, both, padded, columns, sems, first=None
+):
+    gain, tap_ref, bias, ln_gain, ln_shift = params
+    n_s = len(streams)
     rows, features = normed.shape
     width = streams[0].shape[-1]
     n_x = features // width
     keep = rows - 2 * EDGE
     ch = out.shape[-1]
-    outs = [out] if len(out.shape) == 2 else [out.at[b] for b in range(n_x)]
+    outs = [out.at[b] for b in range(n_x)]
     taps = tap_ref.shape[1]
     shift = EDGE - taps // 2
     core, my_x, my_y = info[0], info[1], info[2]
@@ -79,6 +102,8 @@
         copies = [pltpu.make_async_copy(pieces[0].at[:, pl.ds(first_lane, 2 * ch)], weights, sems.at[0])]
     for copy in copies:
         copy.start()
+    if first is not None:
+        first()
 
     def norm(first, step):
         here = pl.ds(first, step)
@@ -146,14 +171,10 @@
         to[keep:] = tail
 
 
-def down_kernel(last, n_s, n_y, n_x, n_g, first_lane, info, *refs):
-    gated, refs = refs[:n_g], refs[n_g:]
-    streams, refs = refs[:n_s], refs[n_s:]
-    pieces, refs = refs[:-5], refs[-5:]
-    out, weights, act, columns, sems = refs
+def down_work(last, n_y, n_x, first_lane, info, exchanged, streams, pieces, out, weights, act, columns, sems):
     core, my_x, my_y = info[0], info[1], info[2]
-    if n_g == 1:
-        gated = [gated[0].at[behind(my_x, s, n_x)] for s in range(n_x)]
+    n_s = len(streams)
+    gated = [exchanged.at[behind(my_x, s, n_x)] for s in range(n_x)]
     rows, ch = gated[0].shape
     keep = rows - EDGE
     width = out.shape[-1]
@@ -234,54 +255,76 @@
     return pl.BlockSpec(memory_space=pltpu.SMEM)
 
 
-def up(layer, total, info, streams, params, pieces, ch, fan, first_lane=0):
+def placed(pieces, features):
+    if len(pieces) == 1:
+        return 0, (features,)
+    n_z, n_i, _ = pieces[0].shape
+    return len(pieces) // 2, (n_z, len(pieces) // 2, 2, n_i)
+
+
+def up_scratch(shape, rows, features, ch, n_y):
+    return [
+        pltpu.VMEM((*shape, 2 * ch), bf16),
+        pltpu.VMEM((rows, features), bf16),
+        pltpu.VMEM((2, rows, ch), f32),
+        pltpu.VMEM((rows, ch), f32),
+        pltpu.VMEM((2 * ch, LANES), f32),
+        pltpu.SemaphoreType.DMA((max(1, 2 * n_y),)),
+    ]
+
+
+def down_scratch(shape, keep, n_x, ch, n_y):
+    return [
+        pltpu.VMEM((*shape, n_x * ch), bf16),
+        pltpu.VMEM((keep, n_x * ch), bf16),
+        pltpu.VMEM((2 * ch, LANES), f32),
+        pltpu.SemaphoreType.DMA((max(1, 2 * n_y),)),
+    ]
+
+
+def up(layer, total, info, streams, params, pieces, ch, first_lane):
     rows, width = streams[0].shape[-2:]
-    n_x = params[0].shape[1] // width
-    keep = rows - 2 * EDGE
-    n_y, shape = 0, (n_x * width,)
-    if len(pieces) > 1:
-        n_z, n_i, _ = pieces[0].shape[-3:]
-        n_y = len(pieces) // 2
-        shape = (n_z, n_y, 2, n_i)
+    features = params[0].shape[1]
+    n_y, shape = placed(pieces, features)
     return pl.pallas_call(
         functools.partial(up_kernel, layer, total, len(streams), n_y, first_lane),
-        out_shape=jax.ShapeDtypeStruct((n_x, keep + EDGE, ch) if fan else (keep + EDGE, ch), bf16),
+        out_shape=jax.ShapeDtypeStruct((features // width, rows - EDGE, ch), bf16),
         in_specs=[smem()] + [vmem()] * (len(streams) + len(params)) + [hbm()] * len(pieces),
         out_specs=vmem(),
-        scratch_shapes=[
-            pltpu.VMEM((*shape, 2 * ch), bf16),
-            pltpu.VMEM((rows, n_x * width), bf16),
-            pltpu.VMEM((2, rows, ch), f32),
-            pltpu.VMEM((rows, ch), f32),
-            pltpu.VMEM((2 * ch, LANES), f32),
-            pltpu.SemaphoreType.DMA((max(1, 2 * n_y),)),
-        ],
+        scratch_shapes=up_scratch(shape, rows, features, ch, n_y),
     )(info, *streams, *params, *pieces)
 
 
-def down(last, info, gated, streams, pieces, paired, first_lane=0):
-    rows, ch = gated[0].shape[-2:]
-    n_x = lax.axis_size("x")
+def mid(layer, total, info, gated, streams, params, outs, down_lane, ups, up_lane):
+    n_x, rows, ch = gated.shape
     keep = rows - EDGE
     width = streams[0].shape[-1]
-    n_y = len(pieces) // 2 if paired else 0
-    shape = (width if last else n_x * width,)
-    if paired:
-        n_z, n_i, _ = pieces[0].shape
-        shape = (n_z, n_y, 2, n_i)
-    out_shape = (keep, width) if last else (n_x, keep, width)
+    features = n_x * width
+    n_out, out_shape = placed(outs, features)
+    n_up, up_shape = placed(ups, features)
     return pl.pallas_call(
-        functools.partial(down_kernel, last, len(streams), n_y, n_x, len(gated), first_lane),
-        out_shape=jax.ShapeDtypeStruct(out_shape, bf16),
-        in_specs=[smem()] + [vmem()] * (len(gated) + len(streams)) + [hbm()] * len(pieces),
+        functools.partial(mid_kernel, layer, total, len(streams), n_out, down_lane, n_up, up_lane, n_x),
+        out_shape=(
+            jax.ShapeDtypeStruct((n_x, keep, width), bf16),
+            jax.ShapeDtypeStruct((n_x, keep - EDGE, ch), bf16),
+        ),
+        in_specs=[smem()] + [vmem()] * (1 + len(streams) + len(params)) + [hbm()] * (len(outs) + len(ups)),
+        out_specs=(vmem(), vmem()),
+        scratch_shapes=down_scratch(out_shape, keep, n_x, ch, n_out) + up_scratch(up_shape, keep, features, ch, n_up),
+    )(info, gated, *streams, *params, *outs, *ups)
+
+
+def down(info, gated, stream, piece, first_lane):
+    n_x, rows, ch = gated.shape
+    keep = rows - EDGE
+    width = stream.shape[-1]
+    return pl.pallas_call(
+        functools.partial(down_kernel, n_x, first_lane),
+        out_shape=jax.ShapeDtypeStruct((keep, width), bf16),
+        in_specs=[smem()] + [vmem()] * 2 + [hbm()],
         out_specs=vmem(),
-        scratch_shapes=[
-            pltpu.VMEM((*shape, n_x * ch), bf16),
-            pltpu.VMEM((keep, n_x * ch), bf16),
-            pltpu.VMEM((2 * ch, LANES), f32),
-            pltpu.SemaphoreType.DMA((len(pieces),)),
-        ],
-    )(info, *gated, *streams, *pieces)
+        scratch_shapes=down_scratch((width,), keep, n_x, ch, 0),
+    )(info, gated, stream, piece)
 
 
 def program(tokens, norm_gain, w_value, w_gate, conv_taps, conv_bias, ln_gain, ln_shift, w_out):
@@ -324,18 +367,20 @@
     ups = spread(ups, "y")
     outs = spread(gather_z(wide[0]), "y")
     ups = [*ups, *swap(ups)]
-
+    near_out = swap(outs[:1])
+
+    gated = up(0, total, info, streams, params, ups, ch, 0)
     for l in range(layers):
-        first, start = lanes[l]
-        gated = up(l, total, info, streams, params, ups if l < near else [rest], ch, True, first)
         gated = lax.all_to_all(gated, "x", split_axis=0, concat_axis=0, tiled=True)
         pieces = [rest]
         if l == 0:
-            pieces = after(outs, gated)
-            pieces = [*pieces, *swap(pieces)]
-        stream = down(l == layers - 1, info, [gated], streams, pieces, l == 0, start)
+            pieces = after(outs[1:], gated)
+            pieces = [outs[0], *pieces, *near_out, *swap(pieces)]
+        if l == layers - 1:
+            return down(info, gated, streams[0], rest, lanes[l][1])
+        up_pieces = ups if l + 1 < near else [rest]
+        stream, gated = mid(l, total, info, gated, streams, params, pieces, lanes[l][1], up_pieces, lanes[l + 1][0])
         streams = [stream]
-    return stream
 
 
 def solution(mesh):

time: 206 us -> 199 us (0.966)
  Pallas kernels: 45 us -> 38.9 us
    pallas_call x3 -> x1, Pallas kernels: 22.2 us -> 7.73 us  [up(): pl.pallas_call(functools.partial(up_kernel, layer, total, len(streams), n...]
    pallas_call x3, Pallas kernels: 22.8 us -> 31.2 us  [the longest x2 25.2 us: mid(): pl.pallas_call(functools.partial(mid_kernel, layer, total, len(streams),...]
  transfers between devices with their start and end apart: 26 -> 26, of which waited for: 15 -> 14; matrix products, arithmetic and copies ran while one was open for 2% -> 2% of each run, Pallas kernels for 12% -> 10%
where the time goes in v4:
time: 199 us; the launch traced here: 198 us
  waiting for transfers between devices  59.7 us (30%)
  starting transfers between devices  45.1 us (23%)
  Pallas kernels  38.9 us (20%)
  blocking collectives  35.4 us (18%)
  between operations  13.6 us (7%)
  local copies, waits for them, and re-layouts  4.13 us (2%)
    ppermute x20, waiting for transfers between devices, shifted(): return lax.ppermute(array, axis, [(i, (i + s) % n) for i in range(n)])  47.7 us
    all_to_all x2, blocking collectives, program(): gated = lax.all_to_all(gated, 'x', split_axis=0, concat_axis=0, tiled=True)  35.4 us
    pallas_call x2, Pallas kernels, mid(): pl.pallas_call(functools.partial(mid_kernel, layer, total, len(streams),...  25.2 us
    ppermute x20, starting transfers between devices, shifted(): return lax.ppermute(array, axis, [(i, (i + s) % n) for i in range(n)])  23.3 us
    all_to_all x2, waiting for transfers between devices, to_all(): return lax.all_to_all(copies, axis, split_axis=0, concat_axis=0, tiled=True)  12 us
    all_to_all x2, starting transfers between devices, to_all(): return lax.all_to_all(copies, axis, split_axis=0, concat_axis=0, tiled=True)  12 us
    pallas_call x1, Pallas kernels, up(): pl.pallas_call(functools.partial(up_kernel, layer, total, len(streams), n...  7.73 us
    pallas_call x1, Pallas kernels, down(): pl.pallas_call(functools.partial(down_kernel, n_x, first_lane), out_shape...  5.98 us
  transfers between devices with their start and end apart: 26, of which 14 were waited for; matrix products, arithmetic and copies ran while one was open for 2% of the time, Pallas kernels for 10%

profile of v4, /device:TPU:8, one launch (start us, length us, event | category | flops | bytes accessed | tf_op | source)
XLA Modules:
  0.0 198.4 jit_solution(18398668109899080811)
XLA Ops:
  6.5 1.5 collective-permute-start.12
  8.0 2.7 %collective-permute-start.13 = (bf16[3,32,256]{2,1,0:T(8,128)(2,1)}, bf16[3,32,256]{2,1,0:T(8,128)(2,1)S(1)}, u32[]{:S(2)}, u32[]{:S(2)}) collective-permute-start(bf16[3,32,256]{2,1,0:T(8,128)(2,1)} %bitcast.26), channel_id=1, source_target_pairs={{0,2},{1,3},{2,0},{3,1},{4,6},{5,7},{6,4},{7,5},{8,10},{9,11},{10,... | collective-permute-start | bytes 147464 | tf_op jit(solution)/shard_map/ppermute | solution.py:26
  10.8 1.4 collective-permute-start.14
  12.2 0.8 slice_bitcast_fusion.3
  13.0 0.8 collective-permute-done.13
  13.8 1.2 collective-permute-done.14
  15.1 0.8 pad_maximum_fusion
  15.9 0.7 pad_maximum_fusion.1
  16.6 0.9 broadcast_in_dim.6
  17.5 8.5 %all-to-all-start = ((bf16[8,32,1024]{2,1,0:T(8,128)(2,1)}), bf16[8,32,1024]{2,1,0:T(8,128)(2,1)S(1)}, u32[]{:S(2)}, u32[]{:S(2)}) async-start(bf16[8,32,1024]{2,1,0:T(8,128)(2,1)} %broadcast_in_dim.6), calls=%async_computation | async-start | bytes 1048576 | tf_op jit(solution)/shard_map/all_to_all | solution.py:21
  26.0 1.9 collective-permute-start
  27.9 3.6 %collective-permute-start.1 = (bf16[48,512]{1,0:T(8,128)(2,1)S(1)}, bf16[48,512]{1,0:T(8,128)(2,1)S(1)}, u32[]{:S(2)}, u32[]{:S(2)}) collective-permute-start(bf16[48,512]{1,0:T(8,128)(2,1)S(1)} %get-tuple-element.19), channel_id=1, source_target_pairs={{4,0},{8,4},{12,8},{16,12},{20,16},{24,20},{28,24},{32,28},{36,32}... | collective-permute-start | bytes 147464 | tf_op jit(solution)/shard_map/ppermute | solution.py:364
  31.6 12.0 %all-to-all-done.refs_9_.refs_18_ = bf16[8,32,1024]{2,1,0:T(8,128)(2,1)S(1)} async-done(((bf16[8,32,1024]{2,1,0:T(8,128)(2,1)}), bf16[8,32,1024]{2,1,0:T(8,128)(2,1)S(1)}, u32[]{:S(2)}, u32[]{:S(2)}) %all-to-all-start) | async-done | bytes 524320 | tf_op jit(solution)/shard_map/all_to_all | solution.py:21
  43.6 3.1 %collective-permute-start.6 = (bf16[8,32,1024]{2,1,0:T(8,128)(2,1)S(1)}, bf16[8,32,1024]{2,1,0:T(8,128)(2,1)S(1)}, u32[]{:S(2)}, u32[]{:S(2)}) collective-permute-start(bf16[8,32,1024]{2,1,0:T(8,128)(2,1)S(1)} %all-to-all-done.refs_9_.refs_18_), channel_id=1, source_target_pairs={{0,16},{8,24},{16,0},{24,8},{1,17},{9,25},{17,1},{25,9},{2,18},{10... | collective-permute-start | bytes 1572872 | tf_op jit(solution)/shard_map/ppermute | solution.py:26
  46.7 0.5 collective-permute-start.7
  47.2 1.5 collective-permute-start.5
  48.7 0.1 collective-permute-start.2
  48.8 3.7 %collective-permute-start.3 = (bf16[480,512]{1,0:T(8,128)(2,1)S(1)}, bf16[480,512]{1,0:T(8,128)(2,1)}, u32[]{:S(2)}, u32[]{:S(2)}) collective-permute-start(bf16[480,512]{1,0:T(8,128)(2,1)S(1)} %constant_dynamic-update-slice_fusion.refs_0_.refs_1_), channel_id=1, source_target_pairs={{0,2},{1,3},{2,0},{3,1},{4,6},{5,7},{6,4},{7,5},{8,10},{9,11},{10,... | collective-permute-start | bytes 1474568 | tf_op jit(solution)/shard_map/ppermute | solution.py:26
  52.5 0.9 broadcast_in_dim.7
  53.3 3.5 %all-to-all-start.2 = ((bf16[8,32,1024]{2,1,0:T(8,128)(2,1)}), bf16[8,32,1024]{2,1,0:T(8,128)(2,1)S(1)}, u32[]{:S(2)}, u32[]{:S(2)}) async-start(bf16[8,32,1024]{2,1,0:T(8,128)(2,1)} %broadcast_in_dim.7), calls=%async_computation.2 | async-start | bytes 1048576 | tf_op jit(solution)/shard_map/all_to_all | solution.py:21
  56.8 6.5 %collective-permute-done.2.refs_1_.refs_2_ = bf16[480,512]{1,0:T(8,128)(2,1)} collective-permute-done((bf16[480,512]{1,0:T(8,128)(2,1)S(1)}, bf16[480,512]{1,0:T(8,128)(2,1)}, u32[]{:S(2)}, u32[]{:S(2)}) %collective-permute-start.2) | collective-permute-done | bytes 491552 | tf_op jit(solution)/shard_map/ppermute | solution.py:26
  63.3 0.5 collective-permute-start.10
  63.8 3.5 %collective-permute-done.7.refs_12_.refs_21_ = bf16[8,32,1024]{2,1,0:T(8,128)(2,1)S(1)} collective-permute-done((bf16[8,32,1024]{2,1,0:T(8,128)(2,1)S(1)}, bf16[8,32,1024]{2,1,0:T(8,128)(2,1)S(1)}, u32[]{:S(2)}, u32[]{:S(2)}) %collective-permute-start.7) | collective-permute-done | bytes 524320 | tf_op jit(solution)/shard_map/ppermute | solution.py:26
  67.3 0.1 collective-permute-done.5.refs_10_.refs_19_
  67.4 0.4 collective-permute-start.9
  67.8 0.8 collective-permute-done.3.refs_2_.refs_3_
  68.6 1.0 collective-permute-start.4
  69.6 0.7 stack.27.info
  70.3 10.9 %collective-permute-done.4.refs_3_.refs_4_ = bf16[480,512]{1,0:T(8,128)(2,1)} collective-permute-done((bf16[480,512]{1,0:T(8,128)(2,1)S(1)}, bf16[480,512]{1,0:T(8,128)(2,1)}, u32[]{:S(2)}, u32[]{:S(2)}) %collective-permute-start.4) | collective-permute-done | bytes 491552 | tf_op jit(solution)/shard_map/ppermute | solution.py:26
  81.2 7.7 %shard_map.91 = bf16[4,464,256]{2,1,0:T(8,128)(2,1)} custom-call(s32[6]{0:T(128)} %stack.27.info, bf16[480,512]{1,0:T(8,128)(2,1)} %copy-done.2, bf16[480,512]{1,0:T(8,128)(2,1)} %collective-permute-done.2.refs_1_.refs_2_, bf16[480,512]{1,0:T(8,128)(2,1)} %collective-permute-done.3.refs_2_.refs_3_, bf16[480,512]{1,0:T(8,128)(2,1)} %collective-permute-done.4.refs_3_.refs_4_, ...), custom_call_target="tpu_custom_call" | custom-call | tf_op jit(solution)/shard_map/pallas_call | solution.py:289
  89.0 4.3 %all-to-all-start.1 = ((bf16[4,464,256]{2,1,0:T(8,128)(2,1)}), bf16[4,464,256]{2,1,0:T(8,128)(2,1)S(1)}, u32[]{:S(2)}, u32[]{:S(2)}) async-start(bf16[4,464,256]{2,1,0:T(8,128)(2,1)} %shard_map.91), calls=%async_computation.1 | async-start | bytes 1900544 | tf_op jit(solution)/shard_map/all_to_all | solution.py:374
  93.3 1.6 collective-permute-start.15
  94.8 2.0 %collective-permute-start.16 = (bf16[8,32,1024]{2,1,0:T(8,128)(2,1)S(1)}, bf16[8,32,1024]{2,1,0:T(8,128)(2,1)S(1)}, u32[]{:S(2)}, u32[]{:S(2)}) collective-permute-start(bf16[8,32,1024]{2,1,0:T(8,128)(2,1)S(1)} %all-to-all-done.2.refs_10_), channel_id=1, source_target_pairs={{0,16},{8,24},{16,0},{24,8},{1,17},{9,25},{17,1},{25,9},{2,18},{10... | collective-permute-start | bytes 1572872 | tf_op jit(solution)/shard_map/ppermute | solution.py:26
  96.9 2.5 %collective-permute-start.17 = (bf16[8,32,1024]{2,1,0:T(8,128)(2,1)S(1)}, bf16[8,32,1024]{2,1,0:T(8,128)(2,1)S(1)}, u32[]{:S(2)}, u32[]{:S(2)}) collective-permute-start(bf16[8,32,1024]{2,1,0:T(8,128)(2,1)S(1)} %all-to-all-done.2.refs_10_), channel_id=1, source_target_pairs={{0,24},{8,0},{16,8},{24,16},{1,25},{9,1},{17,9},{25,17},{2,26},{10... | collective-permute-start | bytes 1572872 | tf_op jit(solution)/shard_map/ppermute | solution.py:26
  99.4 10.7 %collective-permute-done.15.refs_11_ = bf16[8,32,1024]{2,1,0:T(8,128)(2,1)S(1)} collective-permute-done((bf16[8,32,1024]{2,1,0:T(8,128)(2,1)S(1)}, bf16[8,32,1024]{2,1,0:T(8,128)(2,1)S(1)}, u32[]{:S(2)}, u32[]{:S(2)}) %collective-permute-start.15) | collective-permute-done | bytes 524320 | tf_op jit(solution)/shard_map/ppermute | solution.py:26
  110.2 1.0 collective-permute-done.16.refs_12_
  111.2 9.4 %collective-permute-done.17.refs_13_ = bf16[8,32,1024]{2,1,0:T(8,128)(2,1)S(1)} collective-permute-done((bf16[8,32,1024]{2,1,0:T(8,128)(2,1)S(1)}, bf16[8,32,1024]{2,1,0:T(8,128)(2,1)S(1)}, u32[]{:S(2)}, u32[]{:S(2)}) %collective-permute-start.17) | collective-permute-done | bytes 524320 | tf_op jit(solution)/shard_map/ppermute | solution.py:26
  120.5 0.2 collective-permute-start.19
  120.8 0.4 collective-permute-start.20
  121.1 0.1 collective-permute-start.21
  121.3 1.8 collective-permute-done.19.refs_15_
  123.0 1.0 collective-permute-done.20.refs_16_
  124.0 0.8 copy-done.12
  124.9 12.9 %shard_map.92 = (bf16[4,448,512]{2,1,0:T(8,128)(2,1)}, bf16[4,432,256]{2,1,0:T(8,128)(2,1)}) custom-call(s32[6]{0:T(128)} %stack.27.info, bf16[4,464,256]{2,1,0:T(8,128)(2,1)} %copy-done.1, bf16[480,512]{1,0:T(8,128)(2,1)} %copy-done.2, bf16[480,512]{1,0:T(8,128)(2,1)} %collective-permute-done.2.refs_1_.refs_2_, ...), custom_call_target="tpu_custom_call" | custom-call | tf_op jit(solution)/shard_map/pallas_call | solution.py:305
  137.9 18.5 %all_to_all.25.refs_0_ = bf16[4,432,256]{2,1,0:T(8,128)(2,1)} all-to-all(bf16[4,432,256]{2,1,0:T(8,128)(2,1)} %get-tuple-element.15), channel_id=1, replica_groups=mesh['z'=8,'y'=4,'c'=2,'x'=4] {'x'}, dimensions={0} | all-to-all | bytes 1769472 | tf_op jit(solution)/shard_map/all_to_all | solution.py:374
  156.3 12.3 %shard_map.93 = (bf16[4,416,512]{2,1,0:T(8,128)(2,1)}, bf16[4,400,256]{2,1,0:T(8,128)(2,1)}) custom-call(s32[6]{0:T(128)} %stack.27.info, bf16[4,432,256]{2,1,0:T(8,128)(2,1)} %all_to_all.25.refs_0_, bf16[4,448,512]{2,1,0:T(8,128)(2,1)} %get-tuple-element.16.refs_1_, f32[3,2048]{1,0:T(4,128)} %refs_2_.1, f32[3,31,256]{2,1,0:T(8,128)} %refs_3_.1, ...), custom_call_target="tpu_custom_call" | custom-call | tf_op jit(solution)/shard_map/pallas_call | solution.py:305
  168.6 16.9 %all_to_all.26.gated = bf16[4,400,256]{2,1,0:T(8,128)(2,1)} all-to-all(bf16[4,400,256]{2,1,0:T(8,128)(2,1)} %get-tuple-element.17), channel_id=1, replica_groups=mesh['z'=8,'y'=4,'c'=2,'x'=4] {'x'}, dimensions={0} | all-to-all | bytes 1638400 | tf_op jit(solution)/shard_map/all_to_all | solution.py:374
  185.5 6.0 %shard_map.94 = bf16[384,512]{1,0:T(8,128)(2,1)} custom-call(s32[6]{0:T(128)} %stack.27.info, bf16[4,400,256]{2,1,0:T(8,128)(2,1)} %all_to_all.26.gated, bf16[4,416,512]{2,1,0:T(8,128)(2,1)} %get-tuple-element.18.stream, bf16[2048,2560]{1,0:T(8,128)(2,1)} %all-gather.2.cloned.1.call-done.refs_7_.refs_8_.piece), custom_call_target="tpu_custom_call" | custom-call | tf_op jit(solution)/shard_map/pallas_call | solution.py:321
  (49 shorter events, 0.2 us)
Async XLA Ops:
  6.5 19.4 %copy-start.7 = (bf16[384,512]{1,0:T(8,128)(2,1)S(1)}, bf16[384,512]{1,0:T(8,128)(2,1)}, u32[]{:S(2)}) copy-start(bf16[384,512]{1,0:T(8,128)(2,1)} %param.9) | copy-start | bytes 1179652
  6.5 149.8 %all-gather.2.cloned.1.call-start = ((), (), s32[]{:S(2)}) async-start(), calls=%async_computation.5 | async-start | bytes 10649600 | tf_op jit(solution)/shard_map/all_gather | solution.py:361
  6.5 6.5 %collective-permute-start.12 = (bf16[3,32,256]{2,1,0:T(8,128)(2,1)}, bf16[3,32,256]{2,1,0:T(8,128)(2,1)S(1)}, u32[]{:S(2)}, u32[]{:S(2)}) collective-permute-start(bf16[3,32,256]{2,1,0:T(8,128)(2,1)} %bitcast.25), channel_id=1, source_target_pairs={{0,1},{1,2},{2,3},{3,0},{4,5},{5,6},{6,7},{7,4},{8,9},{9,10},{10,1... | collective-permute-start | bytes 147464 | tf_op jit(solution)/shard_map/ppermute | solution.py:26
  8.0 5.8 %collective-permute-start.13 = (bf16[3,32,256]{2,1,0:T(8,128)(2,1)}, bf16[3,32,256]{2,1,0:T(8,128)(2,1)S(1)}, u32[]{:S(2)}, u32[]{:S(2)}) collective-permute-start(bf16[3,32,256]{2,1,0:T(8,128)(2,1)} %bitcast.26), channel_id=1, source_target_pairs={{0,2},{1,3},{2,0},{3,1},{4,6},{5,7},{6,4},{7,5},{8,10},{9,11},{10,... | collective-permute-start | bytes 147464 | tf_op jit(solution)/shard_map/ppermute | solution.py:26
  10.8 4.3 %collective-permute-start.14 = (bf16[3,32,256]{2,1,0:T(8,128)(2,1)}, bf16[3,32,256]{2,1,0:T(8,128)(2,1)S(1)}, u32[]{:S(2)}, u32[]{:S(2)}) collective-permute-start(bf16[3,32,256]{2,1,0:T(8,128)(2,1)} %bitcast.27), channel_id=1, source_target_pairs={{0,3},{1,0},{2,1},{3,2},{4,7},{5,4},{6,5},{7,6},{8,11},{9,8},{10,9... | collective-permute-start | bytes 147464 | tf_op jit(solution)/shard_map/ppermute | solution.py:26
  17.5 26.1 %all-to-all-start = ((bf16[8,32,1024]{2,1,0:T(8,128)(2,1)}), bf16[8,32,1024]{2,1,0:T(8,128)(2,1)S(1)}, u32[]{:S(2)}, u32[]{:S(2)}) async-start(bf16[8,32,1024]{2,1,0:T(8,128)(2,1)} %broadcast_in_dim.6), calls=%async_computation | async-start | bytes 1048576 | tf_op jit(solution)/shard_map/all_to_all | solution.py:21
  26.0 5.6 %collective-permute-start = (bf16[48,512]{1,0:T(8,128)(2,1)S(1)}, bf16[48,512]{1,0:T(8,128)(2,1)S(1)}, u32[]{:S(2)}, u32[]{:S(2)}) collective-permute-start(bf16[48,512]{1,0:T(8,128)(2,1)S(1)} %get-tuple-element.20), channel_id=1, source_target_pairs={{0,4},{4,8},{8,12},{12,16},{16,20},{20,24},{24,28},{28,32},{32,36}... | collective-permute-start | bytes 147464 | tf_op jit(solution)/shard_map/ppermute | solution.py:363
  27.9 20.8 %collective-permute-start.1 = (bf16[48,512]{1,0:T(8,128)(2,1)S(1)}, bf16[48,512]{1,0:T(8,128)(2,1)S(1)}, u32[]{:S(2)}, u32[]{:S(2)}) collective-permute-start(bf16[48,512]{1,0:T(8,128)(2,1)S(1)} %get-tuple-element.19), channel_id=1, source_target_pairs={{4,0},{8,4},{12,8},{16,12},{20,16},{24,20},{28,24},{32,28},{36,32}... | collective-permute-start | bytes 147464 | tf_op jit(solution)/shard_map/ppermute | solution.py:364
  43.6 37.6 %copy-start = (bf16[8,32,1024]{2,1,0:T(8,128)(2,1)}, bf16[8,32,1024]{2,1,0:T(8,128)(2,1)S(1)}, u32[]{:S(2)}) copy-start(bf16[8,32,1024]{2,1,0:T(8,128)(2,1)S(1)} %all-to-all-done.refs_9_.refs_18_) | copy-start | bytes 1572868
  43.6 19.8 %collective-permute-start.6 = (bf16[8,32,1024]{2,1,0:T(8,128)(2,1)S(1)}, bf16[8,32,1024]{2,1,0:T(8,128)(2,1)S(1)}, u32[]{:S(2)}, u32[]{:S(2)}) collective-permute-start(bf16[8,32,1024]{2,1,0:T(8,128)(2,1)S(1)} %all-to-all-done.refs_9_.refs_18_), channel_id=1, source_target_pairs={{0,16},{8,24},{16,0},{24,8},{1,17},{9,25},{17,1},{25,9},{2,18},{10... | collective-permute-start | bytes 1572872 | tf_op jit(solution)/shard_map/ppermute | solution.py:26
  46.7 20.6 %collective-permute-start.7 = (bf16[8,32,1024]{2,1,0:T(8,128)(2,1)S(1)}, bf16[8,32,1024]{2,1,0:T(8,128)(2,1)S(1)}, u32[]{:S(2)}, u32[]{:S(2)}) collective-permute-start(bf16[8,32,1024]{2,1,0:T(8,128)(2,1)S(1)} %all-to-all-done.refs_9_.refs_18_), channel_id=1, source_target_pairs={{0,24},{8,0},{16,8},{24,16},{1,25},{9,1},{17,9},{25,17},{2,26},{10... | collective-permute-start | bytes 1572872 | tf_op jit(solution)/shard_map/ppermute | solution.py:26
  47.2 20.2 %collective-permute-start.5 = (bf16[8,32,1024]{2,1,0:T(8,128)(2,1)S(1)}, bf16[8,32,1024]{2,1,0:T(8,128)(2,1)S(1)}, u32[]{:S(2)}, u32[]{:S(2)}) collective-permute-start(bf16[8,32,1024]{2,1,0:T(8,128)(2,1)S(1)} %all-to-all-done.refs_9_.refs_18_), channel_id=1, source_target_pairs={{0,8},{8,16},{16,24},{24,0},{1,9},{9,17},{17,25},{25,1},{2,10},{10... | collective-permute-start | bytes 1572872 | tf_op jit(solution)/shard_map/ppermute | solution.py:26
  48.7 32.5 %copy-start.2 = (bf16[480,512]{1,0:T(8,128)(2,1)}, bf16[480,512]{1,0:T(8,128)(2,1)S(1)}, u32[]{:S(2)}) copy-start(bf16[480,512]{1,0:T(8,128)(2,1)S(1)} %constant_dynamic-update-slice_fusion.refs_0_.refs_1_) | copy-start | bytes 1474564
  48.7 14.6 %collective-permute-start.2 = (bf16[480,512]{1,0:T(8,128)(2,1)S(1)}, bf16[480,512]{1,0:T(8,128)(2,1)}, u32[]{:S(2)}, u32[]{:S(2)}) collective-permute-start(bf16[480,512]{1,0:T(8,128)(2,1)S(1)} %constant_dynamic-update-slice_fusion.refs_0_.refs_1_), channel_id=1, source_target_pairs={{0,1},{1,2},{2,3},{3,0},{4,5},{5,6},{6,7},{7,4},{8,9},{9,10},{10,1... | collective-permute-start | bytes 1474568 | tf_op jit(solution)/shard_map/ppermute | solution.py:26
  48.8 19.8 %collective-permute-start.3 = (bf16[480,512]{1,0:T(8,128)(2,1)S(1)}, bf16[480,512]{1,0:T(8,128)(2,1)}, u32[]{:S(2)}, u32[]{:S(2)}) collective-permute-start(bf16[480,512]{1,0:T(8,128)(2,1)S(1)} %constant_dynamic-update-slice_fusion.refs_0_.refs_1_), channel_id=1, source_target_pairs={{0,2},{1,3},{2,0},{3,1},{4,6},{5,7},{6,4},{7,5},{8,10},{9,11},{10,... | collective-permute-start | bytes 1474568 | tf_op jit(solution)/shard_map/ppermute | solution.py:26
  53.3 35.6 %all-to-all-start.2 = ((bf16[8,32,1024]{2,1,0:T(8,128)(2,1)}), bf16[8,32,1024]{2,1,0:T(8,128)(2,1)S(1)}, u32[]{:S(2)}, u32[]{:S(2)}) async-start(bf16[8,32,1024]{2,1,0:T(8,128)(2,1)} %broadcast_in_dim.7), calls=%async_computation.2 | async-start | bytes 1048576 | tf_op jit(solution)/shard_map/all_to_all | solution.py:21
  63.3 17.8 %collective-permute-start.8 = (bf16[8,32,1024]{2,1,0:T(8,128)(2,1)S(1)}, bf16[8,32,1024]{2,1,0:T(8,128)(2,1)}, u32[]{:S(2)}, u32[]{:S(2)}) collective-permute-start(bf16[8,32,1024]{2,1,0:T(8,128)(2,1)S(1)} %all-to-all-done.refs_9_.refs_18_), channel_id=1, source_target_pairs={{0,4},{4,0},{1,5},{5,1},{2,6},{6,2},{3,7},{7,3},{8,12},{12,8},{9,1... | collective-permute-start | bytes 1572872 | tf_op jit(solution)/shard_map/ppermute | solution.py:26
  63.3 17.9 %copy-start.4 = (bf16[8,32,1024]{2,1,0:T(8,128)(2,1)}, bf16[8,32,1024]{2,1,0:T(8,128)(2,1)S(1)}, u32[]{:S(2)}) copy-start(bf16[8,32,1024]{2,1,0:T(8,128)(2,1)S(1)} %collective-permute-done.6.refs_11_.refs_20_) | copy-start | bytes 1572868
  63.3 17.8 %collective-permute-start.10 = (bf16[8,32,1024]{2,1,0:T(8,128)(2,1)S(1)}, bf16[8,32,1024]{2,1,0:T(8,128)(2,1)}, u32[]{:S(2)}, u32[]{:S(2)}) collective-permute-start(bf16[8,32,1024]{2,1,0:T(8,128)(2,1)S(1)} %collective-permute-done.6.refs_11_.refs_20_), channel_id=1, source_target_pairs={{0,4},{4,0},{1,5},{5,1},{2,6},{6,2},{3,7},{7,3},{8,12},{12,8},{9,1... | collective-permute-start | bytes 1572872 | tf_op jit(solution)/shard_map/ppermute | solution.py:26
  67.3 13.9 %copy-start.5 = (bf16[8,32,1024]{2,1,0:T(8,128)(2,1)}, bf16[8,32,1024]{2,1,0:T(8,128)(2,1)S(1)}, u32[]{:S(2)}) copy-start(bf16[8,32,1024]{2,1,0:T(8,128)(2,1)S(1)} %collective-permute-done.7.refs_12_.refs_21_) | copy-start | bytes 1572868
  67.3 13.9 %collective-permute-start.11 = (bf16[8,32,1024]{2,1,0:T(8,128)(2,1)S(1)}, bf16[8,32,1024]{2,1,0:T(8,128)(2,1)}, u32[]{:S(2)}, u32[]{:S(2)}) collective-permute-start(bf16[8,32,1024]{2,1,0:T(8,128)(2,1)S(1)} %collective-permute-done.7.refs_12_.refs_21_), channel_id=1, source_target_pairs={{0,4},{4,0},{1,5},{5,1},{2,6},{6,2},{3,7},{7,3},{8,12},{12,8},{9,1... | collective-permute-start | bytes 1572872 | tf_op jit(solution)/shard_map/ppermute | solution.py:26
  67.4 13.8 %copy-start.6 = (bf16[8,32,1024]{2,1,0:T(8,128)(2,1)}, bf16[8,32,1024]{2,1,0:T(8,128)(2,1)S(1)}, u32[]{:S(2)}) copy-start(bf16[8,32,1024]{2,1,0:T(8,128)(2,1)S(1)} %collective-permute-done.5.refs_10_.refs_19_) | copy-start | bytes 1572868
  67.4 13.8 %collective-permute-start.9 = (bf16[8,32,1024]{2,1,0:T(8,128)(2,1)S(1)}, bf16[8,32,1024]{2,1,0:T(8,128)(2,1)}, u32[]{:S(2)}, u32[]{:S(2)}) collective-permute-start(bf16[8,32,1024]{2,1,0:T(8,128)(2,1)S(1)} %collective-permute-done.5.refs_10_.refs_19_), channel_id=1, source_target_pairs={{0,4},{4,0},{1,5},{5,1},{2,6},{6,2},{3,7},{7,3},{8,12},{12,8},{9,1... | collective-permute-start | bytes 1572872 | tf_op jit(solution)/shard_map/ppermute | solution.py:26
  68.6 12.6 %collective-permute-start.4 = (bf16[480,512]{1,0:T(8,128)(2,1)S(1)}, bf16[480,512]{1,0:T(8,128)(2,1)}, u32[]{:S(2)}, u32[]{:S(2)}) collective-permute-start(bf16[480,512]{1,0:T(8,128)(2,1)S(1)} %constant_dynamic-update-slice_fusion.refs_0_.refs_1_), channel_id=1, source_target_pairs={{0,3},{1,0},{2,1},{3,2},{4,7},{5,4},{6,5},{7,6},{8,11},{9,8},{10,9... | collective-permute-start | bytes 1474568 | tf_op jit(solution)/shard_map/ppermute | solution.py:26
  89.0 35.9 %copy-start.3 = (bf16[8,32,1024]{2,1,0:T(8,128)(2,1)}, bf16[8,32,1024]{2,1,0:T(8,128)(2,1)S(1)}, u32[]{:S(2)}) copy-start(bf16[8,32,1024]{2,1,0:T(8,128)(2,1)S(1)} %all-to-all-done.2.refs_10_) | copy-start | bytes 1572868
  89.0 31.6 %all-to-all-start.1 = ((bf16[4,464,256]{2,1,0:T(8,128)(2,1)}), bf16[4,464,256]{2,1,0:T(8,128)(2,1)S(1)}, u32[]{:S(2)}, u32[]{:S(2)}) async-start(bf16[4,464,256]{2,1,0:T(8,128)(2,1)} %shard_map.91), calls=%async_computation.1 | async-start | bytes 1900544 | tf_op jit(solution)/shard_map/all_to_all | solution.py:374
  93.3 16.9 %collective-permute-start.15 = (bf16[8,32,1024]{2,1,0:T(8,128)(2,1)S(1)}, bf16[8,32,1024]{2,1,0:T(8,128)(2,1)S(1)}, u32[]{:S(2)}, u32[]{:S(2)}) collective-permute-start(bf16[8,32,1024]{2,1,0:T(8,128)(2,1)S(1)} %all-to-all-done.2.refs_10_), channel_id=1, source_target_pairs={{0,8},{8,16},{16,24},{24,0},{1,9},{9,17},{17,25},{25,1},{2,10},{10... | collective-permute-start | bytes 1572872 | tf_op jit(solution)/shard_map/ppermute | solution.py:26
  94.8 16.3 %collective-permute-start.16 = (bf16[8,32,1024]{2,1,0:T(8,128)(2,1)S(1)}, bf16[8,32,1024]{2,1,0:T(8,128)(2,1)S(1)}, u32[]{:S(2)}, u32[]{:S(2)}) collective-permute-start(bf16[8,32,1024]{2,1,0:T(8,128)(2,1)S(1)} %all-to-all-done.2.refs_10_), channel_id=1, source_target_pairs={{0,16},{8,24},{16,0},{24,8},{1,17},{9,25},{17,1},{25,9},{2,18},{10... | collective-permute-start | bytes 1572872 | tf_op jit(solution)/shard_map/ppermute | solution.py:26
  96.9 23.7 %collective-permute-start.17 = (bf16[8,32,1024]{2,1,0:T(8,128)(2,1)S(1)}, bf16[8,32,1024]{2,1,0:T(8,128)(2,1)S(1)}, u32[]{:S(2)}, u32[]{:S(2)}) collective-permute-start(bf16[8,32,1024]{2,1,0:T(8,128)(2,1)S(1)} %all-to-all-done.2.refs_10_), channel_id=1, source_target_pairs={{0,24},{8,0},{16,8},{24,16},{1,25},{9,1},{17,9},{25,17},{2,26},{10... | collective-permute-start | bytes 1572872 | tf_op jit(solution)/shard_map/ppermute | solution.py:26
  99.4 21.9 %collective-permute-start.18 = (bf16[8,32,1024]{2,1,0:T(8,128)(2,1)S(1)}, bf16[8,32,1024]{2,1,0:T(8,128)(2,1)}, u32[]{:S(2)}, u32[]{:S(2)}) collective-permute-start(bf16[8,32,1024]{2,1,0:T(8,128)(2,1)S(1)} %all-to-all-done.2.refs_10_), channel_id=1, source_target_pairs={{0,4},{4,0},{1,5},{5,1},{2,6},{6,2},{3,7},{7,3},{8,12},{12,8},{9,1... | collective-permute-start | bytes 1572872 | tf_op jit(solution)/shard_map/ppermute | solution.py:26
  110.2 14.8 %copy-start.8 = (bf16[8,32,1024]{2,1,0:T(8,128)(2,1)}, bf16[8,32,1024]{2,1,0:T(8,128)(2,1)S(1)}, u32[]{:S(2)}) copy-start(bf16[8,32,1024]{2,1,0:T(8,128)(2,1)S(1)} %collective-permute-done.15.refs_11_) | copy-start | bytes 1572868
  111.2 13.7 %copy-start.9 = (bf16[8,32,1024]{2,1,0:T(8,128)(2,1)}, bf16[8,32,1024]{2,1,0:T(8,128)(2,1)S(1)}, u32[]{:S(2)}) copy-start(bf16[8,32,1024]{2,1,0:T(8,128)(2,1)S(1)} %collective-permute-done.16.refs_12_) | copy-start | bytes 1572868
  120.5 4.4 %copy-start.10 = (bf16[8,32,1024]{2,1,0:T(8,128)(2,1)}, bf16[8,32,1024]{2,1,0:T(8,128)(2,1)S(1)}, u32[]{:S(2)}) copy-start(bf16[8,32,1024]{2,1,0:T(8,128)(2,1)S(1)} %collective-permute-done.17.refs_13_) | copy-start | bytes 1572868
  120.5 4.4 %copy-start.1 = (bf16[4,464,256]{2,1,0:T(8,128)(2,1)}, bf16[4,464,256]{2,1,0:T(8,128)(2,1)S(1)}, u32[]{:S(2)}) copy-start(bf16[4,464,256]{2,1,0:T(8,128)(2,1)S(1)} %all-to-all-done.1.refs_0_) | copy-start | bytes 2850820
  120.5 2.5 %collective-permute-start.19 = (bf16[8,32,1024]{2,1,0:T(8,128)(2,1)S(1)}, bf16[8,32,1024]{2,1,0:T(8,128)(2,1)S(1)}, u32[]{:S(2)}, u32[]{:S(2)}) collective-permute-start(bf16[8,32,1024]{2,1,0:T(8,128)(2,1)S(1)} %collective-permute-done.15.refs_11_), channel_id=1, source_target_pairs={{0,4},{4,0},{1,5},{5,1},{2,6},{6,2},{3,7},{7,3},{8,12},{12,8},{9,1... | collective-permute-start | bytes 1572872 | tf_op jit(solution)/shard_map/ppermute | solution.py:26
  120.8 3.3 %collective-permute-start.20 = (bf16[8,32,1024]{2,1,0:T(8,128)(2,1)S(1)}, bf16[8,32,1024]{2,1,0:T(8,128)(2,1)S(1)}, u32[]{:S(2)}, u32[]{:S(2)}) collective-permute-start(bf16[8,32,1024]{2,1,0:T(8,128)(2,1)S(1)} %collective-permute-done.16.refs_12_), channel_id=1, source_target_pairs={{0,4},{4,0},{1,5},{5,1},{2,6},{6,2},{3,7},{7,3},{8,12},{12,8},{9,1... | collective-permute-start | bytes 1572872 | tf_op jit(solution)/shard_map/ppermute | solution.py:26
  121.1 3.8 %collective-permute-start.21 = (bf16[8,32,1024]{2,1,0:T(8,128)(2,1)S(1)}, bf16[8,32,1024]{2,1,0:T(8,128)(2,1)}, u32[]{:S(2)}, u32[]{:S(2)}) collective-permute-start(bf16[8,32,1024]{2,1,0:T(8,128)(2,1)S(1)} %collective-permute-done.17.refs_13_), channel_id=1, source_target_pairs={{0,4},{4,0},{1,5},{5,1},{2,6},{6,2},{3,7},{7,3},{8,12},{12,8},{9,1... | collective-permute-start | bytes 1572872 | tf_op jit(solution)/shard_map/ppermute | solution.py:26
  123.0 1.0 copy-start.11
  124.0 0.8 copy-start.12
Sparse Core Ops, SparseCore 0:
  16.7 107.1 all-gather.1

commit v5 on v4

--- a/solution.py
+++ b/solution.py
@@ -61,7 +61,8 @@
 
 
 def mid_kernel(layer, total, n_s, n_out, down_lane, n_up, up_lane, n_x, info, *refs):
-    gated, streams, params, refs = refs[0], refs[1 : 1 + n_s], refs[1 + n_s : 6 + n_s], refs[6 + n_s :]
+    gated, refs = refs[:n_x], refs[n_x:]
+    streams, params, refs = refs[:n_s], refs[n_s : n_s + 5], refs[n_s + 5 :]
     split = max(1, 2 * n_out)
     down_pieces, up_pieces, refs = refs[:split], refs[split:-12], refs[-12:]
     stream, out, refs = refs[0], refs[1], refs[2:]
@@ -73,7 +74,8 @@
     up_work(layer + 1, total, n_up, up_lane, info, [stream], params, up_pieces, out, *up_scratch, first=first)
 
 
-def down_kernel(n_x, first_lane, info, gated, stream, piece, out, *scratch):
+def down_kernel(n_x, first_lane, info, *refs):
+    gated, (stream, piece, out, *scratch) = refs[:n_x], refs[n_x:]
     down_work(True, 0, n_x, first_lane, info, gated, [stream], [piece], out, *scratch)
 
 
@@ -87,7 +89,6 @@
     n_x = features // width
     keep = rows - 2 * EDGE
     ch = out.shape[-1]
-    outs = [out.at[b] for b in range(n_x)]
     taps = tap_ref.shape[1]
     shift = EDGE - taps // 2
     core, my_x, my_y = info[0], info[1], info[2]
@@ -152,8 +153,7 @@
             accs.append(acc)
         mean = jnp.sum(sum(accs), axis=-1, keepdims=True) * (1.0 / ch)
         for start, acc in zip(range(0, ch, LANES), accs):
-            for to in outs:
-                to[pl.ds(first, size), start : start + LANES] = (acc - mean).astype(bf16)
+            out[pl.ds(first, size), start : start + LANES] = (acc - mean).astype(bf16)
         high = mean.astype(bf16).astype(f32)
         lane = lax.broadcasted_iota(jnp.int32, (size, LANES), 1)
         columns[pl.ds(first, size)] = jnp.where(lane == 0, high, jnp.where(lane == 1, mean - high, 0.0))
@@ -167,14 +167,12 @@
         across = jnp.where(row == 2 + p, part, across)
         params = params - part
     tail = jnp.concatenate([across[:, :ch], across[:, ch:]], axis=0).astype(bf16)
-    for to in outs:
-        to[keep:] = tail
-
-
-def down_work(last, n_y, n_x, first_lane, info, exchanged, streams, pieces, out, weights, act, columns, sems):
+    out[keep:] = tail
+
+
+def down_work(last, n_y, n_x, first_lane, info, gated, streams, pieces, out, weights, act, columns, sems):
     core, my_x, my_y = info[0], info[1], info[2]
     n_s = len(streams)
-    gated = [exchanged.at[behind(my_x, s, n_x)] for s in range(n_x)]
     rows, ch = gated[0].shape
     keep = rows - EDGE
     width = out.shape[-1]
@@ -283,12 +281,12 @@
 
 
 def up(layer, total, info, streams, params, pieces, ch, first_lane):
-    rows, width = streams[0].shape[-2:]
+    rows = streams[0].shape[-2]
     features = params[0].shape[1]
     n_y, shape = placed(pieces, features)
     return pl.pallas_call(
         functools.partial(up_kernel, layer, total, len(streams), n_y, first_lane),
-        out_shape=jax.ShapeDtypeStruct((features // width, rows - EDGE, ch), bf16),
+        out_shape=jax.ShapeDtypeStruct((rows - EDGE, ch), bf16),
         in_specs=[smem()] + [vmem()] * (len(streams) + len(params)) + [hbm()] * len(pieces),
         out_specs=vmem(),
         scratch_shapes=up_scratch(shape, rows, features, ch, n_y),
@@ -296,7 +294,8 @@
 
 
 def mid(layer, total, info, gated, streams, params, outs, down_lane, ups, up_lane):
-    n_x, rows, ch = gated.shape
+    n_x = len(gated)
+    rows, ch = gated[0].shape
     keep = rows - EDGE
     width = streams[0].shape[-1]
     features = n_x * width
@@ -306,25 +305,26 @@
         functools.partial(mid_kernel, layer, total, len(streams), n_out, down_lane, n_up, up_lane, n_x),
         out_shape=(
             jax.ShapeDtypeStruct((n_x, keep, width), bf16),
-            jax.ShapeDtypeStruct((n_x, keep - EDGE, ch), bf16),
+            jax.ShapeDtypeStruct((keep - EDGE, ch), bf16),
         ),
-        in_specs=[smem()] + [vmem()] * (1 + len(streams) + len(params)) + [hbm()] * (len(outs) + len(ups)),
+        in_specs=[smem()] + [vmem()] * (n_x + len(streams) + len(params)) + [hbm()] * (len(outs) + len(ups)),
         out_specs=(vmem(), vmem()),
         scratch_shapes=down_scratch(out_shape, keep, n_x, ch, n_out) + up_scratch(up_shape, keep, features, ch, n_up),
-    )(info, gated, *streams, *params, *outs, *ups)
+    )(info, *gated, *streams, *params, *outs, *ups)
 
 
 def down(info, gated, stream, piece, first_lane):
-    n_x, rows, ch = gated.shape
+    n_x = len(gated)
+    rows, ch = gated[0].shape
     keep = rows - EDGE
     width = stream.shape[-1]
     return pl.pallas_call(
         functools.partial(down_kernel, n_x, first_lane),
         out_shape=jax.ShapeDtypeStruct((keep, width), bf16),
-        in_specs=[smem()] + [vmem()] * 2 + [hbm()],
+        in_specs=[smem()] + [vmem()] * (n_x + 1) + [hbm()],
         out_specs=vmem(),
         scratch_shapes=down_scratch((width,), keep, n_x, ch, 0),
-    )(info, gated, stream, piece)
+    )(info, *gated, stream, piece)
 
 
 def program(tokens, norm_gain, w_value, w_gate, conv_taps, conv_bias, ln_gain, ln_shift, w_out):
@@ -371,10 +371,10 @@
 
     gated = up(0, total, info, streams, params, ups, ch, 0)
     for l in range(layers):
-        gated = lax.all_to_all(gated, "x", split_axis=0, concat_axis=0, tiled=True)
+        block, gated = gated, spread(gated, "x")
         pieces = [rest]
         if l == 0:
-            pieces = after(outs[1:], gated)
+            pieces = after(outs[1:], block)
             pieces = [outs[0], *pieces, *near_out, *swap(pieces)]
         if l == layers - 1:
             return down(info, gated, streams[0], rest, lanes[l][1])

time: 199 us -> 206 us (1.035)
  the two profiles are of different devices: /device:TPU:8 before, /device:TPU:32 now
where the time goes in v5:
time: 206 us; the launch traced here: 205 us
  waiting for transfers between devices  86.6 us (42%)
  starting transfers between devices  58.5 us (28%)
  Pallas kernels  38.6 us (19%)
  between operations  13.6 us (7%)
  local copies, waits for them, and re-layouts  6.5 us (3%)
    ppermute x29, waiting for transfers between devices, shifted(): return lax.ppermute(array, axis, [(i, (i + s) % n) for i in range(n)])  78.6 us
    ppermute x29, starting transfers between devices, shifted(): return lax.ppermute(array, axis, [(i, (i + s) % n) for i in range(n)])  36.8 us
    pallas_call x2, Pallas kernels, mid(): pl.pallas_call(functools.partial(mid_kernel, layer, total, len(streams),...  25.1 us
    all_to_all x2, starting transfers between devices, to_all(): return lax.all_to_all(copies, axis, split_axis=0, concat_axis=0, tiled=True)  14 us
    pallas_call x1, Pallas kernels, up(): pl.pallas_call(functools.partial(up_kernel, layer, total, len(streams), n...  7.47 us
    pallas_call x1, Pallas kernels, down(): pl.pallas_call(functools.partial(down_kernel, n_x, first_lane), out_shape...  6.1 us
    ppermute x1, starting transfers between devices, program(): lax.ppermute(tokens[:halo], SP, [(i + 1, i) for i in range(size - 1)])  5.75 us
    all_to_all x2, waiting for transfers between devices, to_all(): return lax.all_to_all(copies, axis, split_axis=0, concat_axis=0, tiled=True)  5.28 us
  transfers between devices with their start and end apart: 34, of which 19 were waited for; matrix products, arithmetic and copies ran while one was open for 2% of the time, Pallas kernels for 10%

profile of v5, /device:TPU:32, one launch (start us, length us, event | category | flops | bytes accessed | tf_op | source)
XLA Modules:
  0.0 205.4 jit_solution(7498512063310021614)
XLA Ops:
  6.5 1.5 collective-permute-start.15
  8.0 2.7 %collective-permute-start.16 = (bf16[3,32,256]{2,1,0:T(8,128)(2,1)}, bf16[3,32,256]{2,1,0:T(8,128)(2,1)S(1)}, u32[]{:S(2)}, u32[]{:S(2)}) collective-permute-start(bf16[3,32,256]{2,1,0:T(8,128)(2,1)} %bitcast.26), channel_id=1, source_target_pairs={{0,2},{1,3},{2,0},{3,1},{4,6},{5,7},{6,4},{7,5},{8,10},{9,11},{10,... | collective-permute-start | bytes 147464 | tf_op jit(solution)/shard_map/ppermute | solution.py:26
  10.8 1.4 collective-permute-start.17
  12.2 0.8 slice_bitcast_fusion.3
  13.0 0.8 collective-permute-done.16
  13.8 1.2 collective-permute-done.17
  15.1 0.8 pad_maximum_fusion
  15.9 0.7 pad_maximum_fusion.1
  16.6 0.8 broadcast_in_dim.6
  17.5 8.6 %all-to-all-start = ((bf16[8,32,1024]{2,1,0:T(8,128)(2,1)}), bf16[8,32,1024]{2,1,0:T(8,128)(2,1)S(1)}, u32[]{:S(2)}, u32[]{:S(2)}) async-start(bf16[8,32,1024]{2,1,0:T(8,128)(2,1)} %broadcast_in_dim.6), calls=%async_computation | async-start | bytes 1048576 | tf_op jit(solution)/shard_map/all_to_all | solution.py:21
  26.1 1.9 collective-permute-start
  28.0 5.8 %collective-permute-start.1 = (bf16[48,512]{1,0:T(8,128)(2,1)S(1)}, bf16[48,512]{1,0:T(8,128)(2,1)S(1)}, u32[]{:S(2)}, u32[]{:S(2)}) collective-permute-start(bf16[48,512]{1,0:T(8,128)(2,1)S(1)} %get-tuple-element.19), channel_id=1, source_target_pairs={{4,0},{8,4},{12,8},{16,12},{20,16},{24,20},{28,24},{32,28},{36,32}... | collective-permute-start | bytes 147464 | tf_op jit(solution)/shard_map/ppermute | solution.py:364
  33.7 2.8 %collective-permute-done = bf16[48,512]{1,0:T(8,128)(2,1)S(1)} collective-permute-done((bf16[48,512]{1,0:T(8,128)(2,1)S(1)}, bf16[48,512]{1,0:T(8,128)(2,1)S(1)}, u32[]{:S(2)}, u32[]{:S(2)}) %collective-permute-start) | collective-permute-done | bytes 49184 | tf_op jit(solution)/shard_map/ppermute | solution.py:363
  36.6 5.3 %all-to-all-done.refs_9_.refs_21_ = bf16[8,32,1024]{2,1,0:T(8,128)(2,1)S(1)} async-done(((bf16[8,32,1024]{2,1,0:T(8,128)(2,1)}), bf16[8,32,1024]{2,1,0:T(8,128)(2,1)S(1)}, u32[]{:S(2)}, u32[]{:S(2)}) %all-to-all-start) | async-done | bytes 524320 | tf_op jit(solution)/shard_map/all_to_all | solution.py:21
  41.8 3.4 %collective-permute-start.6 = (bf16[8,32,1024]{2,1,0:T(8,128)(2,1)S(1)}, bf16[8,32,1024]{2,1,0:T(8,128)(2,1)S(1)}, u32[]{:S(2)}, u32[]{:S(2)}) collective-permute-start(bf16[8,32,1024]{2,1,0:T(8,128)(2,1)S(1)} %all-to-all-done.refs_9_.refs_21_), channel_id=1, source_target_pairs={{0,16},{8,24},{16,0},{24,8},{1,17},{9,25},{17,1},{25,9},{2,18},{10... | collective-permute-start | bytes 1572872 | tf_op jit(solution)/shard_map/ppermute | solution.py:26
  45.4 3.9 %collective-permute-start.3 = (bf16[480,512]{1,0:T(8,128)(2,1)S(1)}, bf16[480,512]{1,0:T(8,128)(2,1)}, u32[]{:S(2)}, u32[]{:S(2)}) collective-permute-start(bf16[480,512]{1,0:T(8,128)(2,1)S(1)} %constant_dynamic-update-slice_fusion.refs_0_.refs_4_), channel_id=1, source_target_pairs={{0,2},{1,3},{2,0},{3,1},{4,6},{5,7},{6,4},{7,5},{8,10},{9,11},{10,... | collective-permute-start | bytes 1474568 | tf_op jit(solution)/shard_map/ppermute | solution.py:26
  49.3 0.8 broadcast_in_dim.7
  50.1 5.5 %all-to-all-start.1 = ((bf16[8,32,1024]{2,1,0:T(8,128)(2,1)}), bf16[8,32,1024]{2,1,0:T(8,128)(2,1)}, u32[]{:S(2)}, u32[]{:S(2)}) async-start(bf16[8,32,1024]{2,1,0:T(8,128)(2,1)} %broadcast_in_dim.7), calls=%async_computation.1 | async-start | bytes 1048576 | tf_op jit(solution)/shard_map/all_to_all | solution.py:21
  55.6 1.0 collective-permute-start.7
  56.6 1.0 collective-permute-start.5
  57.6 1.7 collective-permute-done.2.refs_1_.refs_5_
  59.9 4.7 %collective-permute-done.3.refs_2_.refs_6_ = bf16[480,512]{1,0:T(8,128)(2,1)} collective-permute-done((bf16[480,512]{1,0:T(8,128)(2,1)S(1)}, bf16[480,512]{1,0:T(8,128)(2,1)}, u32[]{:S(2)}, u32[]{:S(2)}) %collective-permute-start.3) | collective-permute-done | bytes 491552 | tf_op jit(solution)/shard_map/ppermute | solution.py:26
  64.7 2.2 %collective-permute-done.5.refs_10_.refs_22_ = bf16[8,32,1024]{2,1,0:T(8,128)(2,1)S(1)} collective-permute-done((bf16[8,32,1024]{2,1,0:T(8,128)(2,1)S(1)}, bf16[8,32,1024]{2,1,0:T(8,128)(2,1)S(1)}, u32[]{:S(2)}, u32[]{:S(2)}) %collective-permute-start.5) | collective-permute-done | bytes 524320 | tf_op jit(solution)/shard_map/ppermute | solution.py:26
  67.0 6.6 %collective-permute-done.4.refs_3_.refs_7_ = bf16[480,512]{1,0:T(8,128)(2,1)} collective-permute-done((bf16[480,512]{1,0:T(8,128)(2,1)S(1)}, bf16[480,512]{1,0:T(8,128)(2,1)}, u32[]{:S(2)}, u32[]{:S(2)}) %collective-permute-start.4) | collective-permute-done | bytes 491552 | tf_op jit(solution)/shard_map/ppermute | solution.py:26
  73.5 0.7 collective-permute-start.18
  74.2 3.5 %collective-permute-start.19 = (bf16[8,32,1024]{2,1,0:T(8,128)(2,1)}, bf16[8,32,1024]{2,1,0:T(8,128)(2,1)}, u32[]{:S(2)}, u32[]{:S(2)}) collective-permute-start(bf16[8,32,1024]{2,1,0:T(8,128)(2,1)} %all-to-all-done.1.refs_13_), channel_id=1, source_target_pairs={{0,16},{8,24},{16,0},{24,8},{1,17},{9,25},{17,1},{25,9},{2,18},{10... | collective-permute-start | bytes 1572872 | tf_op jit(solution)/shard_map/ppermute | solution.py:26
  78.0 0.6 stack.27.info
  78.7 7.5 %shard_map.91.refs_0_ = bf16[464,256]{1,0:T(8,128)(2,1)} custom-call(s32[6]{0:T(128)} %stack.27.info, bf16[480,512]{1,0:T(8,128)(2,1)} %copy-done.1, bf16[480,512]{1,0:T(8,128)(2,1)} %collective-permute-done.2.refs_1_.refs_5_, bf16[480,512]{1,0:T(8,128)(2,1)} %collective-permute-done.3.refs_2_.refs_6_, ...), custom_call_target="tpu_custom_call" | custom-call | tf_op jit(solution)/shard_map/pallas_call | solution.py:287
  86.1 13.7 %collective-permute-done.18.refs_14_ = bf16[8,32,1024]{2,1,0:T(8,128)(2,1)} collective-permute-done((bf16[8,32,1024]{2,1,0:T(8,128)(2,1)}, bf16[8,32,1024]{2,1,0:T(8,128)(2,1)}, u32[]{:S(2)}, u32[]{:S(2)}) %collective-permute-start.18) | collective-permute-done | bytes 524320 | tf_op jit(solution)/shard_map/ppermute | solution.py:26
  99.8 18.4 %collective-permute-done.19.refs_15_ = bf16[8,32,1024]{2,1,0:T(8,128)(2,1)} collective-permute-done((bf16[8,32,1024]{2,1,0:T(8,128)(2,1)}, bf16[8,32,1024]{2,1,0:T(8,128)(2,1)}, u32[]{:S(2)}, u32[]{:S(2)}) %collective-permute-start.19) | collective-permute-done | bytes 524320 | tf_op jit(solution)/shard_map/ppermute | solution.py:26
  118.8 2.9 %collective-permute-start.12 = (bf16[464,256]{1,0:T(8,128)(2,1)}, bf16[464,256]{1,0:T(8,128)(2,1)S(1)}, u32[]{:S(2)}, u32[]{:S(2)}) collective-permute-start(bf16[464,256]{1,0:T(8,128)(2,1)} %shard_map.91.refs_0_), channel_id=1, source_target_pairs={{0,1},{1,2},{2,3},{3,0},{4,5},{5,6},{6,7},{7,4},{8,9},{9,10},{10,1... | collective-permute-start | bytes 712712 | tf_op jit(solution)/shard_map/ppermute | solution.py:26
  121.6 2.7 %collective-permute-start.13 = (bf16[464,256]{1,0:T(8,128)(2,1)}, bf16[464,256]{1,0:T(8,128)(2,1)S(1)}, u32[]{:S(2)}, u32[]{:S(2)}) collective-permute-start(bf16[464,256]{1,0:T(8,128)(2,1)} %shard_map.91.refs_0_), channel_id=1, source_target_pairs={{0,2},{1,3},{2,0},{3,1},{4,6},{5,7},{6,4},{7,5},{8,10},{9,11},{10,... | collective-permute-start | bytes 712712 | tf_op jit(solution)/shard_map/ppermute | solution.py:26
  124.3 5.2 %collective-permute-done.12.refs_1_ = bf16[464,256]{1,0:T(8,128)(2,1)S(1)} collective-permute-done((bf16[464,256]{1,0:T(8,128)(2,1)}, bf16[464,256]{1,0:T(8,128)(2,1)S(1)}, u32[]{:S(2)}, u32[]{:S(2)}) %collective-permute-start.12) | collective-permute-done | bytes 237600 | tf_op jit(solution)/shard_map/ppermute | solution.py:26
  129.5 2.2 %collective-permute-start.14 = (bf16[464,256]{1,0:T(8,128)(2,1)}, bf16[464,256]{1,0:T(8,128)(2,1)S(1)}, u32[]{:S(2)}, u32[]{:S(2)}) collective-permute-start(bf16[464,256]{1,0:T(8,128)(2,1)} %shard_map.91.refs_0_), channel_id=1, source_target_pairs={{0,3},{1,0},{2,1},{3,2},{4,7},{5,4},{6,5},{7,6},{8,11},{9,8},{10,9... | collective-permute-start | bytes 712712 | tf_op jit(solution)/shard_map/ppermute | solution.py:26
  131.7 4.1 %collective-permute-done.13.refs_2_ = bf16[464,256]{1,0:T(8,128)(2,1)S(1)} collective-permute-done((bf16[464,256]{1,0:T(8,128)(2,1)}, bf16[464,256]{1,0:T(8,128)(2,1)S(1)}, u32[]{:S(2)}, u32[]{:S(2)}) %collective-permute-start.13) | collective-permute-done | bytes 237600 | tf_op jit(solution)/shard_map/ppermute | solution.py:26
  135.8 1.6 collective-permute-done.14.refs_3_
  137.4 0.6 copy-done.12
  138.4 0.8 copy-done.9
  139.2 12.8 %shard_map.92 = (bf16[4,448,512]{2,1,0:T(8,128)(2,1)}, bf16[432,256]{1,0:T(8,128)(2,1)}) custom-call(s32[6]{0:T(128)} %stack.27.info, bf16[464,256]{1,0:T(8,128)(2,1)} %shard_map.91.refs_0_, bf16[464,256]{1,0:T(8,128)(2,1)} %copy-done.10, bf16[464,256]{1,0:T(8,128)(2,1)} %copy-done.11, bf16[464,256]{1,0:T(8,128)(2,1)} %copy-done.12, ...), custom_call_target="tpu_custom_call" | custom-call | tf_op jit(solution)/shard_map/pallas_call | solution.py:304
  152.6 3.7 %collective-permute-start.26 = (bf16[432,256]{1,0:T(8,128)(2,1)}, bf16[432,256]{1,0:T(8,128)(2,1)S(1)}, u32[]{:S(2)}, u32[]{:S(2)}) collective-permute-start(bf16[432,256]{1,0:T(8,128)(2,1)} %get-tuple-element.15.refs_0_), channel_id=1, source_target_pairs={{0,2},{1,3},{2,0},{3,1},{4,6},{5,7},{6,4},{7,5},{8,10},{9,11},{10,... | collective-permute-start | bytes 663560 | tf_op jit(solution)/shard_map/ppermute | solution.py:26
  156.5 5.8 %collective-permute-done.25.refs_1_ = bf16[432,256]{1,0:T(8,128)(2,1)S(1)} collective-permute-done((bf16[432,256]{1,0:T(8,128)(2,1)}, bf16[432,256]{1,0:T(8,128)(2,1)S(1)}, u32[]{:S(2)}, u32[]{:S(2)}) %collective-permute-start.25) | collective-permute-done | bytes 221216 | tf_op jit(solution)/shard_map/ppermute | solution.py:26
  162.3 2.5 %collective-permute-done.26.refs_2_ = bf16[432,256]{1,0:T(8,128)(2,1)S(1)} collective-permute-done((bf16[432,256]{1,0:T(8,128)(2,1)}, bf16[432,256]{1,0:T(8,128)(2,1)S(1)}, u32[]{:S(2)}, u32[]{:S(2)}) %collective-permute-start.26) | collective-permute-done | bytes 221216 | tf_op jit(solution)/shard_map/ppermute | solution.py:26
  166.0 12.2 %shard_map.93 = (bf16[4,416,512]{2,1,0:T(8,128)(2,1)}, bf16[400,256]{1,0:T(8,128)(2,1)}) custom-call(s32[6]{0:T(128)} %stack.27.info, bf16[432,256]{1,0:T(8,128)(2,1)} %get-tuple-element.15.refs_0_, bf16[432,256]{1,0:T(8,128)(2,1)} %copy-done.13, bf16[432,256]{1,0:T(8,128)(2,1)} %copy-done.14, bf16[432,256]{1,0:T(8,128)(2,1)} %copy-done.15, ...), custom_call_target="tpu_custom_call" | custom-call | tf_op jit(solution)/shard_map/pallas_call | solution.py:304
  178.7 3.6 %collective-permute-start.29 = (bf16[400,256]{1,0:T(8,128)(2,1)}, bf16[400,256]{1,0:T(8,128)(2,1)S(1)}, u32[]{:S(2)}, u32[]{:S(2)}) collective-permute-start(bf16[400,256]{1,0:T(8,128)(2,1)} %get-tuple-element.17.refs_0_), channel_id=1, source_target_pairs={{0,2},{1,3},{2,0},{3,1},{4,6},{5,7},{6,4},{7,5},{8,10},{9,11},{10,... | collective-permute-start | bytes 614408 | tf_op jit(solution)/shard_map/ppermute | solution.py:26
  182.3 3.8 %collective-permute-done.28.refs_1_ = bf16[400,256]{1,0:T(8,128)(2,1)S(1)} collective-permute-done((bf16[400,256]{1,0:T(8,128)(2,1)}, bf16[400,256]{1,0:T(8,128)(2,1)S(1)}, u32[]{:S(2)}, u32[]{:S(2)}) %collective-permute-start.28) | collective-permute-done | bytes 204832 | tf_op jit(solution)/shard_map/ppermute | solution.py:26
  186.1 5.6 %collective-permute-done.29.refs_2_ = bf16[400,256]{1,0:T(8,128)(2,1)S(1)} collective-permute-done((bf16[400,256]{1,0:T(8,128)(2,1)}, bf16[400,256]{1,0:T(8,128)(2,1)S(1)}, u32[]{:S(2)}, u32[]{:S(2)}) %collective-permute-start.29) | collective-permute-done | bytes 204832 | tf_op jit(solution)/shard_map/ppermute | solution.py:26
  191.7 0.7 copy-done.17
  192.4 6.1 %shard_map.94 = bf16[384,512]{1,0:T(8,128)(2,1)} custom-call(s32[6]{0:T(128)} %stack.27.info, bf16[400,256]{1,0:T(8,128)(2,1)} %get-tuple-element.17.refs_0_, bf16[400,256]{1,0:T(8,128)(2,1)} %copy-done.16, bf16[400,256]{1,0:T(8,128)(2,1)} %copy-done.17, bf16[400,256]{1,0:T(8,128)(2,1)} %copy-done.18, bf16[4,416,512]{2,1,0:T(8,128)(2,1)} %get-tuple-element.18.refs_4_, ...), custom_call_target="tpu_custom_call" | custom-call | tf_op jit(solution)/shard_map/pallas_call | solution.py:321
  (75 shorter events, 4.6 us)
Async XLA Ops:
  6.5 19.5 %copy-start.6 = (bf16[384,512]{1,0:T(8,128)(2,1)S(1)}, bf16[384,512]{1,0:T(8,128)(2,1)}, u32[]{:S(2)}) copy-start(bf16[384,512]{1,0:T(8,128)(2,1)} %param.9) | copy-start | bytes 1179652
  6.5 158.8 %all-gather.2.cloned.1.call-start = ((), (), s32[]{:S(2)}) async-start(), calls=%async_computation.2 | async-start | bytes 10649600 | tf_op jit(solution)/shard_map/all_gather | solution.py:361
  6.5 6.5 %collective-permute-start.15 = (bf16[3,32,256]{2,1,0:T(8,128)(2,1)}, bf16[3,32,256]{2,1,0:T(8,128)(2,1)S(1)}, u32[]{:S(2)}, u32[]{:S(2)}) collective-permute-start(bf16[3,32,256]{2,1,0:T(8,128)(2,1)} %bitcast.25), channel_id=1, source_target_pairs={{0,1},{1,2},{2,3},{3,0},{4,5},{5,6},{6,7},{7,4},{8,9},{9,10},{10,1... | collective-permute-start | bytes 147464 | tf_op jit(solution)/shard_map/ppermute | solution.py:26
  8.0 5.8 %collective-permute-start.16 = (bf16[3,32,256]{2,1,0:T(8,128)(2,1)}, bf16[3,32,256]{2,1,0:T(8,128)(2,1)S(1)}, u32[]{:S(2)}, u32[]{:S(2)}) collective-permute-start(bf16[3,32,256]{2,1,0:T(8,128)(2,1)} %bitcast.26), channel_id=1, source_target_pairs={{0,2},{1,3},{2,0},{3,1},{4,6},{5,7},{6,4},{7,5},{8,10},{9,11},{10,... | collective-permute-start | bytes 147464 | tf_op jit(solution)/shard_map/ppermute | solution.py:26
  10.8 4.3 %collective-permute-start.17 = (bf16[3,32,256]{2,1,0:T(8,128)(2,1)}, bf16[3,32,256]{2,1,0:T(8,128)(2,1)S(1)}, u32[]{:S(2)}, u32[]{:S(2)}) collective-permute-start(bf16[3,32,256]{2,1,0:T(8,128)(2,1)} %bitcast.27), channel_id=1, source_target_pairs={{0,3},{1,0},{2,1},{3,2},{4,7},{5,4},{6,5},{7,6},{8,11},{9,8},{10,9... | collective-permute-start | bytes 147464 | tf_op jit(solution)/shard_map/ppermute | solution.py:26
  17.5 24.4 %all-to-all-start = ((bf16[8,32,1024]{2,1,0:T(8,128)(2,1)}), bf16[8,32,1024]{2,1,0:T(8,128)(2,1)S(1)}, u32[]{:S(2)}, u32[]{:S(2)}) async-start(bf16[8,32,1024]{2,1,0:T(8,128)(2,1)} %broadcast_in_dim.6), calls=%async_computation | async-start | bytes 1048576 | tf_op jit(solution)/shard_map/all_to_all | solution.py:21
  26.1 10.5 %collective-permute-start = (bf16[48,512]{1,0:T(8,128)(2,1)S(1)}, bf16[48,512]{1,0:T(8,128)(2,1)S(1)}, u32[]{:S(2)}, u32[]{:S(2)}) collective-permute-start(bf16[48,512]{1,0:T(8,128)(2,1)S(1)} %get-tuple-element.20), channel_id=1, source_target_pairs={{0,4},{4,8},{8,12},{12,16},{16,20},{20,24},{24,28},{28,32},{32,36}... | collective-permute-start | bytes 147464 | tf_op jit(solution)/shard_map/ppermute | solution.py:363
  28.0 17.3 %collective-permute-start.1 = (bf16[48,512]{1,0:T(8,128)(2,1)S(1)}, bf16[48,512]{1,0:T(8,128)(2,1)S(1)}, u32[]{:S(2)}, u32[]{:S(2)}) collective-permute-start(bf16[48,512]{1,0:T(8,128)(2,1)S(1)} %get-tuple-element.19), channel_id=1, source_target_pairs={{4,0},{8,4},{12,8},{16,12},{20,16},{24,20},{28,24},{32,28},{36,32}... | collective-permute-start | bytes 147464 | tf_op jit(solution)/shard_map/ppermute | solution.py:364
  41.8 36.8 %copy-start = (bf16[8,32,1024]{2,1,0:T(8,128)(2,1)}, bf16[8,32,1024]{2,1,0:T(8,128)(2,1)S(1)}, u32[]{:S(2)}) copy-start(bf16[8,32,1024]{2,1,0:T(8,128)(2,1)S(1)} %all-to-all-done.refs_9_.refs_21_) | copy-start | bytes 1572868
  41.8 17.5 %collective-permute-start.6 = (bf16[8,32,1024]{2,1,0:T(8,128)(2,1)S(1)}, bf16[8,32,1024]{2,1,0:T(8,128)(2,1)S(1)}, u32[]{:S(2)}, u32[]{:S(2)}) collective-permute-start(bf16[8,32,1024]{2,1,0:T(8,128)(2,1)S(1)} %all-to-all-done.refs_9_.refs_21_), channel_id=1, source_target_pairs={{0,16},{8,24},{16,0},{24,8},{1,17},{9,25},{17,1},{25,9},{2,18},{10... | collective-permute-start | bytes 1572872 | tf_op jit(solution)/shard_map/ppermute | solution.py:26
  45.3 33.4 %copy-start.1 = (bf16[480,512]{1,0:T(8,128)(2,1)}, bf16[480,512]{1,0:T(8,128)(2,1)S(1)}, u32[]{:S(2)}) copy-start(bf16[480,512]{1,0:T(8,128)(2,1)S(1)} %constant_dynamic-update-slice_fusion.refs_0_.refs_4_) | copy-start | bytes 1474564
  45.3 14.1 %collective-permute-start.2 = (bf16[480,512]{1,0:T(8,128)(2,1)S(1)}, bf16[480,512]{1,0:T(8,128)(2,1)}, u32[]{:S(2)}, u32[]{:S(2)}) collective-permute-start(bf16[480,512]{1,0:T(8,128)(2,1)S(1)} %constant_dynamic-update-slice_fusion.refs_0_.refs_4_), channel_id=1, source_target_pairs={{0,1},{1,2},{2,3},{3,0},{4,5},{5,6},{6,7},{7,4},{8,9},{9,10},{10,1... | collective-permute-start | bytes 1474568 | tf_op jit(solution)/shard_map/ppermute | solution.py:26
  45.4 19.2 %collective-permute-start.3 = (bf16[480,512]{1,0:T(8,128)(2,1)S(1)}, bf16[480,512]{1,0:T(8,128)(2,1)}, u32[]{:S(2)}, u32[]{:S(2)}) collective-permute-start(bf16[480,512]{1,0:T(8,128)(2,1)S(1)} %constant_dynamic-update-slice_fusion.refs_0_.refs_4_), channel_id=1, source_target_pairs={{0,2},{1,3},{2,0},{3,1},{4,6},{5,7},{6,4},{7,5},{8,10},{9,11},{10,... | collective-permute-start | bytes 1474568 | tf_op jit(solution)/shard_map/ppermute | solution.py:26
  50.1 23.4 %all-to-all-start.1 = ((bf16[8,32,1024]{2,1,0:T(8,128)(2,1)}), bf16[8,32,1024]{2,1,0:T(8,128)(2,1)}, u32[]{:S(2)}, u32[]{:S(2)}) async-start(bf16[8,32,1024]{2,1,0:T(8,128)(2,1)} %broadcast_in_dim.7), calls=%async_computation.1 | async-start | bytes 1048576 | tf_op jit(solution)/shard_map/all_to_all | solution.py:21
  55.6 9.2 %collective-permute-start.7 = (bf16[8,32,1024]{2,1,0:T(8,128)(2,1)S(1)}, bf16[8,32,1024]{2,1,0:T(8,128)(2,1)S(1)}, u32[]{:S(2)}, u32[]{:S(2)}) collective-permute-start(bf16[8,32,1024]{2,1,0:T(8,128)(2,1)S(1)} %all-to-all-done.refs_9_.refs_21_), channel_id=1, source_target_pairs={{0,24},{8,0},{16,8},{24,16},{1,25},{9,1},{17,9},{25,17},{2,26},{10... | collective-permute-start | bytes 1572872 | tf_op jit(solution)/shard_map/ppermute | solution.py:26
  56.6 10.4 %collective-permute-start.5 = (bf16[8,32,1024]{2,1,0:T(8,128)(2,1)S(1)}, bf16[8,32,1024]{2,1,0:T(8,128)(2,1)S(1)}, u32[]{:S(2)}, u32[]{:S(2)}) collective-permute-start(bf16[8,32,1024]{2,1,0:T(8,128)(2,1)S(1)} %all-to-all-done.refs_9_.refs_21_), channel_id=1, source_target_pairs={{0,8},{8,16},{16,24},{24,0},{1,9},{9,17},{17,25},{25,1},{2,10},{10... | collective-permute-start | bytes 1572872 | tf_op jit(solution)/shard_map/ppermute | solution.py:26
  59.3 14.9 %collective-permute-start.8 = (bf16[8,32,1024]{2,1,0:T(8,128)(2,1)S(1)}, bf16[8,32,1024]{2,1,0:T(8,128)(2,1)S(1)}, u32[]{:S(2)}, u32[]{:S(2)}) collective-permute-start(bf16[8,32,1024]{2,1,0:T(8,128)(2,1)S(1)} %all-to-all-done.refs_9_.refs_21_), channel_id=1, source_target_pairs={{0,4},{4,0},{1,5},{5,1},{2,6},{6,2},{3,7},{7,3},{8,12},{12,8},{9,1... | collective-permute-start | bytes 1572872 | tf_op jit(solution)/shard_map/ppermute | solution.py:26
  59.3 19.3 %copy-start.2 = (bf16[8,32,1024]{2,1,0:T(8,128)(2,1)}, bf16[8,32,1024]{2,1,0:T(8,128)(2,1)S(1)}, u32[]{:S(2)}) copy-start(bf16[8,32,1024]{2,1,0:T(8,128)(2,1)S(1)} %collective-permute-done.6.refs_11_.refs_23_) | copy-start | bytes 1572868
  59.3 18.3 %collective-permute-start.10 = (bf16[8,32,1024]{2,1,0:T(8,128)(2,1)S(1)}, bf16[8,32,1024]{2,1,0:T(8,128)(2,1)}, u32[]{:S(2)}, u32[]{:S(2)}) collective-permute-start(bf16[8,32,1024]{2,1,0:T(8,128)(2,1)S(1)} %collective-permute-done.6.refs_11_.refs_23_), channel_id=1, source_target_pairs={{0,4},{4,0},{1,5},{5,1},{2,6},{6,2},{3,7},{7,3},{8,12},{12,8},{9,1... | collective-permute-start | bytes 1572872 | tf_op jit(solution)/shard_map/ppermute | solution.py:26
  64.6 8.9 %collective-permute-start.4 = (bf16[480,512]{1,0:T(8,128)(2,1)S(1)}, bf16[480,512]{1,0:T(8,128)(2,1)}, u32[]{:S(2)}, u32[]{:S(2)}) collective-permute-start(bf16[480,512]{1,0:T(8,128)(2,1)S(1)} %constant_dynamic-update-slice_fusion.refs_0_.refs_4_), channel_id=1, source_target_pairs={{0,3},{1,0},{2,1},{3,2},{4,7},{5,4},{6,5},{7,6},{8,11},{9,8},{10,9... | collective-permute-start | bytes 1474568 | tf_op jit(solution)/shard_map/ppermute | solution.py:26
  64.7 13.9 %copy-start.3 = (bf16[8,32,1024]{2,1,0:T(8,128)(2,1)}, bf16[8,32,1024]{2,1,0:T(8,128)(2,1)S(1)}, u32[]{:S(2)}) copy-start(bf16[8,32,1024]{2,1,0:T(8,128)(2,1)S(1)} %collective-permute-done.7.refs_12_.refs_24_) | copy-start | bytes 1572868
  64.7 12.9 %collective-permute-start.11 = (bf16[8,32,1024]{2,1,0:T(8,128)(2,1)S(1)}, bf16[8,32,1024]{2,1,0:T(8,128)(2,1)}, u32[]{:S(2)}, u32[]{:S(2)}) collective-permute-start(bf16[8,32,1024]{2,1,0:T(8,128)(2,1)S(1)} %collective-permute-done.7.refs_12_.refs_24_), channel_id=1, source_target_pairs={{0,4},{4,0},{1,5},{5,1},{2,6},{6,2},{3,7},{7,3},{8,12},{12,8},{9,1... | collective-permute-start | bytes 1572872 | tf_op jit(solution)/shard_map/ppermute | solution.py:26
  67.0 11.7 %copy-start.4 = (bf16[8,32,1024]{2,1,0:T(8,128)(2,1)}, bf16[8,32,1024]{2,1,0:T(8,128)(2,1)S(1)}, u32[]{:S(2)}) copy-start(bf16[8,32,1024]{2,1,0:T(8,128)(2,1)S(1)} %collective-permute-done.5.refs_10_.refs_22_) | copy-start | bytes 1572868
  67.0 11.6 %collective-permute-start.9 = (bf16[8,32,1024]{2,1,0:T(8,128)(2,1)S(1)}, bf16[8,32,1024]{2,1,0:T(8,128)(2,1)}, u32[]{:S(2)}, u32[]{:S(2)}) collective-permute-start(bf16[8,32,1024]{2,1,0:T(8,128)(2,1)S(1)} %collective-permute-done.5.refs_10_.refs_22_), channel_id=1, source_target_pairs={{0,4},{4,0},{1,5},{5,1},{2,6},{6,2},{3,7},{7,3},{8,12},{12,8},{9,1... | collective-permute-start | bytes 1572872 | tf_op jit(solution)/shard_map/ppermute | solution.py:26
  73.5 26.3 %collective-permute-start.18 = (bf16[8,32,1024]{2,1,0:T(8,128)(2,1)}, bf16[8,32,1024]{2,1,0:T(8,128)(2,1)}, u32[]{:S(2)}, u32[]{:S(2)}) collective-permute-start(bf16[8,32,1024]{2,1,0:T(8,128)(2,1)} %all-to-all-done.1.refs_13_), channel_id=1, source_target_pairs={{0,8},{8,16},{16,24},{24,0},{1,9},{9,17},{17,25},{25,1},{2,10},{10... | collective-permute-start | bytes 1572872 | tf_op jit(solution)/shard_map/ppermute | solution.py:26
  74.2 4.4 %copy-start.5 = (bf16[8,32,1024]{2,1,0:T(8,128)(2,1)}, bf16[8,32,1024]{2,1,0:T(8,128)(2,1)S(1)}, u32[]{:S(2)}) copy-start(bf16[8,32,1024]{2,1,0:T(8,128)(2,1)S(1)} %collective-permute-done.8.refs_13_.refs_25_) | copy-start | bytes 1572868
  74.2 44.0 %collective-permute-start.19 = (bf16[8,32,1024]{2,1,0:T(8,128)(2,1)}, bf16[8,32,1024]{2,1,0:T(8,128)(2,1)}, u32[]{:S(2)}, u32[]{:S(2)}) collective-permute-start(bf16[8,32,1024]{2,1,0:T(8,128)(2,1)} %all-to-all-done.1.refs_13_), channel_id=1, source_target_pairs={{0,16},{8,24},{16,0},{24,8},{1,17},{9,25},{17,1},{25,9},{2,18},{10... | collective-permute-start | bytes 1572872 | tf_op jit(solution)/shard_map/ppermute | solution.py:26
  77.7 40.6 %collective-permute-start.20 = (bf16[8,32,1024]{2,1,0:T(8,128)(2,1)}, bf16[8,32,1024]{2,1,0:T(8,128)(2,1)}, u32[]{:S(2)}, u32[]{:S(2)}) collective-permute-start(bf16[8,32,1024]{2,1,0:T(8,128)(2,1)} %all-to-all-done.1.refs_13_), channel_id=1, source_target_pairs={{0,24},{8,0},{16,8},{24,16},{1,25},{9,1},{17,9},{25,17},{2,26},{10... | collective-permute-start | bytes 1572872 | tf_op jit(solution)/shard_map/ppermute | solution.py:26
  77.7 44.0 %collective-permute-start.21 = (bf16[8,32,1024]{2,1,0:T(8,128)(2,1)}, bf16[8,32,1024]{2,1,0:T(8,128)(2,1)}, u32[]{:S(2)}, u32[]{:S(2)}) collective-permute-start(bf16[8,32,1024]{2,1,0:T(8,128)(2,1)} %all-to-all-done.1.refs_13_), channel_id=1, source_target_pairs={{0,4},{4,0},{1,5},{5,1},{2,6},{6,2},{3,7},{7,3},{8,12},{12,8},{9,1... | collective-permute-start | bytes 1572872 | tf_op jit(solution)/shard_map/ppermute | solution.py:26
  118.3 19.1 %collective-permute-start.22 = (bf16[8,32,1024]{2,1,0:T(8,128)(2,1)}, bf16[8,32,1024]{2,1,0:T(8,128)(2,1)S(1)}, u32[]{:S(2)}, u32[]{:S(2)}) collective-permute-start(bf16[8,32,1024]{2,1,0:T(8,128)(2,1)} %collective-permute-done.18.refs_14_), channel_id=1, source_target_pairs={{0,4},{4,0},{1,5},{5,1},{2,6},{6,2},{3,7},{7,3},{8,12},{12,8},{9,1... | collective-permute-start | bytes 1572872 | tf_op jit(solution)/shard_map/ppermute | solution.py:26
  118.3 19.1 %collective-permute-start.23 = (bf16[8,32,1024]{2,1,0:T(8,128)(2,1)}, bf16[8,32,1024]{2,1,0:T(8,128)(2,1)S(1)}, u32[]{:S(2)}, u32[]{:S(2)}) collective-permute-start(bf16[8,32,1024]{2,1,0:T(8,128)(2,1)} %collective-permute-done.19.refs_15_), channel_id=1, source_target_pairs={{0,4},{4,0},{1,5},{5,1},{2,6},{6,2},{3,7},{7,3},{8,12},{12,8},{9,1... | collective-permute-start | bytes 1572872 | tf_op jit(solution)/shard_map/ppermute | solution.py:26
  118.8 18.6 %collective-permute-start.24 = (bf16[8,32,1024]{2,1,0:T(8,128)(2,1)}, bf16[8,32,1024]{2,1,0:T(8,128)(2,1)S(1)}, u32[]{:S(2)}, u32[]{:S(2)}) collective-permute-start(bf16[8,32,1024]{2,1,0:T(8,128)(2,1)} %collective-permute-done.20.refs_16_), channel_id=1, source_target_pairs={{0,4},{4,0},{1,5},{5,1},{2,6},{6,2},{3,7},{7,3},{8,12},{12,8},{9,1... | collective-permute-start | bytes 1572872 | tf_op jit(solution)/shard_map/ppermute | solution.py:26
  118.8 10.7 %collective-permute-start.12 = (bf16[464,256]{1,0:T(8,128)(2,1)}, bf16[464,256]{1,0:T(8,128)(2,1)S(1)}, u32[]{:S(2)}, u32[]{:S(2)}) collective-permute-start(bf16[464,256]{1,0:T(8,128)(2,1)} %shard_map.91.refs_0_), channel_id=1, source_target_pairs={{0,1},{1,2},{2,3},{3,0},{4,5},{5,6},{6,7},{7,4},{8,9},{9,10},{10,1... | collective-permute-start | bytes 712712 | tf_op jit(solution)/shard_map/ppermute | solution.py:26
  121.6 14.1 %collective-permute-start.13 = (bf16[464,256]{1,0:T(8,128)(2,1)}, bf16[464,256]{1,0:T(8,128)(2,1)S(1)}, u32[]{:S(2)}, u32[]{:S(2)}) collective-permute-start(bf16[464,256]{1,0:T(8,128)(2,1)} %shard_map.91.refs_0_), channel_id=1, source_target_pairs={{0,2},{1,3},{2,0},{3,1},{4,6},{5,7},{6,4},{7,5},{8,10},{9,11},{10,... | collective-permute-start | bytes 712712 | tf_op jit(solution)/shard_map/ppermute | solution.py:26
  129.5 7.9 %copy-start.10 = (bf16[464,256]{1,0:T(8,128)(2,1)}, bf16[464,256]{1,0:T(8,128)(2,1)S(1)}, u32[]{:S(2)}) copy-start(bf16[464,256]{1,0:T(8,128)(2,1)S(1)} %collective-permute-done.12.refs_1_) | copy-start | bytes 712708
  129.5 7.8 %collective-permute-start.14 = (bf16[464,256]{1,0:T(8,128)(2,1)}, bf16[464,256]{1,0:T(8,128)(2,1)S(1)}, u32[]{:S(2)}, u32[]{:S(2)}) collective-permute-start(bf16[464,256]{1,0:T(8,128)(2,1)} %shard_map.91.refs_0_), channel_id=1, source_target_pairs={{0,3},{1,0},{2,1},{3,2},{4,7},{5,4},{6,5},{7,6},{8,11},{9,8},{10,9... | collective-permute-start | bytes 712712 | tf_op jit(solution)/shard_map/ppermute | solution.py:26
  135.8 1.6 copy-start.11
  137.4 0.9 copy-start.7
  137.4 1.1 copy-start.8
  138.4 0.8 copy-start.9
  152.1 10.3 %collective-permute-start.25 = (bf16[432,256]{1,0:T(8,128)(2,1)}, bf16[432,256]{1,0:T(8,128)(2,1)S(1)}, u32[]{:S(2)}, u32[]{:S(2)}) collective-permute-start(bf16[432,256]{1,0:T(8,128)(2,1)} %get-tuple-element.15.refs_0_), channel_id=1, source_target_pairs={{0,1},{1,2},{2,3},{3,0},{4,5},{5,6},{6,7},{7,4},{8,9},{9,10},{10,1... | collective-permute-start | bytes 663560 | tf_op jit(solution)/shard_map/ppermute | solution.py:26
  152.6 12.2 %collective-permute-start.26 = (bf16[432,256]{1,0:T(8,128)(2,1)}, bf16[432,256]{1,0:T(8,128)(2,1)S(1)}, u32[]{:S(2)}, u32[]{:S(2)}) collective-permute-start(bf16[432,256]{1,0:T(8,128)(2,1)} %get-tuple-element.15.refs_0_), channel_id=1, source_target_pairs={{0,2},{1,3},{2,0},{3,1},{4,6},{5,7},{6,4},{7,5},{8,10},{9,11},{10,... | collective-permute-start | bytes 663560 | tf_op jit(solution)/shard_map/ppermute | solution.py:26
  156.3 9.1 %collective-permute-start.27 = (bf16[432,256]{1,0:T(8,128)(2,1)}, bf16[432,256]{1,0:T(8,128)(2,1)S(1)}, u32[]{:S(2)}, u32[]{:S(2)}) collective-permute-start(bf16[432,256]{1,0:T(8,128)(2,1)} %get-tuple-element.15.refs_0_), channel_id=1, source_target_pairs={{0,3},{1,0},{2,1},{3,2},{4,7},{5,4},{6,5},{7,6},{8,11},{9,8},{10,9... | collective-permute-start | bytes 663560 | tf_op jit(solution)/shard_map/ppermute | solution.py:26
  162.3 3.0 %copy-start.13 = (bf16[432,256]{1,0:T(8,128)(2,1)}, bf16[432,256]{1,0:T(8,128)(2,1)S(1)}, u32[]{:S(2)}) copy-start(bf16[432,256]{1,0:T(8,128)(2,1)S(1)} %collective-permute-done.25.refs_1_) | copy-start | bytes 663556
  178.3 7.8 %collective-permute-start.28 = (bf16[400,256]{1,0:T(8,128)(2,1)}, bf16[400,256]{1,0:T(8,128)(2,1)S(1)}, u32[]{:S(2)}, u32[]{:S(2)}) collective-permute-start(bf16[400,256]{1,0:T(8,128)(2,1)} %get-tuple-element.17.refs_0_), channel_id=1, source_target_pairs={{0,1},{1,2},{2,3},{3,0},{4,5},{5,6},{6,7},{7,4},{8,9},{9,10},{10,1... | collective-permute-start | bytes 614408 | tf_op jit(solution)/shard_map/ppermute | solution.py:26
  178.7 13.0 %collective-permute-start.29 = (bf16[400,256]{1,0:T(8,128)(2,1)}, bf16[400,256]{1,0:T(8,128)(2,1)S(1)}, u32[]{:S(2)}, u32[]{:S(2)}) collective-permute-start(bf16[400,256]{1,0:T(8,128)(2,1)} %get-tuple-element.17.refs_0_), channel_id=1, source_target_pairs={{0,2},{1,3},{2,0},{3,1},{4,6},{5,7},{6,4},{7,5},{8,10},{9,11},{10,... | collective-permute-start | bytes 614408 | tf_op jit(solution)/shard_map/ppermute | solution.py:26
  182.3 9.3 %collective-permute-start.30 = (bf16[400,256]{1,0:T(8,128)(2,1)}, bf16[400,256]{1,0:T(8,128)(2,1)S(1)}, u32[]{:S(2)}, u32[]{:S(2)}) collective-permute-start(bf16[400,256]{1,0:T(8,128)(2,1)} %get-tuple-element.17.refs_0_), channel_id=1, source_target_pairs={{0,3},{1,0},{2,1},{3,2},{4,7},{5,4},{6,5},{7,6},{8,11},{9,8},{10,9... | collective-permute-start | bytes 614408 | tf_op jit(solution)/shard_map/ppermute | solution.py:26
  186.1 5.6 %copy-start.16 = (bf16[400,256]{1,0:T(8,128)(2,1)}, bf16[400,256]{1,0:T(8,128)(2,1)S(1)}, u32[]{:S(2)}) copy-start(bf16[400,256]{1,0:T(8,128)(2,1)S(1)} %collective-permute-done.28.refs_1_) | copy-start | bytes 614404
  (5 other events, 3.5 us)
Sparse Core Ops, SparseCore 0:
  16.7 112.1 all-gather.1

commit v6 on v5

--- a/solution.py
+++ b/solution.py
@@ -120,7 +120,7 @@
             value = (streams[s][here] if n_s > 1 else streams[0][s, here]).astype(f32)
             normed[here, wide] = (value * scale * gain[layer : layer + 1, wide]).astype(bf16)
 
-    by_rows(rows, norm)
+    by_rows(rows, norm, 128)
     for copy in copies:
         copy.wait()
     for half in range(2):
@@ -134,7 +134,7 @@
         gated = jnp.where((t >= 0) & (t < total), gated, 0.0).astype(bf16)
         padded[here] = gated.astype(f32)
 
-    by_rows(rows, gate)
+    by_rows(rows, gate, 128)
     columns[pl.ds(keep, 2 * ch - keep)] = jnp.zeros((2 * ch - keep, LANES), f32)
 
     def filtered(first, size):
@@ -218,7 +218,7 @@
             value = value * params[s][:, :ch] + params[s][:, ch:]
             act[here, s * ch : (s + 1) * ch] = (value * jax.nn.sigmoid(value)).astype(bf16)
 
-    by_rows(keep, activate)
+    by_rows(keep, activate, 128)
     for copy in copies:
         copy.wait()
     dims = (((1,), (1,)), ((), ()))

time: 206 us -> 203 us (0.985)
  Pallas kernels: 38.6 us -> 35.8 us
where the time goes in v6:
time: 203 us
  waiting for transfers between devices  86.7 us (43%)
  starting transfers between devices  58.5 us (29%)
  Pallas kernels  35.8 us (18%)
  between operations  13.6 us (7%)
  local copies, waits for them, and re-layouts  6.5 us (3%)
    ppermute x29, waiting for transfers between devices, shifted(): return lax.ppermute(array, axis, [(i, (i + s) % n) for i in range(n)])  78.6 us
    ppermute x29, starting transfers between devices, shifted(): return lax.ppermute(array, axis, [(i, (i + s) % n) for i in range(n)])  36.8 us
    pallas_call x2, Pallas kernels, mid(): pl.pallas_call(functools.partial(mid_kernel, layer, total, len(streams),...  23.4 us
    all_to_all x2, starting transfers between devices, to_all(): return lax.all_to_all(copies, axis, split_axis=0, concat_axis=0, tiled=True)  14 us
    pallas_call x1, Pallas kernels, up(): pl.pallas_call(functools.partial(up_kernel, layer, total, len(streams), n...  7.42 us
    ppermute x1, starting transfers between devices, program(): lax.ppermute(tokens[:halo], SP, [(i + 1, i) for i in range(size - 1)])  5.75 us
    all_to_all x2, waiting for transfers between devices, to_all(): return lax.all_to_all(copies, axis, split_axis=0, concat_axis=0, tiled=True)  5.28 us
    pallas_call x1, Pallas kernels, down(): pl.pallas_call(functools.partial(down_kernel, n_x, first_lane), out_shape...  4.99 us
  transfers between devices with their start and end apart: 34, of which 19 were waited for; matrix products, arithmetic and copies ran while one was open for 2% of the time, Pallas kernels for 10%

profile of v6, /device:TPU:32, one launch (start us, length us, event | category | flops | bytes accessed | tf_op | source)
XLA Modules:
  0.0 202.6 jit_solution(8708402757700472523)
XLA Ops:
  6.5 1.5 collective-permute-start.15
  8.0 2.7 %collective-permute-start.16 = (bf16[3,32,256]{2,1,0:T(8,128)(2,1)}, bf16[3,32,256]{2,1,0:T(8,128)(2,1)S(1)}, u32[]{:S(2)}, u32[]{:S(2)}) collective-permute-start(bf16[3,32,256]{2,1,0:T(8,128)(2,1)} %bitcast.26), channel_id=1, source_target_pairs={{0,2},{1,3},{2,0},{3,1},{4,6},{5,7},{6,4},{7,5},{8,10},{9,11},{10,... | collective-permute-start | bytes 147464 | tf_op jit(solution)/shard_map/ppermute | solution.py:26
  10.8 1.4 collective-permute-start.17
  12.2 0.8 slice_bitcast_fusion.3
  13.0 0.8 collective-permute-done.16
  13.8 1.2 collective-permute-done.17
  15.1 0.8 pad_maximum_fusion
  15.9 0.7 pad_maximum_fusion.1
  16.6 0.8 broadcast_in_dim.6
  17.5 8.6 %all-to-all-start = ((bf16[8,32,1024]{2,1,0:T(8,128)(2,1)}), bf16[8,32,1024]{2,1,0:T(8,128)(2,1)S(1)}, u32[]{:S(2)}, u32[]{:S(2)}) async-start(bf16[8,32,1024]{2,1,0:T(8,128)(2,1)} %broadcast_in_dim.6), calls=%async_computation | async-start | bytes 1048576 | tf_op jit(solution)/shard_map/all_to_all | solution.py:21
  26.1 1.9 collective-permute-start
  28.0 5.8 %collective-permute-start.1 = (bf16[48,512]{1,0:T(8,128)(2,1)S(1)}, bf16[48,512]{1,0:T(8,128)(2,1)S(1)}, u32[]{:S(2)}, u32[]{:S(2)}) collective-permute-start(bf16[48,512]{1,0:T(8,128)(2,1)S(1)} %get-tuple-element.19), channel_id=1, source_target_pairs={{4,0},{8,4},{12,8},{16,12},{20,16},{24,20},{28,24},{32,28},{36,32}... | collective-permute-start | bytes 147464 | tf_op jit(solution)/shard_map/ppermute | solution.py:364
  33.7 2.8 %collective-permute-done = bf16[48,512]{1,0:T(8,128)(2,1)S(1)} collective-permute-done((bf16[48,512]{1,0:T(8,128)(2,1)S(1)}, bf16[48,512]{1,0:T(8,128)(2,1)S(1)}, u32[]{:S(2)}, u32[]{:S(2)}) %collective-permute-start) | collective-permute-done | bytes 49184 | tf_op jit(solution)/shard_map/ppermute | solution.py:363
  36.6 5.3 %all-to-all-done.refs_9_.refs_21_ = bf16[8,32,1024]{2,1,0:T(8,128)(2,1)S(1)} async-done(((bf16[8,32,1024]{2,1,0:T(8,128)(2,1)}), bf16[8,32,1024]{2,1,0:T(8,128)(2,1)S(1)}, u32[]{:S(2)}, u32[]{:S(2)}) %all-to-all-start) | async-done | bytes 524320 | tf_op jit(solution)/shard_map/all_to_all | solution.py:21
  41.8 3.4 %collective-permute-start.6 = (bf16[8,32,1024]{2,1,0:T(8,128)(2,1)S(1)}, bf16[8,32,1024]{2,1,0:T(8,128)(2,1)S(1)}, u32[]{:S(2)}, u32[]{:S(2)}) collective-permute-start(bf16[8,32,1024]{2,1,0:T(8,128)(2,1)S(1)} %all-to-all-done.refs_9_.refs_21_), channel_id=1, source_target_pairs={{0,16},{8,24},{16,0},{24,8},{1,17},{9,25},{17,1},{25,9},{2,18},{10... | collective-permute-start | bytes 1572872 | tf_op jit(solution)/shard_map/ppermute | solution.py:26
  45.4 3.9 %collective-permute-start.3 = (bf16[480,512]{1,0:T(8,128)(2,1)S(1)}, bf16[480,512]{1,0:T(8,128)(2,1)}, u32[]{:S(2)}, u32[]{:S(2)}) collective-permute-start(bf16[480,512]{1,0:T(8,128)(2,1)S(1)} %constant_dynamic-update-slice_fusion.refs_0_.refs_4_), channel_id=1, source_target_pairs={{0,2},{1,3},{2,0},{3,1},{4,6},{5,7},{6,4},{7,5},{8,10},{9,11},{10,... | collective-permute-start | bytes 1474568 | tf_op jit(solution)/shard_map/ppermute | solution.py:26
  49.3 0.8 broadcast_in_dim.7
  50.1 5.5 %all-to-all-start.1 = ((bf16[8,32,1024]{2,1,0:T(8,128)(2,1)}), bf16[8,32,1024]{2,1,0:T(8,128)(2,1)}, u32[]{:S(2)}, u32[]{:S(2)}) async-start(bf16[8,32,1024]{2,1,0:T(8,128)(2,1)} %broadcast_in_dim.7), calls=%async_computation.1 | async-start | bytes 1048576 | tf_op jit(solution)/shard_map/all_to_all | solution.py:21
  55.6 1.0 collective-permute-start.7
  56.6 1.0 collective-permute-start.5
  57.6 1.7 collective-permute-done.2.refs_1_.refs_5_
  59.9 4.7 %collective-permute-done.3.refs_2_.refs_6_ = bf16[480,512]{1,0:T(8,128)(2,1)} collective-permute-done((bf16[480,512]{1,0:T(8,128)(2,1)S(1)}, bf16[480,512]{1,0:T(8,128)(2,1)}, u32[]{:S(2)}, u32[]{:S(2)}) %collective-permute-start.3) | collective-permute-done | bytes 491552 | tf_op jit(solution)/shard_map/ppermute | solution.py:26
  64.7 2.2 %collective-permute-done.5.refs_10_.refs_22_ = bf16[8,32,1024]{2,1,0:T(8,128)(2,1)S(1)} collective-permute-done((bf16[8,32,1024]{2,1,0:T(8,128)(2,1)S(1)}, bf16[8,32,1024]{2,1,0:T(8,128)(2,1)S(1)}, u32[]{:S(2)}, u32[]{:S(2)}) %collective-permute-start.5) | collective-permute-done | bytes 524320 | tf_op jit(solution)/shard_map/ppermute | solution.py:26
  67.0 6.6 %collective-permute-done.4.refs_3_.refs_7_ = bf16[480,512]{1,0:T(8,128)(2,1)} collective-permute-done((bf16[480,512]{1,0:T(8,128)(2,1)S(1)}, bf16[480,512]{1,0:T(8,128)(2,1)}, u32[]{:S(2)}, u32[]{:S(2)}) %collective-permute-start.4) | collective-permute-done | bytes 491552 | tf_op jit(solution)/shard_map/ppermute | solution.py:26
  73.5 0.7 collective-permute-start.18
  74.2 3.5 %collective-permute-start.19 = (bf16[8,32,1024]{2,1,0:T(8,128)(2,1)}, bf16[8,32,1024]{2,1,0:T(8,128)(2,1)}, u32[]{:S(2)}, u32[]{:S(2)}) collective-permute-start(bf16[8,32,1024]{2,1,0:T(8,128)(2,1)} %all-to-all-done.1.refs_13_), channel_id=1, source_target_pairs={{0,16},{8,24},{16,0},{24,8},{1,17},{9,25},{17,1},{25,9},{2,18},{10... | collective-permute-start | bytes 1572872 | tf_op jit(solution)/shard_map/ppermute | solution.py:26
  78.0 0.6 stack.27.info
  78.7 7.4 %shard_map.91.refs_0_ = bf16[464,256]{1,0:T(8,128)(2,1)} custom-call(s32[6]{0:T(128)} %stack.27.info, bf16[480,512]{1,0:T(8,128)(2,1)} %copy-done.1, bf16[480,512]{1,0:T(8,128)(2,1)} %collective-permute-done.2.refs_1_.refs_5_, bf16[480,512]{1,0:T(8,128)(2,1)} %collective-permute-done.3.refs_2_.refs_6_, ...), custom_call_target="tpu_custom_call" | custom-call | tf_op jit(solution)/shard_map/pallas_call | solution.py:287
  86.1 13.8 %collective-permute-done.18.refs_14_ = bf16[8,32,1024]{2,1,0:T(8,128)(2,1)} collective-permute-done((bf16[8,32,1024]{2,1,0:T(8,128)(2,1)}, bf16[8,32,1024]{2,1,0:T(8,128)(2,1)}, u32[]{:S(2)}, u32[]{:S(2)}) %collective-permute-start.18) | collective-permute-done | bytes 524320 | tf_op jit(solution)/shard_map/ppermute | solution.py:26
  99.8 18.4 %collective-permute-done.19.refs_15_ = bf16[8,32,1024]{2,1,0:T(8,128)(2,1)} collective-permute-done((bf16[8,32,1024]{2,1,0:T(8,128)(2,1)}, bf16[8,32,1024]{2,1,0:T(8,128)(2,1)}, u32[]{:S(2)}, u32[]{:S(2)}) %collective-permute-start.19) | collective-permute-done | bytes 524320 | tf_op jit(solution)/shard_map/ppermute | solution.py:26
  118.8 2.9 %collective-permute-start.12 = (bf16[464,256]{1,0:T(8,128)(2,1)}, bf16[464,256]{1,0:T(8,128)(2,1)S(1)}, u32[]{:S(2)}, u32[]{:S(2)}) collective-permute-start(bf16[464,256]{1,0:T(8,128)(2,1)} %shard_map.91.refs_0_), channel_id=1, source_target_pairs={{0,1},{1,2},{2,3},{3,0},{4,5},{5,6},{6,7},{7,4},{8,9},{9,10},{10,1... | collective-permute-start | bytes 712712 | tf_op jit(solution)/shard_map/ppermute | solution.py:26
  121.6 2.7 %collective-permute-start.13 = (bf16[464,256]{1,0:T(8,128)(2,1)}, bf16[464,256]{1,0:T(8,128)(2,1)S(1)}, u32[]{:S(2)}, u32[]{:S(2)}) collective-permute-start(bf16[464,256]{1,0:T(8,128)(2,1)} %shard_map.91.refs_0_), channel_id=1, source_target_pairs={{0,2},{1,3},{2,0},{3,1},{4,6},{5,7},{6,4},{7,5},{8,10},{9,11},{10,... | collective-permute-start | bytes 712712 | tf_op jit(solution)/shard_map/ppermute | solution.py:26
  124.3 5.2 %collective-permute-done.12.refs_1_ = bf16[464,256]{1,0:T(8,128)(2,1)S(1)} collective-permute-done((bf16[464,256]{1,0:T(8,128)(2,1)}, bf16[464,256]{1,0:T(8,128)(2,1)S(1)}, u32[]{:S(2)}, u32[]{:S(2)}) %collective-permute-start.12) | collective-permute-done | bytes 237600 | tf_op jit(solution)/shard_map/ppermute | solution.py:26
  129.5 2.2 %collective-permute-start.14 = (bf16[464,256]{1,0:T(8,128)(2,1)}, bf16[464,256]{1,0:T(8,128)(2,1)S(1)}, u32[]{:S(2)}, u32[]{:S(2)}) collective-permute-start(bf16[464,256]{1,0:T(8,128)(2,1)} %shard_map.91.refs_0_), channel_id=1, source_target_pairs={{0,3},{1,0},{2,1},{3,2},{4,7},{5,4},{6,5},{7,6},{8,11},{9,8},{10,9... | collective-permute-start | bytes 712712 | tf_op jit(solution)/shard_map/ppermute | solution.py:26
  131.7 4.1 %collective-permute-done.13.refs_2_ = bf16[464,256]{1,0:T(8,128)(2,1)S(1)} collective-permute-done((bf16[464,256]{1,0:T(8,128)(2,1)}, bf16[464,256]{1,0:T(8,128)(2,1)S(1)}, u32[]{:S(2)}, u32[]{:S(2)}) %collective-permute-start.13) | collective-permute-done | bytes 237600 | tf_op jit(solution)/shard_map/ppermute | solution.py:26
  135.8 1.6 collective-permute-done.14.refs_3_
  137.4 0.6 copy-done.12
  138.4 0.8 copy-done.9
  139.2 11.9 %shard_map.92 = (bf16[4,448,512]{2,1,0:T(8,128)(2,1)}, bf16[432,256]{1,0:T(8,128)(2,1)}) custom-call(s32[6]{0:T(128)} %stack.27.info, bf16[464,256]{1,0:T(8,128)(2,1)} %shard_map.91.refs_0_, bf16[464,256]{1,0:T(8,128)(2,1)} %copy-done.10, bf16[464,256]{1,0:T(8,128)(2,1)} %copy-done.11, bf16[464,256]{1,0:T(8,128)(2,1)} %copy-done.12, ...), custom_call_target="tpu_custom_call" | custom-call | tf_op jit(solution)/shard_map/pallas_call | solution.py:304
  151.7 3.7 %collective-permute-start.26 = (bf16[432,256]{1,0:T(8,128)(2,1)}, bf16[432,256]{1,0:T(8,128)(2,1)S(1)}, u32[]{:S(2)}, u32[]{:S(2)}) collective-permute-start(bf16[432,256]{1,0:T(8,128)(2,1)} %get-tuple-element.15.refs_0_), channel_id=1, source_target_pairs={{0,2},{1,3},{2,0},{3,1},{4,6},{5,7},{6,4},{7,5},{8,10},{9,11},{10,... | collective-permute-start | bytes 663560 | tf_op jit(solution)/shard_map/ppermute | solution.py:26
  155.6 5.8 %collective-permute-done.25.refs_1_ = bf16[432,256]{1,0:T(8,128)(2,1)S(1)} collective-permute-done((bf16[432,256]{1,0:T(8,128)(2,1)}, bf16[432,256]{1,0:T(8,128)(2,1)S(1)}, u32[]{:S(2)}, u32[]{:S(2)}) %collective-permute-start.25) | collective-permute-done | bytes 221216 | tf_op jit(solution)/shard_map/ppermute | solution.py:26
  161.4 2.5 %collective-permute-done.26.refs_2_ = bf16[432,256]{1,0:T(8,128)(2,1)S(1)} collective-permute-done((bf16[432,256]{1,0:T(8,128)(2,1)}, bf16[432,256]{1,0:T(8,128)(2,1)S(1)}, u32[]{:S(2)}, u32[]{:S(2)}) %collective-permute-start.26) | collective-permute-done | bytes 221216 | tf_op jit(solution)/shard_map/ppermute | solution.py:26
  165.1 11.5 %shard_map.93 = (bf16[4,416,512]{2,1,0:T(8,128)(2,1)}, bf16[400,256]{1,0:T(8,128)(2,1)}) custom-call(s32[6]{0:T(128)} %stack.27.info, bf16[432,256]{1,0:T(8,128)(2,1)} %get-tuple-element.15.refs_0_, bf16[432,256]{1,0:T(8,128)(2,1)} %copy-done.13, bf16[432,256]{1,0:T(8,128)(2,1)} %copy-done.14, bf16[432,256]{1,0:T(8,128)(2,1)} %copy-done.15, ...), custom_call_target="tpu_custom_call" | custom-call | tf_op jit(solution)/shard_map/pallas_call | solution.py:304
  177.0 3.6 %collective-permute-start.29 = (bf16[400,256]{1,0:T(8,128)(2,1)}, bf16[400,256]{1,0:T(8,128)(2,1)S(1)}, u32[]{:S(2)}, u32[]{:S(2)}) collective-permute-start(bf16[400,256]{1,0:T(8,128)(2,1)} %get-tuple-element.17.refs_0_), channel_id=1, source_target_pairs={{0,2},{1,3},{2,0},{3,1},{4,6},{5,7},{6,4},{7,5},{8,10},{9,11},{10,... | collective-permute-start | bytes 614408 | tf_op jit(solution)/shard_map/ppermute | solution.py:26
  180.7 3.8 %collective-permute-done.28.refs_1_ = bf16[400,256]{1,0:T(8,128)(2,1)S(1)} collective-permute-done((bf16[400,256]{1,0:T(8,128)(2,1)}, bf16[400,256]{1,0:T(8,128)(2,1)S(1)}, u32[]{:S(2)}, u32[]{:S(2)}) %collective-permute-start.28) | collective-permute-done | bytes 204832 | tf_op jit(solution)/shard_map/ppermute | solution.py:26
  184.5 5.6 %collective-permute-done.29.refs_2_ = bf16[400,256]{1,0:T(8,128)(2,1)S(1)} collective-permute-done((bf16[400,256]{1,0:T(8,128)(2,1)}, bf16[400,256]{1,0:T(8,128)(2,1)S(1)}, u32[]{:S(2)}, u32[]{:S(2)}) %collective-permute-start.29) | collective-permute-done | bytes 204832 | tf_op jit(solution)/shard_map/ppermute | solution.py:26
  190.0 0.7 copy-done.17
  190.8 5.0 %shard_map.94 = bf16[384,512]{1,0:T(8,128)(2,1)} custom-call(s32[6]{0:T(128)} %stack.27.info, bf16[400,256]{1,0:T(8,128)(2,1)} %get-tuple-element.17.refs_0_, bf16[400,256]{1,0:T(8,128)(2,1)} %copy-done.16, bf16[400,256]{1,0:T(8,128)(2,1)} %copy-done.17, bf16[400,256]{1,0:T(8,128)(2,1)} %copy-done.18, bf16[4,416,512]{2,1,0:T(8,128)(2,1)} %get-tuple-element.18.refs_4_, ...), custom_call_target="tpu_custom_call" | custom-call | tf_op jit(solution)/shard_map/pallas_call | solution.py:321
  (75 shorter events, 4.6 us)
Async XLA Ops:
  6.5 19.5 %copy-start.6 = (bf16[384,512]{1,0:T(8,128)(2,1)S(1)}, bf16[384,512]{1,0:T(8,128)(2,1)}, u32[]{:S(2)}) copy-start(bf16[384,512]{1,0:T(8,128)(2,1)} %param.9) | copy-start | bytes 1179652
  6.5 157.9 %all-gather.2.cloned.1.call-start = ((), (), s32[]{:S(2)}) async-start(), calls=%async_computation.2 | async-start | bytes 10649600 | tf_op jit(solution)/shard_map/all_gather | solution.py:361
  6.5 6.5 %collective-permute-start.15 = (bf16[3,32,256]{2,1,0:T(8,128)(2,1)}, bf16[3,32,256]{2,1,0:T(8,128)(2,1)S(1)}, u32[]{:S(2)}, u32[]{:S(2)}) collective-permute-start(bf16[3,32,256]{2,1,0:T(8,128)(2,1)} %bitcast.25), channel_id=1, source_target_pairs={{0,1},{1,2},{2,3},{3,0},{4,5},{5,6},{6,7},{7,4},{8,9},{9,10},{10,1... | collective-permute-start | bytes 147464 | tf_op jit(solution)/shard_map/ppermute | solution.py:26
  8.0 5.8 %collective-permute-start.16 = (bf16[3,32,256]{2,1,0:T(8,128)(2,1)}, bf16[3,32,256]{2,1,0:T(8,128)(2,1)S(1)}, u32[]{:S(2)}, u32[]{:S(2)}) collective-permute-start(bf16[3,32,256]{2,1,0:T(8,128)(2,1)} %bitcast.26), channel_id=1, source_target_pairs={{0,2},{1,3},{2,0},{3,1},{4,6},{5,7},{6,4},{7,5},{8,10},{9,11},{10,... | collective-permute-start | bytes 147464 | tf_op jit(solution)/shard_map/ppermute | solution.py:26
  10.8 4.3 %collective-permute-start.17 = (bf16[3,32,256]{2,1,0:T(8,128)(2,1)}, bf16[3,32,256]{2,1,0:T(8,128)(2,1)S(1)}, u32[]{:S(2)}, u32[]{:S(2)}) collective-permute-start(bf16[3,32,256]{2,1,0:T(8,128)(2,1)} %bitcast.27), channel_id=1, source_target_pairs={{0,3},{1,0},{2,1},{3,2},{4,7},{5,4},{6,5},{7,6},{8,11},{9,8},{10,9... | collective-permute-start | bytes 147464 | tf_op jit(solution)/shard_map/ppermute | solution.py:26
  17.5 24.4 %all-to-all-start = ((bf16[8,32,1024]{2,1,0:T(8,128)(2,1)}), bf16[8,32,1024]{2,1,0:T(8,128)(2,1)S(1)}, u32[]{:S(2)}, u32[]{:S(2)}) async-start(bf16[8,32,1024]{2,1,0:T(8,128)(2,1)} %broadcast_in_dim.6), calls=%async_computation | async-start | bytes 1048576 | tf_op jit(solution)/shard_map/all_to_all | solution.py:21
  26.1 10.5 %collective-permute-start = (bf16[48,512]{1,0:T(8,128)(2,1)S(1)}, bf16[48,512]{1,0:T(8,128)(2,1)S(1)}, u32[]{:S(2)}, u32[]{:S(2)}) collective-permute-start(bf16[48,512]{1,0:T(8,128)(2,1)S(1)} %get-tuple-element.20), channel_id=1, source_target_pairs={{0,4},{4,8},{8,12},{12,16},{16,20},{20,24},{24,28},{28,32},{32,36}... | collective-permute-start | bytes 147464 | tf_op jit(solution)/shard_map/ppermute | solution.py:363
  28.0 17.3 %collective-permute-start.1 = (bf16[48,512]{1,0:T(8,128)(2,1)S(1)}, bf16[48,512]{1,0:T(8,128)(2,1)S(1)}, u32[]{:S(2)}, u32[]{:S(2)}) collective-permute-start(bf16[48,512]{1,0:T(8,128)(2,1)S(1)} %get-tuple-element.19), channel_id=1, source_target_pairs={{4,0},{8,4},{12,8},{16,12},{20,16},{24,20},{28,24},{32,28},{36,32}... | collective-permute-start | bytes 147464 | tf_op jit(solution)/shard_map/ppermute | solution.py:364
  41.8 36.8 %copy-start = (bf16[8,32,1024]{2,1,0:T(8,128)(2,1)}, bf16[8,32,1024]{2,1,0:T(8,128)(2,1)S(1)}, u32[]{:S(2)}) copy-start(bf16[8,32,1024]{2,1,0:T(8,128)(2,1)S(1)} %all-to-all-done.refs_9_.refs_21_) | copy-start | bytes 1572868
  41.8 17.5 %collective-permute-start.6 = (bf16[8,32,1024]{2,1,0:T(8,128)(2,1)S(1)}, bf16[8,32,1024]{2,1,0:T(8,128)(2,1)S(1)}, u32[]{:S(2)}, u32[]{:S(2)}) collective-permute-start(bf16[8,32,1024]{2,1,0:T(8,128)(2,1)S(1)} %all-to-all-done.refs_9_.refs_21_), channel_id=1, source_target_pairs={{0,16},{8,24},{16,0},{24,8},{1,17},{9,25},{17,1},{25,9},{2,18},{10... | collective-permute-start | bytes 1572872 | tf_op jit(solution)/shard_map/ppermute | solution.py:26
  45.3 33.4 %copy-start.1 = (bf16[480,512]{1,0:T(8,128)(2,1)}, bf16[480,512]{1,0:T(8,128)(2,1)S(1)}, u32[]{:S(2)}) copy-start(bf16[480,512]{1,0:T(8,128)(2,1)S(1)} %constant_dynamic-update-slice_fusion.refs_0_.refs_4_) | copy-start | bytes 1474564
  45.3 14.1 %collective-permute-start.2 = (bf16[480,512]{1,0:T(8,128)(2,1)S(1)}, bf16[480,512]{1,0:T(8,128)(2,1)}, u32[]{:S(2)}, u32[]{:S(2)}) collective-permute-start(bf16[480,512]{1,0:T(8,128)(2,1)S(1)} %constant_dynamic-update-slice_fusion.refs_0_.refs_4_), channel_id=1, source_target_pairs={{0,1},{1,2},{2,3},{3,0},{4,5},{5,6},{6,7},{7,4},{8,9},{9,10},{10,1... | collective-permute-start | bytes 1474568 | tf_op jit(solution)/shard_map/ppermute | solution.py:26
  45.4 19.2 %collective-permute-start.3 = (bf16[480,512]{1,0:T(8,128)(2,1)S(1)}, bf16[480,512]{1,0:T(8,128)(2,1)}, u32[]{:S(2)}, u32[]{:S(2)}) collective-permute-start(bf16[480,512]{1,0:T(8,128)(2,1)S(1)} %constant_dynamic-update-slice_fusion.refs_0_.refs_4_), channel_id=1, source_target_pairs={{0,2},{1,3},{2,0},{3,1},{4,6},{5,7},{6,4},{7,5},{8,10},{9,11},{10,... | collective-permute-start | bytes 1474568 | tf_op jit(solution)/shard_map/ppermute | solution.py:26
  50.1 23.4 %all-to-all-start.1 = ((bf16[8,32,1024]{2,1,0:T(8,128)(2,1)}), bf16[8,32,1024]{2,1,0:T(8,128)(2,1)}, u32[]{:S(2)}, u32[]{:S(2)}) async-start(bf16[8,32,1024]{2,1,0:T(8,128)(2,1)} %broadcast_in_dim.7), calls=%async_computation.1 | async-start | bytes 1048576 | tf_op jit(solution)/shard_map/all_to_all | solution.py:21
  55.6 9.2 %collective-permute-start.7 = (bf16[8,32,1024]{2,1,0:T(8,128)(2,1)S(1)}, bf16[8,32,1024]{2,1,0:T(8,128)(2,1)S(1)}, u32[]{:S(2)}, u32[]{:S(2)}) collective-permute-start(bf16[8,32,1024]{2,1,0:T(8,128)(2,1)S(1)} %all-to-all-done.refs_9_.refs_21_), channel_id=1, source_target_pairs={{0,24},{8,0},{16,8},{24,16},{1,25},{9,1},{17,9},{25,17},{2,26},{10... | collective-permute-start | bytes 1572872 | tf_op jit(solution)/shard_map/ppermute | solution.py:26
  56.6 10.4 %collective-permute-start.5 = (bf16[8,32,1024]{2,1,0:T(8,128)(2,1)S(1)}, bf16[8,32,1024]{2,1,0:T(8,128)(2,1)S(1)}, u32[]{:S(2)}, u32[]{:S(2)}) collective-permute-start(bf16[8,32,1024]{2,1,0:T(8,128)(2,1)S(1)} %all-to-all-done.refs_9_.refs_21_), channel_id=1, source_target_pairs={{0,8},{8,16},{16,24},{24,0},{1,9},{9,17},{17,25},{25,1},{2,10},{10... | collective-permute-start | bytes 1572872 | tf_op jit(solution)/shard_map/ppermute | solution.py:26
  59.3 14.9 %collective-permute-start.8 = (bf16[8,32,1024]{2,1,0:T(8,128)(2,1)S(1)}, bf16[8,32,1024]{2,1,0:T(8,128)(2,1)S(1)}, u32[]{:S(2)}, u32[]{:S(2)}) collective-permute-start(bf16[8,32,1024]{2,1,0:T(8,128)(2,1)S(1)} %all-to-all-done.refs_9_.refs_21_), channel_id=1, source_target_pairs={{0,4},{4,0},{1,5},{5,1},{2,6},{6,2},{3,7},{7,3},{8,12},{12,8},{9,1... | collective-permute-start | bytes 1572872 | tf_op jit(solution)/shard_map/ppermute | solution.py:26
  59.3 19.3 %copy-start.2 = (bf16[8,32,1024]{2,1,0:T(8,128)(2,1)}, bf16[8,32,1024]{2,1,0:T(8,128)(2,1)S(1)}, u32[]{:S(2)}) copy-start(bf16[8,32,1024]{2,1,0:T(8,128)(2,1)S(1)} %collective-permute-done.6.refs_11_.refs_23_) | copy-start | bytes 1572868
  59.3 18.3 %collective-permute-start.10 = (bf16[8,32,1024]{2,1,0:T(8,128)(2,1)S(1)}, bf16[8,32,1024]{2,1,0:T(8,128)(2,1)}, u32[]{:S(2)}, u32[]{:S(2)}) collective-permute-start(bf16[8,32,1024]{2,1,0:T(8,128)(2,1)S(1)} %collective-permute-done.6.refs_11_.refs_23_), channel_id=1, source_target_pairs={{0,4},{4,0},{1,5},{5,1},{2,6},{6,2},{3,7},{7,3},{8,12},{12,8},{9,1... | collective-permute-start | bytes 1572872 | tf_op jit(solution)/shard_map/ppermute | solution.py:26
  64.6 8.9 %collective-permute-start.4 = (bf16[480,512]{1,0:T(8,128)(2,1)S(1)}, bf16[480,512]{1,0:T(8,128)(2,1)}, u32[]{:S(2)}, u32[]{:S(2)}) collective-permute-start(bf16[480,512]{1,0:T(8,128)(2,1)S(1)} %constant_dynamic-update-slice_fusion.refs_0_.refs_4_), channel_id=1, source_target_pairs={{0,3},{1,0},{2,1},{3,2},{4,7},{5,4},{6,5},{7,6},{8,11},{9,8},{10,9... | collective-permute-start | bytes 1474568 | tf_op jit(solution)/shard_map/ppermute | solution.py:26
  64.7 13.9 %copy-start.3 = (bf16[8,32,1024]{2,1,0:T(8,128)(2,1)}, bf16[8,32,1024]{2,1,0:T(8,128)(2,1)S(1)}, u32[]{:S(2)}) copy-start(bf16[8,32,1024]{2,1,0:T(8,128)(2,1)S(1)} %collective-permute-done.7.refs_12_.refs_24_) | copy-start | bytes 1572868
  64.7 12.9 %collective-permute-start.11 = (bf16[8,32,1024]{2,1,0:T(8,128)(2,1)S(1)}, bf16[8,32,1024]{2,1,0:T(8,128)(2,1)}, u32[]{:S(2)}, u32[]{:S(2)}) collective-permute-start(bf16[8,32,1024]{2,1,0:T(8,128)(2,1)S(1)} %collective-permute-done.7.refs_12_.refs_24_), channel_id=1, source_target_pairs={{0,4},{4,0},{1,5},{5,1},{2,6},{6,2},{3,7},{7,3},{8,12},{12,8},{9,1... | collective-permute-start | bytes 1572872 | tf_op jit(solution)/shard_map/ppermute | solution.py:26
  67.0 11.7 %copy-start.4 = (bf16[8,32,1024]{2,1,0:T(8,128)(2,1)}, bf16[8,32,1024]{2,1,0:T(8,128)(2,1)S(1)}, u32[]{:S(2)}) copy-start(bf16[8,32,1024]{2,1,0:T(8,128)(2,1)S(1)} %collective-permute-done.5.refs_10_.refs_22_) | copy-start | bytes 1572868
  67.0 11.6 %collective-permute-start.9 = (bf16[8,32,1024]{2,1,0:T(8,128)(2,1)S(1)}, bf16[8,32,1024]{2,1,0:T(8,128)(2,1)}, u32[]{:S(2)}, u32[]{:S(2)}) collective-permute-start(bf16[8,32,1024]{2,1,0:T(8,128)(2,1)S(1)} %collective-permute-done.5.refs_10_.refs_22_), channel_id=1, source_target_pairs={{0,4},{4,0},{1,5},{5,1},{2,6},{6,2},{3,7},{7,3},{8,12},{12,8},{9,1... | collective-permute-start | bytes 1572872 | tf_op jit(solution)/shard_map/ppermute | solution.py:26
  73.5 26.3 %collective-permute-start.18 = (bf16[8,32,1024]{2,1,0:T(8,128)(2,1)}, bf16[8,32,1024]{2,1,0:T(8,128)(2,1)}, u32[]{:S(2)}, u32[]{:S(2)}) collective-permute-start(bf16[8,32,1024]{2,1,0:T(8,128)(2,1)} %all-to-all-done.1.refs_13_), channel_id=1, source_target_pairs={{0,8},{8,16},{16,24},{24,0},{1,9},{9,17},{17,25},{25,1},{2,10},{10... | collective-permute-start | bytes 1572872 | tf_op jit(solution)/shard_map/ppermute | solution.py:26
  74.2 4.4 %copy-start.5 = (bf16[8,32,1024]{2,1,0:T(8,128)(2,1)}, bf16[8,32,1024]{2,1,0:T(8,128)(2,1)S(1)}, u32[]{:S(2)}) copy-start(bf16[8,32,1024]{2,1,0:T(8,128)(2,1)S(1)} %collective-permute-done.8.refs_13_.refs_25_) | copy-start | bytes 1572868
  74.2 44.0 %collective-permute-start.19 = (bf16[8,32,1024]{2,1,0:T(8,128)(2,1)}, bf16[8,32,1024]{2,1,0:T(8,128)(2,1)}, u32[]{:S(2)}, u32[]{:S(2)}) collective-permute-start(bf16[8,32,1024]{2,1,0:T(8,128)(2,1)} %all-to-all-done.1.refs_13_), channel_id=1, source_target_pairs={{0,16},{8,24},{16,0},{24,8},{1,17},{9,25},{17,1},{25,9},{2,18},{10... | collective-permute-start | bytes 1572872 | tf_op jit(solution)/shard_map/ppermute | solution.py:26
  77.7 40.6 %collective-permute-start.20 = (bf16[8,32,1024]{2,1,0:T(8,128)(2,1)}, bf16[8,32,1024]{2,1,0:T(8,128)(2,1)}, u32[]{:S(2)}, u32[]{:S(2)}) collective-permute-start(bf16[8,32,1024]{2,1,0:T(8,128)(2,1)} %all-to-all-done.1.refs_13_), channel_id=1, source_target_pairs={{0,24},{8,0},{16,8},{24,16},{1,25},{9,1},{17,9},{25,17},{2,26},{10... | collective-permute-start | bytes 1572872 | tf_op jit(solution)/shard_map/ppermute | solution.py:26
  77.7 44.0 %collective-permute-start.21 = (bf16[8,32,1024]{2,1,0:T(8,128)(2,1)}, bf16[8,32,1024]{2,1,0:T(8,128)(2,1)}, u32[]{:S(2)}, u32[]{:S(2)}) collective-permute-start(bf16[8,32,1024]{2,1,0:T(8,128)(2,1)} %all-to-all-done.1.refs_13_), channel_id=1, source_target_pairs={{0,4},{4,0},{1,5},{5,1},{2,6},{6,2},{3,7},{7,3},{8,12},{12,8},{9,1... | collective-permute-start | bytes 1572872 | tf_op jit(solution)/shard_map/ppermute | solution.py:26
  118.3 19.1 %collective-permute-start.22 = (bf16[8,32,1024]{2,1,0:T(8,128)(2,1)}, bf16[8,32,1024]{2,1,0:T(8,128)(2,1)S(1)}, u32[]{:S(2)}, u32[]{:S(2)}) collective-permute-start(bf16[8,32,1024]{2,1,0:T(8,128)(2,1)} %collective-permute-done.18.refs_14_), channel_id=1, source_target_pairs={{0,4},{4,0},{1,5},{5,1},{2,6},{6,2},{3,7},{7,3},{8,12},{12,8},{9,1... | collective-permute-start | bytes 1572872 | tf_op jit(solution)/shard_map/ppermute | solution.py:26
  118.3 19.1 %collective-permute-start.23 = (bf16[8,32,1024]{2,1,0:T(8,128)(2,1)}, bf16[8,32,1024]{2,1,0:T(8,128)(2,1)S(1)}, u32[]{:S(2)}, u32[]{:S(2)}) collective-permute-start(bf16[8,32,1024]{2,1,0:T(8,128)(2,1)} %collective-permute-done.19.refs_15_), channel_id=1, source_target_pairs={{0,4},{4,0},{1,5},{5,1},{2,6},{6,2},{3,7},{7,3},{8,12},{12,8},{9,1... | collective-permute-start | bytes 1572872 | tf_op jit(solution)/shard_map/ppermute | solution.py:26
  118.8 18.6 %collective-permute-start.24 = (bf16[8,32,1024]{2,1,0:T(8,128)(2,1)}, bf16[8,32,1024]{2,1,0:T(8,128)(2,1)S(1)}, u32[]{:S(2)}, u32[]{:S(2)}) collective-permute-start(bf16[8,32,1024]{2,1,0:T(8,128)(2,1)} %collective-permute-done.20.refs_16_), channel_id=1, source_target_pairs={{0,4},{4,0},{1,5},{5,1},{2,6},{6,2},{3,7},{7,3},{8,12},{12,8},{9,1... | collective-permute-start | bytes 1572872 | tf_op jit(solution)/shard_map/ppermute | solution.py:26
  118.8 10.7 %collective-permute-start.12 = (bf16[464,256]{1,0:T(8,128)(2,1)}, bf16[464,256]{1,0:T(8,128)(2,1)S(1)}, u32[]{:S(2)}, u32[]{:S(2)}) collective-permute-start(bf16[464,256]{1,0:T(8,128)(2,1)} %shard_map.91.refs_0_), channel_id=1, source_target_pairs={{0,1},{1,2},{2,3},{3,0},{4,5},{5,6},{6,7},{7,4},{8,9},{9,10},{10,1... | collective-permute-start | bytes 712712 | tf_op jit(solution)/shard_map/ppermute | solution.py:26
  121.6 14.1 %collective-permute-start.13 = (bf16[464,256]{1,0:T(8,128)(2,1)}, bf16[464,256]{1,0:T(8,128)(2,1)S(1)}, u32[]{:S(2)}, u32[]{:S(2)}) collective-permute-start(bf16[464,256]{1,0:T(8,128)(2,1)} %shard_map.91.refs_0_), channel_id=1, source_target_pairs={{0,2},{1,3},{2,0},{3,1},{4,6},{5,7},{6,4},{7,5},{8,10},{9,11},{10,... | collective-permute-start | bytes 712712 | tf_op jit(solution)/shard_map/ppermute | solution.py:26
  129.5 7.9 %copy-start.10 = (bf16[464,256]{1,0:T(8,128)(2,1)}, bf16[464,256]{1,0:T(8,128)(2,1)S(1)}, u32[]{:S(2)}) copy-start(bf16[464,256]{1,0:T(8,128)(2,1)S(1)} %collective-permute-done.12.refs_1_) | copy-start | bytes 712708
  129.5 7.8 %collective-permute-start.14 = (bf16[464,256]{1,0:T(8,128)(2,1)}, bf16[464,256]{1,0:T(8,128)(2,1)S(1)}, u32[]{:S(2)}, u32[]{:S(2)}) collective-permute-start(bf16[464,256]{1,0:T(8,128)(2,1)} %shard_map.91.refs_0_), channel_id=1, source_target_pairs={{0,3},{1,0},{2,1},{3,2},{4,7},{5,4},{6,5},{7,6},{8,11},{9,8},{10,9... | collective-permute-start | bytes 712712 | tf_op jit(solution)/shard_map/ppermute | solution.py:26
  135.8 1.6 copy-start.11
  137.4 0.9 copy-start.7
  137.4 1.1 copy-start.8
  138.4 0.8 copy-start.9
  151.1 10.3 %collective-permute-start.25 = (bf16[432,256]{1,0:T(8,128)(2,1)}, bf16[432,256]{1,0:T(8,128)(2,1)S(1)}, u32[]{:S(2)}, u32[]{:S(2)}) collective-permute-start(bf16[432,256]{1,0:T(8,128)(2,1)} %get-tuple-element.15.refs_0_), channel_id=1, source_target_pairs={{0,1},{1,2},{2,3},{3,0},{4,5},{5,6},{6,7},{7,4},{8,9},{9,10},{10,1... | collective-permute-start | bytes 663560 | tf_op jit(solution)/shard_map/ppermute | solution.py:26
  151.7 12.2 %collective-permute-start.26 = (bf16[432,256]{1,0:T(8,128)(2,1)}, bf16[432,256]{1,0:T(8,128)(2,1)S(1)}, u32[]{:S(2)}, u32[]{:S(2)}) collective-permute-start(bf16[432,256]{1,0:T(8,128)(2,1)} %get-tuple-element.15.refs_0_), channel_id=1, source_target_pairs={{0,2},{1,3},{2,0},{3,1},{4,6},{5,7},{6,4},{7,5},{8,10},{9,11},{10,... | collective-permute-start | bytes 663560 | tf_op jit(solution)/shard_map/ppermute | solution.py:26
  155.4 9.0 %collective-permute-start.27 = (bf16[432,256]{1,0:T(8,128)(2,1)}, bf16[432,256]{1,0:T(8,128)(2,1)S(1)}, u32[]{:S(2)}, u32[]{:S(2)}) collective-permute-start(bf16[432,256]{1,0:T(8,128)(2,1)} %get-tuple-element.15.refs_0_), channel_id=1, source_target_pairs={{0,3},{1,0},{2,1},{3,2},{4,7},{5,4},{6,5},{7,6},{8,11},{9,8},{10,9... | collective-permute-start | bytes 663560 | tf_op jit(solution)/shard_map/ppermute | solution.py:26
  161.4 3.0 %copy-start.13 = (bf16[432,256]{1,0:T(8,128)(2,1)}, bf16[432,256]{1,0:T(8,128)(2,1)S(1)}, u32[]{:S(2)}) copy-start(bf16[432,256]{1,0:T(8,128)(2,1)S(1)} %collective-permute-done.25.refs_1_) | copy-start | bytes 663556
  176.6 7.8 %collective-permute-start.28 = (bf16[400,256]{1,0:T(8,128)(2,1)}, bf16[400,256]{1,0:T(8,128)(2,1)S(1)}, u32[]{:S(2)}, u32[]{:S(2)}) collective-permute-start(bf16[400,256]{1,0:T(8,128)(2,1)} %get-tuple-element.17.refs_0_), channel_id=1, source_target_pairs={{0,1},{1,2},{2,3},{3,0},{4,5},{5,6},{6,7},{7,4},{8,9},{9,10},{10,1... | collective-permute-start | bytes 614408 | tf_op jit(solution)/shard_map/ppermute | solution.py:26
  177.0 13.0 %collective-permute-start.29 = (bf16[400,256]{1,0:T(8,128)(2,1)}, bf16[400,256]{1,0:T(8,128)(2,1)S(1)}, u32[]{:S(2)}, u32[]{:S(2)}) collective-permute-start(bf16[400,256]{1,0:T(8,128)(2,1)} %get-tuple-element.17.refs_0_), channel_id=1, source_target_pairs={{0,2},{1,3},{2,0},{3,1},{4,6},{5,7},{6,4},{7,5},{8,10},{9,11},{10,... | collective-permute-start | bytes 614408 | tf_op jit(solution)/shard_map/ppermute | solution.py:26
  180.7 9.3 %collective-permute-start.30 = (bf16[400,256]{1,0:T(8,128)(2,1)}, bf16[400,256]{1,0:T(8,128)(2,1)S(1)}, u32[]{:S(2)}, u32[]{:S(2)}) collective-permute-start(bf16[400,256]{1,0:T(8,128)(2,1)} %get-tuple-element.17.refs_0_), channel_id=1, source_target_pairs={{0,3},{1,0},{2,1},{3,2},{4,7},{5,4},{6,5},{7,6},{8,11},{9,8},{10,9... | collective-permute-start | bytes 614408 | tf_op jit(solution)/shard_map/ppermute | solution.py:26
  184.5 5.6 %copy-start.16 = (bf16[400,256]{1,0:T(8,128)(2,1)}, bf16[400,256]{1,0:T(8,128)(2,1)S(1)}, u32[]{:S(2)}) copy-start(bf16[400,256]{1,0:T(8,128)(2,1)S(1)} %collective-permute-done.28.refs_1_) | copy-start | bytes 614404
  (5 other events, 3.5 us)
Sparse Core Ops, SparseCore 0:
  16.7 112.1 all-gather.1

commit v7 on v6

--- a/solution.py
+++ b/solution.py
@@ -120,7 +120,7 @@
             value = (streams[s][here] if n_s > 1 else streams[0][s, here]).astype(f32)
             normed[here, wide] = (value * scale * gain[layer : layer + 1, wide]).astype(bf16)
 
-    by_rows(rows, norm, 128)
+    by_rows(rows, norm, rows // 2)
     for copy in copies:
         copy.wait()
     for half in range(2):
@@ -134,7 +134,7 @@
         gated = jnp.where((t >= 0) & (t < total), gated, 0.0).astype(bf16)
         padded[here] = gated.astype(f32)
 
-    by_rows(rows, gate, 128)
+    by_rows(rows, gate, rows // 2)
     columns[pl.ds(keep, 2 * ch - keep)] = jnp.zeros((2 * ch - keep, LANES), f32)
 
     def filtered(first, size):
@@ -218,7 +218,7 @@
             value = value * params[s][:, :ch] + params[s][:, ch:]
             act[here, s * ch : (s + 1) * ch] = (value * jax.nn.sigmoid(value)).astype(bf16)
 
-    by_rows(keep, activate, 128)
+    by_rows(keep, activate, keep // 2)
     for copy in copies:
         copy.wait()
     dims = (((1,), (1,)), ((), ()))

time: 203 us -> 203 us (level)
  no operation moved by 1% of the time
where the time goes in v7:
time: 203 us; the launch traced here: 202 us
  waiting for transfers between devices  86.7 us (43%)
  starting transfers between devices  58.5 us (29%)
  Pallas kernels  35.4 us (17%)
  between operations  13.6 us (7%)
  local copies, waits for them, and re-layouts  6.5 us (3%)
    ppermute x29, waiting for transfers between devices, shifted(): return lax.ppermute(array, axis, [(i, (i + s) % n) for i in range(n)])  78.6 us
    ppermute x29, starting transfers between devices, shifted(): return lax.ppermute(array, axis, [(i, (i + s) % n) for i in range(n)])  36.8 us
    pallas_call x2, Pallas kernels, mid(): pl.pallas_call(functools.partial(mid_kernel, layer, total, len(streams),...  23.2 us
    all_to_all x2, starting transfers between devices, to_all(): return lax.all_to_all(copies, axis, split_axis=0, concat_axis=0, tiled=True)  14 us
    pallas_call x1, Pallas kernels, up(): pl.pallas_call(functools.partial(up_kernel, layer, total, len(streams), n...  7.42 us
    ppermute x1, starting transfers between devices, program(): lax.ppermute(tokens[:halo], SP, [(i + 1, i) for i in range(size - 1)])  5.75 us
    all_to_all x2, waiting for transfers between devices, to_all(): return lax.all_to_all(copies, axis, split_axis=0, concat_axis=0, tiled=True)  5.28 us
    pallas_call x1, Pallas kernels, down(): pl.pallas_call(functools.partial(down_kernel, n_x, first_lane), out_shape...  4.78 us
  transfers between devices with their start and end apart: 34, of which 19 were waited for; matrix products, arithmetic and copies ran while one was open for 2% of the time, Pallas kernels for 10%

profile of v7, /device:TPU:32, one launch (start us, length us, event | category | flops | bytes accessed | tf_op | source)
XLA Modules:
  0.0 202.3 jit_solution(5944362969661120352)
XLA Ops:
  6.5 1.5 collective-permute-start.15
  8.0 2.7 %collective-permute-start.16 = (bf16[3,32,256]{2,1,0:T(8,128)(2,1)}, bf16[3,32,256]{2,1,0:T(8,128)(2,1)S(1)}, u32[]{:S(2)}, u32[]{:S(2)}) collective-permute-start(bf16[3,32,256]{2,1,0:T(8,128)(2,1)} %bitcast.26), channel_id=1, source_target_pairs={{0,2},{1,3},{2,0},{3,1},{4,6},{5,7},{6,4},{7,5},{8,10},{9,11},{10,... | collective-permute-start | bytes 147464 | tf_op jit(solution)/shard_map/ppermute | solution.py:26
  10.8 1.4 collective-permute-start.17
  12.2 0.8 slice_bitcast_fusion.3
  13.0 0.8 collective-permute-done.16
  13.8 1.2 collective-permute-done.17
  15.1 0.8 pad_maximum_fusion
  15.9 0.7 pad_maximum_fusion.1
  16.6 0.8 broadcast_in_dim.6
  17.5 8.6 %all-to-all-start = ((bf16[8,32,1024]{2,1,0:T(8,128)(2,1)}), bf16[8,32,1024]{2,1,0:T(8,128)(2,1)S(1)}, u32[]{:S(2)}, u32[]{:S(2)}) async-start(bf16[8,32,1024]{2,1,0:T(8,128)(2,1)} %broadcast_in_dim.6), calls=%async_computation | async-start | bytes 1048576 | tf_op jit(solution)/shard_map/all_to_all | solution.py:21
  26.1 1.9 collective-permute-start
  28.0 5.8 %collective-permute-start.1 = (bf16[48,512]{1,0:T(8,128)(2,1)S(1)}, bf16[48,512]{1,0:T(8,128)(2,1)S(1)}, u32[]{:S(2)}, u32[]{:S(2)}) collective-permute-start(bf16[48,512]{1,0:T(8,128)(2,1)S(1)} %get-tuple-element.19), channel_id=1, source_target_pairs={{4,0},{8,4},{12,8},{16,12},{20,16},{24,20},{28,24},{32,28},{36,32}... | collective-permute-start | bytes 147464 | tf_op jit(solution)/shard_map/ppermute | solution.py:364
  33.7 2.8 %collective-permute-done = bf16[48,512]{1,0:T(8,128)(2,1)S(1)} collective-permute-done((bf16[48,512]{1,0:T(8,128)(2,1)S(1)}, bf16[48,512]{1,0:T(8,128)(2,1)S(1)}, u32[]{:S(2)}, u32[]{:S(2)}) %collective-permute-start) | collective-permute-done | bytes 49184 | tf_op jit(solution)/shard_map/ppermute | solution.py:363
  36.6 5.3 %all-to-all-done.refs_9_.refs_21_ = bf16[8,32,1024]{2,1,0:T(8,128)(2,1)S(1)} async-done(((bf16[8,32,1024]{2,1,0:T(8,128)(2,1)}), bf16[8,32,1024]{2,1,0:T(8,128)(2,1)S(1)}, u32[]{:S(2)}, u32[]{:S(2)}) %all-to-all-start) | async-done | bytes 524320 | tf_op jit(solution)/shard_map/all_to_all | solution.py:21
  41.8 3.4 %collective-permute-start.6 = (bf16[8,32,1024]{2,1,0:T(8,128)(2,1)S(1)}, bf16[8,32,1024]{2,1,0:T(8,128)(2,1)S(1)}, u32[]{:S(2)}, u32[]{:S(2)}) collective-permute-start(bf16[8,32,1024]{2,1,0:T(8,128)(2,1)S(1)} %all-to-all-done.refs_9_.refs_21_), channel_id=1, source_target_pairs={{0,16},{8,24},{16,0},{24,8},{1,17},{9,25},{17,1},{25,9},{2,18},{10... | collective-permute-start | bytes 1572872 | tf_op jit(solution)/shard_map/ppermute | solution.py:26
  45.4 3.9 %collective-permute-start.3 = (bf16[480,512]{1,0:T(8,128)(2,1)S(1)}, bf16[480,512]{1,0:T(8,128)(2,1)}, u32[]{:S(2)}, u32[]{:S(2)}) collective-permute-start(bf16[480,512]{1,0:T(8,128)(2,1)S(1)} %constant_dynamic-update-slice_fusion.refs_0_.refs_4_), channel_id=1, source_target_pairs={{0,2},{1,3},{2,0},{3,1},{4,6},{5,7},{6,4},{7,5},{8,10},{9,11},{10,... | collective-permute-start | bytes 1474568 | tf_op jit(solution)/shard_map/ppermute | solution.py:26
  49.3 0.8 broadcast_in_dim.7
  50.1 5.5 %all-to-all-start.1 = ((bf16[8,32,1024]{2,1,0:T(8,128)(2,1)}), bf16[8,32,1024]{2,1,0:T(8,128)(2,1)}, u32[]{:S(2)}, u32[]{:S(2)}) async-start(bf16[8,32,1024]{2,1,0:T(8,128)(2,1)} %broadcast_in_dim.7), calls=%async_computation.1 | async-start | bytes 1048576 | tf_op jit(solution)/shard_map/all_to_all | solution.py:21
  55.6 1.0 collective-permute-start.7
  56.6 1.0 collective-permute-start.5
  57.6 1.7 collective-permute-done.2.refs_1_.refs_5_
  59.9 4.7 %collective-permute-done.3.refs_2_.refs_6_ = bf16[480,512]{1,0:T(8,128)(2,1)} collective-permute-done((bf16[480,512]{1,0:T(8,128)(2,1)S(1)}, bf16[480,512]{1,0:T(8,128)(2,1)}, u32[]{:S(2)}, u32[]{:S(2)}) %collective-permute-start.3) | collective-permute-done | bytes 491552 | tf_op jit(solution)/shard_map/ppermute | solution.py:26
  64.7 2.2 %collective-permute-done.5.refs_10_.refs_22_ = bf16[8,32,1024]{2,1,0:T(8,128)(2,1)S(1)} collective-permute-done((bf16[8,32,1024]{2,1,0:T(8,128)(2,1)S(1)}, bf16[8,32,1024]{2,1,0:T(8,128)(2,1)S(1)}, u32[]{:S(2)}, u32[]{:S(2)}) %collective-permute-start.5) | collective-permute-done | bytes 524320 | tf_op jit(solution)/shard_map/ppermute | solution.py:26
  67.0 6.6 %collective-permute-done.4.refs_3_.refs_7_ = bf16[480,512]{1,0:T(8,128)(2,1)} collective-permute-done((bf16[480,512]{1,0:T(8,128)(2,1)S(1)}, bf16[480,512]{1,0:T(8,128)(2,1)}, u32[]{:S(2)}, u32[]{:S(2)}) %collective-permute-start.4) | collective-permute-done | bytes 491552 | tf_op jit(solution)/shard_map/ppermute | solution.py:26
  73.5 0.7 collective-permute-start.18
  74.2 3.5 %collective-permute-start.19 = (bf16[8,32,1024]{2,1,0:T(8,128)(2,1)}, bf16[8,32,1024]{2,1,0:T(8,128)(2,1)}, u32[]{:S(2)}, u32[]{:S(2)}) collective-permute-start(bf16[8,32,1024]{2,1,0:T(8,128)(2,1)} %all-to-all-done.1.refs_13_), channel_id=1, source_target_pairs={{0,16},{8,24},{16,0},{24,8},{1,17},{9,25},{17,1},{25,9},{2,18},{10... | collective-permute-start | bytes 1572872 | tf_op jit(solution)/shard_map/ppermute | solution.py:26
  78.0 0.6 stack.27.info
  78.7 7.4 %shard_map.91.refs_0_ = bf16[464,256]{1,0:T(8,128)(2,1)} custom-call(s32[6]{0:T(128)} %stack.27.info, bf16[480,512]{1,0:T(8,128)(2,1)} %copy-done.1, bf16[480,512]{1,0:T(8,128)(2,1)} %collective-permute-done.2.refs_1_.refs_5_, bf16[480,512]{1,0:T(8,128)(2,1)} %collective-permute-done.3.refs_2_.refs_6_, ...), custom_call_target="tpu_custom_call" | custom-call | tf_op jit(solution)/shard_map/pallas_call | solution.py:287
  86.1 13.8 %collective-permute-done.18.refs_14_ = bf16[8,32,1024]{2,1,0:T(8,128)(2,1)} collective-permute-done((bf16[8,32,1024]{2,1,0:T(8,128)(2,1)}, bf16[8,32,1024]{2,1,0:T(8,128)(2,1)}, u32[]{:S(2)}, u32[]{:S(2)}) %collective-permute-start.18) | collective-permute-done | bytes 524320 | tf_op jit(solution)/shard_map/ppermute | solution.py:26
  99.8 18.4 %collective-permute-done.19.refs_15_ = bf16[8,32,1024]{2,1,0:T(8,128)(2,1)} collective-permute-done((bf16[8,32,1024]{2,1,0:T(8,128)(2,1)}, bf16[8,32,1024]{2,1,0:T(8,128)(2,1)}, u32[]{:S(2)}, u32[]{:S(2)}) %collective-permute-start.19) | collective-permute-done | bytes 524320 | tf_op jit(solution)/shard_map/ppermute | solution.py:26
  118.8 2.9 %collective-permute-start.12 = (bf16[464,256]{1,0:T(8,128)(2,1)}, bf16[464,256]{1,0:T(8,128)(2,1)S(1)}, u32[]{:S(2)}, u32[]{:S(2)}) collective-permute-start(bf16[464,256]{1,0:T(8,128)(2,1)} %shard_map.91.refs_0_), channel_id=1, source_target_pairs={{0,1},{1,2},{2,3},{3,0},{4,5},{5,6},{6,7},{7,4},{8,9},{9,10},{10,1... | collective-permute-start | bytes 712712 | tf_op jit(solution)/shard_map/ppermute | solution.py:26
  121.6 2.7 %collective-permute-start.13 = (bf16[464,256]{1,0:T(8,128)(2,1)}, bf16[464,256]{1,0:T(8,128)(2,1)S(1)}, u32[]{:S(2)}, u32[]{:S(2)}) collective-permute-start(bf16[464,256]{1,0:T(8,128)(2,1)} %shard_map.91.refs_0_), channel_id=1, source_target_pairs={{0,2},{1,3},{2,0},{3,1},{4,6},{5,7},{6,4},{7,5},{8,10},{9,11},{10,... | collective-permute-start | bytes 712712 | tf_op jit(solution)/shard_map/ppermute | solution.py:26
  124.3 5.2 %collective-permute-done.12.refs_1_ = bf16[464,256]{1,0:T(8,128)(2,1)S(1)} collective-permute-done((bf16[464,256]{1,0:T(8,128)(2,1)}, bf16[464,256]{1,0:T(8,128)(2,1)S(1)}, u32[]{:S(2)}, u32[]{:S(2)}) %collective-permute-start.12) | collective-permute-done | bytes 237600 | tf_op jit(solution)/shard_map/ppermute | solution.py:26
  129.5 2.2 %collective-permute-start.14 = (bf16[464,256]{1,0:T(8,128)(2,1)}, bf16[464,256]{1,0:T(8,128)(2,1)S(1)}, u32[]{:S(2)}, u32[]{:S(2)}) collective-permute-start(bf16[464,256]{1,0:T(8,128)(2,1)} %shard_map.91.refs_0_), channel_id=1, source_target_pairs={{0,3},{1,0},{2,1},{3,2},{4,7},{5,4},{6,5},{7,6},{8,11},{9,8},{10,9... | collective-permute-start | bytes 712712 | tf_op jit(solution)/shard_map/ppermute | solution.py:26
  131.7 4.1 %collective-permute-done.13.refs_2_ = bf16[464,256]{1,0:T(8,128)(2,1)S(1)} collective-permute-done((bf16[464,256]{1,0:T(8,128)(2,1)}, bf16[464,256]{1,0:T(8,128)(2,1)S(1)}, u32[]{:S(2)}, u32[]{:S(2)}) %collective-permute-start.13) | collective-permute-done | bytes 237600 | tf_op jit(solution)/shard_map/ppermute | solution.py:26
  135.8 1.6 collective-permute-done.14.refs_3_
  137.4 0.6 copy-done.12
  138.4 0.8 copy-done.9
  139.2 11.9 %shard_map.92 = (bf16[4,448,512]{2,1,0:T(8,128)(2,1)}, bf16[432,256]{1,0:T(8,128)(2,1)}) custom-call(s32[6]{0:T(128)} %stack.27.info, bf16[464,256]{1,0:T(8,128)(2,1)} %shard_map.91.refs_0_, bf16[464,256]{1,0:T(8,128)(2,1)} %copy-done.10, bf16[464,256]{1,0:T(8,128)(2,1)} %copy-done.11, bf16[464,256]{1,0:T(8,128)(2,1)} %copy-done.12, ...), custom_call_target="tpu_custom_call" | custom-call | tf_op jit(solution)/shard_map/pallas_call | solution.py:304
  151.6 3.7 %collective-permute-start.26 = (bf16[432,256]{1,0:T(8,128)(2,1)}, bf16[432,256]{1,0:T(8,128)(2,1)S(1)}, u32[]{:S(2)}, u32[]{:S(2)}) collective-permute-start(bf16[432,256]{1,0:T(8,128)(2,1)} %get-tuple-element.15.refs_0_), channel_id=1, source_target_pairs={{0,2},{1,3},{2,0},{3,1},{4,6},{5,7},{6,4},{7,5},{8,10},{9,11},{10,... | collective-permute-start | bytes 663560 | tf_op jit(solution)/shard_map/ppermute | solution.py:26
  155.5 5.8 %collective-permute-done.25.refs_1_ = bf16[432,256]{1,0:T(8,128)(2,1)S(1)} collective-permute-done((bf16[432,256]{1,0:T(8,128)(2,1)}, bf16[432,256]{1,0:T(8,128)(2,1)S(1)}, u32[]{:S(2)}, u32[]{:S(2)}) %collective-permute-start.25) | collective-permute-done | bytes 221216 | tf_op jit(solution)/shard_map/ppermute | solution.py:26
  161.4 2.5 %collective-permute-done.26.refs_2_ = bf16[432,256]{1,0:T(8,128)(2,1)S(1)} collective-permute-done((bf16[432,256]{1,0:T(8,128)(2,1)}, bf16[432,256]{1,0:T(8,128)(2,1)S(1)}, u32[]{:S(2)}, u32[]{:S(2)}) %collective-permute-start.26) | collective-permute-done | bytes 221216 | tf_op jit(solution)/shard_map/ppermute | solution.py:26
  165.1 11.4 %shard_map.93 = (bf16[4,416,512]{2,1,0:T(8,128)(2,1)}, bf16[400,256]{1,0:T(8,128)(2,1)}) custom-call(s32[6]{0:T(128)} %stack.27.info, bf16[432,256]{1,0:T(8,128)(2,1)} %get-tuple-element.15.refs_0_, bf16[432,256]{1,0:T(8,128)(2,1)} %copy-done.13, bf16[432,256]{1,0:T(8,128)(2,1)} %copy-done.14, bf16[432,256]{1,0:T(8,128)(2,1)} %copy-done.15, ...), custom_call_target="tpu_custom_call" | custom-call | tf_op jit(solution)/shard_map/pallas_call | solution.py:304
  176.9 3.6 %collective-permute-start.29 = (bf16[400,256]{1,0:T(8,128)(2,1)}, bf16[400,256]{1,0:T(8,128)(2,1)S(1)}, u32[]{:S(2)}, u32[]{:S(2)}) collective-permute-start(bf16[400,256]{1,0:T(8,128)(2,1)} %get-tuple-element.17.refs_0_), channel_id=1, source_target_pairs={{0,2},{1,3},{2,0},{3,1},{4,6},{5,7},{6,4},{7,5},{8,10},{9,11},{10,... | collective-permute-start | bytes 614408 | tf_op jit(solution)/shard_map/ppermute | solution.py:26
  180.5 3.8 %collective-permute-done.28.refs_1_ = bf16[400,256]{1,0:T(8,128)(2,1)S(1)} collective-permute-done((bf16[400,256]{1,0:T(8,128)(2,1)}, bf16[400,256]{1,0:T(8,128)(2,1)S(1)}, u32[]{:S(2)}, u32[]{:S(2)}) %collective-permute-start.28) | collective-permute-done | bytes 204832 | tf_op jit(solution)/shard_map/ppermute | solution.py:26
  184.3 5.6 %collective-permute-done.29.refs_2_ = bf16[400,256]{1,0:T(8,128)(2,1)S(1)} collective-permute-done((bf16[400,256]{1,0:T(8,128)(2,1)}, bf16[400,256]{1,0:T(8,128)(2,1)S(1)}, u32[]{:S(2)}, u32[]{:S(2)}) %collective-permute-start.29) | collective-permute-done | bytes 204832 | tf_op jit(solution)/shard_map/ppermute | solution.py:26
  189.9 0.7 copy-done.17
  190.6 4.8 %shard_map.94 = bf16[384,512]{1,0:T(8,128)(2,1)} custom-call(s32[6]{0:T(128)} %stack.27.info, bf16[400,256]{1,0:T(8,128)(2,1)} %get-tuple-element.17.refs_0_, bf16[400,256]{1,0:T(8,128)(2,1)} %copy-done.16, bf16[400,256]{1,0:T(8,128)(2,1)} %copy-done.17, bf16[400,256]{1,0:T(8,128)(2,1)} %copy-done.18, bf16[4,416,512]{2,1,0:T(8,128)(2,1)} %get-tuple-element.18.refs_4_, ...), custom_call_target="tpu_custom_call" | custom-call | tf_op jit(solution)/shard_map/pallas_call | solution.py:321
  (75 shorter events, 4.6 us)
Async XLA Ops:
  6.5 19.5 %copy-start.6 = (bf16[384,512]{1,0:T(8,128)(2,1)S(1)}, bf16[384,512]{1,0:T(8,128)(2,1)}, u32[]{:S(2)}) copy-start(bf16[384,512]{1,0:T(8,128)(2,1)} %param.9) | copy-start | bytes 1179652
  6.5 157.8 %all-gather.2.cloned.1.call-start = ((), (), s32[]{:S(2)}) async-start(), calls=%async_computation.2 | async-start | bytes 10649600 | tf_op jit(solution)/shard_map/all_gather | solution.py:361
  6.5 6.5 %collective-permute-start.15 = (bf16[3,32,256]{2,1,0:T(8,128)(2,1)}, bf16[3,32,256]{2,1,0:T(8,128)(2,1)S(1)}, u32[]{:S(2)}, u32[]{:S(2)}) collective-permute-start(bf16[3,32,256]{2,1,0:T(8,128)(2,1)} %bitcast.25), channel_id=1, source_target_pairs={{0,1},{1,2},{2,3},{3,0},{4,5},{5,6},{6,7},{7,4},{8,9},{9,10},{10,1... | collective-permute-start | bytes 147464 | tf_op jit(solution)/shard_map/ppermute | solution.py:26
  8.0 5.8 %collective-permute-start.16 = (bf16[3,32,256]{2,1,0:T(8,128)(2,1)}, bf16[3,32,256]{2,1,0:T(8,128)(2,1)S(1)}, u32[]{:S(2)}, u32[]{:S(2)}) collective-permute-start(bf16[3,32,256]{2,1,0:T(8,128)(2,1)} %bitcast.26), channel_id=1, source_target_pairs={{0,2},{1,3},{2,0},{3,1},{4,6},{5,7},{6,4},{7,5},{8,10},{9,11},{10,... | collective-permute-start | bytes 147464 | tf_op jit(solution)/shard_map/ppermute | solution.py:26
  10.8 4.3 %collective-permute-start.17 = (bf16[3,32,256]{2,1,0:T(8,128)(2,1)}, bf16[3,32,256]{2,1,0:T(8,128)(2,1)S(1)}, u32[]{:S(2)}, u32[]{:S(2)}) collective-permute-start(bf16[3,32,256]{2,1,0:T(8,128)(2,1)} %bitcast.27), channel_id=1, source_target_pairs={{0,3},{1,0},{2,1},{3,2},{4,7},{5,4},{6,5},{7,6},{8,11},{9,8},{10,9... | collective-permute-start | bytes 147464 | tf_op jit(solution)/shard_map/ppermute | solution.py:26
  17.5 24.4 %all-to-all-start = ((bf16[8,32,1024]{2,1,0:T(8,128)(2,1)}), bf16[8,32,1024]{2,1,0:T(8,128)(2,1)S(1)}, u32[]{:S(2)}, u32[]{:S(2)}) async-start(bf16[8,32,1024]{2,1,0:T(8,128)(2,1)} %broadcast_in_dim.6), calls=%async_computation | async-start | bytes 1048576 | tf_op jit(solution)/shard_map/all_to_all | solution.py:21
  26.1 10.5 %collective-permute-start = (bf16[48,512]{1,0:T(8,128)(2,1)S(1)}, bf16[48,512]{1,0:T(8,128)(2,1)S(1)}, u32[]{:S(2)}, u32[]{:S(2)}) collective-permute-start(bf16[48,512]{1,0:T(8,128)(2,1)S(1)} %get-tuple-element.20), channel_id=1, source_target_pairs={{0,4},{4,8},{8,12},{12,16},{16,20},{20,24},{24,28},{28,32},{32,36}... | collective-permute-start | bytes 147464 | tf_op jit(solution)/shard_map/ppermute | solution.py:363
  28.0 17.3 %collective-permute-start.1 = (bf16[48,512]{1,0:T(8,128)(2,1)S(1)}, bf16[48,512]{1,0:T(8,128)(2,1)S(1)}, u32[]{:S(2)}, u32[]{:S(2)}) collective-permute-start(bf16[48,512]{1,0:T(8,128)(2,1)S(1)} %get-tuple-element.19), channel_id=1, source_target_pairs={{4,0},{8,4},{12,8},{16,12},{20,16},{24,20},{28,24},{32,28},{36,32}... | collective-permute-start | bytes 147464 | tf_op jit(solution)/shard_map/ppermute | solution.py:364
  41.8 36.8 %copy-start = (bf16[8,32,1024]{2,1,0:T(8,128)(2,1)}, bf16[8,32,1024]{2,1,0:T(8,128)(2,1)S(1)}, u32[]{:S(2)}) copy-start(bf16[8,32,1024]{2,1,0:T(8,128)(2,1)S(1)} %all-to-all-done.refs_9_.refs_21_) | copy-start | bytes 1572868
  41.8 17.5 %collective-permute-start.6 = (bf16[8,32,1024]{2,1,0:T(8,128)(2,1)S(1)}, bf16[8,32,1024]{2,1,0:T(8,128)(2,1)S(1)}, u32[]{:S(2)}, u32[]{:S(2)}) collective-permute-start(bf16[8,32,1024]{2,1,0:T(8,128)(2,1)S(1)} %all-to-all-done.refs_9_.refs_21_), channel_id=1, source_target_pairs={{0,16},{8,24},{16,0},{24,8},{1,17},{9,25},{17,1},{25,9},{2,18},{10... | collective-permute-start | bytes 1572872 | tf_op jit(solution)/shard_map/ppermute | solution.py:26
  45.3 33.4 %copy-start.1 = (bf16[480,512]{1,0:T(8,128)(2,1)}, bf16[480,512]{1,0:T(8,128)(2,1)S(1)}, u32[]{:S(2)}) copy-start(bf16[480,512]{1,0:T(8,128)(2,1)S(1)} %constant_dynamic-update-slice_fusion.refs_0_.refs_4_) | copy-start | bytes 1474564
  45.3 14.1 %collective-permute-start.2 = (bf16[480,512]{1,0:T(8,128)(2,1)S(1)}, bf16[480,512]{1,0:T(8,128)(2,1)}, u32[]{:S(2)}, u32[]{:S(2)}) collective-permute-start(bf16[480,512]{1,0:T(8,128)(2,1)S(1)} %constant_dynamic-update-slice_fusion.refs_0_.refs_4_), channel_id=1, source_target_pairs={{0,1},{1,2},{2,3},{3,0},{4,5},{5,6},{6,7},{7,4},{8,9},{9,10},{10,1... | collective-permute-start | bytes 1474568 | tf_op jit(solution)/shard_map/ppermute | solution.py:26
  45.4 19.2 %collective-permute-start.3 = (bf16[480,512]{1,0:T(8,128)(2,1)S(1)}, bf16[480,512]{1,0:T(8,128)(2,1)}, u32[]{:S(2)}, u32[]{:S(2)}) collective-permute-start(bf16[480,512]{1,0:T(8,128)(2,1)S(1)} %constant_dynamic-update-slice_fusion.refs_0_.refs_4_), channel_id=1, source_target_pairs={{0,2},{1,3},{2,0},{3,1},{4,6},{5,7},{6,4},{7,5},{8,10},{9,11},{10,... | collective-permute-start | bytes 1474568 | tf_op jit(solution)/shard_map/ppermute | solution.py:26
  50.1 23.4 %all-to-all-start.1 = ((bf16[8,32,1024]{2,1,0:T(8,128)(2,1)}), bf16[8,32,1024]{2,1,0:T(8,128)(2,1)}, u32[]{:S(2)}, u32[]{:S(2)}) async-start(bf16[8,32,1024]{2,1,0:T(8,128)(2,1)} %broadcast_in_dim.7), calls=%async_computation.1 | async-start | bytes 1048576 | tf_op jit(solution)/shard_map/all_to_all | solution.py:21
  55.6 9.2 %collective-permute-start.7 = (bf16[8,32,1024]{2,1,0:T(8,128)(2,1)S(1)}, bf16[8,32,1024]{2,1,0:T(8,128)(2,1)S(1)}, u32[]{:S(2)}, u32[]{:S(2)}) collective-permute-start(bf16[8,32,1024]{2,1,0:T(8,128)(2,1)S(1)} %all-to-all-done.refs_9_.refs_21_), channel_id=1, source_target_pairs={{0,24},{8,0},{16,8},{24,16},{1,25},{9,1},{17,9},{25,17},{2,26},{10... | collective-permute-start | bytes 1572872 | tf_op jit(solution)/shard_map/ppermute | solution.py:26
  56.6 10.4 %collective-permute-start.5 = (bf16[8,32,1024]{2,1,0:T(8,128)(2,1)S(1)}, bf16[8,32,1024]{2,1,0:T(8,128)(2,1)S(1)}, u32[]{:S(2)}, u32[]{:S(2)}) collective-permute-start(bf16[8,32,1024]{2,1,0:T(8,128)(2,1)S(1)} %all-to-all-done.refs_9_.refs_21_), channel_id=1, source_target_pairs={{0,8},{8,16},{16,24},{24,0},{1,9},{9,17},{17,25},{25,1},{2,10},{10... | collective-permute-start | bytes 1572872 | tf_op jit(solution)/shard_map/ppermute | solution.py:26
  59.3 14.9 %collective-permute-start.8 = (bf16[8,32,1024]{2,1,0:T(8,128)(2,1)S(1)}, bf16[8,32,1024]{2,1,0:T(8,128)(2,1)S(1)}, u32[]{:S(2)}, u32[]{:S(2)}) collective-permute-start(bf16[8,32,1024]{2,1,0:T(8,128)(2,1)S(1)} %all-to-all-done.refs_9_.refs_21_), channel_id=1, source_target_pairs={{0,4},{4,0},{1,5},{5,1},{2,6},{6,2},{3,7},{7,3},{8,12},{12,8},{9,1... | collective-permute-start | bytes 1572872 | tf_op jit(solution)/shard_map/ppermute | solution.py:26
  59.3 19.3 %copy-start.2 = (bf16[8,32,1024]{2,1,0:T(8,128)(2,1)}, bf16[8,32,1024]{2,1,0:T(8,128)(2,1)S(1)}, u32[]{:S(2)}) copy-start(bf16[8,32,1024]{2,1,0:T(8,128)(2,1)S(1)} %collective-permute-done.6.refs_11_.refs_23_) | copy-start | bytes 1572868
  59.3 18.3 %collective-permute-start.10 = (bf16[8,32,1024]{2,1,0:T(8,128)(2,1)S(1)}, bf16[8,32,1024]{2,1,0:T(8,128)(2,1)}, u32[]{:S(2)}, u32[]{:S(2)}) collective-permute-start(bf16[8,32,1024]{2,1,0:T(8,128)(2,1)S(1)} %collective-permute-done.6.refs_11_.refs_23_), channel_id=1, source_target_pairs={{0,4},{4,0},{1,5},{5,1},{2,6},{6,2},{3,7},{7,3},{8,12},{12,8},{9,1... | collective-permute-start | bytes 1572872 | tf_op jit(solution)/shard_map/ppermute | solution.py:26
  64.6 8.9 %collective-permute-start.4 = (bf16[480,512]{1,0:T(8,128)(2,1)S(1)}, bf16[480,512]{1,0:T(8,128)(2,1)}, u32[]{:S(2)}, u32[]{:S(2)}) collective-permute-start(bf16[480,512]{1,0:T(8,128)(2,1)S(1)} %constant_dynamic-update-slice_fusion.refs_0_.refs_4_), channel_id=1, source_target_pairs={{0,3},{1,0},{2,1},{3,2},{4,7},{5,4},{6,5},{7,6},{8,11},{9,8},{10,9... | collective-permute-start | bytes 1474568 | tf_op jit(solution)/shard_map/ppermute | solution.py:26
  64.7 13.9 %copy-start.3 = (bf16[8,32,1024]{2,1,0:T(8,128)(2,1)}, bf16[8,32,1024]{2,1,0:T(8,128)(2,1)S(1)}, u32[]{:S(2)}) copy-start(bf16[8,32,1024]{2,1,0:T(8,128)(2,1)S(1)} %collective-permute-done.7.refs_12_.refs_24_) | copy-start | bytes 1572868
  64.7 12.9 %collective-permute-start.11 = (bf16[8,32,1024]{2,1,0:T(8,128)(2,1)S(1)}, bf16[8,32,1024]{2,1,0:T(8,128)(2,1)}, u32[]{:S(2)}, u32[]{:S(2)}) collective-permute-start(bf16[8,32,1024]{2,1,0:T(8,128)(2,1)S(1)} %collective-permute-done.7.refs_12_.refs_24_), channel_id=1, source_target_pairs={{0,4},{4,0},{1,5},{5,1},{2,6},{6,2},{3,7},{7,3},{8,12},{12,8},{9,1... | collective-permute-start | bytes 1572872 | tf_op jit(solution)/shard_map/ppermute | solution.py:26
  67.0 11.7 %copy-start.4 = (bf16[8,32,1024]{2,1,0:T(8,128)(2,1)}, bf16[8,32,1024]{2,1,0:T(8,128)(2,1)S(1)}, u32[]{:S(2)}) copy-start(bf16[8,32,1024]{2,1,0:T(8,128)(2,1)S(1)} %collective-permute-done.5.refs_10_.refs_22_) | copy-start | bytes 1572868
  67.0 11.6 %collective-permute-start.9 = (bf16[8,32,1024]{2,1,0:T(8,128)(2,1)S(1)}, bf16[8,32,1024]{2,1,0:T(8,128)(2,1)}, u32[]{:S(2)}, u32[]{:S(2)}) collective-permute-start(bf16[8,32,1024]{2,1,0:T(8,128)(2,1)S(1)} %collective-permute-done.5.refs_10_.refs_22_), channel_id=1, source_target_pairs={{0,4},{4,0},{1,5},{5,1},{2,6},{6,2},{3,7},{7,3},{8,12},{12,8},{9,1... | collective-permute-start | bytes 1572872 | tf_op jit(solution)/shard_map/ppermute | solution.py:26
  73.5 26.3 %collective-permute-start.18 = (bf16[8,32,1024]{2,1,0:T(8,128)(2,1)}, bf16[8,32,1024]{2,1,0:T(8,128)(2,1)}, u32[]{:S(2)}, u32[]{:S(2)}) collective-permute-start(bf16[8,32,1024]{2,1,0:T(8,128)(2,1)} %all-to-all-done.1.refs_13_), channel_id=1, source_target_pairs={{0,8},{8,16},{16,24},{24,0},{1,9},{9,17},{17,25},{25,1},{2,10},{10... | collective-permute-start | bytes 1572872 | tf_op jit(solution)/shard_map/ppermute | solution.py:26
  74.2 4.4 %copy-start.5 = (bf16[8,32,1024]{2,1,0:T(8,128)(2,1)}, bf16[8,32,1024]{2,1,0:T(8,128)(2,1)S(1)}, u32[]{:S(2)}) copy-start(bf16[8,32,1024]{2,1,0:T(8,128)(2,1)S(1)} %collective-permute-done.8.refs_13_.refs_25_) | copy-start | bytes 1572868
  74.2 44.0 %collective-permute-start.19 = (bf16[8,32,1024]{2,1,0:T(8,128)(2,1)}, bf16[8,32,1024]{2,1,0:T(8,128)(2,1)}, u32[]{:S(2)}, u32[]{:S(2)}) collective-permute-start(bf16[8,32,1024]{2,1,0:T(8,128)(2,1)} %all-to-all-done.1.refs_13_), channel_id=1, source_target_pairs={{0,16},{8,24},{16,0},{24,8},{1,17},{9,25},{17,1},{25,9},{2,18},{10... | collective-permute-start | bytes 1572872 | tf_op jit(solution)/shard_map/ppermute | solution.py:26
  77.7 40.6 %collective-permute-start.20 = (bf16[8,32,1024]{2,1,0:T(8,128)(2,1)}, bf16[8,32,1024]{2,1,0:T(8,128)(2,1)}, u32[]{:S(2)}, u32[]{:S(2)}) collective-permute-start(bf16[8,32,1024]{2,1,0:T(8,128)(2,1)} %all-to-all-done.1.refs_13_), channel_id=1, source_target_pairs={{0,24},{8,0},{16,8},{24,16},{1,25},{9,1},{17,9},{25,17},{2,26},{10... | collective-permute-start | bytes 1572872 | tf_op jit(solution)/shard_map/ppermute | solution.py:26
  77.7 44.0 %collective-permute-start.21 = (bf16[8,32,1024]{2,1,0:T(8,128)(2,1)}, bf16[8,32,1024]{2,1,0:T(8,128)(2,1)}, u32[]{:S(2)}, u32[]{:S(2)}) collective-permute-start(bf16[8,32,1024]{2,1,0:T(8,128)(2,1)} %all-to-all-done.1.refs_13_), channel_id=1, source_target_pairs={{0,4},{4,0},{1,5},{5,1},{2,6},{6,2},{3,7},{7,3},{8,12},{12,8},{9,1... | collective-permute-start | bytes 1572872 | tf_op jit(solution)/shard_map/ppermute | solution.py:26
  118.3 19.1 %collective-permute-start.22 = (bf16[8,32,1024]{2,1,0:T(8,128)(2,1)}, bf16[8,32,1024]{2,1,0:T(8,128)(2,1)S(1)}, u32[]{:S(2)}, u32[]{:S(2)}) collective-permute-start(bf16[8,32,1024]{2,1,0:T(8,128)(2,1)} %collective-permute-done.18.refs_14_), channel_id=1, source_target_pairs={{0,4},{4,0},{1,5},{5,1},{2,6},{6,2},{3,7},{7,3},{8,12},{12,8},{9,1... | collective-permute-start | bytes 1572872 | tf_op jit(solution)/shard_map/ppermute | solution.py:26
  118.3 19.1 %collective-permute-start.23 = (bf16[8,32,1024]{2,1,0:T(8,128)(2,1)}, bf16[8,32,1024]{2,1,0:T(8,128)(2,1)S(1)}, u32[]{:S(2)}, u32[]{:S(2)}) collective-permute-start(bf16[8,32,1024]{2,1,0:T(8,128)(2,1)} %collective-permute-done.19.refs_15_), channel_id=1, source_target_pairs={{0,4},{4,0},{1,5},{5,1},{2,6},{6,2},{3,7},{7,3},{8,12},{12,8},{9,1... | collective-permute-start | bytes 1572872 | tf_op jit(solution)/shard_map/ppermute | solution.py:26
  118.8 18.6 %collective-permute-start.24 = (bf16[8,32,1024]{2,1,0:T(8,128)(2,1)}, bf16[8,32,1024]{2,1,0:T(8,128)(2,1)S(1)}, u32[]{:S(2)}, u32[]{:S(2)}) collective-permute-start(bf16[8,32,1024]{2,1,0:T(8,128)(2,1)} %collective-permute-done.20.refs_16_), channel_id=1, source_target_pairs={{0,4},{4,0},{1,5},{5,1},{2,6},{6,2},{3,7},{7,3},{8,12},{12,8},{9,1... | collective-permute-start | bytes 1572872 | tf_op jit(solution)/shard_map/ppermute | solution.py:26
  118.8 10.7 %collective-permute-start.12 = (bf16[464,256]{1,0:T(8,128)(2,1)}, bf16[464,256]{1,0:T(8,128)(2,1)S(1)}, u32[]{:S(2)}, u32[]{:S(2)}) collective-permute-start(bf16[464,256]{1,0:T(8,128)(2,1)} %shard_map.91.refs_0_), channel_id=1, source_target_pairs={{0,1},{1,2},{2,3},{3,0},{4,5},{5,6},{6,7},{7,4},{8,9},{9,10},{10,1... | collective-permute-start | bytes 712712 | tf_op jit(solution)/shard_map/ppermute | solution.py:26
  121.6 14.1 %collective-permute-start.13 = (bf16[464,256]{1,0:T(8,128)(2,1)}, bf16[464,256]{1,0:T(8,128)(2,1)S(1)}, u32[]{:S(2)}, u32[]{:S(2)}) collective-permute-start(bf16[464,256]{1,0:T(8,128)(2,1)} %shard_map.91.refs_0_), channel_id=1, source_target_pairs={{0,2},{1,3},{2,0},{3,1},{4,6},{5,7},{6,4},{7,5},{8,10},{9,11},{10,... | collective-permute-start | bytes 712712 | tf_op jit(solution)/shard_map/ppermute | solution.py:26
  129.5 7.9 %copy-start.10 = (bf16[464,256]{1,0:T(8,128)(2,1)}, bf16[464,256]{1,0:T(8,128)(2,1)S(1)}, u32[]{:S(2)}) copy-start(bf16[464,256]{1,0:T(8,128)(2,1)S(1)} %collective-permute-done.12.refs_1_) | copy-start | bytes 712708
  129.5 7.8 %collective-permute-start.14 = (bf16[464,256]{1,0:T(8,128)(2,1)}, bf16[464,256]{1,0:T(8,128)(2,1)S(1)}, u32[]{:S(2)}, u32[]{:S(2)}) collective-permute-start(bf16[464,256]{1,0:T(8,128)(2,1)} %shard_map.91.refs_0_), channel_id=1, source_target_pairs={{0,3},{1,0},{2,1},{3,2},{4,7},{5,4},{6,5},{7,6},{8,11},{9,8},{10,9... | collective-permute-start | bytes 712712 | tf_op jit(solution)/shard_map/ppermute | solution.py:26
  135.8 1.6 copy-start.11
  137.4 0.9 copy-start.7
  137.4 1.1 copy-start.8
  138.4 0.8 copy-start.9
  151.1 10.3 %collective-permute-start.25 = (bf16[432,256]{1,0:T(8,128)(2,1)}, bf16[432,256]{1,0:T(8,128)(2,1)S(1)}, u32[]{:S(2)}, u32[]{:S(2)}) collective-permute-start(bf16[432,256]{1,0:T(8,128)(2,1)} %get-tuple-element.15.refs_0_), channel_id=1, source_target_pairs={{0,1},{1,2},{2,3},{3,0},{4,5},{5,6},{6,7},{7,4},{8,9},{9,10},{10,1... | collective-permute-start | bytes 663560 | tf_op jit(solution)/shard_map/ppermute | solution.py:26
  151.6 12.2 %collective-permute-start.26 = (bf16[432,256]{1,0:T(8,128)(2,1)}, bf16[432,256]{1,0:T(8,128)(2,1)S(1)}, u32[]{:S(2)}, u32[]{:S(2)}) collective-permute-start(bf16[432,256]{1,0:T(8,128)(2,1)} %get-tuple-element.15.refs_0_), channel_id=1, source_target_pairs={{0,2},{1,3},{2,0},{3,1},{4,6},{5,7},{6,4},{7,5},{8,10},{9,11},{10,... | collective-permute-start | bytes 663560 | tf_op jit(solution)/shard_map/ppermute | solution.py:26
  155.3 9.1 %collective-permute-start.27 = (bf16[432,256]{1,0:T(8,128)(2,1)}, bf16[432,256]{1,0:T(8,128)(2,1)S(1)}, u32[]{:S(2)}, u32[]{:S(2)}) collective-permute-start(bf16[432,256]{1,0:T(8,128)(2,1)} %get-tuple-element.15.refs_0_), channel_id=1, source_target_pairs={{0,3},{1,0},{2,1},{3,2},{4,7},{5,4},{6,5},{7,6},{8,11},{9,8},{10,9... | collective-permute-start | bytes 663560 | tf_op jit(solution)/shard_map/ppermute | solution.py:26
  161.4 3.0 %copy-start.13 = (bf16[432,256]{1,0:T(8,128)(2,1)}, bf16[432,256]{1,0:T(8,128)(2,1)S(1)}, u32[]{:S(2)}) copy-start(bf16[432,256]{1,0:T(8,128)(2,1)S(1)} %collective-permute-done.25.refs_1_) | copy-start | bytes 663556
  176.5 7.8 %collective-permute-start.28 = (bf16[400,256]{1,0:T(8,128)(2,1)}, bf16[400,256]{1,0:T(8,128)(2,1)S(1)}, u32[]{:S(2)}, u32[]{:S(2)}) collective-permute-start(bf16[400,256]{1,0:T(8,128)(2,1)} %get-tuple-element.17.refs_0_), channel_id=1, source_target_pairs={{0,1},{1,2},{2,3},{3,0},{4,5},{5,6},{6,7},{7,4},{8,9},{9,10},{10,1... | collective-permute-start | bytes 614408 | tf_op jit(solution)/shard_map/ppermute | solution.py:26
  176.9 13.0 %collective-permute-start.29 = (bf16[400,256]{1,0:T(8,128)(2,1)}, bf16[400,256]{1,0:T(8,128)(2,1)S(1)}, u32[]{:S(2)}, u32[]{:S(2)}) collective-permute-start(bf16[400,256]{1,0:T(8,128)(2,1)} %get-tuple-element.17.refs_0_), channel_id=1, source_target_pairs={{0,2},{1,3},{2,0},{3,1},{4,6},{5,7},{6,4},{7,5},{8,10},{9,11},{10,... | collective-permute-start | bytes 614408 | tf_op jit(solution)/shard_map/ppermute | solution.py:26
  180.5 9.3 %collective-permute-start.30 = (bf16[400,256]{1,0:T(8,128)(2,1)}, bf16[400,256]{1,0:T(8,128)(2,1)S(1)}, u32[]{:S(2)}, u32[]{:S(2)}) collective-permute-start(bf16[400,256]{1,0:T(8,128)(2,1)} %get-tuple-element.17.refs_0_), channel_id=1, source_target_pairs={{0,3},{1,0},{2,1},{3,2},{4,7},{5,4},{6,5},{7,6},{8,11},{9,8},{10,9... | collective-permute-start | bytes 614408 | tf_op jit(solution)/shard_map/ppermute | solution.py:26
  184.3 5.6 %copy-start.16 = (bf16[400,256]{1,0:T(8,128)(2,1)}, bf16[400,256]{1,0:T(8,128)(2,1)S(1)}, u32[]{:S(2)}) copy-start(bf16[400,256]{1,0:T(8,128)(2,1)S(1)} %collective-permute-done.28.refs_1_) | copy-start | bytes 614404
  (5 other events, 3.5 us)
Sparse Core Ops, SparseCore 0:
  16.7 112.1 all-gather.1
